TPU v7x, 512 devices: a whole 4x4x16 slice. The times are simulated.
512 devices in a mesh: rep: 2 (over z_hi), fs: 32 (over z_lo, y), tp: 8 (over x, core).
Axes of the slice: x: 4, y: 4, z: 16 (z_hi: 2, z_lo: 8; z = z_hi * 8 + z_lo), core: 2. Of those that a mesh axis runs over, the one named last changes fastest.
Arguments:
- inputs: bfloat16 [32768, 2048], P(('rep', 'fs')), may hold values from -6 to 6
- gain: float32 [2048], replicated, may hold values from 0.1 to 1.9
- gate_weight: bfloat16 [2048, 3072], P('fs', 'tp'), may hold values from -0.125 to 0.125
- up_weight: bfloat16 [2048, 3072], P('fs', 'tp'), may hold values from -0.125 to 0.125
- down_weight: bfloat16 [2048, 3072], P('fs', 'tp'), may hold values from -0.109375 to 0.109375
- cotangent: bfloat16 [32768, 2048], P(('rep', 'fs')), may hold values from -16 to 16
Outputs:
- input_gradient: bfloat16 [32768, 2048], P(('rep', 'fs'))
- gain_gradient: float32 [2048], replicated
- d_down: float32 [2048, 3072], P('fs', 'tp')
All inputs are finite; a program needn't handle non-finite values.
Results may differ from a plain program's by a relative error of at most 0.014.
Values may be sent and summed in bfloat16 or wider, within the bound.
No kernel may reach another device: no remote copies, remote signals or barrier semaphores. Data moves between devices by JAX's collectives and lax.ppermute only.
A program may use at most 64 MiB of HBM per device.

v0:
```python
import jax
import jax.numpy as jnp
from jax import lax
from jax.experimental import pallas as pl
from jax.experimental.pallas import tpu as pltpu
from jax.sharding import Mesh
from jax.sharding import PartitionSpec as P

FS = ("fs_0", "fs_1")
REP_FS = ("rep", "fs_0", "fs_1")
TP = ("x", "c")
RING = ("rep", "fs_0")
PLANE = ("fs_1", "x", "c")
EPS = 1e-06
F32 = jnp.float32
BF16 = jnp.bfloat16


def shifted(v, axis, by):
    n = lax.axis_size(axis)
    return lax.ppermute(v, axis, [(i, (i + by) % n) for i in range(n)])


def exchanged(v, axis):
    return lax.all_to_all(v, axis, 0, 0, tiled=True)


def from_all(v, axis):
    n = lax.axis_size(axis)
    return exchanged(jnp.broadcast_to(v[None], (n, *v.shape)), axis)


def rolled(v, start):
    return lax.dynamic_slice_in_dim(jnp.concatenate([v, v], axis=0), start, v.shape[0], axis=0)


def blocks_of(refs):
    for d in range(4):
        yield d, 0, refs[d]
    yield 4, 0, refs[4]
    yield 4, refs[4].shape[0], refs[5]
    for d in range(5, 8):
        yield d, 0, refs[d + 1]


def prepare_tokens(at_ref, x_ref, gain_ref, out_ref):
    nz, _, cols = out_ref.shape
    v = x_ref[...].astype(F32)
    inv = lax.rsqrt(jnp.mean(v * v, axis=-1, keepdims=True) + EPS)
    for d in range(nz):
        own = pl.ds(pl.multiple_of(((at_ref[0] + d) % nz) * cols, cols), cols)
        part = x_ref[:, own].astype(F32)
        out_ref[d] = (part * inv * gain_ref[:, own]).astype(BF16)


def prepare_cotangent(at_ref, lo_ref, hi_ref, out_ref, turned_ref):
    nz, _, cols = out_ref.shape
    for d in range(nz):
        own = pl.ds(pl.multiple_of(((at_ref[0] + d) % nz) * cols, cols), cols)
        part = jnp.concatenate([lo_ref[:, own], hi_ref[:, own]], axis=0)
        out_ref[d] = part
        turned_ref[d] = part.T


def grad_kernel(x_ref, c_ref, *refs):
    w_refs, (mine_ref, other_ref, hid_ref) = refs[:9], refs[9:]
    units = hid_ref.shape[1]
    nx, _, part, _ = mine_ref.shape
    gu = dh = None
    for d, lo, w in blocks_of(w_refs):
        rows = w.shape[0]
        a = jnp.dot(x_ref[d, :, lo : lo + rows], w[:, : 2 * units], preferred_element_type=F32)
        b = jnp.dot(c_ref[d, :, lo : lo + rows], w[:, 2 * units :], preferred_element_type=F32)
        gu = a if gu is None else gu + a
        dh = b if dh is None else dh + b
    gate, up = gu[:, :units], gu[:, units:]
    dh = 0.5 * dh
    sig = jax.nn.sigmoid(gate)
    act = gate * sig
    hid_ref[...] = (act * up).astype(BF16)
    d_gate = (dh * up * sig * (1.0 + gate * (1.0 - sig))).astype(BF16)
    d_up = (dh * act).astype(BF16)
    both = jnp.concatenate([d_gate, d_up], axis=1)
    for d, lo, w in blocks_of(w_refs):
        rows = w.shape[0]
        out = lax.dot_general(
            both, w[:, : 2 * units], (((1,), (1,)), ((), ())), preferred_element_type=F32
        ).astype(BF16)
        for k in range(nx):
            mine_ref[k, d, :, lo : lo + rows] = out[k * part : (k + 1) * part]
            other_ref[k, d, :, lo : lo + rows] = out[(nx + k) * part : (nx + k + 1) * part]


def down_kernel(ct_ref, hid_ref, out_ref):
    ny, nz, rows, _ = out_ref.shape
    for d in range(nz):
        res = jnp.dot(ct_ref[d], hid_ref[...], preferred_element_type=F32)
        res = (0.5 * res).astype(BF16)
        for y in range(ny):
            out_ref[y, d] = res[y * rows : (y + 1) * rows]


def chip_kernel(mine_ref, theirs_ref, *out_refs):
    for k, out_ref in enumerate(out_refs):
        out_ref[...] = (mine_ref[k].astype(F32) + theirs_ref[k].astype(F32)).astype(BF16)


def finish_kernel(at_ref, got0, got1, got2, got3, x_ref, c_ref, gain_ref, out_ref, sum_ref, dn_ref):
    nz, _, cols = got0.shape
    for d in range(nz):
        own = pl.ds(pl.multiple_of(((at_ref[0] + d) % nz) * cols, cols), cols)
        total = got0[d].astype(F32)
        for got in (got1, got2, got3):
            total = total + got[d].astype(F32)
        dn_ref[:, own] = total.astype(BF16)
    v = x_ref[...].astype(F32)
    inv = lax.rsqrt(jnp.mean(v * v, axis=-1, keepdims=True) + EPS)
    xhat = v * inv
    dn = dn_ref[...].astype(F32)
    sums = jnp.sum(dn * xhat, axis=0, keepdims=True)
    gs = gain_ref[...] * dn
    m = jnp.mean(gs * xhat, axis=-1, keepdims=True)
    out_ref[...] = (c_ref[...].astype(F32) + inv * (gs - xhat * m)).astype(BF16)
    for k in range(sum_ref.shape[0]):
        sum_ref[k] = sums


def place_kernel(at_ref, p0, p1, p2, p3, other_ref, out_ref):
    n = 4
    part = p0.shape[0]
    for k, piece in enumerate((p0, p1, p2, p3)):
        spot = (at_ref[2] + k) % n
        own = pl.multiple_of((at_ref[1] * n + spot) * part, part)
        out_ref[pl.ds(own, part), :] = piece[...]
        far = pl.multiple_of(((1 - at_ref[1]) * n + spot) * part, part)
        out_ref[pl.ds(far, part), :] = other_ref[k]


def vmem(n):
    return [pl.BlockSpec(memory_space=pltpu.VMEM)] * n


def work(inputs, gain, gate_weight, up_weight, down_weight, cotangent):
    nz, ny, nx = lax.axis_size("fs_0"), lax.axis_size("fs_1"), lax.axis_size("x")
    rep, zl = lax.axis_index("rep"), lax.axis_index("fs_0")
    x, c = lax.axis_index("x"), lax.axis_index("c")
    tokens, width = inputs.shape
    rows, units = gate_weight.shape
    cols = width // nz
    half, part = tokens // 2, tokens // 2 // nx
    gain2 = gain[None]
    at = jnp.stack([zl, c, x]).astype(jnp.int32)

    w = jnp.concatenate([gate_weight, up_weight, down_weight], axis=1)
    w0 = from_all(w, "fs_1").reshape(ny * rows, 3 * units)
    fwd, bwd = [w0], [w0]
    for _ in range(3):
        fwd.append(shifted(fwd[-1], RING, 1))
        bwd.append(shifted(bwd[-1], RING, -1))
    mid = cols // 2
    last_f = shifted(fwd[-1][:mid], RING, 1)
    last_b = shifted(bwd[-1][mid:], RING, -1)
    weights = [w0, bwd[1], bwd[2], bwd[3], last_f, last_b, fwd[3], fwd[2], fwd[1]]

    def spot(i, at):
        return ((i // nx + at[1]) % 2) * nx + (i + at[2]) % nx

    xr = pl.pallas_call(
        prepare_tokens,
        out_shape=jax.ShapeDtypeStruct((nz, tokens, cols), BF16),
        grid_spec=pltpu.PrefetchScalarGridSpec(
            num_scalar_prefetch=1,
            grid=(2 * nx,),
            in_specs=[
                pl.BlockSpec((part, width), lambda i, at: (spot(i, at), 0)),
                pl.BlockSpec((1, width), lambda i, at: (0, 0)),
            ],
            out_specs=pl.BlockSpec((nz, part, cols), lambda i, at: (0, i, 0)),
        ),
        name="prepare_x",
    )(at, inputs, gain2)
    cr, ct = pl.pallas_call(
        prepare_cotangent,
        out_shape=(
            jax.ShapeDtypeStruct((nz, tokens, cols), BF16),
            jax.ShapeDtypeStruct((nz, cols, tokens), BF16),
        ),
        grid_spec=pltpu.PrefetchScalarGridSpec(
            num_scalar_prefetch=1,
            grid=(nx,),
            in_specs=[
                pl.BlockSpec((part, width), lambda i, at: (spot(2 * i, at), 0)),
                pl.BlockSpec((part, width), lambda i, at: (spot(2 * i + 1, at), 0)),
            ],
            out_specs=(
                pl.BlockSpec((nz, 2 * part, cols), lambda i, at: (0, i, 0)),
                pl.BlockSpec((nz, cols, 2 * part), lambda i, at: (0, 0, i)),
            ),
        ),
        name="prepare_c",
    )(at, cotangent, cotangent)

    mine, other, hidden = pl.pallas_call(
        grad_kernel,
        out_shape=(
            jax.ShapeDtypeStruct((nx, nz, part, cols), BF16),
            jax.ShapeDtypeStruct((nx, nz, part, cols), BF16),
            jax.ShapeDtypeStruct((tokens, units), BF16),
        ),
        in_specs=vmem(11),
        out_specs=tuple(vmem(3)),
        name="grad",
    )(xr, cr, *weights)
    theirs = shifted(other, "c", 1)
    (dd,) = pl.pallas_call(
        down_kernel,
        out_shape=(jax.ShapeDtypeStruct((ny, nz, rows, units), BF16),),
        in_specs=vmem(2),
        out_specs=tuple(vmem(1)),
        name="down",
    )(ct, hidden)
    dy = exchanged(dd, "fs_1")

    chunk = jax.ShapeDtypeStruct((nz, part, cols), BF16)
    chip = pl.pallas_call(
        chip_kernel,
        out_shape=(chunk,) * 4,
        in_specs=vmem(2),
        out_specs=tuple(vmem(4)),
        name="chip",
    )(mine, theirs)
    got = [chip[0]]
    for k in (1, 2, 3):
        got.append(shifted(chip[k], "x", k))
    first = c * half + x * part
    xs = lax.dynamic_slice_in_dim(inputs, first, part, axis=0)
    cs = lax.dynamic_slice_in_dim(cotangent, first, part, axis=0)
    planes = lax.axis_size(PLANE)
    ig, gain_part = pl.pallas_call(
        finish_kernel,
        out_shape=(
            jax.ShapeDtypeStruct((part, width), BF16),
            jax.ShapeDtypeStruct((planes, 1, width), F32),
        ),
        in_specs=[pl.BlockSpec(memory_space=pltpu.SMEM)] + vmem(7),
        out_specs=tuple(vmem(2)),
        scratch_shapes=[pltpu.VMEM((part, width), BF16)],
        name="finish",
    )(at, *got, xs, cs, gain2)
    pieces = [ig]
    for k in (1, 2, 3):
        pieces.append(shifted(ig, "x", -k))
    ig_other = shifted(jnp.stack(pieces), "c", 1)
    out = pl.pallas_call(
        place_kernel,
        out_shape=jax.ShapeDtypeStruct((tokens, width), BF16),
        in_specs=[pl.BlockSpec(memory_space=pltpu.SMEM)] + vmem(5),
        out_specs=pl.BlockSpec(memory_space=pltpu.VMEM),
        name="place",
    )(at, *pieces, ig_other)

    gain_plane = exchanged(gain_part, PLANE)
    gain_plane = jnp.sum(gain_plane, axis=0)
    gain_gradient = from_all(gain_plane, RING)
    gain_gradient = jnp.sum(gain_gradient, axis=(0, 1))

    dy = jnp.sum(dy.astype(F32), axis=0).astype(BF16)
    dz = rolled(dy, (nz - zl) % nz).reshape(nz, 2, rows // 2, units).transpose(1, 0, 2, 3)
    dz = exchanged(dz.reshape(2 * nz, rows // 2, units), RING)
    own = jnp.sum(dz.astype(F32), axis=0)
    far = shifted(own, "rep", 1)
    pair = rolled(jnp.stack([own, far]), rep)
    d_down = pair.reshape(rows, units)
    return (out, gain_gradient, d_down)


def solution(mesh):
    torus = Mesh(
        mesh.devices.reshape(mesh.shape["rep"], 8, 4, 4, 2),
        ("rep", "fs_0", "fs_1", "x", "c"),
    )
    return jax.shard_map(
        work,
        mesh=torus,
        in_specs=(P(REP_FS, None), P(), P(FS, TP), P(FS, TP), P(FS, TP), P(REP_FS, None)),
        out_specs=(P(REP_FS, None), P(), P(FS, TP)),
        check_vma=False,
    )
```

profile of v0, /device:TPU:1, one launch (start us, length us, event | category | flops | bytes accessed | tf_op | source)
XLA Modules:
  0.0 218.8 jit_solution(15455993155824749124)
XLA Ops:
  0.6 0.9 pad_maximum_fusion.1
  1.5 12.1 %all_to_all.25 = bf16[4,64,1152]{2,1,0:T(8,128)(2,1)S(1)} all-to-all(bf16[4,64,1152]{2,1,0:T(8,128)(2,1)S(1)} %broadcast_in_dim.7), channel_id=1, replica_groups=mesh['rep'=2,'fs_0'=8,'fs_1'=4,'x'=4,'c'=2] {'fs_1'}, dimensions={0} | all-to-all | bytes 1179648 | tf_op jit(solution)/shard_map/all_to_all | solution.py:25
  13.6 5.3 %collective-permute-start.3 = (bf16[256,1152]{1,0:T(8,128)(2,1)S(1)}, bf16[256,1152]{1,0:T(8,128)(2,1)S(1)}, u32[]{:S(2)}, u32[]{:S(2)}) collective-permute-start(bf16[256,1152]{1,0:T(8,128)(2,1)S(1)} %bitcast.16), channel_id=1, source_target_pairs={{0,32},{32,64},{64,96},{96,128},{128,160},{160,192},{192,224},{224... | collective-permute-start | bytes 1769480 | tf_op jit(solution)/shard_map/ppermute | solution.py:21
  18.9 9.5 %collective-permute-start = (bf16[256,1152]{1,0:T(8,128)(2,1)S(1)}, bf16[256,1152]{1,0:T(8,128)(2,1)S(1)}, u32[]{:S(2)}, u32[]{:S(2)}) collective-permute-start(bf16[256,1152]{1,0:T(8,128)(2,1)S(1)} %bitcast.17), channel_id=1, source_target_pairs={{0,480},{32,0},{64,32},{96,64},{128,96},{160,128},{192,160},{224,1... | collective-permute-start | bytes 1769480 | tf_op jit(solution)/shard_map/ppermute | solution.py:21
  28.4 9.7 %collective-permute-done.3.refs_8_ = bf16[256,1152]{1,0:T(8,128)(2,1)S(1)} collective-permute-done((bf16[256,1152]{1,0:T(8,128)(2,1)S(1)}, bf16[256,1152]{1,0:T(8,128)(2,1)S(1)}, u32[]{:S(2)}, u32[]{:S(2)}) %collective-permute-start.3) | collective-permute-done | bytes 589856 | tf_op jit(solution)/shard_map/ppermute | solution.py:21
  38.1 1.9 collective-permute-start.4
  40.0 0.0 collective-permute-done.refs_1_
  40.0 4.6 %collective-permute-start.1 = (bf16[256,1152]{1,0:T(8,128)(2,1)S(1)}, bf16[256,1152]{1,0:T(8,128)(2,1)S(1)}, u32[]{:S(2)}, u32[]{:S(2)}) collective-permute-start(bf16[256,1152]{1,0:T(8,128)(2,1)S(1)} %collective-permute-done.refs_1_), channel_id=1, source_target_pairs={{0,480},{32,0},{64,32},{96,64},{128,96},{160,128},{192,160},{224,1... | collective-permute-start | bytes 1769480 | tf_op jit(solution)/shard_map/ppermute | solution.py:21
  44.6 8.8 %collective-permute-done.4.refs_7_ = bf16[256,1152]{1,0:T(8,128)(2,1)S(1)} collective-permute-done((bf16[256,1152]{1,0:T(8,128)(2,1)S(1)}, bf16[256,1152]{1,0:T(8,128)(2,1)S(1)}, u32[]{:S(2)}, u32[]{:S(2)}) %collective-permute-start.4) | collective-permute-done | bytes 589856 | tf_op jit(solution)/shard_map/ppermute | solution.py:21
  53.4 1.9 collective-permute-start.5
  55.3 0.0 collective-permute-done.1.refs_2_
  55.3 4.6 %collective-permute-start.2 = (bf16[256,1152]{1,0:T(8,128)(2,1)S(1)}, bf16[256,1152]{1,0:T(8,128)(2,1)S(1)}, u32[]{:S(2)}, u32[]{:S(2)}) collective-permute-start(bf16[256,1152]{1,0:T(8,128)(2,1)S(1)} %collective-permute-done.1.refs_2_), channel_id=1, source_target_pairs={{0,480},{32,0},{64,32},{96,64},{128,96},{160,128},{192,160},{224,1... | collective-permute-start | bytes 1769480 | tf_op jit(solution)/shard_map/ppermute | solution.py:21
  59.9 7.9 %collective-permute-done.5.refs_6_ = bf16[256,1152]{1,0:T(8,128)(2,1)S(1)} collective-permute-done((bf16[256,1152]{1,0:T(8,128)(2,1)S(1)}, bf16[256,1152]{1,0:T(8,128)(2,1)S(1)}, u32[]{:S(2)}, u32[]{:S(2)}) %collective-permute-start.5) | collective-permute-done | bytes 589856 | tf_op jit(solution)/shard_map/ppermute | solution.py:21
  67.9 0.8 slice.8
  68.7 1.9 collective-permute-start.6
  70.6 0.0 collective-permute-done.2.refs_3_
  70.6 0.8 slice.9
  71.4 4.6 %collective-permute-start.7 = (bf16[128,1152]{1,0:T(8,128)(2,1)}, bf16[128,1152]{1,0:T(8,128)(2,1)}, u32[]{:S(2)}, u32[]{:S(2)}) collective-permute-start(bf16[128,1152]{1,0:T(8,128)(2,1)} %slice.9), channel_id=1, source_target_pairs={{0,480},{32,0},{64,32},{96,64},{128,96},{160,128},{192,160},{224,1... | collective-permute-start | bytes 884744 | tf_op jit(solution)/shard_map/ppermute | solution.py:21
  76.0 0.6 pad_add_fusion.at_ref
  76.6 5.2 %prepare_c.1 = (bf16[8,512,256]{2,1,0:T(8,128)(2,1)}, bf16[8,256,512]{2,1,0:T(8,128)(2,1)}) custom-call(s32[3]{0:T(128)} %pad_add_fusion.at_ref, bf16[512,2048]{1,0:T(8,128)(2,1)} %hi_ref.1, bf16[512,2048]{1,0:T(8,128)(2,1)} %hi_ref.1), custom_call_target="tpu_custom_call" | custom-call | tf_op jit(solution)/shard_map/prepare_c/pallas_call | solution.py:182
  81.8 6.8 %prepare_x.1.x_ref = bf16[8,512,256]{2,1,0:T(8,128)(2,1)} custom-call(s32[3]{0:T(128)} %pad_add_fusion.at_ref, bf16[512,2048]{1,0:T(8,128)(2,1)} %x_ref.1, f32[1,2048]{1,0:T(1,128)} %bitcast.27), custom_call_target="tpu_custom_call" | custom-call | tf_op jit(solution)/shard_map/prepare_x/pallas_call | solution.py:168
  88.7 0.0 collective-permute-done.6.refs_4_
  88.7 10.3 %grad.1 = (bf16[4,8,64,256]{3,2,1,0:T(8,128)(2,1)}, bf16[4,8,64,256]{3,2,1,0:T(8,128)(2,1)}, bf16[512,384]{1,0:T(8,128)(2,1)}) custom-call(bf16[8,512,256]{2,1,0:T(8,128)(2,1)} %prepare_x.1.x_ref, bf16[8,512,256]{2,1,0:T(8,128)(2,1)} %get-tuple-element.14.c_ref, bf16[256,1152]{1,0:T(8,128)(2,1)} %bitcast.18, bf16[256,1152]{1,0:T(8,128)(2,1)} %copy-done.10, ...), custom_call_target="tpu_custom_call" | custom-call | tf_op jit(solution)/shard_map/grad/pallas_call | solution.py:203
  98.9 6.8 %collective-permute-start.8 = (bf16[4,8,64,256]{3,2,1,0:T(8,128)(2,1)}, bf16[4,8,64,256]{3,2,1,0:T(8,128)(2,1)S(1)}, u32[]{:S(2)}, u32[]{:S(2)}) collective-permute-start(bf16[4,8,64,256]{3,2,1,0:T(8,128)(2,1)} %get-tuple-element.16), channel_id=1, source_target_pairs={{0,1},{1,0},{2,3},{3,2},{4,5},{5,4},{6,7},{7,6},{8,9},{9,8},{10,11... | collective-permute-start | bytes 3145736 | tf_op jit(solution)/shard_map/ppermute | solution.py:21
  105.8 4.0 %down.1 = bf16[4,8,64,384]{3,2,1,0:T(8,128)(2,1)} custom-call(bf16[8,256,512]{2,1,0:T(8,128)(2,1)} %get-tuple-element.23.ct_ref, bf16[512,384]{1,0:T(8,128)(2,1)} %get-tuple-element.24.hid_ref), custom_call_target="tpu_custom_call" | custom-call | tf_op jit(solution)/shard_map/down/pallas_call | solution.py:215
  109.8 3.6 %all-to-all-start.3 = ((bf16[4,8,64,384]{3,2,1,0:T(8,128)(2,1)}), bf16[4,8,64,384]{3,2,1,0:T(8,128)(2,1)S(1)}, u32[]{:S(2)}, u32[]{:S(2)}) async-start(bf16[4,8,64,384]{3,2,1,0:T(8,128)(2,1)} %down.1), calls=%async_computation.3 | async-start | bytes 3145728 | tf_op jit(solution)/shard_map/all_to_all | solution.py:25
  113.4 1.0 copy-done.4
  114.4 2.6 %chip.1 = (bf16[8,64,256]{2,1,0:T(8,128)(2,1)}, bf16[8,64,256]{2,1,0:T(8,128)(2,1)}, bf16[8,64,256]{2,1,0:T(8,128)(2,1)}, bf16[8,64,256]{2,1,0:T(8,128)(2,1)}) custom-call(bf16[4,8,64,256]{3,2,1,0:T(8,128)(2,1)} %get-tuple-element.15.mine_ref, bf16[4,8,64,256]{3,2,1,0:T(8,128)(2,1)} %copy-done.4), custom_call_target="tpu_custom_call" | custom-call | tf_op jit(solution)/shard_map/chip/pallas_call | solution.py:225
  117.0 4.6 %collective-permute-start.10 = (bf16[8,64,256]{2,1,0:T(8,128)(2,1)}, bf16[8,64,256]{2,1,0:T(8,128)(2,1)S(1)}, u32[]{:S(2)}, u32[]{:S(2)}) collective-permute-start(bf16[8,64,256]{2,1,0:T(8,128)(2,1)} %get-tuple-element.19), channel_id=1, source_target_pairs={{0,4},{2,6},{4,0},{6,2},{1,5},{3,7},{5,1},{7,3},{8,12},{10,14},{12... | collective-permute-start | bytes 786440 | tf_op jit(solution)/shard_map/ppermute | solution.py:21
  121.6 2.8 %collective-permute-start.11 = (bf16[8,64,256]{2,1,0:T(8,128)(2,1)}, bf16[8,64,256]{2,1,0:T(8,128)(2,1)S(1)}, u32[]{:S(2)}, u32[]{:S(2)}) collective-permute-start(bf16[8,64,256]{2,1,0:T(8,128)(2,1)} %get-tuple-element.20), channel_id=1, source_target_pairs={{0,6},{2,0},{4,2},{6,4},{1,7},{3,1},{5,3},{7,5},{8,14},{10,8},{12,... | collective-permute-start | bytes 786440 | tf_op jit(solution)/shard_map/ppermute | solution.py:21
  124.4 2.5 %collective-permute-start.9 = (bf16[8,64,256]{2,1,0:T(8,128)(2,1)}, bf16[8,64,256]{2,1,0:T(8,128)(2,1)S(1)}, u32[]{:S(2)}, u32[]{:S(2)}) collective-permute-start(bf16[8,64,256]{2,1,0:T(8,128)(2,1)} %get-tuple-element.18), channel_id=1, source_target_pairs={{0,2},{2,4},{4,6},{6,0},{1,3},{3,5},{5,7},{7,1},{8,10},{10,12},{12... | collective-permute-start | bytes 786440 | tf_op jit(solution)/shard_map/ppermute | solution.py:21
  126.9 1.7 constant_dynamic-slice_fusion.c_ref
  128.6 1.7 constant_dynamic-slice_fusion.1.x_ref
  130.2 3.9 %collective-permute-done.11.got3 = bf16[8,64,256]{2,1,0:T(8,128)(2,1)S(1)} collective-permute-done((bf16[8,64,256]{2,1,0:T(8,128)(2,1)}, bf16[8,64,256]{2,1,0:T(8,128)(2,1)S(1)}, u32[]{:S(2)}, u32[]{:S(2)}) %collective-permute-start.11) | collective-permute-done | bytes 262176 | tf_op jit(solution)/shard_map/ppermute | solution.py:21
  134.2 0.8 collective-permute-done.9.got1
  135.0 0.7 copy-done.15
  135.7 2.7 %finish.1 = (bf16[64,2048]{1,0:T(8,128)(2,1)}, f32[32,1,2048]{2,1,0:T(1,128)}) custom-call(s32[3]{0:T(128)} %pad_add_fusion.at_ref, bf16[8,64,256]{2,1,0:T(8,128)(2,1)} %get-tuple-element.17.got0, bf16[8,64,256]{2,1,0:T(8,128)(2,1)} %copy-done.15, bf16[8,64,256]{2,1,0:T(8,128)(2,1)} %copy-done.13, bf16[8,64,256]{2,1,0:T(8,128)(2,1)} %copy-done.14, ...), custom_call_target="tpu_custom_call" | custom-call | tf_op jit(solution)/shard_map/finish/pallas_call | solution.py:239
  138.4 0.0 all-to-all-done.3
  138.4 7.0 %all-to-all-start.1 = ((f32[32,1,2048]{2,1,0:T(1,128)}), f32[32,1,2048]{2,1,0:T(1,128)S(1)}, u32[]{:S(2)}, u32[]{:S(2)}) async-start(f32[32,1,2048]{2,1,0:T(1,128)} %get-tuple-element.22), calls=%async_computation.1 | async-start | bytes 524288 | tf_op jit(solution)/shard_map/all_to_all | solution.py:25
  145.5 0.3 reduce_sum.41
  145.8 0.2 fusion
  146.0 0.8 copy.12
  146.8 7.5 %all-to-all-done.1 = f32[32,1,2048]{2,1,0:T(1,128)S(1)} async-done(((f32[32,1,2048]{2,1,0:T(1,128)}), f32[32,1,2048]{2,1,0:T(1,128)S(1)}, u32[]{:S(2)}, u32[]{:S(2)}) %all-to-all-start.1) | async-done | bytes 262176 | tf_op jit(solution)/shard_map/all_to_all | solution.py:25
  154.3 7.8 %all-to-all-start.4 = ((bf16[16,32,384]{2,1,0:T(8,128)(2,1)}), bf16[16,32,384]{2,1,0:T(8,128)(2,1)S(1)}, u32[]{:S(2)}, u32[]{:S(2)}) async-start(bf16[16,32,384]{2,1,0:T(8,128)(2,1)} %bitcast.11), calls=%async_computation.4 | async-start | bytes 786432 | tf_op jit(solution)/shard_map/all_to_all | solution.py:25
  162.1 3.0 %collective-permute-start.12 = (bf16[64,2048]{1,0:T(8,128)(2,1)S(1)}, bf16[64,2048]{1,0:T(8,128)(2,1)S(1)}, u32[]{:S(2)}, u32[]{:S(2)}) collective-permute-start(bf16[64,2048]{1,0:T(8,128)(2,1)S(1)} %copy-done.5), channel_id=1, source_target_pairs={{0,6},{2,0},{4,2},{6,4},{1,7},{3,1},{5,3},{7,5},{8,14},{10,8},{12,... | collective-permute-start | bytes 786440 | tf_op jit(solution)/shard_map/ppermute | solution.py:21
  165.2 3.0 %collective-permute-start.13 = (bf16[64,2048]{1,0:T(8,128)(2,1)S(1)}, bf16[64,2048]{1,0:T(8,128)(2,1)S(1)}, u32[]{:S(2)}, u32[]{:S(2)}) collective-permute-start(bf16[64,2048]{1,0:T(8,128)(2,1)S(1)} %copy-done.5), channel_id=1, source_target_pairs={{0,4},{2,6},{4,0},{6,2},{1,5},{3,7},{5,1},{7,3},{8,12},{10,14},{12... | collective-permute-start | bytes 786440 | tf_op jit(solution)/shard_map/ppermute | solution.py:21
  168.2 1.9 collective-permute-start.14
  170.2 1.3 collective-permute-done.12.p1
  171.5 4.4 %collective-permute-done.13.p2 = bf16[64,2048]{1,0:T(8,128)(2,1)S(1)} collective-permute-done((bf16[64,2048]{1,0:T(8,128)(2,1)S(1)}, bf16[64,2048]{1,0:T(8,128)(2,1)S(1)}, u32[]{:S(2)}, u32[]{:S(2)}) %collective-permute-start.13) | collective-permute-done | bytes 262176 | tf_op jit(solution)/shard_map/ppermute | solution.py:21
  175.9 6.5 %collective-permute-done.14.p3 = bf16[64,2048]{1,0:T(8,128)(2,1)S(1)} collective-permute-done((bf16[64,2048]{1,0:T(8,128)(2,1)S(1)}, bf16[64,2048]{1,0:T(8,128)(2,1)S(1)}, u32[]{:S(2)}, u32[]{:S(2)}) %collective-permute-start.14) | collective-permute-done | bytes 262176 | tf_op jit(solution)/shard_map/ppermute | solution.py:21
  182.4 0.7 copy-done.8
  183.1 0.1 pad_maximum_fusion
  183.3 2.4 %collective-permute-start.15 = (bf16[4,64,2048]{2,1,0:T(8,128)(2,1)S(1)}, bf16[4,64,2048]{2,1,0:T(8,128)(2,1)S(1)}, u32[]{:S(2)}, u32[]{:S(2)}) collective-permute-start(bf16[4,64,2048]{2,1,0:T(8,128)(2,1)S(1)} %pad_maximum_fusion), channel_id=1, source_target_pairs={{0,1},{1,0},{2,3},{3,2},{4,5},{5,4},{6,7},{7,6},{8,9},{9,8},{10,11... | collective-permute-start | bytes 3145736 | tf_op jit(solution)/shard_map/ppermute | solution.py:21
  185.7 0.2 reduce_sum.39
  185.9 0.7 broadcast_in_dim.8
  186.6 11.5 %all-to-all-start.2 = ((f32[16,1,2048]{2,1,0:T(1,128)}), f32[16,1,2048]{2,1,0:T(1,128)S(1)}, u32[]{:S(2)}, u32[]{:S(2)}) async-start(f32[16,1,2048]{2,1,0:T(1,128)} %broadcast_in_dim.8), calls=%async_computation.2 | async-start | bytes 262144 | tf_op jit(solution)/shard_map/all_to_all | solution.py:25
  198.1 0.1 convert_reduce_fusion
  198.1 12.0 %collective-permute-start.16 = (f32[32,384]{1,0:T(8,128)S(1)}, f32[32,384]{1,0:T(8,128)S(1)}, u32[]{:S(2)}, u32[]{:S(2)}) collective-permute-start(f32[32,384]{1,0:T(8,128)S(1)} %convert_reduce_fusion), channel_id=1, source_target_pairs={{0,256},{256,0},{1,257},{257,1},{2,258},{258,2},{3,259},{259,3},{4... | collective-permute-start | bytes 147464 | tf_op jit(solution)/shard_map/ppermute | solution.py:21
  210.1 0.3 all-to-all-done.2
  210.4 0.7 reduce_sum.40
  211.1 1.0 copy-done.3
  212.1 3.0 %place.1 = bf16[512,2048]{1,0:T(8,128)(2,1)} custom-call(s32[3]{0:T(128)} %pad_add_fusion.at_ref, bf16[64,2048]{1,0:T(8,128)(2,1)} %get-tuple-element.21.p0, bf16[64,2048]{1,0:T(8,128)(2,1)} %copy-done.6, bf16[64,2048]{1,0:T(8,128)(2,1)} %copy-done.7, bf16[64,2048]{1,0:T(8,128)(2,1)} %copy-done.8, bf16[4,64,2048]{2,1,0:T(8,128)(2,1)} %copy-done.3), custom_call_target="tpu_custom_call" | custom-call | tf_op jit(solution)/shard_map/place/pallas_call | solution.py:254
  215.1 3.0 %collective-permute-done.16 = f32[32,384]{1,0:T(8,128)S(1)} collective-permute-done((f32[32,384]{1,0:T(8,128)S(1)}, f32[32,384]{1,0:T(8,128)S(1)}, u32[]{:S(2)}, u32[]{:S(2)}) %collective-permute-start.16) | collective-permute-done | bytes 49184 | tf_op jit(solution)/shard_map/ppermute | solution.py:21
  218.1 0.7 fusion.3
  (34 shorter events, 0.1 us)
Async XLA Ops:
  13.6 68.1 %copy-start = (bf16[4,64,1152]{2,1,0:T(8,128)(2,1)}, bf16[4,64,1152]{2,1,0:T(8,128)(2,1)S(1)}, u32[]{:S(2)}) copy-start(bf16[4,64,1152]{2,1,0:T(8,128)(2,1)S(1)} %all_to_all.25) | copy-start | bytes 1769476
  13.6 24.5 %collective-permute-start.3 = (bf16[256,1152]{1,0:T(8,128)(2,1)S(1)}, bf16[256,1152]{1,0:T(8,128)(2,1)S(1)}, u32[]{:S(2)}, u32[]{:S(2)}) collective-permute-start(bf16[256,1152]{1,0:T(8,128)(2,1)S(1)} %bitcast.16), channel_id=1, source_target_pairs={{0,32},{32,64},{64,96},{96,128},{128,160},{160,192},{192,224},{224... | collective-permute-start | bytes 1769480 | tf_op jit(solution)/shard_map/ppermute | solution.py:21
  18.9 21.1 %collective-permute-start = (bf16[256,1152]{1,0:T(8,128)(2,1)S(1)}, bf16[256,1152]{1,0:T(8,128)(2,1)S(1)}, u32[]{:S(2)}, u32[]{:S(2)}) collective-permute-start(bf16[256,1152]{1,0:T(8,128)(2,1)S(1)} %bitcast.17), channel_id=1, source_target_pairs={{0,480},{32,0},{64,32},{96,64},{128,96},{160,128},{192,160},{224,1... | collective-permute-start | bytes 1769480 | tf_op jit(solution)/shard_map/ppermute | solution.py:21
  38.1 43.7 %copy-start.9 = (bf16[256,1152]{1,0:T(8,128)(2,1)}, bf16[256,1152]{1,0:T(8,128)(2,1)S(1)}, u32[]{:S(2)}) copy-start(bf16[256,1152]{1,0:T(8,128)(2,1)S(1)} %collective-permute-done.3.refs_8_) | copy-start | bytes 1769476
  38.1 15.3 %collective-permute-start.4 = (bf16[256,1152]{1,0:T(8,128)(2,1)S(1)}, bf16[256,1152]{1,0:T(8,128)(2,1)S(1)}, u32[]{:S(2)}, u32[]{:S(2)}) collective-permute-start(bf16[256,1152]{1,0:T(8,128)(2,1)S(1)} %collective-permute-done.3.refs_8_), channel_id=1, source_target_pairs={{0,32},{32,64},{64,96},{96,128},{128,160},{160,192},{192,224},{224... | collective-permute-start | bytes 1769480 | tf_op jit(solution)/shard_map/ppermute | solution.py:21
  40.0 41.8 %copy-start.10 = (bf16[256,1152]{1,0:T(8,128)(2,1)}, bf16[256,1152]{1,0:T(8,128)(2,1)S(1)}, u32[]{:S(2)}) copy-start(bf16[256,1152]{1,0:T(8,128)(2,1)S(1)} %collective-permute-done.refs_1_) | copy-start | bytes 1769476
  40.0 15.3 %collective-permute-start.1 = (bf16[256,1152]{1,0:T(8,128)(2,1)S(1)}, bf16[256,1152]{1,0:T(8,128)(2,1)S(1)}, u32[]{:S(2)}, u32[]{:S(2)}) collective-permute-start(bf16[256,1152]{1,0:T(8,128)(2,1)S(1)} %collective-permute-done.refs_1_), channel_id=1, source_target_pairs={{0,480},{32,0},{64,32},{96,64},{128,96},{160,128},{192,160},{224,1... | collective-permute-start | bytes 1769480 | tf_op jit(solution)/shard_map/ppermute | solution.py:21
  53.4 28.4 %copy-start.11 = (bf16[256,1152]{1,0:T(8,128)(2,1)}, bf16[256,1152]{1,0:T(8,128)(2,1)S(1)}, u32[]{:S(2)}) copy-start(bf16[256,1152]{1,0:T(8,128)(2,1)S(1)} %collective-permute-done.4.refs_7_) | copy-start | bytes 1769476
  53.4 14.4 %collective-permute-start.5 = (bf16[256,1152]{1,0:T(8,128)(2,1)S(1)}, bf16[256,1152]{1,0:T(8,128)(2,1)S(1)}, u32[]{:S(2)}, u32[]{:S(2)}) collective-permute-start(bf16[256,1152]{1,0:T(8,128)(2,1)S(1)} %collective-permute-done.4.refs_7_), channel_id=1, source_target_pairs={{0,32},{32,64},{64,96},{96,128},{128,160},{160,192},{192,224},{224... | collective-permute-start | bytes 1769480 | tf_op jit(solution)/shard_map/ppermute | solution.py:21
  55.3 15.3 %copy-start.12 = (bf16[256,1152]{1,0:T(8,128)(2,1)}, bf16[256,1152]{1,0:T(8,128)(2,1)S(1)}, u32[]{:S(2)}) copy-start(bf16[256,1152]{1,0:T(8,128)(2,1)S(1)} %collective-permute-done.1.refs_2_) | copy-start | bytes 1769476
  55.3 15.2 %collective-permute-start.2 = (bf16[256,1152]{1,0:T(8,128)(2,1)S(1)}, bf16[256,1152]{1,0:T(8,128)(2,1)S(1)}, u32[]{:S(2)}, u32[]{:S(2)}) collective-permute-start(bf16[256,1152]{1,0:T(8,128)(2,1)S(1)} %collective-permute-done.1.refs_2_), channel_id=1, source_target_pairs={{0,480},{32,0},{64,32},{96,64},{128,96},{160,128},{192,160},{224,1... | collective-permute-start | bytes 1769480 | tf_op jit(solution)/shard_map/ppermute | solution.py:21
  67.9 14.0 %copy-start.1 = (bf16[256,1152]{1,0:T(8,128)(2,1)}, bf16[256,1152]{1,0:T(8,128)(2,1)S(1)}, u32[]{:S(2)}) copy-start(bf16[256,1152]{1,0:T(8,128)(2,1)S(1)} %collective-permute-done.5.refs_6_) | copy-start | bytes 1769476
  68.7 20.0 %collective-permute-start.6 = (bf16[128,1152]{1,0:T(8,128)(2,1)}, bf16[128,1152]{1,0:T(8,128)(2,1)}, u32[]{:S(2)}, u32[]{:S(2)}) collective-permute-start(bf16[128,1152]{1,0:T(8,128)(2,1)} %slice.8), channel_id=1, source_target_pairs={{0,32},{32,64},{64,96},{96,128},{128,160},{160,192},{192,224},{224... | collective-permute-start | bytes 884744 | tf_op jit(solution)/shard_map/ppermute | solution.py:21
  70.6 11.2 %copy-start.2 = (bf16[256,1152]{1,0:T(8,128)(2,1)}, bf16[256,1152]{1,0:T(8,128)(2,1)S(1)}, u32[]{:S(2)}) copy-start(bf16[256,1152]{1,0:T(8,128)(2,1)S(1)} %collective-permute-done.2.refs_3_) | copy-start | bytes 1769476
  71.4 17.3 %collective-permute-start.7 = (bf16[128,1152]{1,0:T(8,128)(2,1)}, bf16[128,1152]{1,0:T(8,128)(2,1)}, u32[]{:S(2)}, u32[]{:S(2)}) collective-permute-start(bf16[128,1152]{1,0:T(8,128)(2,1)} %slice.9), channel_id=1, source_target_pairs={{0,480},{32,0},{64,32},{96,64},{128,96},{160,128},{192,160},{224,1... | collective-permute-start | bytes 884744 | tf_op jit(solution)/shard_map/ppermute | solution.py:21
  98.9 14.5 %collective-permute-start.8 = (bf16[4,8,64,256]{3,2,1,0:T(8,128)(2,1)}, bf16[4,8,64,256]{3,2,1,0:T(8,128)(2,1)S(1)}, u32[]{:S(2)}, u32[]{:S(2)}) collective-permute-start(bf16[4,8,64,256]{3,2,1,0:T(8,128)(2,1)} %get-tuple-element.16), channel_id=1, source_target_pairs={{0,1},{1,0},{2,3},{3,2},{4,5},{5,4},{6,7},{7,6},{8,9},{9,8},{10,11... | collective-permute-start | bytes 3145736 | tf_op jit(solution)/shard_map/ppermute | solution.py:21
  109.8 28.6 %all-to-all-start.3 = ((bf16[4,8,64,384]{3,2,1,0:T(8,128)(2,1)}), bf16[4,8,64,384]{3,2,1,0:T(8,128)(2,1)S(1)}, u32[]{:S(2)}, u32[]{:S(2)}) async-start(bf16[4,8,64,384]{3,2,1,0:T(8,128)(2,1)} %down.1), calls=%async_computation.3 | async-start | bytes 3145728 | tf_op jit(solution)/shard_map/all_to_all | solution.py:25
  113.4 1.0 copy-start.4
  117.0 13.3 %collective-permute-start.10 = (bf16[8,64,256]{2,1,0:T(8,128)(2,1)}, bf16[8,64,256]{2,1,0:T(8,128)(2,1)S(1)}, u32[]{:S(2)}, u32[]{:S(2)}) collective-permute-start(bf16[8,64,256]{2,1,0:T(8,128)(2,1)} %get-tuple-element.19), channel_id=1, source_target_pairs={{0,4},{2,6},{4,0},{6,2},{1,5},{3,7},{5,1},{7,3},{8,12},{10,14},{12... | collective-permute-start | bytes 786440 | tf_op jit(solution)/shard_map/ppermute | solution.py:21
  121.6 12.5 %collective-permute-start.11 = (bf16[8,64,256]{2,1,0:T(8,128)(2,1)}, bf16[8,64,256]{2,1,0:T(8,128)(2,1)S(1)}, u32[]{:S(2)}, u32[]{:S(2)}) collective-permute-start(bf16[8,64,256]{2,1,0:T(8,128)(2,1)} %get-tuple-element.20), channel_id=1, source_target_pairs={{0,6},{2,0},{4,2},{6,4},{1,7},{3,1},{5,3},{7,5},{8,14},{10,8},{12,... | collective-permute-start | bytes 786440 | tf_op jit(solution)/shard_map/ppermute | solution.py:21
  124.4 10.6 %collective-permute-start.9 = (bf16[8,64,256]{2,1,0:T(8,128)(2,1)}, bf16[8,64,256]{2,1,0:T(8,128)(2,1)S(1)}, u32[]{:S(2)}, u32[]{:S(2)}) collective-permute-start(bf16[8,64,256]{2,1,0:T(8,128)(2,1)} %get-tuple-element.18), channel_id=1, source_target_pairs={{0,2},{2,4},{4,6},{6,0},{1,3},{3,5},{5,7},{7,1},{8,10},{10,12},{12... | collective-permute-start | bytes 786440 | tf_op jit(solution)/shard_map/ppermute | solution.py:21
  130.2 4.8 %copy-start.13 = (bf16[8,64,256]{2,1,0:T(8,128)(2,1)}, bf16[8,64,256]{2,1,0:T(8,128)(2,1)S(1)}, u32[]{:S(2)}) copy-start(bf16[8,64,256]{2,1,0:T(8,128)(2,1)S(1)} %collective-permute-done.10.got2) | copy-start | bytes 786436
  134.2 0.8 copy-start.14
  135.0 0.7 copy-start.15
  138.4 15.9 %all-to-all-start.1 = ((f32[32,1,2048]{2,1,0:T(1,128)}), f32[32,1,2048]{2,1,0:T(1,128)S(1)}, u32[]{:S(2)}, u32[]{:S(2)}) async-start(f32[32,1,2048]{2,1,0:T(1,128)} %get-tuple-element.22), calls=%async_computation.1 | async-start | bytes 524288 | tf_op jit(solution)/shard_map/all_to_all | solution.py:25
  145.5 16.7 %copy-start.5 = (bf16[64,2048]{1,0:T(8,128)(2,1)S(1)}, bf16[64,2048]{1,0:T(8,128)(2,1)}, u32[]{:S(2)}) copy-start(bf16[64,2048]{1,0:T(8,128)(2,1)} %get-tuple-element.21.p0) | copy-start | bytes 786436
  154.3 31.5 %all-to-all-start.4 = ((bf16[16,32,384]{2,1,0:T(8,128)(2,1)}), bf16[16,32,384]{2,1,0:T(8,128)(2,1)S(1)}, u32[]{:S(2)}, u32[]{:S(2)}) async-start(bf16[16,32,384]{2,1,0:T(8,128)(2,1)} %bitcast.11), calls=%async_computation.4 | async-start | bytes 786432 | tf_op jit(solution)/shard_map/all_to_all | solution.py:25
  162.1 9.3 %collective-permute-start.12 = (bf16[64,2048]{1,0:T(8,128)(2,1)S(1)}, bf16[64,2048]{1,0:T(8,128)(2,1)S(1)}, u32[]{:S(2)}, u32[]{:S(2)}) collective-permute-start(bf16[64,2048]{1,0:T(8,128)(2,1)S(1)} %copy-done.5), channel_id=1, source_target_pairs={{0,6},{2,0},{4,2},{6,4},{1,7},{3,1},{5,3},{7,5},{8,14},{10,8},{12,... | collective-permute-start | bytes 786440 | tf_op jit(solution)/shard_map/ppermute | solution.py:21
  165.2 10.7 %collective-permute-start.13 = (bf16[64,2048]{1,0:T(8,128)(2,1)S(1)}, bf16[64,2048]{1,0:T(8,128)(2,1)S(1)}, u32[]{:S(2)}, u32[]{:S(2)}) collective-permute-start(bf16[64,2048]{1,0:T(8,128)(2,1)S(1)} %copy-done.5), channel_id=1, source_target_pairs={{0,4},{2,6},{4,0},{6,2},{1,5},{3,7},{5,1},{7,3},{8,12},{10,14},{12... | collective-permute-start | bytes 786440 | tf_op jit(solution)/shard_map/ppermute | solution.py:21
  168.2 14.2 %collective-permute-start.14 = (bf16[64,2048]{1,0:T(8,128)(2,1)S(1)}, bf16[64,2048]{1,0:T(8,128)(2,1)S(1)}, u32[]{:S(2)}, u32[]{:S(2)}) collective-permute-start(bf16[64,2048]{1,0:T(8,128)(2,1)S(1)} %copy-done.5), channel_id=1, source_target_pairs={{0,2},{2,4},{4,6},{6,0},{1,3},{3,5},{5,7},{7,1},{8,10},{10,12},{12... | collective-permute-start | bytes 786440 | tf_op jit(solution)/shard_map/ppermute | solution.py:21
  171.5 39.7 %copy-start.6 = (bf16[64,2048]{1,0:T(8,128)(2,1)}, bf16[64,2048]{1,0:T(8,128)(2,1)S(1)}, u32[]{:S(2)}) copy-start(bf16[64,2048]{1,0:T(8,128)(2,1)S(1)} %collective-permute-done.12.p1) | copy-start | bytes 786436
  175.9 35.2 %copy-start.7 = (bf16[64,2048]{1,0:T(8,128)(2,1)}, bf16[64,2048]{1,0:T(8,128)(2,1)S(1)}, u32[]{:S(2)}) copy-start(bf16[64,2048]{1,0:T(8,128)(2,1)S(1)} %collective-permute-done.13.p2) | copy-start | bytes 786436
  182.4 0.7 copy-start.8
  183.3 27.8 %collective-permute-start.15 = (bf16[4,64,2048]{2,1,0:T(8,128)(2,1)S(1)}, bf16[4,64,2048]{2,1,0:T(8,128)(2,1)S(1)}, u32[]{:S(2)}, u32[]{:S(2)}) collective-permute-start(bf16[4,64,2048]{2,1,0:T(8,128)(2,1)S(1)} %pad_maximum_fusion), channel_id=1, source_target_pairs={{0,1},{1,0},{2,3},{3,2},{4,5},{5,4},{6,7},{7,6},{8,9},{9,8},{10,11... | collective-permute-start | bytes 3145736 | tf_op jit(solution)/shard_map/ppermute | solution.py:21
  186.6 23.8 %all-to-all-start.2 = ((f32[16,1,2048]{2,1,0:T(1,128)}), f32[16,1,2048]{2,1,0:T(1,128)S(1)}, u32[]{:S(2)}, u32[]{:S(2)}) async-start(f32[16,1,2048]{2,1,0:T(1,128)} %broadcast_in_dim.8), calls=%async_computation.2 | async-start | bytes 262144 | tf_op jit(solution)/shard_map/all_to_all | solution.py:25
  198.1 20.0 %collective-permute-start.16 = (f32[32,384]{1,0:T(8,128)S(1)}, f32[32,384]{1,0:T(8,128)S(1)}, u32[]{:S(2)}, u32[]{:S(2)}) collective-permute-start(f32[32,384]{1,0:T(8,128)S(1)} %convert_reduce_fusion), channel_id=1, source_target_pairs={{0,256},{256,0},{1,257},{257,1},{2,258},{258,2},{3,259},{259,3},{4... | collective-permute-start | bytes 147464 | tf_op jit(solution)/shard_map/ppermute | solution.py:21
  211.1 1.0 copy-start.3
where the time goes:
time: 220 us; the launch traced here: 219 us
  starting transfers between devices  103 us (47%)
  waiting for transfers between devices  54.3 us (25%)
  Pallas kernels  34.7 us (16%)
  blocking collectives  12.1 us (6%)
  local copies, waits for them, and re-layouts  9.87 us (4%)
  other arithmetic  3.7 us (2%)
    ppermute x17, starting transfers between devices, shifted(): return lax.ppermute(v, axis, [(i, (i + by) % n) for i in range(n)])  73.4 us
    ppermute x17, waiting for transfers between devices, shifted(): return lax.ppermute(v, axis, [(i, (i + by) % n) for i in range(n)])  46.4 us
    all_to_all x4, starting transfers between devices, exchanged(): return lax.all_to_all(v, axis, 0, 0, tiled=True)  29.8 us
    all_to_all x1, blocking collectives, exchanged(): return lax.all_to_all(v, axis, 0, 0, tiled=True)  12.1 us
    pallas_call x1, Pallas kernels, work(): pl.pallas_call(grad_kernel, out_shape=(jax.ShapeDtypeStruct((nx, nz, part...  10.3 us
    all_to_all x4, waiting for transfers between devices, exchanged(): return lax.all_to_all(v, axis, 0, 0, tiled=True)  7.86 us
    pallas_call x1, Pallas kernels, work(): pl.pallas_call(prepare_tokens, out_shape=jax.ShapeDtypeStruct((nz, tokens...  6.83 us
    pallas_call x1, Pallas kernels, work(): pl.pallas_call(prepare_cotangent, out_shape=(jax.ShapeDtypeStruct((nz, to...  5.2 us
  transfers between devices with their start and end apart: 21, of which 11 were waited for; matrix products, arithmetic and copies ran while one was open for 4% of the time, Pallas kernels for 11%

commit v1 on v0

--- a/solution.py
+++ b/solution.py
@@ -125,15 +125,46 @@
         sum_ref[k] = sums
 
 
-def place_kernel(at_ref, p0, p1, p2, p3, other_ref, out_ref):
+def place_kernel(at_ref, p0, p1, p2, p3, other_ref, out_ref, sems):
     n = 4
     part = p0.shape[0]
+    copies = []
     for k, piece in enumerate((p0, p1, p2, p3)):
         spot = (at_ref[2] + k) % n
         own = pl.multiple_of((at_ref[1] * n + spot) * part, part)
-        out_ref[pl.ds(own, part), :] = piece[...]
         far = pl.multiple_of(((1 - at_ref[1]) * n + spot) * part, part)
-        out_ref[pl.ds(far, part), :] = other_ref[k]
+        copies.append(
+            pltpu.make_async_copy(piece, out_ref.at[pl.ds(own, part), :], sems.at[2 * k])
+        )
+        copies.append(
+            pltpu.make_async_copy(
+                other_ref.at[k], out_ref.at[pl.ds(far, part), :], sems.at[2 * k + 1]
+            )
+        )
+    for copy in copies:
+        copy.start()
+    for copy in copies:
+        copy.wait()
+
+
+def rows_kernel(at_ref, got_ref, out_ref):
+    ny, nz, rows, _ = got_ref.shape
+    half = rows // 2
+    for d in range(nz):
+        total = got_ref[0, d].astype(F32)
+        for k in range(1, ny):
+            total = total + got_ref[k, d].astype(F32)
+        total = total.astype(BF16)
+        to = (at_ref[0] + d) % nz
+        out_ref[to] = total[:half]
+        out_ref[nz + to] = total[half:]
+
+
+def ring_kernel(got_ref, out_ref):
+    total = got_ref[0].astype(F32)
+    for k in range(1, got_ref.shape[0]):
+        total = total + got_ref[k].astype(F32)
+    out_ref[...] = total
 
 
 def vmem(n):
@@ -147,7 +178,7 @@
     tokens, width = inputs.shape
     rows, units = gate_weight.shape
     cols = width // nz
-    half, part = tokens // 2, tokens // 2 // nx
+    part = tokens // 2 // nx
     gain2 = gain[None]
     at = jnp.stack([zl, c, x]).astype(jnp.int32)
 
@@ -232,21 +263,27 @@
     got = [chip[0]]
     for k in (1, 2, 3):
         got.append(shifted(chip[k], "x", k))
-    first = c * half + x * part
-    xs = lax.dynamic_slice_in_dim(inputs, first, part, axis=0)
-    cs = lax.dynamic_slice_in_dim(cotangent, first, part, axis=0)
     planes = lax.axis_size(PLANE)
+    whole = pl.BlockSpec((nz, part, cols), lambda i, at: (0, 0, 0))
+    own = pl.BlockSpec((part, width), lambda i, at: (at[1] * nx + at[2], 0))
     ig, gain_part = pl.pallas_call(
         finish_kernel,
         out_shape=(
             jax.ShapeDtypeStruct((part, width), BF16),
             jax.ShapeDtypeStruct((planes, 1, width), F32),
         ),
-        in_specs=[pl.BlockSpec(memory_space=pltpu.SMEM)] + vmem(7),
-        out_specs=tuple(vmem(2)),
-        scratch_shapes=[pltpu.VMEM((part, width), BF16)],
+        grid_spec=pltpu.PrefetchScalarGridSpec(
+            num_scalar_prefetch=1,
+            grid=(1,),
+            in_specs=[whole] * 4 + [own, own, pl.BlockSpec((1, width), lambda i, at: (0, 0))],
+            out_specs=(
+                pl.BlockSpec((part, width), lambda i, at: (0, 0)),
+                pl.BlockSpec((planes, 1, width), lambda i, at: (0, 0, 0)),
+            ),
+            scratch_shapes=[pltpu.VMEM((part, width), BF16)],
+        ),
         name="finish",
-    )(at, *got, xs, cs, gain2)
+    )(at, *got, inputs, cotangent, gain2)
     pieces = [ig]
     for k in (1, 2, 3):
         pieces.append(shifted(ig, "x", -k))
@@ -254,8 +291,9 @@
     out = pl.pallas_call(
         place_kernel,
         out_shape=jax.ShapeDtypeStruct((tokens, width), BF16),
-        in_specs=[pl.BlockSpec(memory_space=pltpu.SMEM)] + vmem(5),
-        out_specs=pl.BlockSpec(memory_space=pltpu.VMEM),
+        in_specs=[pl.BlockSpec(memory_space=pltpu.SMEM)] + [pl.BlockSpec(memory_space=pl.ANY)] * 5,
+        out_specs=pl.BlockSpec(memory_space=pl.ANY),
+        scratch_shapes=[pltpu.SemaphoreType.DMA((8,))],
         name="place",
     )(at, *pieces, ig_other)
 
@@ -264,10 +302,21 @@
     gain_gradient = from_all(gain_plane, RING)
     gain_gradient = jnp.sum(gain_gradient, axis=(0, 1))
 
-    dy = jnp.sum(dy.astype(F32), axis=0).astype(BF16)
-    dz = rolled(dy, (nz - zl) % nz).reshape(nz, 2, rows // 2, units).transpose(1, 0, 2, 3)
-    dz = exchanged(dz.reshape(2 * nz, rows // 2, units), RING)
-    own = jnp.sum(dz.astype(F32), axis=0)
+    dz = pl.pallas_call(
+        rows_kernel,
+        out_shape=jax.ShapeDtypeStruct((2 * nz, rows // 2, units), BF16),
+        in_specs=[pl.BlockSpec(memory_space=pltpu.SMEM)] + vmem(1),
+        out_specs=pl.BlockSpec(memory_space=pltpu.VMEM),
+        name="ysum",
+    )(at, dy)
+    dz = exchanged(dz, RING)
+    own = pl.pallas_call(
+        ring_kernel,
+        out_shape=jax.ShapeDtypeStruct((rows // 2, units), F32),
+        in_specs=vmem(1),
+        out_specs=pl.BlockSpec(memory_space=pltpu.VMEM),
+        name="zsum",
+    )(dz)
     far = shifted(own, "rep", 1)
     pair = rolled(jnp.stack([own, far]), rep)
     d_down = pair.reshape(rows, units)

time: 220 us -> 283 us (1.29)
  Pallas kernels: 34.7 us -> 102 us
  starting transfers between devices: 103 us -> 107 us
  local copies, waits for them, and re-layouts: 9.87 us -> 5.93 us
  waiting for transfers between devices: 54.3 us -> 51.1 us
    pallas_call x1, Pallas kernels: 3.02 us -> 65.4 us  [work(): pl.pallas_call(place_kernel, out_shape=jax.ShapeDtypeStruct((tokens, widt...]
    pallas_call x0 -> x2, Pallas kernels: none -> 4.03 us  [the longest x1 2.36 us: work(): pl.pallas_call(rows_kernel, out_shape=jax.ShapeDtypeStruct((2 * nz, rows...]
    dynamic_slice x2 -> x0, local copies, waits for them, and re-layouts: 3.33 us -> none  [the longest x1 1.68 us: work(): cs = lax.dynamic_slice_in_dim(cotangent, first, part, axis=0)]
  transfers between devices with their start and end apart: 21 -> 21, of which waited for: 11 -> 10; matrix products, arithmetic and copies ran while one was open for 4% -> 1% of each run, Pallas kernels for 11% -> 32%
where the time goes in v1:
time: 283 us; the launch traced here: 282 us
  starting transfers between devices  107 us (38%)
  Pallas kernels  102 us (36%)
  waiting for transfers between devices  51.1 us (18%)
  blocking collectives  12.1 us (4%)
  local copies, waits for them, and re-layouts  5.93 us (2%)
  other arithmetic  3.14 us (1%)
    ppermute x17, starting transfers between devices, shifted(): return lax.ppermute(v, axis, [(i, (i + by) % n) for i in range(n)])  75.6 us
    pallas_call x1, Pallas kernels, work(): pl.pallas_call(place_kernel, out_shape=jax.ShapeDtypeStruct((tokens, widt...  65.4 us
    ppermute x17, waiting for transfers between devices, shifted(): return lax.ppermute(v, axis, [(i, (i + by) % n) for i in range(n)])  44.6 us
    all_to_all x4, starting transfers between devices, exchanged(): return lax.all_to_all(v, axis, 0, 0, tiled=True)  31.3 us
    all_to_all x1, blocking collectives, exchanged(): return lax.all_to_all(v, axis, 0, 0, tiled=True)  12.1 us
    pallas_call x1, Pallas kernels, work(): pl.pallas_call(grad_kernel, out_shape=(jax.ShapeDtypeStruct((nx, nz, part...  10.3 us
    pallas_call x1, Pallas kernels, work(): pl.pallas_call(prepare_tokens, out_shape=jax.ShapeDtypeStruct((nz, tokens...  6.83 us
    all_to_all x4, waiting for transfers between devices, exchanged(): return lax.all_to_all(v, axis, 0, 0, tiled=True)  6.51 us
  transfers between devices with their start and end apart: 21, of which 10 were waited for; matrix products, arithmetic and copies ran while one was open for 1% of the time, Pallas kernels for 32%

profile of v1, /device:TPU:1, one launch (start us, length us, event | category | flops | bytes accessed | tf_op | source)
XLA Modules:
  0.0 282.0 jit_solution(5862637583808039742)
XLA Ops:
  0.6 0.9 pad_maximum_fusion.1
  1.5 12.1 %all_to_all.25 = bf16[4,64,1152]{2,1,0:T(8,128)(2,1)S(1)} all-to-all(bf16[4,64,1152]{2,1,0:T(8,128)(2,1)S(1)} %broadcast_in_dim.7), channel_id=1, replica_groups=mesh['rep'=2,'fs_0'=8,'fs_1'=4,'x'=4,'c'=2] {'fs_1'}, dimensions={0} | all-to-all | bytes 1179648 | tf_op jit(solution)/shard_map/all_to_all | solution.py:25
  13.6 5.3 %collective-permute-start.3 = (bf16[256,1152]{1,0:T(8,128)(2,1)S(1)}, bf16[256,1152]{1,0:T(8,128)(2,1)S(1)}, u32[]{:S(2)}, u32[]{:S(2)}) collective-permute-start(bf16[256,1152]{1,0:T(8,128)(2,1)S(1)} %bitcast.12), channel_id=1, source_target_pairs={{0,32},{32,64},{64,96},{96,128},{128,160},{160,192},{192,224},{224... | collective-permute-start | bytes 1769480 | tf_op jit(solution)/shard_map/ppermute | solution.py:21
  18.9 9.5 %collective-permute-start = (bf16[256,1152]{1,0:T(8,128)(2,1)S(1)}, bf16[256,1152]{1,0:T(8,128)(2,1)S(1)}, u32[]{:S(2)}, u32[]{:S(2)}) collective-permute-start(bf16[256,1152]{1,0:T(8,128)(2,1)S(1)} %bitcast.13), channel_id=1, source_target_pairs={{0,480},{32,0},{64,32},{96,64},{128,96},{160,128},{192,160},{224,1... | collective-permute-start | bytes 1769480 | tf_op jit(solution)/shard_map/ppermute | solution.py:21
  28.4 9.7 %collective-permute-done.3.refs_8_ = bf16[256,1152]{1,0:T(8,128)(2,1)S(1)} collective-permute-done((bf16[256,1152]{1,0:T(8,128)(2,1)S(1)}, bf16[256,1152]{1,0:T(8,128)(2,1)S(1)}, u32[]{:S(2)}, u32[]{:S(2)}) %collective-permute-start.3) | collective-permute-done | bytes 589856 | tf_op jit(solution)/shard_map/ppermute | solution.py:21
  38.1 1.9 collective-permute-start.4
  40.0 0.0 collective-permute-done.refs_1_
  40.0 4.6 %collective-permute-start.1 = (bf16[256,1152]{1,0:T(8,128)(2,1)S(1)}, bf16[256,1152]{1,0:T(8,128)(2,1)S(1)}, u32[]{:S(2)}, u32[]{:S(2)}) collective-permute-start(bf16[256,1152]{1,0:T(8,128)(2,1)S(1)} %collective-permute-done.refs_1_), channel_id=1, source_target_pairs={{0,480},{32,0},{64,32},{96,64},{128,96},{160,128},{192,160},{224,1... | collective-permute-start | bytes 1769480 | tf_op jit(solution)/shard_map/ppermute | solution.py:21
  44.6 8.8 %collective-permute-done.4.refs_7_ = bf16[256,1152]{1,0:T(8,128)(2,1)S(1)} collective-permute-done((bf16[256,1152]{1,0:T(8,128)(2,1)S(1)}, bf16[256,1152]{1,0:T(8,128)(2,1)S(1)}, u32[]{:S(2)}, u32[]{:S(2)}) %collective-permute-start.4) | collective-permute-done | bytes 589856 | tf_op jit(solution)/shard_map/ppermute | solution.py:21
  53.4 1.9 collective-permute-start.5
  55.3 0.0 collective-permute-done.1.refs_2_
  55.3 4.6 %collective-permute-start.2 = (bf16[256,1152]{1,0:T(8,128)(2,1)S(1)}, bf16[256,1152]{1,0:T(8,128)(2,1)S(1)}, u32[]{:S(2)}, u32[]{:S(2)}) collective-permute-start(bf16[256,1152]{1,0:T(8,128)(2,1)S(1)} %collective-permute-done.1.refs_2_), channel_id=1, source_target_pairs={{0,480},{32,0},{64,32},{96,64},{128,96},{160,128},{192,160},{224,1... | collective-permute-start | bytes 1769480 | tf_op jit(solution)/shard_map/ppermute | solution.py:21
  59.9 7.9 %collective-permute-done.5.refs_6_ = bf16[256,1152]{1,0:T(8,128)(2,1)S(1)} collective-permute-done((bf16[256,1152]{1,0:T(8,128)(2,1)S(1)}, bf16[256,1152]{1,0:T(8,128)(2,1)S(1)}, u32[]{:S(2)}, u32[]{:S(2)}) %collective-permute-start.5) | collective-permute-done | bytes 589856 | tf_op jit(solution)/shard_map/ppermute | solution.py:21
  67.9 0.8 slice.8
  68.7 1.9 collective-permute-start.6
  70.6 0.0 collective-permute-done.2.refs_3_
  70.6 0.8 slice.9
  71.5 4.6 %collective-permute-start.7 = (bf16[128,1152]{1,0:T(8,128)(2,1)}, bf16[128,1152]{1,0:T(8,128)(2,1)}, u32[]{:S(2)}, u32[]{:S(2)}) collective-permute-start(bf16[128,1152]{1,0:T(8,128)(2,1)} %slice.9), channel_id=1, source_target_pairs={{0,480},{32,0},{64,32},{96,64},{128,96},{160,128},{192,160},{224,1... | collective-permute-start | bytes 884744 | tf_op jit(solution)/shard_map/ppermute | solution.py:21
  76.0 0.6 pad_add_fusion.at_ref
  76.7 5.3 %prepare_c.1 = (bf16[8,512,256]{2,1,0:T(8,128)(2,1)}, bf16[8,256,512]{2,1,0:T(8,128)(2,1)}) custom-call(s32[3]{0:T(128)} %pad_add_fusion.at_ref, bf16[512,2048]{1,0:T(8,128)(2,1)} %c_ref.1, bf16[512,2048]{1,0:T(8,128)(2,1)} %c_ref.1), custom_call_target="tpu_custom_call" | custom-call | tf_op jit(solution)/shard_map/prepare_c/pallas_call | solution.py:213
  82.0 6.8 %prepare_x.1.x_ref = bf16[8,512,256]{2,1,0:T(8,128)(2,1)} custom-call(s32[3]{0:T(128)} %pad_add_fusion.at_ref, bf16[512,2048]{1,0:T(8,128)(2,1)} %x_ref.3, f32[1,2048]{1,0:T(1,128)} %bitcast.22), custom_call_target="tpu_custom_call" | custom-call | tf_op jit(solution)/shard_map/prepare_x/pallas_call | solution.py:199
  88.8 0.0 collective-permute-done.6.refs_4_
  88.8 0.0 collective-permute-done.7.refs_5_
  88.8 10.3 %grad.1 = (bf16[4,8,64,256]{3,2,1,0:T(8,128)(2,1)}, bf16[4,8,64,256]{3,2,1,0:T(8,128)(2,1)}, bf16[512,384]{1,0:T(8,128)(2,1)}) custom-call(bf16[8,512,256]{2,1,0:T(8,128)(2,1)} %prepare_x.1.x_ref, bf16[8,512,256]{2,1,0:T(8,128)(2,1)} %get-tuple-element.14.c_ref, bf16[256,1152]{1,0:T(8,128)(2,1)} %bitcast.14, bf16[256,1152]{1,0:T(8,128)(2,1)} %copy-done.12, ...), custom_call_target="tpu_custom_call" | custom-call | tf_op jit(solution)/shard_map/grad/pallas_call | solution.py:234
  99.1 6.8 %collective-permute-start.8 = (bf16[4,8,64,256]{3,2,1,0:T(8,128)(2,1)}, bf16[4,8,64,256]{3,2,1,0:T(8,128)(2,1)S(1)}, u32[]{:S(2)}, u32[]{:S(2)}) collective-permute-start(bf16[4,8,64,256]{3,2,1,0:T(8,128)(2,1)} %get-tuple-element.16), channel_id=1, source_target_pairs={{0,1},{1,0},{2,3},{3,2},{4,5},{5,4},{6,7},{7,6},{8,9},{9,8},{10,11... | collective-permute-start | bytes 3145736 | tf_op jit(solution)/shard_map/ppermute | solution.py:21
  106.0 4.0 %down.1 = bf16[4,8,64,384]{3,2,1,0:T(8,128)(2,1)} custom-call(bf16[8,256,512]{2,1,0:T(8,128)(2,1)} %get-tuple-element.23.ct_ref, bf16[512,384]{1,0:T(8,128)(2,1)} %get-tuple-element.24.hid_ref), custom_call_target="tpu_custom_call" | custom-call | tf_op jit(solution)/shard_map/down/pallas_call | solution.py:246
  110.0 3.6 %all-to-all-start.3 = ((bf16[4,8,64,384]{3,2,1,0:T(8,128)(2,1)}), bf16[4,8,64,384]{3,2,1,0:T(8,128)(2,1)S(1)}, u32[]{:S(2)}, u32[]{:S(2)}) async-start(bf16[4,8,64,384]{3,2,1,0:T(8,128)(2,1)} %down.1), calls=%async_computation.3 | async-start | bytes 3145728 | tf_op jit(solution)/shard_map/all_to_all | solution.py:25
  113.6 0.0 collective-permute-done.8.theirs_ref
  113.6 1.0 copy-done.6
  114.6 2.6 chip.1
  117.2 3.1 %collective-permute-start.9 = (bf16[8,64,256]{2,1,0:T(8,128)(2,1)}, bf16[8,64,256]{2,1,0:T(8,128)(2,1)S(1)}, u32[]{:S(2)}, u32[]{:S(2)}) collective-permute-start(bf16[8,64,256]{2,1,0:T(8,128)(2,1)} %get-tuple-element.18), channel_id=1, source_target_pairs={{0,2},{2,4},{4,6},{6,0},{1,3},{3,5},{5,7},{7,1},{8,10},{10,12},{12... | collective-permute-start | bytes 786440 | tf_op jit(solution)/shard_map/ppermute | solution.py:21
  120.3 4.4 %collective-permute-start.10 = (bf16[8,64,256]{2,1,0:T(8,128)(2,1)}, bf16[8,64,256]{2,1,0:T(8,128)(2,1)S(1)}, u32[]{:S(2)}, u32[]{:S(2)}) collective-permute-start(bf16[8,64,256]{2,1,0:T(8,128)(2,1)} %get-tuple-element.19), channel_id=1, source_target_pairs={{0,4},{2,6},{4,0},{6,2},{1,5},{3,7},{5,1},{7,3},{8,12},{10,14},{12... | collective-permute-start | bytes 786440 | tf_op jit(solution)/shard_map/ppermute | solution.py:21
  124.6 3.1 %collective-permute-start.11 = (bf16[8,64,256]{2,1,0:T(8,128)(2,1)}, bf16[8,64,256]{2,1,0:T(8,128)(2,1)S(1)}, u32[]{:S(2)}, u32[]{:S(2)}) collective-permute-start(bf16[8,64,256]{2,1,0:T(8,128)(2,1)} %get-tuple-element.20), channel_id=1, source_target_pairs={{0,6},{2,0},{4,2},{6,4},{1,7},{3,1},{5,3},{7,5},{8,14},{10,8},{12,... | collective-permute-start | bytes 786440 | tf_op jit(solution)/shard_map/ppermute | solution.py:21
  127.7 0.6 collective-permute-done.9.got1
  128.3 6.6 %collective-permute-done.10.got2 = bf16[8,64,256]{2,1,0:T(8,128)(2,1)S(1)} collective-permute-done((bf16[8,64,256]{2,1,0:T(8,128)(2,1)}, bf16[8,64,256]{2,1,0:T(8,128)(2,1)S(1)}, u32[]{:S(2)}, u32[]{:S(2)}) %collective-permute-start.10) | collective-permute-done | bytes 262176 | tf_op jit(solution)/shard_map/ppermute | solution.py:21
  134.9 1.2 collective-permute-done.11.got3
  136.1 0.7 copy-done.17
  136.8 3.4 %finish.1 = (bf16[64,2048]{1,0:T(8,128)(2,1)}, f32[32,1,2048]{2,1,0:T(1,128)}) custom-call(s32[3]{0:T(128)} %pad_add_fusion.at_ref, bf16[8,64,256]{2,1,0:T(8,128)(2,1)} %get-tuple-element.17.got0, bf16[8,64,256]{2,1,0:T(8,128)(2,1)} %copy-done.15, bf16[8,64,256]{2,1,0:T(8,128)(2,1)} %copy-done.16, bf16[8,64,256]{2,1,0:T(8,128)(2,1)} %copy-done.17, ...), custom_call_target="tpu_custom_call" | custom-call | tf_op jit(solution)/shard_map/finish/pallas_call | solution.py:269
  140.2 0.0 all-to-all-done.3.got_ref
  140.2 8.4 %all-to-all-start.1 = ((f32[32,1,2048]{2,1,0:T(1,128)}), f32[32,1,2048]{2,1,0:T(1,128)S(1)}, u32[]{:S(2)}, u32[]{:S(2)}) async-start(f32[32,1,2048]{2,1,0:T(1,128)} %get-tuple-element.22), calls=%async_computation.1 | async-start | bytes 524288 | tf_op jit(solution)/shard_map/all_to_all | solution.py:25
  148.7 2.4 ysum.1
  151.0 6.5 %all-to-all-done.1 = f32[32,1,2048]{2,1,0:T(1,128)S(1)} async-done(((f32[32,1,2048]{2,1,0:T(1,128)}), f32[32,1,2048]{2,1,0:T(1,128)S(1)}, u32[]{:S(2)}, u32[]{:S(2)}) %all-to-all-start.1) | async-done | bytes 262176 | tf_op jit(solution)/shard_map/all_to_all | solution.py:25
  157.5 7.8 %all-to-all-start.4 = ((bf16[16,32,384]{2,1,0:T(8,128)(2,1)}), bf16[16,32,384]{2,1,0:T(8,128)(2,1)S(1)}, u32[]{:S(2)}, u32[]{:S(2)}) async-start(bf16[16,32,384]{2,1,0:T(8,128)(2,1)} %ysum.1), calls=%async_computation.4 | async-start | bytes 786432 | tf_op jit(solution)/shard_map/all_to_all | solution.py:25
  165.4 2.4 collective-permute-start.14
  167.8 3.8 %collective-permute-start.13 = (bf16[64,2048]{1,0:T(8,128)(2,1)S(1)}, bf16[64,2048]{1,0:T(8,128)(2,1)S(1)}, u32[]{:S(2)}, u32[]{:S(2)}) collective-permute-start(bf16[64,2048]{1,0:T(8,128)(2,1)S(1)} %copy-done.7), channel_id=1, source_target_pairs={{0,4},{2,6},{4,0},{6,2},{1,5},{3,7},{5,1},{7,3},{8,12},{10,14},{12... | collective-permute-start | bytes 786440 | tf_op jit(solution)/shard_map/ppermute | solution.py:21
  171.5 2.5 collective-permute-start.12
  174.0 2.1 collective-permute-done.14.p3
  176.1 5.2 %collective-permute-done.13.p2 = bf16[64,2048]{1,0:T(8,128)(2,1)S(1)} collective-permute-done((bf16[64,2048]{1,0:T(8,128)(2,1)S(1)}, bf16[64,2048]{1,0:T(8,128)(2,1)S(1)}, u32[]{:S(2)}, u32[]{:S(2)}) %collective-permute-start.13) | collective-permute-done | bytes 262176 | tf_op jit(solution)/shard_map/ppermute | solution.py:21
  181.3 2.5 collective-permute-done.12.p1
  183.8 0.7 copy-done.10
  184.5 0.1 pad_maximum_fusion
  184.6 3.5 %collective-permute-start.15 = (bf16[4,64,2048]{2,1,0:T(8,128)(2,1)S(1)}, bf16[4,64,2048]{2,1,0:T(8,128)(2,1)S(1)}, u32[]{:S(2)}, u32[]{:S(2)}) collective-permute-start(bf16[4,64,2048]{2,1,0:T(8,128)(2,1)S(1)} %pad_maximum_fusion), channel_id=1, source_target_pairs={{0,1},{1,0},{2,3},{3,2},{4,5},{5,4},{6,7},{7,6},{8,9},{9,8},{10,11... | collective-permute-start | bytes 3145736 | tf_op jit(solution)/shard_map/ppermute | solution.py:21
  188.1 0.2 reduce_sum.18
  188.3 0.0 copy-start.2
  188.3 0.8 broadcast_in_dim.8
  189.1 11.5 %all-to-all-start.2 = ((f32[16,1,2048]{2,1,0:T(1,128)}), f32[16,1,2048]{2,1,0:T(1,128)S(1)}, u32[]{:S(2)}, u32[]{:S(2)}) async-start(f32[16,1,2048]{2,1,0:T(1,128)} %broadcast_in_dim.8), calls=%async_computation.2 | async-start | bytes 262144 | tf_op jit(solution)/shard_map/all_to_all | solution.py:25
  200.5 1.7 zsum.1
  202.2 12.0 %collective-permute-start.16 = (f32[32,384]{1,0:T(8,128)}, f32[32,384]{1,0:T(8,128)S(1)}, u32[]{:S(2)}, u32[]{:S(2)}) collective-permute-start(f32[32,384]{1,0:T(8,128)} %zsum.1), channel_id=1, source_target_pairs={{0,256},{256,0},{1,257},{257,1},{2,258},{258,2},{3,259},{259,3},{4... | collective-permute-start | bytes 147464 | tf_op jit(solution)/shard_map/ppermute | solution.py:21
  214.2 0.0 all-to-all-done.2
  214.2 0.7 reduce_sum.19
  214.9 0.0 collective-permute-done.15.other_ref
  214.9 1.0 copy-done.5
  215.9 65.4 %place.1 = bf16[512,2048]{1,0:T(8,128)(2,1)} custom-call(s32[3]{0:T(128)} %pad_add_fusion.at_ref, bf16[64,2048]{1,0:T(8,128)(2,1)} %get-tuple-element.21.p0, bf16[64,2048]{1,0:T(8,128)(2,1)} %copy-done.10, bf16[64,2048]{1,0:T(8,128)(2,1)} %copy-done.9, bf16[64,2048]{1,0:T(8,128)(2,1)} %copy-done.8, bf16[4,64,2048]{2,1,0:T(8,128)(2,1)} %copy-done.5), custom_call_target="tpu_custom_call" | custom-call | tf_op jit(solution)/shard_map/place/pallas_call | solution.py:291
  281.3 0.7 fusion.2
  (36 shorter events, 0.1 us)
Async XLA Ops:
  13.6 68.3 %copy-start.1 = (bf16[4,64,1152]{2,1,0:T(8,128)(2,1)}, bf16[4,64,1152]{2,1,0:T(8,128)(2,1)S(1)}, u32[]{:S(2)}) copy-start(bf16[4,64,1152]{2,1,0:T(8,128)(2,1)S(1)} %all_to_all.25) | copy-start | bytes 1769476
  13.6 24.5 %collective-permute-start.3 = (bf16[256,1152]{1,0:T(8,128)(2,1)S(1)}, bf16[256,1152]{1,0:T(8,128)(2,1)S(1)}, u32[]{:S(2)}, u32[]{:S(2)}) collective-permute-start(bf16[256,1152]{1,0:T(8,128)(2,1)S(1)} %bitcast.12), channel_id=1, source_target_pairs={{0,32},{32,64},{64,96},{96,128},{128,160},{160,192},{192,224},{224... | collective-permute-start | bytes 1769480 | tf_op jit(solution)/shard_map/ppermute | solution.py:21
  18.9 21.1 %collective-permute-start = (bf16[256,1152]{1,0:T(8,128)(2,1)S(1)}, bf16[256,1152]{1,0:T(8,128)(2,1)S(1)}, u32[]{:S(2)}, u32[]{:S(2)}) collective-permute-start(bf16[256,1152]{1,0:T(8,128)(2,1)S(1)} %bitcast.13), channel_id=1, source_target_pairs={{0,480},{32,0},{64,32},{96,64},{128,96},{160,128},{192,160},{224,1... | collective-permute-start | bytes 1769480 | tf_op jit(solution)/shard_map/ppermute | solution.py:21
  38.1 43.9 %copy-start.11 = (bf16[256,1152]{1,0:T(8,128)(2,1)}, bf16[256,1152]{1,0:T(8,128)(2,1)S(1)}, u32[]{:S(2)}) copy-start(bf16[256,1152]{1,0:T(8,128)(2,1)S(1)} %collective-permute-done.3.refs_8_) | copy-start | bytes 1769476
  38.1 15.3 %collective-permute-start.4 = (bf16[256,1152]{1,0:T(8,128)(2,1)S(1)}, bf16[256,1152]{1,0:T(8,128)(2,1)S(1)}, u32[]{:S(2)}, u32[]{:S(2)}) collective-permute-start(bf16[256,1152]{1,0:T(8,128)(2,1)S(1)} %collective-permute-done.3.refs_8_), channel_id=1, source_target_pairs={{0,32},{32,64},{64,96},{96,128},{128,160},{160,192},{192,224},{224... | collective-permute-start | bytes 1769480 | tf_op jit(solution)/shard_map/ppermute | solution.py:21
  40.0 41.9 %copy-start.12 = (bf16[256,1152]{1,0:T(8,128)(2,1)}, bf16[256,1152]{1,0:T(8,128)(2,1)S(1)}, u32[]{:S(2)}) copy-start(bf16[256,1152]{1,0:T(8,128)(2,1)S(1)} %collective-permute-done.refs_1_) | copy-start | bytes 1769476
  40.0 15.3 %collective-permute-start.1 = (bf16[256,1152]{1,0:T(8,128)(2,1)S(1)}, bf16[256,1152]{1,0:T(8,128)(2,1)S(1)}, u32[]{:S(2)}, u32[]{:S(2)}) collective-permute-start(bf16[256,1152]{1,0:T(8,128)(2,1)S(1)} %collective-permute-done.refs_1_), channel_id=1, source_target_pairs={{0,480},{32,0},{64,32},{96,64},{128,96},{160,128},{192,160},{224,1... | collective-permute-start | bytes 1769480 | tf_op jit(solution)/shard_map/ppermute | solution.py:21
  53.4 28.6 %copy-start.13 = (bf16[256,1152]{1,0:T(8,128)(2,1)}, bf16[256,1152]{1,0:T(8,128)(2,1)S(1)}, u32[]{:S(2)}) copy-start(bf16[256,1152]{1,0:T(8,128)(2,1)S(1)} %collective-permute-done.4.refs_7_) | copy-start | bytes 1769476
  53.4 14.4 %collective-permute-start.5 = (bf16[256,1152]{1,0:T(8,128)(2,1)S(1)}, bf16[256,1152]{1,0:T(8,128)(2,1)S(1)}, u32[]{:S(2)}, u32[]{:S(2)}) collective-permute-start(bf16[256,1152]{1,0:T(8,128)(2,1)S(1)} %collective-permute-done.4.refs_7_), channel_id=1, source_target_pairs={{0,32},{32,64},{64,96},{96,128},{128,160},{160,192},{192,224},{224... | collective-permute-start | bytes 1769480 | tf_op jit(solution)/shard_map/ppermute | solution.py:21
  55.3 15.3 %copy-start.14 = (bf16[256,1152]{1,0:T(8,128)(2,1)}, bf16[256,1152]{1,0:T(8,128)(2,1)S(1)}, u32[]{:S(2)}) copy-start(bf16[256,1152]{1,0:T(8,128)(2,1)S(1)} %collective-permute-done.1.refs_2_) | copy-start | bytes 1769476
  55.3 15.3 %collective-permute-start.2 = (bf16[256,1152]{1,0:T(8,128)(2,1)S(1)}, bf16[256,1152]{1,0:T(8,128)(2,1)S(1)}, u32[]{:S(2)}, u32[]{:S(2)}) collective-permute-start(bf16[256,1152]{1,0:T(8,128)(2,1)S(1)} %collective-permute-done.1.refs_2_), channel_id=1, source_target_pairs={{0,480},{32,0},{64,32},{96,64},{128,96},{160,128},{192,160},{224,1... | collective-permute-start | bytes 1769480 | tf_op jit(solution)/shard_map/ppermute | solution.py:21
  67.9 14.1 %copy-start.3 = (bf16[256,1152]{1,0:T(8,128)(2,1)}, bf16[256,1152]{1,0:T(8,128)(2,1)S(1)}, u32[]{:S(2)}) copy-start(bf16[256,1152]{1,0:T(8,128)(2,1)S(1)} %collective-permute-done.5.refs_6_) | copy-start | bytes 1769476
  68.7 20.2 %collective-permute-start.6 = (bf16[128,1152]{1,0:T(8,128)(2,1)}, bf16[128,1152]{1,0:T(8,128)(2,1)}, u32[]{:S(2)}, u32[]{:S(2)}) collective-permute-start(bf16[128,1152]{1,0:T(8,128)(2,1)} %slice.8), channel_id=1, source_target_pairs={{0,32},{32,64},{64,96},{96,128},{128,160},{160,192},{192,224},{224... | collective-permute-start | bytes 884744 | tf_op jit(solution)/shard_map/ppermute | solution.py:21
  70.6 11.4 %copy-start.4 = (bf16[256,1152]{1,0:T(8,128)(2,1)}, bf16[256,1152]{1,0:T(8,128)(2,1)S(1)}, u32[]{:S(2)}) copy-start(bf16[256,1152]{1,0:T(8,128)(2,1)S(1)} %collective-permute-done.2.refs_3_) | copy-start | bytes 1769476
  71.5 17.4 %collective-permute-start.7 = (bf16[128,1152]{1,0:T(8,128)(2,1)}, bf16[128,1152]{1,0:T(8,128)(2,1)}, u32[]{:S(2)}, u32[]{:S(2)}) collective-permute-start(bf16[128,1152]{1,0:T(8,128)(2,1)} %slice.9), channel_id=1, source_target_pairs={{0,480},{32,0},{64,32},{96,64},{128,96},{160,128},{192,160},{224,1... | collective-permute-start | bytes 884744 | tf_op jit(solution)/shard_map/ppermute | solution.py:21
  99.1 14.4 %collective-permute-start.8 = (bf16[4,8,64,256]{3,2,1,0:T(8,128)(2,1)}, bf16[4,8,64,256]{3,2,1,0:T(8,128)(2,1)S(1)}, u32[]{:S(2)}, u32[]{:S(2)}) collective-permute-start(bf16[4,8,64,256]{3,2,1,0:T(8,128)(2,1)} %get-tuple-element.16), channel_id=1, source_target_pairs={{0,1},{1,0},{2,3},{3,2},{4,5},{5,4},{6,7},{7,6},{8,9},{9,8},{10,11... | collective-permute-start | bytes 3145736 | tf_op jit(solution)/shard_map/ppermute | solution.py:21
  110.0 30.2 %all-to-all-start.3 = ((bf16[4,8,64,384]{3,2,1,0:T(8,128)(2,1)}), bf16[4,8,64,384]{3,2,1,0:T(8,128)(2,1)S(1)}, u32[]{:S(2)}, u32[]{:S(2)}) async-start(bf16[4,8,64,384]{3,2,1,0:T(8,128)(2,1)} %down.1), calls=%async_computation.3 | async-start | bytes 3145728 | tf_op jit(solution)/shard_map/all_to_all | solution.py:25
  113.6 1.0 copy-start.6
  117.2 11.2 %collective-permute-start.9 = (bf16[8,64,256]{2,1,0:T(8,128)(2,1)}, bf16[8,64,256]{2,1,0:T(8,128)(2,1)S(1)}, u32[]{:S(2)}, u32[]{:S(2)}) collective-permute-start(bf16[8,64,256]{2,1,0:T(8,128)(2,1)} %get-tuple-element.18), channel_id=1, source_target_pairs={{0,2},{2,4},{4,6},{6,0},{1,3},{3,5},{5,7},{7,1},{8,10},{10,12},{12... | collective-permute-start | bytes 786440 | tf_op jit(solution)/shard_map/ppermute | solution.py:21
  120.3 14.6 %collective-permute-start.10 = (bf16[8,64,256]{2,1,0:T(8,128)(2,1)}, bf16[8,64,256]{2,1,0:T(8,128)(2,1)S(1)}, u32[]{:S(2)}, u32[]{:S(2)}) collective-permute-start(bf16[8,64,256]{2,1,0:T(8,128)(2,1)} %get-tuple-element.19), channel_id=1, source_target_pairs={{0,4},{2,6},{4,0},{6,2},{1,5},{3,7},{5,1},{7,3},{8,12},{10,14},{12... | collective-permute-start | bytes 786440 | tf_op jit(solution)/shard_map/ppermute | solution.py:21
  124.6 11.5 %collective-permute-start.11 = (bf16[8,64,256]{2,1,0:T(8,128)(2,1)}, bf16[8,64,256]{2,1,0:T(8,128)(2,1)S(1)}, u32[]{:S(2)}, u32[]{:S(2)}) collective-permute-start(bf16[8,64,256]{2,1,0:T(8,128)(2,1)} %get-tuple-element.20), channel_id=1, source_target_pairs={{0,6},{2,0},{4,2},{6,4},{1,7},{3,1},{5,3},{7,5},{8,14},{10,8},{12,... | collective-permute-start | bytes 786440 | tf_op jit(solution)/shard_map/ppermute | solution.py:21
  128.3 7.8 %copy-start.15 = (bf16[8,64,256]{2,1,0:T(8,128)(2,1)}, bf16[8,64,256]{2,1,0:T(8,128)(2,1)S(1)}, u32[]{:S(2)}) copy-start(bf16[8,64,256]{2,1,0:T(8,128)(2,1)S(1)} %collective-permute-done.9.got1) | copy-start | bytes 786436
  134.9 1.2 copy-start.16
  136.1 0.7 copy-start.17
  140.2 25.1 %copy-start.7 = (bf16[64,2048]{1,0:T(8,128)(2,1)S(1)}, bf16[64,2048]{1,0:T(8,128)(2,1)}, u32[]{:S(2)}) copy-start(bf16[64,2048]{1,0:T(8,128)(2,1)} %get-tuple-element.21.p0) | copy-start | bytes 786436
  140.2 8.5 %copy-start = (bf16[4,8,64,384]{3,2,1,0:T(8,128)(2,1)}, bf16[4,8,64,384]{3,2,1,0:T(8,128)(2,1)S(1)}, u32[]{:S(2)}) copy-start(bf16[4,8,64,384]{3,2,1,0:T(8,128)(2,1)S(1)} %all-to-all-done.3.got_ref) | copy-start | bytes 4718596
  140.2 17.3 %all-to-all-start.1 = ((f32[32,1,2048]{2,1,0:T(1,128)}), f32[32,1,2048]{2,1,0:T(1,128)S(1)}, u32[]{:S(2)}, u32[]{:S(2)}) async-start(f32[32,1,2048]{2,1,0:T(1,128)} %get-tuple-element.22), calls=%async_computation.1 | async-start | bytes 524288 | tf_op jit(solution)/shard_map/all_to_all | solution.py:25
  157.5 30.7 %all-to-all-start.4 = ((bf16[16,32,384]{2,1,0:T(8,128)(2,1)}), bf16[16,32,384]{2,1,0:T(8,128)(2,1)S(1)}, u32[]{:S(2)}, u32[]{:S(2)}) async-start(bf16[16,32,384]{2,1,0:T(8,128)(2,1)} %ysum.1), calls=%async_computation.4 | async-start | bytes 786432 | tf_op jit(solution)/shard_map/all_to_all | solution.py:25
  165.4 10.8 %collective-permute-start.14 = (bf16[64,2048]{1,0:T(8,128)(2,1)S(1)}, bf16[64,2048]{1,0:T(8,128)(2,1)S(1)}, u32[]{:S(2)}, u32[]{:S(2)}) collective-permute-start(bf16[64,2048]{1,0:T(8,128)(2,1)S(1)} %copy-done.7), channel_id=1, source_target_pairs={{0,2},{2,4},{4,6},{6,0},{1,3},{3,5},{5,7},{7,1},{8,10},{10,12},{12... | collective-permute-start | bytes 786440 | tf_op jit(solution)/shard_map/ppermute | solution.py:21
  167.8 13.6 %collective-permute-start.13 = (bf16[64,2048]{1,0:T(8,128)(2,1)S(1)}, bf16[64,2048]{1,0:T(8,128)(2,1)S(1)}, u32[]{:S(2)}, u32[]{:S(2)}) collective-permute-start(bf16[64,2048]{1,0:T(8,128)(2,1)S(1)} %copy-done.7), channel_id=1, source_target_pairs={{0,4},{2,6},{4,0},{6,2},{1,5},{3,7},{5,1},{7,3},{8,12},{10,14},{12... | collective-permute-start | bytes 786440 | tf_op jit(solution)/shard_map/ppermute | solution.py:21
  171.5 12.3 %collective-permute-start.12 = (bf16[64,2048]{1,0:T(8,128)(2,1)S(1)}, bf16[64,2048]{1,0:T(8,128)(2,1)S(1)}, u32[]{:S(2)}, u32[]{:S(2)}) collective-permute-start(bf16[64,2048]{1,0:T(8,128)(2,1)S(1)} %copy-done.7), channel_id=1, source_target_pairs={{0,6},{2,0},{4,2},{6,4},{1,7},{3,1},{5,3},{7,5},{8,14},{10,8},{12,... | collective-permute-start | bytes 786440 | tf_op jit(solution)/shard_map/ppermute | solution.py:21
  176.1 38.8 %copy-start.8 = (bf16[64,2048]{1,0:T(8,128)(2,1)}, bf16[64,2048]{1,0:T(8,128)(2,1)S(1)}, u32[]{:S(2)}) copy-start(bf16[64,2048]{1,0:T(8,128)(2,1)S(1)} %collective-permute-done.14.p3) | copy-start | bytes 786436
  181.3 33.6 %copy-start.9 = (bf16[64,2048]{1,0:T(8,128)(2,1)}, bf16[64,2048]{1,0:T(8,128)(2,1)S(1)}, u32[]{:S(2)}) copy-start(bf16[64,2048]{1,0:T(8,128)(2,1)S(1)} %collective-permute-done.13.p2) | copy-start | bytes 786436
  183.8 0.7 copy-start.10
  184.6 30.3 %collective-permute-start.15 = (bf16[4,64,2048]{2,1,0:T(8,128)(2,1)S(1)}, bf16[4,64,2048]{2,1,0:T(8,128)(2,1)S(1)}, u32[]{:S(2)}, u32[]{:S(2)}) collective-permute-start(bf16[4,64,2048]{2,1,0:T(8,128)(2,1)S(1)} %pad_maximum_fusion), channel_id=1, source_target_pairs={{0,1},{1,0},{2,3},{3,2},{4,5},{5,4},{6,7},{7,6},{8,9},{9,8},{10,11... | collective-permute-start | bytes 3145736 | tf_op jit(solution)/shard_map/ppermute | solution.py:21
  188.3 12.2 %copy-start.2 = (bf16[16,32,384]{2,1,0:T(8,128)(2,1)}, bf16[16,32,384]{2,1,0:T(8,128)(2,1)S(1)}, u32[]{:S(2)}) copy-start(bf16[16,32,384]{2,1,0:T(8,128)(2,1)S(1)} %all-to-all-done.4.got_ref) | copy-start | bytes 1179652
  189.1 25.1 %all-to-all-start.2 = ((f32[16,1,2048]{2,1,0:T(1,128)}), f32[16,1,2048]{2,1,0:T(1,128)S(1)}, u32[]{:S(2)}, u32[]{:S(2)}) async-start(f32[16,1,2048]{2,1,0:T(1,128)} %broadcast_in_dim.8), calls=%async_computation.2 | async-start | bytes 262144 | tf_op jit(solution)/shard_map/all_to_all | solution.py:25
  202.2 79.1 %collective-permute-start.16 = (f32[32,384]{1,0:T(8,128)}, f32[32,384]{1,0:T(8,128)S(1)}, u32[]{:S(2)}, u32[]{:S(2)}) collective-permute-start(f32[32,384]{1,0:T(8,128)} %zsum.1), channel_id=1, source_target_pairs={{0,256},{256,0},{1,257},{257,1},{2,258},{258,2},{3,259},{259,3},{4... | collective-permute-start | bytes 147464 | tf_op jit(solution)/shard_map/ppermute | solution.py:21
  214.9 66.4 %copy-start.18 = (f32[32,384]{1,0:T(8,128)S(1)}, f32[32,384]{1,0:T(8,128)}, u32[]{:S(2)}) copy-start(f32[32,384]{1,0:T(8,128)} %zsum.1) | copy-start | bytes 147460
  214.9 1.0 copy-start.5

commit v2 on v0

--- a/solution.py
+++ b/solution.py
@@ -10,7 +10,6 @@
 REP_FS = ("rep", "fs_0", "fs_1")
 TP = ("x", "c")
 RING = ("rep", "fs_0")
-PLANE = ("fs_1", "x", "c")
 EPS = 1e-06
 F32 = jnp.float32
 BF16 = jnp.bfloat16
@@ -105,7 +104,7 @@
         out_ref[...] = (mine_ref[k].astype(F32) + theirs_ref[k].astype(F32)).astype(BF16)
 
 
-def finish_kernel(at_ref, got0, got1, got2, got3, x_ref, c_ref, gain_ref, out_ref, sum_ref, dn_ref):
+def finish_kernel(at_ref, got0, got1, got2, got3, x_ref, c_ref, gain_ref, out_ref, dn_ref):
     nz, _, cols = got0.shape
     for d in range(nz):
         own = pl.ds(pl.multiple_of(((at_ref[0] + d) % nz) * cols, cols), cols)
@@ -120,20 +119,34 @@
     sums = jnp.sum(dn * xhat, axis=0, keepdims=True)
     gs = gain_ref[...] * dn
     m = jnp.mean(gs * xhat, axis=-1, keepdims=True)
-    out_ref[...] = (c_ref[...].astype(F32) + inv * (gs - xhat * m)).astype(BF16)
-    for k in range(sum_ref.shape[0]):
-        sum_ref[k] = sums
+    part = v.shape[0]
+    out_ref[:part] = (c_ref[...].astype(F32) + inv * (gs - xhat * m)).astype(BF16)
+    high = sums.astype(BF16)
+    left = sums - high.astype(F32)
+    mid = left.astype(BF16)
+    low = (left - mid.astype(F32)).astype(BF16)
+    none = jnp.zeros((out_ref.shape[0] - part - 3, v.shape[1]), BF16)
+    out_ref[part:] = jnp.concatenate([high, mid, low, none], axis=0)
 
 
 def place_kernel(at_ref, p0, p1, p2, p3, other_ref, out_ref):
     n = 4
-    part = p0.shape[0]
+    part = out_ref.shape[0] // (2 * n)
     for k, piece in enumerate((p0, p1, p2, p3)):
         spot = (at_ref[2] + k) % n
         own = pl.multiple_of((at_ref[1] * n + spot) * part, part)
-        out_ref[pl.ds(own, part), :] = piece[...]
         far = pl.multiple_of(((1 - at_ref[1]) * n + spot) * part, part)
-        out_ref[pl.ds(far, part), :] = other_ref[k]
+        out_ref[pl.ds(own, part), :] = piece[:part]
+        out_ref[pl.ds(far, part), :] = other_ref[k, :part]
+
+
+def gain_kernel(p0, p1, p2, p3, other_ref, out_ref):
+    total = jnp.zeros(p0.shape, F32)
+    for k, piece in enumerate((p0, p1, p2, p3)):
+        total = total + (piece[...].astype(F32) + other_ref[k].astype(F32))
+    total = jnp.sum(total, axis=0, keepdims=True)
+    for k in range(out_ref.shape[0]):
+        out_ref[k] = total
 
 
 def vmem(n):
@@ -147,7 +160,7 @@
     tokens, width = inputs.shape
     rows, units = gate_weight.shape
     cols = width // nz
-    half, part = tokens // 2, tokens // 2 // nx
+    part = tokens // 2 // nx
     gain2 = gain[None]
     at = jnp.stack([zl, c, x]).astype(jnp.int32)
 
@@ -232,21 +245,21 @@
     got = [chip[0]]
     for k in (1, 2, 3):
         got.append(shifted(chip[k], "x", k))
-    first = c * half + x * part
-    xs = lax.dynamic_slice_in_dim(inputs, first, part, axis=0)
-    cs = lax.dynamic_slice_in_dim(cotangent, first, part, axis=0)
-    planes = lax.axis_size(PLANE)
-    ig, gain_part = pl.pallas_call(
+    whole = pl.BlockSpec((nz, part, cols), lambda i, at: (0, 0, 0))
+    own = pl.BlockSpec((part, width), lambda i, at: (at[1] * nx + at[2], 0))
+    longer = part + 8
+    ig = pl.pallas_call(
         finish_kernel,
-        out_shape=(
-            jax.ShapeDtypeStruct((part, width), BF16),
-            jax.ShapeDtypeStruct((planes, 1, width), F32),
-        ),
-        in_specs=[pl.BlockSpec(memory_space=pltpu.SMEM)] + vmem(7),
-        out_specs=tuple(vmem(2)),
-        scratch_shapes=[pltpu.VMEM((part, width), BF16)],
+        out_shape=jax.ShapeDtypeStruct((longer, width), BF16),
+        grid_spec=pltpu.PrefetchScalarGridSpec(
+            num_scalar_prefetch=1,
+            grid=(1,),
+            in_specs=[whole] * 4 + [own, own, pl.BlockSpec((1, width), lambda i, at: (0, 0))],
+            out_specs=pl.BlockSpec((longer, width), lambda i, at: (0, 0)),
+            scratch_shapes=[pltpu.VMEM((part, width), BF16)],
+        ),
         name="finish",
-    )(at, *got, xs, cs, gain2)
+    )(at, *got, inputs, cotangent, gain2)
     pieces = [ig]
     for k in (1, 2, 3):
         pieces.append(shifted(ig, "x", -k))
@@ -259,14 +272,24 @@
         name="place",
     )(at, *pieces, ig_other)
 
-    gain_plane = exchanged(gain_part, PLANE)
-    gain_plane = jnp.sum(gain_plane, axis=0)
-    gain_gradient = from_all(gain_plane, RING)
-    gain_gradient = jnp.sum(gain_gradient, axis=(0, 1))
+    groups = lax.axis_size(REP_FS)
+    last = part // 8
+    tail = pl.BlockSpec((8, width), lambda i: (last, 0))
+    gain_chip = pl.pallas_call(
+        gain_kernel,
+        out_shape=jax.ShapeDtypeStruct((groups, 1, width), F32),
+        grid=(1,),
+        in_specs=[tail] * 4 + [pl.BlockSpec((4, 8, width), lambda i: (0, last, 0))],
+        out_specs=pl.BlockSpec((groups, 1, width), lambda i: (0, 0, 0)),
+        name="gain",
+    )(*pieces, ig_other)
+    gain_all = exchanged(gain_chip, REP_FS)
+    gain_gradient = jnp.sum(gain_all, axis=(0, 1))
 
     dy = jnp.sum(dy.astype(F32), axis=0).astype(BF16)
     dz = rolled(dy, (nz - zl) % nz).reshape(nz, 2, rows // 2, units).transpose(1, 0, 2, 3)
-    dz = exchanged(dz.reshape(2 * nz, rows // 2, units), RING)
+    dz = dz.reshape(2 * nz, rows // 2, units)
+    dz = exchanged(dz, RING)
     own = jnp.sum(dz.astype(F32), axis=0)
     far = shifted(own, "rep", 1)
     pair = rolled(jnp.stack([own, far]), rep)

time: 220 us -> 235 us (1.068)
  the two profiles are of different devices: /device:TPU:1 before, /device:TPU:8 now
where the time goes in v2:
time: 235 us; the launch traced here: 234 us
  starting transfers between devices  94.4 us (40%)
  waiting for transfers between devices  76.6 us (33%)
  Pallas kernels  37.1 us (16%)
  blocking collectives  15.2 us (6%)
  local copies, waits for them, and re-layouts  5.87 us (2%)
  other arithmetic  3.83 us (2%)
    ppermute x17, starting transfers between devices, shifted(): return lax.ppermute(v, axis, [(i, (i + by) % n) for i in range(n)])  71.5 us
    ppermute x17, waiting for transfers between devices, shifted(): return lax.ppermute(v, axis, [(i, (i + by) % n) for i in range(n)])  62.8 us
    all_to_all x3, starting transfers between devices, exchanged(): return lax.all_to_all(v, axis, 0, 0, tiled=True)  22.9 us
    all_to_all x1, blocking collectives, exchanged(): return lax.all_to_all(v, axis, 0, 0, tiled=True)  15.2 us
    all_to_all x3, waiting for transfers between devices, exchanged(): return lax.all_to_all(v, axis, 0, 0, tiled=True)  13.8 us
    pallas_call x1, Pallas kernels, work(): pl.pallas_call(grad_kernel, out_shape=(jax.ShapeDtypeStruct((nx, nz, part...  10.3 us
    pallas_call x1, Pallas kernels, work(): pl.pallas_call(prepare_tokens, out_shape=jax.ShapeDtypeStruct((nz, tokens...  6.83 us
    pallas_call x1, Pallas kernels, work(): pl.pallas_call(prepare_cotangent, out_shape=(jax.ShapeDtypeStruct((nz, to...  5.2 us
  transfers between devices with their start and end apart: 20, of which 9 were waited for; matrix products, arithmetic and copies ran while one was open for 2% of the time, Pallas kernels for 11%

profile of v2, /device:TPU:8, one launch (start us, length us, event | category | flops | bytes accessed | tf_op | source)
XLA Modules:
  0.0 234.1 jit_solution(9287598177025705978)
XLA Ops:
  0.6 0.9 pad_maximum_fusion.1
  1.5 15.2 %all_to_all.20 = bf16[4,64,1152]{2,1,0:T(8,128)(2,1)S(1)} all-to-all(bf16[4,64,1152]{2,1,0:T(8,128)(2,1)S(1)} %broadcast_in_dim.10), channel_id=1, replica_groups=mesh['rep'=2,'fs_0'=8,'fs_1'=4,'x'=4,'c'=2] {'fs_1'}, dimensions={0} | all-to-all | bytes 1179648 | tf_op jit(solution)/shard_map/all_to_all | solution.py:24
  16.7 2.1 collective-permute-start.3
  18.8 9.5 %collective-permute-start = (bf16[256,1152]{1,0:T(8,128)(2,1)S(1)}, bf16[256,1152]{1,0:T(8,128)(2,1)S(1)}, u32[]{:S(2)}, u32[]{:S(2)}) collective-permute-start(bf16[256,1152]{1,0:T(8,128)(2,1)S(1)} %bitcast.21), channel_id=1, source_target_pairs={{0,480},{32,0},{64,32},{96,64},{128,96},{160,128},{192,160},{224,1... | collective-permute-start | bytes 1769480 | tf_op jit(solution)/shard_map/ppermute | solution.py:20
  28.3 10.0 %collective-permute-done.3.refs_8_ = bf16[256,1152]{1,0:T(8,128)(2,1)S(1)} collective-permute-done((bf16[256,1152]{1,0:T(8,128)(2,1)S(1)}, bf16[256,1152]{1,0:T(8,128)(2,1)S(1)}, u32[]{:S(2)}, u32[]{:S(2)}) %collective-permute-start.3) | collective-permute-done | bytes 589856 | tf_op jit(solution)/shard_map/ppermute | solution.py:20
  38.3 1.9 collective-permute-start.4
  40.2 0.0 collective-permute-done.refs_1_
  40.2 5.1 %collective-permute-start.1 = (bf16[256,1152]{1,0:T(8,128)(2,1)S(1)}, bf16[256,1152]{1,0:T(8,128)(2,1)S(1)}, u32[]{:S(2)}, u32[]{:S(2)}) collective-permute-start(bf16[256,1152]{1,0:T(8,128)(2,1)S(1)} %collective-permute-done.refs_1_), channel_id=1, source_target_pairs={{0,480},{32,0},{64,32},{96,64},{128,96},{160,128},{192,160},{224,1... | collective-permute-start | bytes 1769480 | tf_op jit(solution)/shard_map/ppermute | solution.py:20
  45.3 9.1 %collective-permute-done.4.refs_7_ = bf16[256,1152]{1,0:T(8,128)(2,1)S(1)} collective-permute-done((bf16[256,1152]{1,0:T(8,128)(2,1)S(1)}, bf16[256,1152]{1,0:T(8,128)(2,1)S(1)}, u32[]{:S(2)}, u32[]{:S(2)}) %collective-permute-start.4) | collective-permute-done | bytes 589856 | tf_op jit(solution)/shard_map/ppermute | solution.py:20
  54.4 1.9 collective-permute-start.5
  56.3 0.0 collective-permute-done.1.refs_2_
  56.4 5.1 %collective-permute-start.2 = (bf16[256,1152]{1,0:T(8,128)(2,1)S(1)}, bf16[256,1152]{1,0:T(8,128)(2,1)S(1)}, u32[]{:S(2)}, u32[]{:S(2)}) collective-permute-start(bf16[256,1152]{1,0:T(8,128)(2,1)S(1)} %collective-permute-done.1.refs_2_), channel_id=1, source_target_pairs={{0,480},{32,0},{64,32},{96,64},{128,96},{160,128},{192,160},{224,1... | collective-permute-start | bytes 1769480 | tf_op jit(solution)/shard_map/ppermute | solution.py:20
  61.5 8.2 %collective-permute-done.5.refs_6_ = bf16[256,1152]{1,0:T(8,128)(2,1)S(1)} collective-permute-done((bf16[256,1152]{1,0:T(8,128)(2,1)S(1)}, bf16[256,1152]{1,0:T(8,128)(2,1)S(1)}, u32[]{:S(2)}, u32[]{:S(2)}) %collective-permute-start.5) | collective-permute-done | bytes 589856 | tf_op jit(solution)/shard_map/ppermute | solution.py:20
  69.7 0.8 slice.8
  70.5 1.9 collective-permute-start.6
  72.4 0.0 collective-permute-done.2.refs_3_
  72.5 0.8 slice.9
  73.3 5.1 %collective-permute-start.7 = (bf16[128,1152]{1,0:T(8,128)(2,1)}, bf16[128,1152]{1,0:T(8,128)(2,1)}, u32[]{:S(2)}, u32[]{:S(2)}) collective-permute-start(bf16[128,1152]{1,0:T(8,128)(2,1)} %slice.9), channel_id=1, source_target_pairs={{0,480},{32,0},{64,32},{96,64},{128,96},{160,128},{192,160},{224,1... | collective-permute-start | bytes 884744 | tf_op jit(solution)/shard_map/ppermute | solution.py:20
  78.4 0.6 pad_add_fusion.at_ref
  79.0 5.2 %prepare_c.1 = (bf16[8,512,256]{2,1,0:T(8,128)(2,1)}, bf16[8,256,512]{2,1,0:T(8,128)(2,1)}) custom-call(s32[3]{0:T(128)} %pad_add_fusion.at_ref, bf16[512,2048]{1,0:T(8,128)(2,1)} %c_ref.1, bf16[512,2048]{1,0:T(8,128)(2,1)} %c_ref.1), custom_call_target="tpu_custom_call" | custom-call | tf_op jit(solution)/shard_map/prepare_c/pallas_call | solution.py:195
  84.3 6.8 %prepare_x.1.x_ref = bf16[8,512,256]{2,1,0:T(8,128)(2,1)} custom-call(s32[3]{0:T(128)} %pad_add_fusion.at_ref, bf16[512,2048]{1,0:T(8,128)(2,1)} %x_ref.3, f32[1,2048]{1,0:T(1,128)} %bitcast.27), custom_call_target="tpu_custom_call" | custom-call | tf_op jit(solution)/shard_map/prepare_x/pallas_call | solution.py:181
  91.1 0.0 collective-permute-done.7.refs_5_
  91.1 10.3 %grad.1 = (bf16[4,8,64,256]{3,2,1,0:T(8,128)(2,1)}, bf16[4,8,64,256]{3,2,1,0:T(8,128)(2,1)}, bf16[512,384]{1,0:T(8,128)(2,1)}) custom-call(bf16[8,512,256]{2,1,0:T(8,128)(2,1)} %prepare_x.1.x_ref, bf16[8,512,256]{2,1,0:T(8,128)(2,1)} %get-tuple-element.12.c_ref, bf16[256,1152]{1,0:T(8,128)(2,1)} %bitcast.22, bf16[256,1152]{1,0:T(8,128)(2,1)} %copy-done.10, ...), custom_call_target="tpu_custom_call" | custom-call | tf_op jit(solution)/shard_map/grad/pallas_call | solution.py:216
  101.4 1.9 collective-permute-start.8
  103.3 4.0 %down.1 = bf16[4,8,64,384]{3,2,1,0:T(8,128)(2,1)} custom-call(bf16[8,256,512]{2,1,0:T(8,128)(2,1)} %get-tuple-element.19.ct_ref, bf16[512,384]{1,0:T(8,128)(2,1)} %get-tuple-element.20.hid_ref), custom_call_target="tpu_custom_call" | custom-call | tf_op jit(solution)/shard_map/down/pallas_call | solution.py:228
  107.3 5.0 %all-to-all-start.2 = ((bf16[4,8,64,384]{3,2,1,0:T(8,128)(2,1)}), bf16[4,8,64,384]{3,2,1,0:T(8,128)(2,1)S(1)}, u32[]{:S(2)}, u32[]{:S(2)}) async-start(bf16[4,8,64,384]{3,2,1,0:T(8,128)(2,1)} %down.1), calls=%async_computation.2 | async-start | bytes 3145728 | tf_op jit(solution)/shard_map/all_to_all | solution.py:24
  112.3 0.0 collective-permute-done.8.theirs_ref
  112.3 1.0 copy-done.8
  113.3 2.6 %chip.1 = (bf16[8,64,256]{2,1,0:T(8,128)(2,1)}, bf16[8,64,256]{2,1,0:T(8,128)(2,1)}, bf16[8,64,256]{2,1,0:T(8,128)(2,1)}, bf16[8,64,256]{2,1,0:T(8,128)(2,1)}) custom-call(bf16[4,8,64,256]{3,2,1,0:T(8,128)(2,1)} %get-tuple-element.13.mine_ref, bf16[4,8,64,256]{3,2,1,0:T(8,128)(2,1)} %copy-done.8), custom_call_target="tpu_custom_call" | custom-call | tf_op jit(solution)/shard_map/chip/pallas_call | solution.py:238
  115.9 3.4 %collective-permute-start.9 = (bf16[8,64,256]{2,1,0:T(8,128)(2,1)}, bf16[8,64,256]{2,1,0:T(8,128)(2,1)S(1)}, u32[]{:S(2)}, u32[]{:S(2)}) collective-permute-start(bf16[8,64,256]{2,1,0:T(8,128)(2,1)} %get-tuple-element.16), channel_id=1, source_target_pairs={{0,2},{2,4},{4,6},{6,0},{1,3},{3,5},{5,7},{7,1},{8,10},{10,12},{12... | collective-permute-start | bytes 786440 | tf_op jit(solution)/shard_map/ppermute | solution.py:20
  119.3 4.6 %collective-permute-start.10 = (bf16[8,64,256]{2,1,0:T(8,128)(2,1)}, bf16[8,64,256]{2,1,0:T(8,128)(2,1)S(1)}, u32[]{:S(2)}, u32[]{:S(2)}) collective-permute-start(bf16[8,64,256]{2,1,0:T(8,128)(2,1)} %get-tuple-element.17), channel_id=1, source_target_pairs={{0,4},{2,6},{4,0},{6,2},{1,5},{3,7},{5,1},{7,3},{8,12},{10,14},{12... | collective-permute-start | bytes 786440 | tf_op jit(solution)/shard_map/ppermute | solution.py:20
  123.9 3.3 %collective-permute-start.11 = (bf16[8,64,256]{2,1,0:T(8,128)(2,1)}, bf16[8,64,256]{2,1,0:T(8,128)(2,1)S(1)}, u32[]{:S(2)}, u32[]{:S(2)}) collective-permute-start(bf16[8,64,256]{2,1,0:T(8,128)(2,1)} %get-tuple-element.18), channel_id=1, source_target_pairs={{0,6},{2,0},{4,2},{6,4},{1,7},{3,1},{5,3},{7,5},{8,14},{10,8},{12,... | collective-permute-start | bytes 786440 | tf_op jit(solution)/shard_map/ppermute | solution.py:20
  127.3 0.3 collective-permute-done.9.got1
  127.6 6.6 %collective-permute-done.10.got2 = bf16[8,64,256]{2,1,0:T(8,128)(2,1)S(1)} collective-permute-done((bf16[8,64,256]{2,1,0:T(8,128)(2,1)}, bf16[8,64,256]{2,1,0:T(8,128)(2,1)S(1)}, u32[]{:S(2)}, u32[]{:S(2)}) %collective-permute-start.10) | collective-permute-done | bytes 262176 | tf_op jit(solution)/shard_map/ppermute | solution.py:20
  134.2 1.5 collective-permute-done.11.got3
  135.7 0.7 copy-done.15
  136.4 3.3 %finish.1.p0 = bf16[72,2048]{1,0:T(8,128)(2,1)} custom-call(s32[3]{0:T(128)} %pad_add_fusion.at_ref, bf16[8,64,256]{2,1,0:T(8,128)(2,1)} %get-tuple-element.15.got0, bf16[8,64,256]{2,1,0:T(8,128)(2,1)} %copy-done.13, bf16[8,64,256]{2,1,0:T(8,128)(2,1)} %copy-done.14, bf16[8,64,256]{2,1,0:T(8,128)(2,1)} %copy-done.15, bf16[512,2048]{1,0:T(8,128)(2,1)} %x_ref.3, ...), custom_call_target="tpu_custom_call" | custom-call | tf_op jit(solution)/shard_map/finish/pallas_call | solution.py:251
  139.7 4.3 %collective-permute-start.14 = (bf16[72,2048]{1,0:T(8,128)(2,1)}, bf16[72,2048]{1,0:T(8,128)(2,1)S(1)}, u32[]{:S(2)}, u32[]{:S(2)}) collective-permute-start(bf16[72,2048]{1,0:T(8,128)(2,1)} %finish.1.p0), channel_id=1, source_target_pairs={{0,2},{2,4},{4,6},{6,0},{1,3},{3,5},{5,7},{7,1},{8,10},{10,12},{12... | collective-permute-start | bytes 884744 | tf_op jit(solution)/shard_map/ppermute | solution.py:20
  144.0 3.6 %collective-permute-start.13 = (bf16[72,2048]{1,0:T(8,128)(2,1)}, bf16[72,2048]{1,0:T(8,128)(2,1)S(1)}, u32[]{:S(2)}, u32[]{:S(2)}) collective-permute-start(bf16[72,2048]{1,0:T(8,128)(2,1)} %finish.1.p0), channel_id=1, source_target_pairs={{0,4},{2,6},{4,0},{6,2},{1,5},{3,7},{5,1},{7,3},{8,12},{10,14},{12... | collective-permute-start | bytes 884744 | tf_op jit(solution)/shard_map/ppermute | solution.py:20
  147.7 3.5 %collective-permute-start.12 = (bf16[72,2048]{1,0:T(8,128)(2,1)}, bf16[72,2048]{1,0:T(8,128)(2,1)S(1)}, u32[]{:S(2)}, u32[]{:S(2)}) collective-permute-start(bf16[72,2048]{1,0:T(8,128)(2,1)} %finish.1.p0), channel_id=1, source_target_pairs={{0,6},{2,0},{4,2},{6,4},{1,7},{3,1},{5,3},{7,5},{8,14},{10,8},{12,... | collective-permute-start | bytes 884744 | tf_op jit(solution)/shard_map/ppermute | solution.py:20
  151.2 0.0 all-to-all-done.2
  151.2 0.3 reduce_sum.31
  151.5 0.2 fusion
  151.7 0.8 copy.9
  152.5 8.1 %all-to-all-start.3 = ((bf16[16,32,384]{2,1,0:T(8,128)(2,1)}), bf16[16,32,384]{2,1,0:T(8,128)(2,1)S(1)}, u32[]{:S(2)}, u32[]{:S(2)}) async-start(bf16[16,32,384]{2,1,0:T(8,128)(2,1)} %bitcast.11), calls=%async_computation.3 | async-start | bytes 786432 | tf_op jit(solution)/shard_map/all_to_all | solution.py:24
  160.6 0.0 collective-permute-done.14.p3
  160.6 0.0 collective-permute-done.13.p2
  160.7 0.2 pad_maximum_fusion
  160.8 0.5 copy-done.2
  161.3 0.1 copy-done.3
  161.4 0.1 copy-done.4
  161.5 1.9 collective-permute-start.15
  163.4 2.8 %collective-permute-done.15.other_ref = bf16[4,72,2048]{2,1,0:T(8,128)(2,1)S(1)} collective-permute-done((bf16[4,72,2048]{2,1,0:T(8,128)(2,1)S(1)}, bf16[4,72,2048]{2,1,0:T(8,128)(2,1)S(1)}, u32[]{:S(2)}, u32[]{:S(2)}) %collective-permute-start.15) | collective-permute-done | bytes 1179680 | tf_op jit(solution)/shard_map/ppermute | solution.py:20
  166.3 1.0 copy-done.1
  167.3 1.8 gain.1
  169.1 13.8 %all-to-all-done.3 = bf16[16,32,384]{2,1,0:T(8,128)(2,1)S(1)} async-done(((bf16[16,32,384]{2,1,0:T(8,128)(2,1)}), bf16[16,32,384]{2,1,0:T(8,128)(2,1)S(1)}, u32[]{:S(2)}, u32[]{:S(2)}) %all-to-all-start.3) | async-done | bytes 393248 | tf_op jit(solution)/shard_map/all_to_all | solution.py:24
  183.0 9.8 %all-to-all-start.1 = ((f32[64,1,2048]{2,1,0:T(1,128)}), f32[64,1,2048]{2,1,0:T(1,128)S(1)}, u32[]{:S(2)}, u32[]{:S(2)}) async-start(f32[64,1,2048]{2,1,0:T(1,128)} %gain.1), calls=%async_computation.1 | async-start | bytes 1048576 | tf_op jit(solution)/shard_map/all_to_all | solution.py:24
  192.8 0.1 convert_reduce_fusion
  192.9 12.2 %collective-permute-start.16 = (f32[32,384]{1,0:T(8,128)S(1)}, f32[32,384]{1,0:T(8,128)S(1)}, u32[]{:S(2)}, u32[]{:S(2)}) collective-permute-start(f32[32,384]{1,0:T(8,128)S(1)} %convert_reduce_fusion), channel_id=1, source_target_pairs={{0,256},{256,0},{1,257},{257,1},{2,258},{258,2},{3,259},{259,3},{4... | collective-permute-start | bytes 147464 | tf_op jit(solution)/shard_map/ppermute | solution.py:20
  205.1 24.3 %collective-permute-done.16 = f32[32,384]{1,0:T(8,128)S(1)} collective-permute-done((f32[32,384]{1,0:T(8,128)S(1)}, f32[32,384]{1,0:T(8,128)S(1)}, u32[]{:S(2)}, u32[]{:S(2)}) %collective-permute-start.16) | collective-permute-done | bytes 49184 | tf_op jit(solution)/shard_map/ppermute | solution.py:20
  229.4 0.7 fusion.3
  230.0 3.1 %place.1 = bf16[512,2048]{1,0:T(8,128)(2,1)} custom-call(s32[3]{0:T(128)} %pad_add_fusion.at_ref, bf16[72,2048]{1,0:T(8,128)(2,1)} %finish.1.p0, bf16[72,2048]{1,0:T(8,128)(2,1)} %copy-done.4, bf16[72,2048]{1,0:T(8,128)(2,1)} %copy-done.3, bf16[72,2048]{1,0:T(8,128)(2,1)} %copy-done.2, bf16[4,72,2048]{2,1,0:T(8,128)(2,1)} %copy-done.1), custom_call_target="tpu_custom_call" | custom-call | tf_op jit(solution)/shard_map/place/pallas_call | solution.py:267
  233.1 0.0 all-to-all-done.1
  233.1 1.0 reduce_sum.30
  (29 shorter events, 0.1 us)
Async XLA Ops:
  16.7 67.5 %copy-start.5 = (bf16[4,64,1152]{2,1,0:T(8,128)(2,1)}, bf16[4,64,1152]{2,1,0:T(8,128)(2,1)S(1)}, u32[]{:S(2)}) copy-start(bf16[4,64,1152]{2,1,0:T(8,128)(2,1)S(1)} %all_to_all.20) | copy-start | bytes 1769476
  16.7 21.6 %collective-permute-start.3 = (bf16[256,1152]{1,0:T(8,128)(2,1)S(1)}, bf16[256,1152]{1,0:T(8,128)(2,1)S(1)}, u32[]{:S(2)}, u32[]{:S(2)}) collective-permute-start(bf16[256,1152]{1,0:T(8,128)(2,1)S(1)} %bitcast.20), channel_id=1, source_target_pairs={{0,32},{32,64},{64,96},{96,128},{128,160},{160,192},{192,224},{224... | collective-permute-start | bytes 1769480 | tf_op jit(solution)/shard_map/ppermute | solution.py:20
  18.8 21.4 %collective-permute-start = (bf16[256,1152]{1,0:T(8,128)(2,1)S(1)}, bf16[256,1152]{1,0:T(8,128)(2,1)S(1)}, u32[]{:S(2)}, u32[]{:S(2)}) collective-permute-start(bf16[256,1152]{1,0:T(8,128)(2,1)S(1)} %bitcast.21), channel_id=1, source_target_pairs={{0,480},{32,0},{64,32},{96,64},{128,96},{160,128},{192,160},{224,1... | collective-permute-start | bytes 1769480 | tf_op jit(solution)/shard_map/ppermute | solution.py:20
  38.3 46.0 %copy-start.9 = (bf16[256,1152]{1,0:T(8,128)(2,1)}, bf16[256,1152]{1,0:T(8,128)(2,1)S(1)}, u32[]{:S(2)}) copy-start(bf16[256,1152]{1,0:T(8,128)(2,1)S(1)} %collective-permute-done.3.refs_8_) | copy-start | bytes 1769476
  38.3 16.2 %collective-permute-start.4 = (bf16[256,1152]{1,0:T(8,128)(2,1)S(1)}, bf16[256,1152]{1,0:T(8,128)(2,1)S(1)}, u32[]{:S(2)}, u32[]{:S(2)}) collective-permute-start(bf16[256,1152]{1,0:T(8,128)(2,1)S(1)} %collective-permute-done.3.refs_8_), channel_id=1, source_target_pairs={{0,32},{32,64},{64,96},{96,128},{128,160},{160,192},{192,224},{224... | collective-permute-start | bytes 1769480 | tf_op jit(solution)/shard_map/ppermute | solution.py:20
  40.2 44.0 %copy-start.10 = (bf16[256,1152]{1,0:T(8,128)(2,1)}, bf16[256,1152]{1,0:T(8,128)(2,1)S(1)}, u32[]{:S(2)}) copy-start(bf16[256,1152]{1,0:T(8,128)(2,1)S(1)} %collective-permute-done.refs_1_) | copy-start | bytes 1769476
  40.2 16.1 %collective-permute-start.1 = (bf16[256,1152]{1,0:T(8,128)(2,1)S(1)}, bf16[256,1152]{1,0:T(8,128)(2,1)S(1)}, u32[]{:S(2)}, u32[]{:S(2)}) collective-permute-start(bf16[256,1152]{1,0:T(8,128)(2,1)S(1)} %collective-permute-done.refs_1_), channel_id=1, source_target_pairs={{0,480},{32,0},{64,32},{96,64},{128,96},{160,128},{192,160},{224,1... | collective-permute-start | bytes 1769480 | tf_op jit(solution)/shard_map/ppermute | solution.py:20
  54.4 29.8 %copy-start.11 = (bf16[256,1152]{1,0:T(8,128)(2,1)}, bf16[256,1152]{1,0:T(8,128)(2,1)S(1)}, u32[]{:S(2)}) copy-start(bf16[256,1152]{1,0:T(8,128)(2,1)S(1)} %collective-permute-done.4.refs_7_) | copy-start | bytes 1769476
  54.4 15.3 %collective-permute-start.5 = (bf16[256,1152]{1,0:T(8,128)(2,1)S(1)}, bf16[256,1152]{1,0:T(8,128)(2,1)S(1)}, u32[]{:S(2)}, u32[]{:S(2)}) collective-permute-start(bf16[256,1152]{1,0:T(8,128)(2,1)S(1)} %collective-permute-done.4.refs_7_), channel_id=1, source_target_pairs={{0,32},{32,64},{64,96},{96,128},{128,160},{160,192},{192,224},{224... | collective-permute-start | bytes 1769480 | tf_op jit(solution)/shard_map/ppermute | solution.py:20
  56.3 16.1 %copy-start.12 = (bf16[256,1152]{1,0:T(8,128)(2,1)}, bf16[256,1152]{1,0:T(8,128)(2,1)S(1)}, u32[]{:S(2)}) copy-start(bf16[256,1152]{1,0:T(8,128)(2,1)S(1)} %collective-permute-done.1.refs_2_) | copy-start | bytes 1769476
  56.4 16.1 %collective-permute-start.2 = (bf16[256,1152]{1,0:T(8,128)(2,1)S(1)}, bf16[256,1152]{1,0:T(8,128)(2,1)S(1)}, u32[]{:S(2)}, u32[]{:S(2)}) collective-permute-start(bf16[256,1152]{1,0:T(8,128)(2,1)S(1)} %collective-permute-done.1.refs_2_), channel_id=1, source_target_pairs={{0,480},{32,0},{64,32},{96,64},{128,96},{160,128},{192,160},{224,1... | collective-permute-start | bytes 1769480 | tf_op jit(solution)/shard_map/ppermute | solution.py:20
  69.7 14.5 %copy-start.6 = (bf16[256,1152]{1,0:T(8,128)(2,1)}, bf16[256,1152]{1,0:T(8,128)(2,1)S(1)}, u32[]{:S(2)}) copy-start(bf16[256,1152]{1,0:T(8,128)(2,1)S(1)} %collective-permute-done.5.refs_6_) | copy-start | bytes 1769476
  70.5 20.6 %collective-permute-start.6 = (bf16[128,1152]{1,0:T(8,128)(2,1)}, bf16[128,1152]{1,0:T(8,128)(2,1)}, u32[]{:S(2)}, u32[]{:S(2)}) collective-permute-start(bf16[128,1152]{1,0:T(8,128)(2,1)} %slice.8), channel_id=1, source_target_pairs={{0,32},{32,64},{64,96},{96,128},{128,160},{160,192},{192,224},{224... | collective-permute-start | bytes 884744 | tf_op jit(solution)/shard_map/ppermute | solution.py:20
  72.5 11.8 %copy-start.7 = (bf16[256,1152]{1,0:T(8,128)(2,1)}, bf16[256,1152]{1,0:T(8,128)(2,1)S(1)}, u32[]{:S(2)}) copy-start(bf16[256,1152]{1,0:T(8,128)(2,1)S(1)} %collective-permute-done.2.refs_3_) | copy-start | bytes 1769476
  73.3 17.8 %collective-permute-start.7 = (bf16[128,1152]{1,0:T(8,128)(2,1)}, bf16[128,1152]{1,0:T(8,128)(2,1)}, u32[]{:S(2)}, u32[]{:S(2)}) collective-permute-start(bf16[128,1152]{1,0:T(8,128)(2,1)} %slice.9), channel_id=1, source_target_pairs={{0,480},{32,0},{64,32},{96,64},{128,96},{160,128},{192,160},{224,1... | collective-permute-start | bytes 884744 | tf_op jit(solution)/shard_map/ppermute | solution.py:20
  101.4 10.9 %collective-permute-start.8 = (bf16[4,8,64,256]{3,2,1,0:T(8,128)(2,1)}, bf16[4,8,64,256]{3,2,1,0:T(8,128)(2,1)S(1)}, u32[]{:S(2)}, u32[]{:S(2)}) collective-permute-start(bf16[4,8,64,256]{3,2,1,0:T(8,128)(2,1)} %get-tuple-element.14), channel_id=1, source_target_pairs={{0,1},{1,0},{2,3},{3,2},{4,5},{5,4},{6,7},{7,6},{8,9},{9,8},{10,11... | collective-permute-start | bytes 3145736 | tf_op jit(solution)/shard_map/ppermute | solution.py:20
  107.3 43.8 %all-to-all-start.2 = ((bf16[4,8,64,384]{3,2,1,0:T(8,128)(2,1)}), bf16[4,8,64,384]{3,2,1,0:T(8,128)(2,1)S(1)}, u32[]{:S(2)}, u32[]{:S(2)}) async-start(bf16[4,8,64,384]{3,2,1,0:T(8,128)(2,1)} %down.1), calls=%async_computation.2 | async-start | bytes 3145728 | tf_op jit(solution)/shard_map/all_to_all | solution.py:24
  112.3 1.0 copy-start.8
  115.9 11.7 %collective-permute-start.9 = (bf16[8,64,256]{2,1,0:T(8,128)(2,1)}, bf16[8,64,256]{2,1,0:T(8,128)(2,1)S(1)}, u32[]{:S(2)}, u32[]{:S(2)}) collective-permute-start(bf16[8,64,256]{2,1,0:T(8,128)(2,1)} %get-tuple-element.16), channel_id=1, source_target_pairs={{0,2},{2,4},{4,6},{6,0},{1,3},{3,5},{5,7},{7,1},{8,10},{10,12},{12... | collective-permute-start | bytes 786440 | tf_op jit(solution)/shard_map/ppermute | solution.py:20
  119.3 14.9 %collective-permute-start.10 = (bf16[8,64,256]{2,1,0:T(8,128)(2,1)}, bf16[8,64,256]{2,1,0:T(8,128)(2,1)S(1)}, u32[]{:S(2)}, u32[]{:S(2)}) collective-permute-start(bf16[8,64,256]{2,1,0:T(8,128)(2,1)} %get-tuple-element.17), channel_id=1, source_target_pairs={{0,4},{2,6},{4,0},{6,2},{1,5},{3,7},{5,1},{7,3},{8,12},{10,14},{12... | collective-permute-start | bytes 786440 | tf_op jit(solution)/shard_map/ppermute | solution.py:20
  123.9 11.8 %collective-permute-start.11 = (bf16[8,64,256]{2,1,0:T(8,128)(2,1)}, bf16[8,64,256]{2,1,0:T(8,128)(2,1)S(1)}, u32[]{:S(2)}, u32[]{:S(2)}) collective-permute-start(bf16[8,64,256]{2,1,0:T(8,128)(2,1)} %get-tuple-element.18), channel_id=1, source_target_pairs={{0,6},{2,0},{4,2},{6,4},{1,7},{3,1},{5,3},{7,5},{8,14},{10,8},{12,... | collective-permute-start | bytes 786440 | tf_op jit(solution)/shard_map/ppermute | solution.py:20
  127.6 8.1 %copy-start.13 = (bf16[8,64,256]{2,1,0:T(8,128)(2,1)}, bf16[8,64,256]{2,1,0:T(8,128)(2,1)S(1)}, u32[]{:S(2)}) copy-start(bf16[8,64,256]{2,1,0:T(8,128)(2,1)S(1)} %collective-permute-done.9.got1) | copy-start | bytes 786436
  134.2 1.5 copy-start.14
  135.7 0.7 copy-start.15
  139.7 20.9 %collective-permute-start.14 = (bf16[72,2048]{1,0:T(8,128)(2,1)}, bf16[72,2048]{1,0:T(8,128)(2,1)S(1)}, u32[]{:S(2)}, u32[]{:S(2)}) collective-permute-start(bf16[72,2048]{1,0:T(8,128)(2,1)} %finish.1.p0), channel_id=1, source_target_pairs={{0,2},{2,4},{4,6},{6,0},{1,3},{3,5},{5,7},{7,1},{8,10},{10,12},{12... | collective-permute-start | bytes 884744 | tf_op jit(solution)/shard_map/ppermute | solution.py:20
  144.0 16.6 %collective-permute-start.13 = (bf16[72,2048]{1,0:T(8,128)(2,1)}, bf16[72,2048]{1,0:T(8,128)(2,1)S(1)}, u32[]{:S(2)}, u32[]{:S(2)}) collective-permute-start(bf16[72,2048]{1,0:T(8,128)(2,1)} %finish.1.p0), channel_id=1, source_target_pairs={{0,4},{2,6},{4,0},{6,2},{1,5},{3,7},{5,1},{7,3},{8,12},{10,14},{12... | collective-permute-start | bytes 884744 | tf_op jit(solution)/shard_map/ppermute | solution.py:20
  147.7 13.0 %collective-permute-start.12 = (bf16[72,2048]{1,0:T(8,128)(2,1)}, bf16[72,2048]{1,0:T(8,128)(2,1)S(1)}, u32[]{:S(2)}, u32[]{:S(2)}) collective-permute-start(bf16[72,2048]{1,0:T(8,128)(2,1)} %finish.1.p0), channel_id=1, source_target_pairs={{0,6},{2,0},{4,2},{6,4},{1,7},{3,1},{5,3},{7,5},{8,14},{10,8},{12,... | collective-permute-start | bytes 884744 | tf_op jit(solution)/shard_map/ppermute | solution.py:20
  151.5 9.1 %copy-start = (bf16[72,2048]{1,0:T(8,128)(2,1)S(1)}, bf16[72,2048]{1,0:T(8,128)(2,1)}, u32[]{:S(2)}) copy-start(bf16[72,2048]{1,0:T(8,128)(2,1)} %finish.1.p0) | copy-start | bytes 884740
  152.5 30.5 %all-to-all-start.3 = ((bf16[16,32,384]{2,1,0:T(8,128)(2,1)}), bf16[16,32,384]{2,1,0:T(8,128)(2,1)S(1)}, u32[]{:S(2)}, u32[]{:S(2)}) async-start(bf16[16,32,384]{2,1,0:T(8,128)(2,1)} %bitcast.11), calls=%async_computation.3 | async-start | bytes 786432 | tf_op jit(solution)/shard_map/all_to_all | solution.py:24
  160.6 0.7 copy-start.2
  160.6 0.8 copy-start.3
  160.6 0.9 copy-start.4
  161.5 4.7 %collective-permute-start.15 = (bf16[4,72,2048]{2,1,0:T(8,128)(2,1)S(1)}, bf16[4,72,2048]{2,1,0:T(8,128)(2,1)S(1)}, u32[]{:S(2)}, u32[]{:S(2)}) collective-permute-start(bf16[4,72,2048]{2,1,0:T(8,128)(2,1)S(1)} %pad_maximum_fusion), channel_id=1, source_target_pairs={{0,1},{1,0},{2,3},{3,2},{4,5},{5,4},{6,7},{7,6},{8,9},{9,8},{10,11... | collective-permute-start | bytes 3538952 | tf_op jit(solution)/shard_map/ppermute | solution.py:20
  166.2 1.0 copy-start.1
  183.0 50.2 %all-to-all-start.1 = ((f32[64,1,2048]{2,1,0:T(1,128)}), f32[64,1,2048]{2,1,0:T(1,128)S(1)}, u32[]{:S(2)}, u32[]{:S(2)}) async-start(f32[64,1,2048]{2,1,0:T(1,128)} %gain.1), calls=%async_computation.1 | async-start | bytes 1048576 | tf_op jit(solution)/shard_map/all_to_all | solution.py:24
  192.9 36.5 %collective-permute-start.16 = (f32[32,384]{1,0:T(8,128)S(1)}, f32[32,384]{1,0:T(8,128)S(1)}, u32[]{:S(2)}, u32[]{:S(2)}) collective-permute-start(f32[32,384]{1,0:T(8,128)S(1)} %convert_reduce_fusion), channel_id=1, source_target_pairs={{0,256},{256,0},{1,257},{257,1},{2,258},{258,2},{3,259},{259,3},{4... | collective-permute-start | bytes 147464 | tf_op jit(solution)/shard_map/ppermute | solution.py:20

commit v3 on v2

--- a/solution.py
+++ b/solution.py
@@ -61,8 +61,8 @@
         turned_ref[d] = part.T
 
 
-def grad_kernel(x_ref, c_ref, *refs):
-    w_refs, (mine_ref, other_ref, hid_ref) = refs[:9], refs[9:]
+def grad_kernel(x_ref, c_ref, gain_ref, *refs):
+    w_refs, (mine_ref, other_ref, hid_ref, sum_ref) = refs[:9], refs[9:]
     units = hid_ref.shape[1]
     nx, _, part, _ = mine_ref.shape
     gu = dh = None
@@ -84,19 +84,64 @@
         rows = w.shape[0]
         out = lax.dot_general(
             both, w[:, : 2 * units], (((1,), (1,)), ((), ())), preferred_element_type=F32
-        ).astype(BF16)
+        )
+        terms = x_ref[d, :, lo : lo + rows].astype(F32) * out
+        sums = jnp.sum(terms, axis=0, keepdims=True)
+        sum_ref[d, :, lo : lo + rows] = sums / gain_ref[d, :, lo : lo + rows]
+        out = out.astype(BF16)
         for k in range(nx):
             mine_ref[k, d, :, lo : lo + rows] = out[k * part : (k + 1) * part]
             other_ref[k, d, :, lo : lo + rows] = out[(nx + k) * part : (nx + k + 1) * part]
 
 
-def down_kernel(ct_ref, hid_ref, out_ref):
-    ny, nz, rows, _ = out_ref.shape
+def down_kernel(ct_ref, hid_ref, sum_ref, out_ref):
+    ny, nz, longer, units = out_ref.shape
+    rows = longer - 8
+    cols = sum_ref.shape[2]
     for d in range(nz):
         res = jnp.dot(ct_ref[d], hid_ref[...], preferred_element_type=F32)
         res = (0.5 * res).astype(BF16)
+        sums = sum_ref[d]
+        high = sums.astype(BF16)
+        left = sums - high.astype(F32)
+        mid = left.astype(BF16)
+        low = (left - mid.astype(F32)).astype(BF16)
+        extra = jnp.concatenate([high, mid, low, jnp.zeros((5, cols), BF16)], axis=0)
+        extra = jnp.concatenate([extra, jnp.zeros((8, units - cols), BF16)], axis=1)
         for y in range(ny):
-            out_ref[y, d] = res[y * rows : (y + 1) * rows]
+            out_ref[y, d, :rows] = res[y * rows : (y + 1) * rows]
+            out_ref[y, d, rows:] = extra
+
+
+def rows_kernel(at_ref, got_ref, out_ref):
+    ny, nz, longer, _ = got_ref.shape
+    rows = longer - 8
+    half = rows // 2
+    sums = []
+    for d in range(nz):
+        total = got_ref[0, d].astype(F32)
+        for k in range(1, ny):
+            total = total + got_ref[k, d].astype(F32)
+        part = total[:rows].astype(BF16)
+        to = (at_ref[0] + d) % nz
+        out_ref[to, :half] = part[:half]
+        out_ref[nz + to, :half] = part[half:]
+        sums.append(jnp.sum(total[rows:], axis=0, keepdims=True))
+    extra = jnp.concatenate(sums, axis=0)
+    extra = pltpu.roll(extra, at_ref[0], 0).astype(BF16)
+    for k in range(2 * nz):
+        out_ref[k, half:] = extra
+
+
+def ring_kernel(got_ref, out_ref, sum_ref):
+    half = out_ref.shape[0]
+    cols = sum_ref.shape[2]
+    total = got_ref[0].astype(F32)
+    for k in range(1, got_ref.shape[0]):
+        total = total + got_ref[k].astype(F32)
+    out_ref[...] = total[:half]
+    for k in range(sum_ref.shape[0]):
+        sum_ref[k] = total[half:, :cols]
 
 
 def chip_kernel(mine_ref, theirs_ref, *out_refs):
@@ -116,17 +161,9 @@
     inv = lax.rsqrt(jnp.mean(v * v, axis=-1, keepdims=True) + EPS)
     xhat = v * inv
     dn = dn_ref[...].astype(F32)
-    sums = jnp.sum(dn * xhat, axis=0, keepdims=True)
     gs = gain_ref[...] * dn
     m = jnp.mean(gs * xhat, axis=-1, keepdims=True)
-    part = v.shape[0]
-    out_ref[:part] = (c_ref[...].astype(F32) + inv * (gs - xhat * m)).astype(BF16)
-    high = sums.astype(BF16)
-    left = sums - high.astype(F32)
-    mid = left.astype(BF16)
-    low = (left - mid.astype(F32)).astype(BF16)
-    none = jnp.zeros((out_ref.shape[0] - part - 3, v.shape[1]), BF16)
-    out_ref[part:] = jnp.concatenate([high, mid, low, none], axis=0)
+    out_ref[...] = (c_ref[...].astype(F32) + inv * (gs - xhat * m)).astype(BF16)
 
 
 def place_kernel(at_ref, p0, p1, p2, p3, other_ref, out_ref):
@@ -140,13 +177,8 @@
         out_ref[pl.ds(far, part), :] = other_ref[k, :part]
 
 
-def gain_kernel(p0, p1, p2, p3, other_ref, out_ref):
-    total = jnp.zeros(p0.shape, F32)
-    for k, piece in enumerate((p0, p1, p2, p3)):
-        total = total + (piece[...].astype(F32) + other_ref[k].astype(F32))
-    total = jnp.sum(total, axis=0, keepdims=True)
-    for k in range(out_ref.shape[0]):
-        out_ref[k] = total
+def near(*arrays):
+    return [pltpu.with_memory_space_constraint(a, pltpu.VMEM) for a in arrays]
 
 
 def vmem(n):
@@ -213,25 +245,27 @@
         name="prepare_c",
     )(at, cotangent, cotangent)
 
-    mine, other, hidden = pl.pallas_call(
+    gain_ring = rolled(gain.reshape(nz, 1, cols), zl)
+    mine, other, hidden, sums = pl.pallas_call(
         grad_kernel,
         out_shape=(
             jax.ShapeDtypeStruct((nx, nz, part, cols), BF16),
             jax.ShapeDtypeStruct((nx, nz, part, cols), BF16),
             jax.ShapeDtypeStruct((tokens, units), BF16),
-        ),
-        in_specs=vmem(11),
-        out_specs=tuple(vmem(3)),
+            jax.ShapeDtypeStruct((nz, 1, cols), F32),
+        ),
+        in_specs=vmem(12),
+        out_specs=tuple(vmem(4)),
         name="grad",
-    )(xr, cr, *weights)
+    )(xr, cr, gain_ring, *weights[:4], *near(last_f, last_b), *weights[6:])
     theirs = shifted(other, "c", 1)
     (dd,) = pl.pallas_call(
         down_kernel,
-        out_shape=(jax.ShapeDtypeStruct((ny, nz, rows, units), BF16),),
-        in_specs=vmem(2),
+        out_shape=(jax.ShapeDtypeStruct((ny, nz, rows + 8, units), BF16),),
+        in_specs=vmem(3),
         out_specs=tuple(vmem(1)),
         name="down",
-    )(ct, hidden)
+    )(ct, hidden, sums)
     dy = exchanged(dd, "fs_1")
 
     chunk = jax.ShapeDtypeStruct((nz, part, cols), BF16)
@@ -241,25 +275,23 @@
         in_specs=vmem(2),
         out_specs=tuple(vmem(4)),
         name="chip",
-    )(mine, theirs)
+    )(mine, *near(theirs))
     got = [chip[0]]
     for k in (1, 2, 3):
         got.append(shifted(chip[k], "x", k))
-    whole = pl.BlockSpec((nz, part, cols), lambda i, at: (0, 0, 0))
     own = pl.BlockSpec((part, width), lambda i, at: (at[1] * nx + at[2], 0))
-    longer = part + 8
     ig = pl.pallas_call(
         finish_kernel,
-        out_shape=jax.ShapeDtypeStruct((longer, width), BF16),
+        out_shape=jax.ShapeDtypeStruct((part, width), BF16),
         grid_spec=pltpu.PrefetchScalarGridSpec(
             num_scalar_prefetch=1,
             grid=(1,),
-            in_specs=[whole] * 4 + [own, own, pl.BlockSpec((1, width), lambda i, at: (0, 0))],
-            out_specs=pl.BlockSpec((longer, width), lambda i, at: (0, 0)),
+            in_specs=vmem(4) + [own, own, pl.BlockSpec((1, width), lambda i, at: (0, 0))],
+            out_specs=pl.BlockSpec((part, width), lambda i, at: (0, 0)),
             scratch_shapes=[pltpu.VMEM((part, width), BF16)],
         ),
         name="finish",
-    )(at, *got, inputs, cotangent, gain2)
+    )(at, got[0], *near(*got[1:]), inputs, cotangent, gain2)
     pieces = [ig]
     for k in (1, 2, 3):
         pieces.append(shifted(ig, "x", -k))
@@ -270,27 +302,28 @@
         in_specs=[pl.BlockSpec(memory_space=pltpu.SMEM)] + vmem(5),
         out_specs=pl.BlockSpec(memory_space=pltpu.VMEM),
         name="place",
-    )(at, *pieces, ig_other)
-
-    groups = lax.axis_size(REP_FS)
-    last = part // 8
-    tail = pl.BlockSpec((8, width), lambda i: (last, 0))
-    gain_chip = pl.pallas_call(
-        gain_kernel,
-        out_shape=jax.ShapeDtypeStruct((groups, 1, width), F32),
-        grid=(1,),
-        in_specs=[tail] * 4 + [pl.BlockSpec((4, 8, width), lambda i: (0, last, 0))],
-        out_specs=pl.BlockSpec((groups, 1, width), lambda i: (0, 0, 0)),
-        name="gain",
-    )(*pieces, ig_other)
-    gain_all = exchanged(gain_chip, REP_FS)
-    gain_gradient = jnp.sum(gain_all, axis=(0, 1))
-
-    dy = jnp.sum(dy.astype(F32), axis=0).astype(BF16)
-    dz = rolled(dy, (nz - zl) % nz).reshape(nz, 2, rows // 2, units).transpose(1, 0, 2, 3)
-    dz = dz.reshape(2 * nz, rows // 2, units)
+    )(at, pieces[0], *near(*pieces[1:], ig_other))
+
+    dz = pl.pallas_call(
+        rows_kernel,
+        out_shape=jax.ShapeDtypeStruct((2 * nz, rows // 2 + 8, units), BF16),
+        in_specs=[pl.BlockSpec(memory_space=pltpu.SMEM)] + vmem(1),
+        out_specs=pl.BlockSpec(memory_space=pltpu.VMEM),
+        name="ysum",
+    )(at, *near(dy))
     dz = exchanged(dz, RING)
-    own = jnp.sum(dz.astype(F32), axis=0)
+    own, gain_own = pl.pallas_call(
+        ring_kernel,
+        out_shape=(
+            jax.ShapeDtypeStruct((rows // 2, units), F32),
+            jax.ShapeDtypeStruct((lax.axis_size(TP), nz, cols), F32),
+        ),
+        in_specs=vmem(1),
+        out_specs=tuple(vmem(2)),
+        name="zsum",
+    )(*near(dz))
+    gain_all = exchanged(gain_own, TP)
+    gain_gradient = jnp.sum(gain_all, axis=0).reshape(width)
     far = shifted(own, "rep", 1)
     pair = rolled(jnp.stack([own, far]), rep)
     d_down = pair.reshape(rows, units)

time: 235 us -> 207 us (0.88)
  the two profiles are of different devices: /device:TPU:8 before, /device:TPU:1 now
where the time goes in v3:
time: 207 us; the launch traced here: 206 us
  starting transfers between devices  99.2 us (48%)
  waiting for transfers between devices  51.3 us (25%)
  Pallas kernels  36.5 us (18%)
  blocking collectives  12.1 us (6%)
  other arithmetic  3.87 us (2%)
  local copies, waits for them, and re-layouts  2.26 us (1%)
    ppermute x17, starting transfers between devices, shifted(): return lax.ppermute(v, axis, [(i, (i + by) % n) for i in range(n)])  84.8 us
    ppermute x17, waiting for transfers between devices, shifted(): return lax.ppermute(v, axis, [(i, (i + by) % n) for i in range(n)])  36.3 us
    all_to_all x3, waiting for transfers between devices, exchanged(): return lax.all_to_all(v, axis, 0, 0, tiled=True)  15 us
    all_to_all x3, starting transfers between devices, exchanged(): return lax.all_to_all(v, axis, 0, 0, tiled=True)  14.4 us
    all_to_all x1, blocking collectives, exchanged(): return lax.all_to_all(v, axis, 0, 0, tiled=True)  12.1 us
    pallas_call x1, Pallas kernels, work(): pl.pallas_call(grad_kernel, out_shape=(jax.ShapeDtypeStruct((nx, nz, part...  10.1 us
    pallas_call x1, Pallas kernels, work(): pl.pallas_call(prepare_tokens, out_shape=jax.ShapeDtypeStruct((nz, tokens...  6.97 us
    pallas_call x1, Pallas kernels, work(): pl.pallas_call(prepare_cotangent, out_shape=(jax.ShapeDtypeStruct((nz, to...  5.2 us
  transfers between devices with their start and end apart: 20, of which 9 were waited for; matrix products, arithmetic and copies ran while one was open for 2% of the time, Pallas kernels for 11%

profile of v3, /device:TPU:1, one launch (start us, length us, event | category | flops | bytes accessed | tf_op | source)
XLA Modules:
  0.0 206.1 jit_solution(9399094500643725702)
XLA Ops:
  0.6 0.9 pad_maximum_fusion.1
  1.5 12.1 %all_to_all.20 = bf16[4,64,1152]{2,1,0:T(8,128)(2,1)S(1)} all-to-all(bf16[4,64,1152]{2,1,0:T(8,128)(2,1)S(1)} %broadcast_in_dim.10), channel_id=1, replica_groups=mesh['rep'=2,'fs_0'=8,'fs_1'=4,'x'=4,'c'=2] {'fs_1'}, dimensions={0} | all-to-all | bytes 1179648 | tf_op jit(solution)/shard_map/all_to_all | solution.py:24
  13.6 5.3 %collective-permute-start.3 = (bf16[256,1152]{1,0:T(8,128)(2,1)S(1)}, bf16[256,1152]{1,0:T(8,128)(2,1)S(1)}, u32[]{:S(2)}, u32[]{:S(2)}) collective-permute-start(bf16[256,1152]{1,0:T(8,128)(2,1)S(1)} %bitcast.18), channel_id=1, source_target_pairs={{0,32},{32,64},{64,96},{96,128},{128,160},{160,192},{192,224},{224... | collective-permute-start | bytes 1769480 | tf_op jit(solution)/shard_map/ppermute | solution.py:20
  18.9 9.5 %collective-permute-start = (bf16[256,1152]{1,0:T(8,128)(2,1)S(1)}, bf16[256,1152]{1,0:T(8,128)(2,1)S(1)}, u32[]{:S(2)}, u32[]{:S(2)}) collective-permute-start(bf16[256,1152]{1,0:T(8,128)(2,1)S(1)} %bitcast.19), channel_id=1, source_target_pairs={{0,480},{32,0},{64,32},{96,64},{128,96},{160,128},{192,160},{224,1... | collective-permute-start | bytes 1769480 | tf_op jit(solution)/shard_map/ppermute | solution.py:20
  28.4 9.7 %collective-permute-done.3.refs_8_ = bf16[256,1152]{1,0:T(8,128)(2,1)S(1)} collective-permute-done((bf16[256,1152]{1,0:T(8,128)(2,1)S(1)}, bf16[256,1152]{1,0:T(8,128)(2,1)S(1)}, u32[]{:S(2)}, u32[]{:S(2)}) %collective-permute-start.3) | collective-permute-done | bytes 589856 | tf_op jit(solution)/shard_map/ppermute | solution.py:20
  38.1 1.9 collective-permute-start.4
  40.0 0.0 collective-permute-done.refs_1_
  40.0 0.0 copy-start.4
  40.0 4.6 %collective-permute-start.1 = (bf16[256,1152]{1,0:T(8,128)(2,1)S(1)}, bf16[256,1152]{1,0:T(8,128)(2,1)S(1)}, u32[]{:S(2)}, u32[]{:S(2)}) collective-permute-start(bf16[256,1152]{1,0:T(8,128)(2,1)S(1)} %collective-permute-done.refs_1_), channel_id=1, source_target_pairs={{0,480},{32,0},{64,32},{96,64},{128,96},{160,128},{192,160},{224,1... | collective-permute-start | bytes 1769480 | tf_op jit(solution)/shard_map/ppermute | solution.py:20
  44.6 8.8 %collective-permute-done.4.refs_7_ = bf16[256,1152]{1,0:T(8,128)(2,1)S(1)} collective-permute-done((bf16[256,1152]{1,0:T(8,128)(2,1)S(1)}, bf16[256,1152]{1,0:T(8,128)(2,1)S(1)}, u32[]{:S(2)}, u32[]{:S(2)}) %collective-permute-start.4) | collective-permute-done | bytes 589856 | tf_op jit(solution)/shard_map/ppermute | solution.py:20
  53.4 1.9 collective-permute-start.5
  55.3 0.0 collective-permute-done.1.refs_2_
  55.3 0.0 copy-start.6
  55.3 4.6 %collective-permute-start.2 = (bf16[256,1152]{1,0:T(8,128)(2,1)S(1)}, bf16[256,1152]{1,0:T(8,128)(2,1)S(1)}, u32[]{:S(2)}, u32[]{:S(2)}) collective-permute-start(bf16[256,1152]{1,0:T(8,128)(2,1)S(1)} %collective-permute-done.1.refs_2_), channel_id=1, source_target_pairs={{0,480},{32,0},{64,32},{96,64},{128,96},{160,128},{192,160},{224,1... | collective-permute-start | bytes 1769480 | tf_op jit(solution)/shard_map/ppermute | solution.py:20
  59.9 7.9 %collective-permute-done.5.refs_6_ = bf16[256,1152]{1,0:T(8,128)(2,1)S(1)} collective-permute-done((bf16[256,1152]{1,0:T(8,128)(2,1)S(1)}, bf16[256,1152]{1,0:T(8,128)(2,1)S(1)}, u32[]{:S(2)}, u32[]{:S(2)}) %collective-permute-start.5) | collective-permute-done | bytes 589856 | tf_op jit(solution)/shard_map/ppermute | solution.py:20
  67.9 0.8 slice.8
  68.6 1.9 collective-permute-start.6
  70.6 0.0 collective-permute-done.2.refs_3_
  70.6 0.8 slice.9
  71.4 4.6 %collective-permute-start.7 = (bf16[128,1152]{1,0:T(8,128)(2,1)}, bf16[128,1152]{1,0:T(8,128)(2,1)S(1)}, u32[]{:S(2)}, u32[]{:S(2)}) collective-permute-start(bf16[128,1152]{1,0:T(8,128)(2,1)} %slice.9), channel_id=1, source_target_pairs={{0,480},{32,0},{64,32},{96,64},{128,96},{160,128},{192,160},{224,1... | collective-permute-start | bytes 884744 | tf_op jit(solution)/shard_map/ppermute | solution.py:20
  75.9 0.6 pad_add_fusion.at_ref
  76.6 5.2 %prepare_c.1 = (bf16[8,512,256]{2,1,0:T(8,128)(2,1)}, bf16[8,256,512]{2,1,0:T(8,128)(2,1)}) custom-call(s32[3]{0:T(128)} %pad_add_fusion.at_ref, bf16[512,2048]{1,0:T(8,128)(2,1)} %c_ref.1, bf16[512,2048]{1,0:T(8,128)(2,1)} %c_ref.1), custom_call_target="tpu_custom_call" | custom-call | tf_op jit(solution)/shard_map/prepare_c/pallas_call | solution.py:227
  81.8 0.0 copy-done
  81.8 0.0 copy-start.7
  81.8 7.0 %prepare_x.1.x_ref = bf16[8,512,256]{2,1,0:T(8,128)(2,1)} custom-call(s32[3]{0:T(128)} %pad_add_fusion.at_ref, bf16[512,2048]{1,0:T(8,128)(2,1)} %x_ref.3, f32[1,2048]{1,0:T(1,128)} %bitcast.23), custom_call_target="tpu_custom_call" | custom-call | tf_op jit(solution)/shard_map/prepare_x/pallas_call | solution.py:213
  88.8 0.6 fusion.3.gain_ref
  89.4 0.0 collective-permute-done.6.refs_4_
  89.4 0.0 collective-permute-done.7.refs_5_
  89.4 10.1 %grad.1 = (bf16[4,8,64,256]{3,2,1,0:T(8,128)(2,1)}, bf16[4,8,64,256]{3,2,1,0:T(8,128)(2,1)}, bf16[512,384]{1,0:T(8,128)(2,1)}, f32[8,1,256]{2,1,0:T(1,128)}) custom-call(bf16[8,512,256]{2,1,0:T(8,128)(2,1)} %prepare_x.1.x_ref, bf16[8,512,256]{2,1,0:T(8,128)(2,1)} %get-tuple-element.15.c_ref, f32[8,1,256]{2,1,0:T(1,128)} %fusion.3.gain_ref, ...), custom_call_target="tpu_custom_call" | custom-call | tf_op jit(solution)/shard_map/grad/pallas_call | solution.py:249
  99.5 4.2 %down.1 = bf16[4,8,72,384]{3,2,1,0:T(8,128)(2,1)} custom-call(bf16[8,256,512]{2,1,0:T(8,128)(2,1)} %get-tuple-element.22.ct_ref, bf16[512,384]{1,0:T(8,128)(2,1)} %get-tuple-element.23.hid_ref, f32[8,1,256]{2,1,0:T(1,128)} %get-tuple-element.24.sum_ref), custom_call_target="tpu_custom_call" | custom-call | tf_op jit(solution)/shard_map/down/pallas_call | solution.py:262
  103.7 3.6 %all-to-all-start.1 = ((bf16[4,8,72,384]{3,2,1,0:T(8,128)(2,1)}), bf16[4,8,72,384]{3,2,1,0:T(8,128)(2,1)S(1)}, u32[]{:S(2)}, u32[]{:S(2)}) async-start(bf16[4,8,72,384]{3,2,1,0:T(8,128)(2,1)} %down.1), calls=%async_computation.1 | async-start | bytes 3538944 | tf_op jit(solution)/shard_map/all_to_all | solution.py:24
  107.3 6.9 %collective-permute-start.8 = (bf16[4,8,64,256]{3,2,1,0:T(8,128)(2,1)}, bf16[4,8,64,256]{3,2,1,0:T(8,128)(2,1)S(1)}, u32[]{:S(2)}, u32[]{:S(2)}) collective-permute-start(bf16[4,8,64,256]{3,2,1,0:T(8,128)(2,1)} %get-tuple-element.17), channel_id=1, source_target_pairs={{0,1},{1,0},{2,3},{3,2},{4,5},{5,4},{6,7},{7,6},{8,9},{9,8},{10,11... | collective-permute-start | bytes 3145736 | tf_op jit(solution)/shard_map/ppermute | solution.py:20
  114.2 10.8 %all-to-all-done.1.got_ref = bf16[4,8,72,384]{3,2,1,0:T(8,128)(2,1)S(1)} async-done(((bf16[4,8,72,384]{3,2,1,0:T(8,128)(2,1)}), bf16[4,8,72,384]{3,2,1,0:T(8,128)(2,1)S(1)}, u32[]{:S(2)}, u32[]{:S(2)}) %all-to-all-start.1) | async-done | bytes 1769504 | tf_op jit(solution)/shard_map/all_to_all | solution.py:24
  124.9 1.7 ysum.1
  126.6 7.3 %all-to-all-start.2 = ((bf16[16,40,384]{2,1,0:T(8,128)(2,1)}), bf16[16,40,384]{2,1,0:T(8,128)(2,1)S(1)}, u32[]{:S(2)}, u32[]{:S(2)}) async-start(bf16[16,40,384]{2,1,0:T(8,128)(2,1)} %ysum.1), calls=%async_computation.2 | async-start | bytes 983040 | tf_op jit(solution)/shard_map/all_to_all | solution.py:24
  133.9 0.0 collective-permute-done.8.theirs_ref
  133.9 2.3 %chip.1 = (bf16[8,64,256]{2,1,0:T(8,128)(2,1)}, bf16[8,64,256]{2,1,0:T(8,128)(2,1)}, bf16[8,64,256]{2,1,0:T(8,128)(2,1)}, bf16[8,64,256]{2,1,0:T(8,128)(2,1)}) custom-call(bf16[4,8,64,256]{3,2,1,0:T(8,128)(2,1)} %get-tuple-element.16.mine_ref, bf16[4,8,64,256]{3,2,1,0:T(8,128)(2,1)S(1)} %collective-permute-done.8.theirs_ref), custom_call_target="tpu_custom_call" | custom-call | tf_op jit(solution)/shard_map/chip/pallas_call | solution.py:272
  136.2 3.1 %collective-permute-start.9 = (bf16[8,64,256]{2,1,0:T(8,128)(2,1)}, bf16[8,64,256]{2,1,0:T(8,128)(2,1)S(1)}, u32[]{:S(2)}, u32[]{:S(2)}) collective-permute-start(bf16[8,64,256]{2,1,0:T(8,128)(2,1)} %get-tuple-element.19), channel_id=1, source_target_pairs={{0,2},{2,4},{4,6},{6,0},{1,3},{3,5},{5,7},{7,1},{8,10},{10,12},{12... | collective-permute-start | bytes 786440 | tf_op jit(solution)/shard_map/ppermute | solution.py:20
  139.3 4.4 %collective-permute-start.10 = (bf16[8,64,256]{2,1,0:T(8,128)(2,1)}, bf16[8,64,256]{2,1,0:T(8,128)(2,1)S(1)}, u32[]{:S(2)}, u32[]{:S(2)}) collective-permute-start(bf16[8,64,256]{2,1,0:T(8,128)(2,1)} %get-tuple-element.20), channel_id=1, source_target_pairs={{0,4},{2,6},{4,0},{6,2},{1,5},{3,7},{5,1},{7,3},{8,12},{10,14},{12... | collective-permute-start | bytes 786440 | tf_op jit(solution)/shard_map/ppermute | solution.py:20
  143.7 3.1 %collective-permute-start.11 = (bf16[8,64,256]{2,1,0:T(8,128)(2,1)}, bf16[8,64,256]{2,1,0:T(8,128)(2,1)S(1)}, u32[]{:S(2)}, u32[]{:S(2)}) collective-permute-start(bf16[8,64,256]{2,1,0:T(8,128)(2,1)} %get-tuple-element.21), channel_id=1, source_target_pairs={{0,6},{2,0},{4,2},{6,4},{1,7},{3,1},{5,3},{7,5},{8,14},{10,8},{12,... | collective-permute-start | bytes 786440 | tf_op jit(solution)/shard_map/ppermute | solution.py:20
  146.7 0.0 collective-permute-done.9.got1
  146.7 2.1 collective-permute-done.10.got2
  148.8 2.5 %collective-permute-done.11.got3 = bf16[8,64,256]{2,1,0:T(8,128)(2,1)S(1)} collective-permute-done((bf16[8,64,256]{2,1,0:T(8,128)(2,1)}, bf16[8,64,256]{2,1,0:T(8,128)(2,1)S(1)}, u32[]{:S(2)}, u32[]{:S(2)}) %collective-permute-start.11) | collective-permute-done | bytes 262176 | tf_op jit(solution)/shard_map/ppermute | solution.py:20
  151.3 2.9 %finish.1.p0 = bf16[64,2048]{1,0:T(8,128)(2,1)} custom-call(s32[3]{0:T(128)} %pad_add_fusion.at_ref, bf16[8,64,256]{2,1,0:T(8,128)(2,1)} %get-tuple-element.18.got0, bf16[8,64,256]{2,1,0:T(8,128)(2,1)S(1)} %collective-permute-done.9.got1, bf16[8,64,256]{2,1,0:T(8,128)(2,1)S(1)} %collective-permute-done.10.got2, ...), custom_call_target="tpu_custom_call" | custom-call | tf_op jit(solution)/shard_map/finish/pallas_call | solution.py:283
  154.2 3.1 %collective-permute-start.14 = (bf16[64,2048]{1,0:T(8,128)(2,1)}, bf16[64,2048]{1,0:T(8,128)(2,1)S(1)}, u32[]{:S(2)}, u32[]{:S(2)}) collective-permute-start(bf16[64,2048]{1,0:T(8,128)(2,1)} %finish.1.p0), channel_id=1, source_target_pairs={{0,2},{2,4},{4,6},{6,0},{1,3},{3,5},{5,7},{7,1},{8,10},{10,12},{12... | collective-permute-start | bytes 786440 | tf_op jit(solution)/shard_map/ppermute | solution.py:20
  157.2 4.3 %collective-permute-start.13 = (bf16[64,2048]{1,0:T(8,128)(2,1)}, bf16[64,2048]{1,0:T(8,128)(2,1)S(1)}, u32[]{:S(2)}, u32[]{:S(2)}) collective-permute-start(bf16[64,2048]{1,0:T(8,128)(2,1)} %finish.1.p0), channel_id=1, source_target_pairs={{0,4},{2,6},{4,0},{6,2},{1,5},{3,7},{5,1},{7,3},{8,12},{10,14},{12... | collective-permute-start | bytes 786440 | tf_op jit(solution)/shard_map/ppermute | solution.py:20
  161.6 2.2 %collective-permute-start.12 = (bf16[64,2048]{1,0:T(8,128)(2,1)}, bf16[64,2048]{1,0:T(8,128)(2,1)S(1)}, u32[]{:S(2)}, u32[]{:S(2)}) collective-permute-start(bf16[64,2048]{1,0:T(8,128)(2,1)} %finish.1.p0), channel_id=1, source_target_pairs={{0,6},{2,0},{4,2},{6,4},{1,7},{3,1},{5,3},{7,5},{8,14},{10,8},{12,... | collective-permute-start | bytes 786440 | tf_op jit(solution)/shard_map/ppermute | solution.py:20
  163.8 0.0 collective-permute-done.14.p3
  163.8 2.6 %collective-permute-done.13.p2 = bf16[64,2048]{1,0:T(8,128)(2,1)S(1)} collective-permute-done((bf16[64,2048]{1,0:T(8,128)(2,1)}, bf16[64,2048]{1,0:T(8,128)(2,1)S(1)}, u32[]{:S(2)}, u32[]{:S(2)}) %collective-permute-start.13) | collective-permute-done | bytes 262176 | tf_op jit(solution)/shard_map/ppermute | solution.py:20
  166.4 2.8 %collective-permute-done.12.p1 = bf16[64,2048]{1,0:T(8,128)(2,1)S(1)} collective-permute-done((bf16[64,2048]{1,0:T(8,128)(2,1)}, bf16[64,2048]{1,0:T(8,128)(2,1)S(1)}, u32[]{:S(2)}, u32[]{:S(2)}) %collective-permute-start.12) | collective-permute-done | bytes 262176 | tf_op jit(solution)/shard_map/ppermute | solution.py:20
  169.2 1.1 pad_maximum_fusion
  170.3 11.4 %collective-permute-start.15 = (bf16[4,64,2048]{2,1,0:T(8,128)(2,1)S(1)}, bf16[4,64,2048]{2,1,0:T(8,128)(2,1)S(1)}, u32[]{:S(2)}, u32[]{:S(2)}) collective-permute-start(bf16[4,64,2048]{2,1,0:T(8,128)(2,1)S(1)} %pad_maximum_fusion), channel_id=1, source_target_pairs={{0,1},{1,0},{2,3},{3,2},{4,5},{5,4},{6,7},{7,6},{8,9},{9,8},{10,11... | collective-permute-start | bytes 3145736 | tf_op jit(solution)/shard_map/ppermute | solution.py:20
  181.7 0.0 all-to-all-done.2.got_ref
  181.7 0.7 zsum.1
  182.4 12.3 %collective-permute-start.16 = (f32[32,384]{1,0:T(8,128)}, f32[32,384]{1,0:T(8,128)S(1)}, u32[]{:S(2)}, u32[]{:S(2)}) collective-permute-start(f32[32,384]{1,0:T(8,128)} %get-tuple-element.26), channel_id=1, source_target_pairs={{0,256},{256,0},{1,257},{257,1},{2,258},{258,2},{3,259},{259,3},{4... | collective-permute-start | bytes 147464 | tf_op jit(solution)/shard_map/ppermute | solution.py:20
  194.6 0.0 copy-start.8
  194.6 0.0 collective-permute-done.15.other_ref
  194.7 2.4 %place.1 = bf16[512,2048]{1,0:T(8,128)(2,1)} custom-call(s32[3]{0:T(128)} %pad_add_fusion.at_ref, bf16[64,2048]{1,0:T(8,128)(2,1)} %finish.1.p0, bf16[64,2048]{1,0:T(8,128)(2,1)S(1)} %collective-permute-done.12.p1, bf16[64,2048]{1,0:T(8,128)(2,1)S(1)} %collective-permute-done.13.p2, bf16[64,2048]{1,0:T(8,128)(2,1)S(1)} %collective-permute-done.14.p3, ...), custom_call_target="tpu_custom_call" | custom-call | tf_op jit(solution)/shard_map/place/pallas_call | solution.py:299
  197.1 3.5 %all-to-all-start.3 = ((f32[8,8,256]{2,1,0:T(8,128)}), f32[8,8,256]{2,1,0:T(8,128)S(1)}, u32[]{:S(2)}, u32[]{:S(2)}) async-start(f32[8,8,256]{2,1,0:T(8,128)} %get-tuple-element.25), calls=%async_computation.3 | async-start | bytes 131072 | tf_op jit(solution)/shard_map/all_to_all | solution.py:24
  200.6 0.0 collective-permute-done.16
  200.6 0.0 copy-done.8
  200.6 0.7 fusion.2
  201.3 4.2 %all-to-all-done.3 = f32[8,8,256]{2,1,0:T(8,128)S(1)} async-done(((f32[8,8,256]{2,1,0:T(8,128)}), f32[8,8,256]{2,1,0:T(8,128)S(1)}, u32[]{:S(2)}, u32[]{:S(2)}) %all-to-all-start.3) | async-done | bytes 65568 | tf_op jit(solution)/shard_map/all_to_all | solution.py:24
  205.5 0.6 copy.9
  (14 shorter events, 0.1 us)
Async XLA Ops:
  13.6 68.1 %copy-start = (bf16[4,64,1152]{2,1,0:T(8,128)(2,1)}, bf16[4,64,1152]{2,1,0:T(8,128)(2,1)S(1)}, u32[]{:S(2)}) copy-start(bf16[4,64,1152]{2,1,0:T(8,128)(2,1)S(1)} %all_to_all.20) | copy-start | bytes 1769476
  13.6 24.5 %collective-permute-start.3 = (bf16[256,1152]{1,0:T(8,128)(2,1)S(1)}, bf16[256,1152]{1,0:T(8,128)(2,1)S(1)}, u32[]{:S(2)}, u32[]{:S(2)}) collective-permute-start(bf16[256,1152]{1,0:T(8,128)(2,1)S(1)} %bitcast.18), channel_id=1, source_target_pairs={{0,32},{32,64},{64,96},{96,128},{128,160},{160,192},{192,224},{224... | collective-permute-start | bytes 1769480 | tf_op jit(solution)/shard_map/ppermute | solution.py:20
  18.9 21.1 %collective-permute-start = (bf16[256,1152]{1,0:T(8,128)(2,1)S(1)}, bf16[256,1152]{1,0:T(8,128)(2,1)S(1)}, u32[]{:S(2)}, u32[]{:S(2)}) collective-permute-start(bf16[256,1152]{1,0:T(8,128)(2,1)S(1)} %bitcast.19), channel_id=1, source_target_pairs={{0,480},{32,0},{64,32},{96,64},{128,96},{160,128},{192,160},{224,1... | collective-permute-start | bytes 1769480 | tf_op jit(solution)/shard_map/ppermute | solution.py:20
  38.1 43.7 %copy-start.3 = (bf16[256,1152]{1,0:T(8,128)(2,1)}, bf16[256,1152]{1,0:T(8,128)(2,1)S(1)}, u32[]{:S(2)}) copy-start(bf16[256,1152]{1,0:T(8,128)(2,1)S(1)} %collective-permute-done.3.refs_8_) | copy-start | bytes 1769476
  38.1 15.3 %collective-permute-start.4 = (bf16[256,1152]{1,0:T(8,128)(2,1)S(1)}, bf16[256,1152]{1,0:T(8,128)(2,1)S(1)}, u32[]{:S(2)}, u32[]{:S(2)}) collective-permute-start(bf16[256,1152]{1,0:T(8,128)(2,1)S(1)} %collective-permute-done.3.refs_8_), channel_id=1, source_target_pairs={{0,32},{32,64},{64,96},{96,128},{128,160},{160,192},{192,224},{224... | collective-permute-start | bytes 1769480 | tf_op jit(solution)/shard_map/ppermute | solution.py:20
  40.0 41.7 %copy-start.4 = (bf16[256,1152]{1,0:T(8,128)(2,1)}, bf16[256,1152]{1,0:T(8,128)(2,1)S(1)}, u32[]{:S(2)}) copy-start(bf16[256,1152]{1,0:T(8,128)(2,1)S(1)} %collective-permute-done.refs_1_) | copy-start | bytes 1769476
  40.0 15.3 %collective-permute-start.1 = (bf16[256,1152]{1,0:T(8,128)(2,1)S(1)}, bf16[256,1152]{1,0:T(8,128)(2,1)S(1)}, u32[]{:S(2)}, u32[]{:S(2)}) collective-permute-start(bf16[256,1152]{1,0:T(8,128)(2,1)S(1)} %collective-permute-done.refs_1_), channel_id=1, source_target_pairs={{0,480},{32,0},{64,32},{96,64},{128,96},{160,128},{192,160},{224,1... | collective-permute-start | bytes 1769480 | tf_op jit(solution)/shard_map/ppermute | solution.py:20
  53.4 14.5 %copy-start.5 = (bf16[256,1152]{1,0:T(8,128)(2,1)}, bf16[256,1152]{1,0:T(8,128)(2,1)S(1)}, u32[]{:S(2)}) copy-start(bf16[256,1152]{1,0:T(8,128)(2,1)S(1)} %collective-permute-done.4.refs_7_) | copy-start | bytes 1769476
  53.4 14.4 %collective-permute-start.5 = (bf16[256,1152]{1,0:T(8,128)(2,1)S(1)}, bf16[256,1152]{1,0:T(8,128)(2,1)S(1)}, u32[]{:S(2)}, u32[]{:S(2)}) collective-permute-start(bf16[256,1152]{1,0:T(8,128)(2,1)S(1)} %collective-permute-done.4.refs_7_), channel_id=1, source_target_pairs={{0,32},{32,64},{64,96},{96,128},{128,160},{160,192},{192,224},{224... | collective-permute-start | bytes 1769480 | tf_op jit(solution)/shard_map/ppermute | solution.py:20
  55.3 15.2 %copy-start.6 = (bf16[256,1152]{1,0:T(8,128)(2,1)}, bf16[256,1152]{1,0:T(8,128)(2,1)S(1)}, u32[]{:S(2)}) copy-start(bf16[256,1152]{1,0:T(8,128)(2,1)S(1)} %collective-permute-done.1.refs_2_) | copy-start | bytes 1769476
  55.3 15.2 %collective-permute-start.2 = (bf16[256,1152]{1,0:T(8,128)(2,1)S(1)}, bf16[256,1152]{1,0:T(8,128)(2,1)S(1)}, u32[]{:S(2)}, u32[]{:S(2)}) collective-permute-start(bf16[256,1152]{1,0:T(8,128)(2,1)S(1)} %collective-permute-done.1.refs_2_), channel_id=1, source_target_pairs={{0,480},{32,0},{64,32},{96,64},{128,96},{160,128},{192,160},{224,1... | collective-permute-start | bytes 1769480 | tf_op jit(solution)/shard_map/ppermute | solution.py:20
  67.9 13.9 %copy-start.1 = (bf16[256,1152]{1,0:T(8,128)(2,1)}, bf16[256,1152]{1,0:T(8,128)(2,1)S(1)}, u32[]{:S(2)}) copy-start(bf16[256,1152]{1,0:T(8,128)(2,1)S(1)} %collective-permute-done.5.refs_6_) | copy-start | bytes 1769476
  68.6 20.8 %collective-permute-start.6 = (bf16[128,1152]{1,0:T(8,128)(2,1)}, bf16[128,1152]{1,0:T(8,128)(2,1)S(1)}, u32[]{:S(2)}, u32[]{:S(2)}) collective-permute-start(bf16[128,1152]{1,0:T(8,128)(2,1)} %slice.8), channel_id=1, source_target_pairs={{0,32},{32,64},{64,96},{96,128},{128,160},{160,192},{192,224},{224... | collective-permute-start | bytes 884744 | tf_op jit(solution)/shard_map/ppermute | solution.py:20
  70.6 11.2 %copy-start.2 = (bf16[256,1152]{1,0:T(8,128)(2,1)}, bf16[256,1152]{1,0:T(8,128)(2,1)S(1)}, u32[]{:S(2)}) copy-start(bf16[256,1152]{1,0:T(8,128)(2,1)S(1)} %collective-permute-done.2.refs_3_) | copy-start | bytes 1769476
  71.4 18.0 %collective-permute-start.7 = (bf16[128,1152]{1,0:T(8,128)(2,1)}, bf16[128,1152]{1,0:T(8,128)(2,1)S(1)}, u32[]{:S(2)}, u32[]{:S(2)}) collective-permute-start(bf16[128,1152]{1,0:T(8,128)(2,1)} %slice.9), channel_id=1, source_target_pairs={{0,480},{32,0},{64,32},{96,64},{128,96},{160,128},{192,160},{224,1... | collective-permute-start | bytes 884744 | tf_op jit(solution)/shard_map/ppermute | solution.py:20
  81.8 7.0 %copy-start.7 = (f32[2048]{0:T(1024)S(1)}, f32[2048]{0:T(1024)}, u32[]{:S(2)}) copy-start(f32[2048]{0:T(1024)} %param.7) | copy-start | bytes 24580
  103.7 21.2 %all-to-all-start.1 = ((bf16[4,8,72,384]{3,2,1,0:T(8,128)(2,1)}), bf16[4,8,72,384]{3,2,1,0:T(8,128)(2,1)S(1)}, u32[]{:S(2)}, u32[]{:S(2)}) async-start(bf16[4,8,72,384]{3,2,1,0:T(8,128)(2,1)} %down.1), calls=%async_computation.1 | async-start | bytes 3538944 | tf_op jit(solution)/shard_map/all_to_all | solution.py:24
  107.3 26.6 %collective-permute-start.8 = (bf16[4,8,64,256]{3,2,1,0:T(8,128)(2,1)}, bf16[4,8,64,256]{3,2,1,0:T(8,128)(2,1)S(1)}, u32[]{:S(2)}, u32[]{:S(2)}) collective-permute-start(bf16[4,8,64,256]{3,2,1,0:T(8,128)(2,1)} %get-tuple-element.17), channel_id=1, source_target_pairs={{0,1},{1,0},{2,3},{3,2},{4,5},{5,4},{6,7},{7,6},{8,9},{9,8},{10,11... | collective-permute-start | bytes 3145736 | tf_op jit(solution)/shard_map/ppermute | solution.py:20
  126.6 55.0 %all-to-all-start.2 = ((bf16[16,40,384]{2,1,0:T(8,128)(2,1)}), bf16[16,40,384]{2,1,0:T(8,128)(2,1)S(1)}, u32[]{:S(2)}, u32[]{:S(2)}) async-start(bf16[16,40,384]{2,1,0:T(8,128)(2,1)} %ysum.1), calls=%async_computation.2 | async-start | bytes 983040 | tf_op jit(solution)/shard_map/all_to_all | solution.py:24
  136.2 10.6 %collective-permute-start.9 = (bf16[8,64,256]{2,1,0:T(8,128)(2,1)}, bf16[8,64,256]{2,1,0:T(8,128)(2,1)S(1)}, u32[]{:S(2)}, u32[]{:S(2)}) collective-permute-start(bf16[8,64,256]{2,1,0:T(8,128)(2,1)} %get-tuple-element.19), channel_id=1, source_target_pairs={{0,2},{2,4},{4,6},{6,0},{1,3},{3,5},{5,7},{7,1},{8,10},{10,12},{12... | collective-permute-start | bytes 786440 | tf_op jit(solution)/shard_map/ppermute | solution.py:20
  139.3 9.5 %collective-permute-start.10 = (bf16[8,64,256]{2,1,0:T(8,128)(2,1)}, bf16[8,64,256]{2,1,0:T(8,128)(2,1)S(1)}, u32[]{:S(2)}, u32[]{:S(2)}) collective-permute-start(bf16[8,64,256]{2,1,0:T(8,128)(2,1)} %get-tuple-element.20), channel_id=1, source_target_pairs={{0,4},{2,6},{4,0},{6,2},{1,5},{3,7},{5,1},{7,3},{8,12},{10,14},{12... | collective-permute-start | bytes 786440 | tf_op jit(solution)/shard_map/ppermute | solution.py:20
  143.7 7.6 %collective-permute-start.11 = (bf16[8,64,256]{2,1,0:T(8,128)(2,1)}, bf16[8,64,256]{2,1,0:T(8,128)(2,1)S(1)}, u32[]{:S(2)}, u32[]{:S(2)}) collective-permute-start(bf16[8,64,256]{2,1,0:T(8,128)(2,1)} %get-tuple-element.21), channel_id=1, source_target_pairs={{0,6},{2,0},{4,2},{6,4},{1,7},{3,1},{5,3},{7,5},{8,14},{10,8},{12,... | collective-permute-start | bytes 786440 | tf_op jit(solution)/shard_map/ppermute | solution.py:20
  154.2 9.6 %collective-permute-start.14 = (bf16[64,2048]{1,0:T(8,128)(2,1)}, bf16[64,2048]{1,0:T(8,128)(2,1)S(1)}, u32[]{:S(2)}, u32[]{:S(2)}) collective-permute-start(bf16[64,2048]{1,0:T(8,128)(2,1)} %finish.1.p0), channel_id=1, source_target_pairs={{0,2},{2,4},{4,6},{6,0},{1,3},{3,5},{5,7},{7,1},{8,10},{10,12},{12... | collective-permute-start | bytes 786440 | tf_op jit(solution)/shard_map/ppermute | solution.py:20
  157.2 9.1 %collective-permute-start.13 = (bf16[64,2048]{1,0:T(8,128)(2,1)}, bf16[64,2048]{1,0:T(8,128)(2,1)S(1)}, u32[]{:S(2)}, u32[]{:S(2)}) collective-permute-start(bf16[64,2048]{1,0:T(8,128)(2,1)} %finish.1.p0), channel_id=1, source_target_pairs={{0,4},{2,6},{4,0},{6,2},{1,5},{3,7},{5,1},{7,3},{8,12},{10,14},{12... | collective-permute-start | bytes 786440 | tf_op jit(solution)/shard_map/ppermute | solution.py:20
  161.6 7.6 %collective-permute-start.12 = (bf16[64,2048]{1,0:T(8,128)(2,1)}, bf16[64,2048]{1,0:T(8,128)(2,1)S(1)}, u32[]{:S(2)}, u32[]{:S(2)}) collective-permute-start(bf16[64,2048]{1,0:T(8,128)(2,1)} %finish.1.p0), channel_id=1, source_target_pairs={{0,6},{2,0},{4,2},{6,4},{1,7},{3,1},{5,3},{7,5},{8,14},{10,8},{12,... | collective-permute-start | bytes 786440 | tf_op jit(solution)/shard_map/ppermute | solution.py:20
  170.3 24.4 %collective-permute-start.15 = (bf16[4,64,2048]{2,1,0:T(8,128)(2,1)S(1)}, bf16[4,64,2048]{2,1,0:T(8,128)(2,1)S(1)}, u32[]{:S(2)}, u32[]{:S(2)}) collective-permute-start(bf16[4,64,2048]{2,1,0:T(8,128)(2,1)S(1)} %pad_maximum_fusion), channel_id=1, source_target_pairs={{0,1},{1,0},{2,3},{3,2},{4,5},{5,4},{6,7},{7,6},{8,9},{9,8},{10,11... | collective-permute-start | bytes 3145736 | tf_op jit(solution)/shard_map/ppermute | solution.py:20
  182.4 18.3 %collective-permute-start.16 = (f32[32,384]{1,0:T(8,128)}, f32[32,384]{1,0:T(8,128)S(1)}, u32[]{:S(2)}, u32[]{:S(2)}) collective-permute-start(f32[32,384]{1,0:T(8,128)} %get-tuple-element.26), channel_id=1, source_target_pairs={{0,256},{256,0},{1,257},{257,1},{2,258},{258,2},{3,259},{259,3},{4... | collective-permute-start | bytes 147464 | tf_op jit(solution)/shard_map/ppermute | solution.py:20
  194.6 6.0 %copy-start.8 = (f32[32,384]{1,0:T(8,128)S(1)}, f32[32,384]{1,0:T(8,128)}, u32[]{:S(2)}) copy-start(f32[32,384]{1,0:T(8,128)} %get-tuple-element.26) | copy-start | bytes 147460
  197.1 8.4 %all-to-all-start.3 = ((f32[8,8,256]{2,1,0:T(8,128)}), f32[8,8,256]{2,1,0:T(8,128)S(1)}, u32[]{:S(2)}, u32[]{:S(2)}) async-start(f32[8,8,256]{2,1,0:T(8,128)} %get-tuple-element.25), calls=%async_computation.3 | async-start | bytes 131072 | tf_op jit(solution)/shard_map/all_to_all | solution.py:24

commit v4 on v3

--- a/solution.py
+++ b/solution.py
@@ -11,6 +11,7 @@
 TP = ("x", "c")
 RING = ("rep", "fs_0")
 EPS = 1e-06
+EARLY = (0, 1, 7, 2, 6)
 F32 = jnp.float32
 BF16 = jnp.bfloat16
 
@@ -31,15 +32,6 @@
 
 def rolled(v, start):
     return lax.dynamic_slice_in_dim(jnp.concatenate([v, v], axis=0), start, v.shape[0], axis=0)
-
-
-def blocks_of(refs):
-    for d in range(4):
-        yield d, 0, refs[d]
-    yield 4, 0, refs[4]
-    yield 4, refs[4].shape[0], refs[5]
-    for d in range(5, 8):
-        yield d, 0, refs[d + 1]
 
 
 def prepare_tokens(at_ref, x_ref, gain_ref, out_ref):
@@ -61,56 +53,109 @@
         turned_ref[d] = part.T
 
 
-def grad_kernel(x_ref, c_ref, gain_ref, *refs):
-    w_refs, (mine_ref, other_ref, hid_ref, sum_ref) = refs[:9], refs[9:]
-    units = hid_ref.shape[1]
-    nx, _, part, _ = mine_ref.shape
+def forward_kernel(x_ref, c_ref, *refs):
+    w_refs, acc_ref = refs[:-1], refs[-1]
+    units = acc_ref.shape[1] // 3
     gu = dh = None
-    for d, lo, w in blocks_of(w_refs):
-        rows = w.shape[0]
-        a = jnp.dot(x_ref[d, :, lo : lo + rows], w[:, : 2 * units], preferred_element_type=F32)
-        b = jnp.dot(c_ref[d, :, lo : lo + rows], w[:, 2 * units :], preferred_element_type=F32)
+    for d, w in zip(EARLY, w_refs):
+        a = jnp.dot(x_ref[d], w[:, : 2 * units], preferred_element_type=F32)
+        b = jnp.dot(c_ref[d], w[:, 2 * units :], preferred_element_type=F32)
         gu = a if gu is None else gu + a
         dh = b if dh is None else dh + b
+    acc_ref[:, : 2 * units] = gu
+    acc_ref[:, 2 * units :] = dh
+
+
+def grad_kernel(gain_ref, lo_ref, hi_ref, acc_hbm, x_hbm, c_hbm, ct_hbm, *refs):
+    w_hbm, (mine_hbm, other_hbm, dd_hbm) = refs[:7], refs[7:10]
+    acc, xv, cv, ctv, wv, ov, dv, sems = refs[10:]
+    units = acc.shape[1] // 3
+    nz, _, cols = xv.shape
+    ny, _, longer, _ = dv.shape
+    nx, part = mine_hbm.shape[0], mine_hbm.shape[2]
+    rows = longer - 8
+    used = [0]
+
+    def begin(src, dst):
+        copy = pltpu.make_async_copy(src, dst, sems.at[used[0]])
+        used[0] += 1
+        copy.start()
+        return copy
+
+    slot = {0: 0, 1: 1, 2: 2, 3: 3, 5: 4, 6: 5, 7: 6}
+    acc_in = begin(acc_hbm, acc)
+    x_in, c_in, w_in = {}, {}, {}
+    for d in (3, 5):
+        w_in[d] = begin(w_hbm[slot[d]], wv.at[slot[d]])
+        x_in[d] = begin(x_hbm.at[d], xv.at[d])
+        c_in[d] = begin(c_hbm.at[d], cv.at[d - 3])
+    x_in[4] = begin(x_hbm.at[4], xv.at[4])
+    c_in[4] = begin(c_hbm.at[4], cv.at[1])
+    for d in EARLY:
+        w_in[d] = begin(w_hbm[slot[d]], wv.at[slot[d]])
+        x_in[d] = begin(x_hbm.at[d], xv.at[d])
+    ct_in = begin(ct_hbm, ctv)
+
+    half = cols // 2
+    halves = ((lo_ref, slice(0, half)), (hi_ref, slice(half, cols)))
+    acc_in.wait()
+    gu, dh = acc[:, : 2 * units], acc[:, 2 * units :]
+    for d in (3, 5):
+        w_in[d].wait()
+        x_in[d].wait()
+        c_in[d].wait()
+        w = wv.at[slot[d]]
+        gu = gu + jnp.dot(xv[d], w[:, : 2 * units], preferred_element_type=F32)
+        dh = dh + jnp.dot(cv[d - 3], w[:, 2 * units :], preferred_element_type=F32)
+    x_in[4].wait()
+    c_in[4].wait()
+    for w, at in halves:
+        gu = gu + jnp.dot(xv[4, :, at], w[:, : 2 * units], preferred_element_type=F32)
+        dh = dh + jnp.dot(cv[1, :, at], w[:, 2 * units :], preferred_element_type=F32)
     gate, up = gu[:, :units], gu[:, units:]
     dh = 0.5 * dh
     sig = jax.nn.sigmoid(gate)
     act = gate * sig
-    hid_ref[...] = (act * up).astype(BF16)
+    hidden = (act * up).astype(BF16)
     d_gate = (dh * up * sig * (1.0 + gate * (1.0 - sig))).astype(BF16)
     d_up = (dh * act).astype(BF16)
     both = jnp.concatenate([d_gate, d_up], axis=1)
-    for d, lo, w in blocks_of(w_refs):
-        rows = w.shape[0]
-        out = lax.dot_general(
-            both, w[:, : 2 * units], (((1,), (1,)), ((), ())), preferred_element_type=F32
-        )
-        terms = x_ref[d, :, lo : lo + rows].astype(F32) * out
-        sums = jnp.sum(terms, axis=0, keepdims=True)
-        sum_ref[d, :, lo : lo + rows] = sums / gain_ref[d, :, lo : lo + rows]
-        out = out.astype(BF16)
-        for k in range(nx):
-            mine_ref[k, d, :, lo : lo + rows] = out[k * part : (k + 1) * part]
-            other_ref[k, d, :, lo : lo + rows] = out[(nx + k) * part : (nx + k + 1) * part]
-
-
-def down_kernel(ct_ref, hid_ref, sum_ref, out_ref):
-    ny, nz, longer, units = out_ref.shape
-    rows = longer - 8
-    cols = sum_ref.shape[2]
-    for d in range(nz):
-        res = jnp.dot(ct_ref[d], hid_ref[...], preferred_element_type=F32)
+    out_copies = []
+    sums = {}
+    for d in (4, 3, 5) + EARLY:
+        if d in EARLY:
+            w_in[d].wait()
+            x_in[d].wait()
+        pieces = halves if d == 4 else ((wv.at[slot[d]], slice(0, cols)),)
+        got = []
+        for w, at in pieces:
+            out = lax.dot_general(
+                both, w[:, : 2 * units], (((1,), (1,)), ((), ())), preferred_element_type=F32
+            )
+            terms = jnp.sum(xv[d, :, at].astype(F32) * out, axis=0, keepdims=True)
+            got.append(terms / gain_ref[d, :, at])
+            out = out.astype(BF16)
+            for k in range(2 * nx):
+                ov[k, d, :, at] = out[k * part : (k + 1) * part]
+        sums[d] = got[0] if len(got) == 1 else jnp.concatenate(got, axis=1)
+        out_copies.append(begin(ov.at[pl.ds(nx, nx), d], other_hbm.at[:, d]))
+        out_copies.append(begin(ov.at[pl.ds(0, nx), d], mine_hbm.at[:, d]))
+    ct_in.wait()
+    for d in range(nz):
+        res = jnp.dot(ctv[d], hidden, preferred_element_type=F32)
         res = (0.5 * res).astype(BF16)
-        sums = sum_ref[d]
-        high = sums.astype(BF16)
-        left = sums - high.astype(F32)
+        high = sums[d].astype(BF16)
+        left = sums[d] - high.astype(F32)
         mid = left.astype(BF16)
         low = (left - mid.astype(F32)).astype(BF16)
         extra = jnp.concatenate([high, mid, low, jnp.zeros((5, cols), BF16)], axis=0)
         extra = jnp.concatenate([extra, jnp.zeros((8, units - cols), BF16)], axis=1)
         for y in range(ny):
-            out_ref[y, d, :rows] = res[y * rows : (y + 1) * rows]
-            out_ref[y, d, rows:] = extra
+            dv[y, d, :rows] = res[y * rows : (y + 1) * rows]
+            dv[y, d, rows:] = extra
+        out_copies.append(begin(dv.at[:, d], dd_hbm.at[:, d]))
+    for copy in out_copies:
+        copy.wait()
 
 
 def rows_kernel(at_ref, got_ref, out_ref):
@@ -205,7 +250,7 @@
     mid = cols // 2
     last_f = shifted(fwd[-1][:mid], RING, 1)
     last_b = shifted(bwd[-1][mid:], RING, -1)
-    weights = [w0, bwd[1], bwd[2], bwd[3], last_f, last_b, fwd[3], fwd[2], fwd[1]]
+    weights = [w0, bwd[1], bwd[2], bwd[3], fwd[3], fwd[2], fwd[1]]
 
     def spot(i, at):
         return ((i // nx + at[1]) % 2) * nx + (i + at[2]) % nx
@@ -246,26 +291,36 @@
     )(at, cotangent, cotangent)
 
     gain_ring = rolled(gain.reshape(nz, 1, cols), zl)
-    mine, other, hidden, sums = pl.pallas_call(
+    acc = pl.pallas_call(
+        forward_kernel,
+        out_shape=jax.ShapeDtypeStruct((tokens, 3 * units), F32),
+        in_specs=vmem(7),
+        out_specs=pl.BlockSpec(memory_space=pltpu.VMEM),
+        name="forward",
+    )(xr, cr, w0, bwd[1], fwd[1], bwd[2], fwd[2])
+    anywhere = pl.BlockSpec(memory_space=pl.ANY)
+    mine, other, dd = pl.pallas_call(
         grad_kernel,
         out_shape=(
             jax.ShapeDtypeStruct((nx, nz, part, cols), BF16),
             jax.ShapeDtypeStruct((nx, nz, part, cols), BF16),
-            jax.ShapeDtypeStruct((tokens, units), BF16),
-            jax.ShapeDtypeStruct((nz, 1, cols), F32),
-        ),
-        in_specs=vmem(12),
-        out_specs=tuple(vmem(4)),
+            jax.ShapeDtypeStruct((ny, nz, rows + 8, units), BF16),
+        ),
+        in_specs=vmem(3) + [anywhere] * 11,
+        out_specs=(anywhere,) * 3,
+        scratch_shapes=[
+            pltpu.VMEM((tokens, 3 * units), F32),
+            pltpu.VMEM((nz, tokens, cols), BF16),
+            pltpu.VMEM((3, tokens, cols), BF16),
+            pltpu.VMEM((nz, cols, tokens), BF16),
+            pltpu.VMEM((7, cols, 3 * units), BF16),
+            pltpu.VMEM((2 * nx, nz, part, cols), BF16),
+            pltpu.VMEM((ny, nz, rows + 8, units), BF16),
+            pltpu.SemaphoreType.DMA((48,)),
+        ],
         name="grad",
-    )(xr, cr, gain_ring, *weights[:4], *near(last_f, last_b), *weights[6:])
+    )(gain_ring, *near(last_f, last_b), acc, xr, cr, ct, *weights)
     theirs = shifted(other, "c", 1)
-    (dd,) = pl.pallas_call(
-        down_kernel,
-        out_shape=(jax.ShapeDtypeStruct((ny, nz, rows + 8, units), BF16),),
-        in_specs=vmem(3),
-        out_specs=tuple(vmem(1)),
-        name="down",
-    )(ct, hidden, sums)
     dy = exchanged(dd, "fs_1")
 
     chunk = jax.ShapeDtypeStruct((nz, part, cols), BF16)

time: 207 us -> 209 us (level)
  waiting for transfers between devices: 51.3 us -> 48.2 us
  Pallas kernels: 36.5 us -> 39.5 us
    ppermute x17, waiting for transfers between devices: 36.3 us -> 33.3 us  [shifted(): return lax.ppermute(v, axis, [(i, (i + by) % n) for i in range(n)])]
    ppermute x17, starting transfers between devices: 84.8 us -> 87 us  [shifted(): return lax.ppermute(v, axis, [(i, (i + by) % n) for i in range(n)])]
    pallas_call x1, Pallas kernels: 4.19 us -> 6.29 us  [work(): pl.pallas_call(forward_kernel, out_shape=jax.ShapeDtypeStruct((tokens, 3...]
  transfers between devices with their start and end apart: 20 -> 20, of which waited for: 9 -> 9; matrix products, arithmetic and copies ran while one was open for 2% -> 2% of each run, Pallas kernels for 11% -> 14%
where the time goes in v4:
time: 209 us; the launch traced here: 208 us
  starting transfers between devices  101 us (48%)
  waiting for transfers between devices  48.2 us (23%)
  Pallas kernels  39.5 us (19%)
  blocking collectives  12.1 us (6%)
  other arithmetic  3.85 us (2%)
  local copies, waits for them, and re-layouts  2.41 us (1%)
    ppermute x17, starting transfers between devices, shifted(): return lax.ppermute(v, axis, [(i, (i + by) % n) for i in range(n)])  87 us
    ppermute x17, waiting for transfers between devices, shifted(): return lax.ppermute(v, axis, [(i, (i + by) % n) for i in range(n)])  33.3 us
    all_to_all x3, waiting for transfers between devices, exchanged(): return lax.all_to_all(v, axis, 0, 0, tiled=True)  15 us
    all_to_all x3, starting transfers between devices, exchanged(): return lax.all_to_all(v, axis, 0, 0, tiled=True)  13.9 us
    all_to_all x1, blocking collectives, exchanged(): return lax.all_to_all(v, axis, 0, 0, tiled=True)  12.1 us
    pallas_call x1, Pallas kernels, work(): pl.pallas_call(grad_kernel, out_shape=(jax.ShapeDtypeStruct((nx, nz, part...  11 us
    pallas_call x1, Pallas kernels, work(): pl.pallas_call(prepare_tokens, out_shape=jax.ShapeDtypeStruct((nz, tokens...  6.97 us
    pallas_call x1, Pallas kernels, work(): pl.pallas_call(forward_kernel, out_shape=jax.ShapeDtypeStruct((tokens, 3...  6.29 us
  transfers between devices with their start and end apart: 20, of which 9 were waited for; matrix products, arithmetic and copies ran while one was open for 2% of the time, Pallas kernels for 14%

profile of v4, /device:TPU:1, one launch (start us, length us, event | category | flops | bytes accessed | tf_op | source)
XLA Modules:
  0.0 207.9 jit_solution(18280409580936776621)
XLA Ops:
  0.6 0.9 pad_maximum_fusion.1
  1.5 12.1 %all_to_all.20 = bf16[4,64,1152]{2,1,0:T(8,128)(2,1)S(1)} all-to-all(bf16[4,64,1152]{2,1,0:T(8,128)(2,1)S(1)} %broadcast_in_dim.4), channel_id=1, replica_groups=mesh['rep'=2,'fs_0'=8,'fs_1'=4,'x'=4,'c'=2] {'fs_1'}, dimensions={0} | all-to-all | bytes 1179648 | tf_op jit(solution)/shard_map/all_to_all | solution.py:25
  13.6 12.9 %collective-permute-start.4 = (bf16[256,1152]{1,0:T(8,128)(2,1)S(1)}, bf16[256,1152]{1,0:T(8,128)(2,1)S(1)}, u32[]{:S(2)}, u32[]{:S(2)}) collective-permute-start(bf16[256,1152]{1,0:T(8,128)(2,1)S(1)} %bitcast.18), channel_id=1, source_target_pairs={{0,480},{32,0},{64,32},{96,64},{128,96},{160,128},{192,160},{224,1... | collective-permute-start | bytes 1769480 | tf_op jit(solution)/shard_map/ppermute | solution.py:21
  26.5 1.9 collective-permute-start
  28.4 8.6 %collective-permute-done.4.refs_1_ = bf16[256,1152]{1,0:T(8,128)(2,1)S(1)} collective-permute-done((bf16[256,1152]{1,0:T(8,128)(2,1)S(1)}, bf16[256,1152]{1,0:T(8,128)(2,1)S(1)}, u32[]{:S(2)}, u32[]{:S(2)}) %collective-permute-start.4) | collective-permute-done | bytes 589856 | tf_op jit(solution)/shard_map/ppermute | solution.py:21
  37.1 5.3 %collective-permute-start.5 = (bf16[256,1152]{1,0:T(8,128)(2,1)S(1)}, bf16[256,1152]{1,0:T(8,128)(2,1)S(1)}, u32[]{:S(2)}, u32[]{:S(2)}) collective-permute-start(bf16[256,1152]{1,0:T(8,128)(2,1)S(1)} %collective-permute-done.4.refs_1_), channel_id=1, source_target_pairs={{0,480},{32,0},{64,32},{96,64},{128,96},{160,128},{192,160},{224,1... | collective-permute-start | bytes 1769480 | tf_op jit(solution)/shard_map/ppermute | solution.py:21
  42.4 0.0 collective-permute-done.refs_2_.refs_6_
  42.4 0.0 copy-start.2
  42.4 1.9 collective-permute-start.1
  44.3 7.8 %collective-permute-done.5.refs_3_.refs_2_ = bf16[256,1152]{1,0:T(8,128)(2,1)S(1)} collective-permute-done((bf16[256,1152]{1,0:T(8,128)(2,1)S(1)}, bf16[256,1152]{1,0:T(8,128)(2,1)S(1)}, u32[]{:S(2)}, u32[]{:S(2)}) %collective-permute-start.5) | collective-permute-done | bytes 589856 | tf_op jit(solution)/shard_map/ppermute | solution.py:21
  52.1 5.3 %collective-permute-start.6 = (bf16[256,1152]{1,0:T(8,128)(2,1)S(1)}, bf16[256,1152]{1,0:T(8,128)(2,1)S(1)}, u32[]{:S(2)}, u32[]{:S(2)}) collective-permute-start(bf16[256,1152]{1,0:T(8,128)(2,1)S(1)} %collective-permute-done.5.refs_3_.refs_2_), channel_id=1, source_target_pairs={{0,480},{32,0},{64,32},{96,64},{128,96},{160,128},{192,160},{224,1... | collective-permute-start | bytes 1769480 | tf_op jit(solution)/shard_map/ppermute | solution.py:21
  57.4 0.0 collective-permute-done.1.refs_4_.refs_5_
  57.4 1.9 collective-permute-start.2
  59.4 6.9 %collective-permute-done.6.refs_3_ = bf16[256,1152]{1,0:T(8,128)(2,1)S(1)} collective-permute-done((bf16[256,1152]{1,0:T(8,128)(2,1)S(1)}, bf16[256,1152]{1,0:T(8,128)(2,1)S(1)}, u32[]{:S(2)}, u32[]{:S(2)}) %collective-permute-start.6) | collective-permute-done | bytes 589856 | tf_op jit(solution)/shard_map/ppermute | solution.py:21
  66.3 0.8 slice.9
  67.1 5.3 %collective-permute-start.7 = (bf16[128,1152]{1,0:T(8,128)(2,1)}, bf16[128,1152]{1,0:T(8,128)(2,1)S(1)}, u32[]{:S(2)}, u32[]{:S(2)}) collective-permute-start(bf16[128,1152]{1,0:T(8,128)(2,1)} %slice.9), channel_id=1, source_target_pairs={{0,480},{32,0},{64,32},{96,64},{128,96},{160,128},{192,160},{224,1... | collective-permute-start | bytes 884744 | tf_op jit(solution)/shard_map/ppermute | solution.py:21
  72.4 0.0 collective-permute-done.2.refs_4_
  72.4 0.8 slice.8
  73.2 0.1 copy-done.6
  73.3 1.9 collective-permute-start.3
  75.3 0.6 pad_add_fusion.at_ref
  75.8 5.2 %prepare_c.1 = (bf16[8,512,256]{2,1,0:T(8,128)(2,1)}, bf16[8,256,512]{2,1,0:T(8,128)(2,1)}) custom-call(s32[3]{0:T(128)} %pad_add_fusion.at_ref, bf16[512,2048]{1,0:T(8,128)(2,1)} %c_ref.1, bf16[512,2048]{1,0:T(8,128)(2,1)} %c_ref.1), custom_call_target="tpu_custom_call" | custom-call | tf_op jit(solution)/shard_map/prepare_c/pallas_call | solution.py:272
  81.1 0.0 copy-done
  81.1 0.0 copy-start.7
  81.1 7.0 %prepare_x.1.x_ref.x_hbm = bf16[8,512,256]{2,1,0:T(8,128)(2,1)} custom-call(s32[3]{0:T(128)} %pad_add_fusion.at_ref, bf16[512,2048]{1,0:T(8,128)(2,1)} %x_ref.3, f32[1,2048]{1,0:T(1,128)} %bitcast.24), custom_call_target="tpu_custom_call" | custom-call | tf_op jit(solution)/shard_map/prepare_x/pallas_call | solution.py:258
  88.1 0.6 fusion.3.gain_ref
  88.7 6.3 %forward.1.acc_hbm = f32[512,1152]{1,0:T(8,128)} custom-call(bf16[8,512,256]{2,1,0:T(8,128)(2,1)} %prepare_x.1.x_ref.x_hbm, bf16[8,512,256]{2,1,0:T(8,128)(2,1)} %get-tuple-element.14.c_ref.c_hbm, bf16[256,1152]{1,0:T(8,128)(2,1)} %bitcast.20, bf16[256,1152]{1,0:T(8,128)(2,1)} %copy-done.1, bf16[256,1152]{1,0:T(8,128)(2,1)} %copy-done.2, ...), custom_call_target="tpu_custom_call" | custom-call | tf_op jit(solution)/shard_map/forward/pallas_call | solution.py:294
  95.0 0.0 collective-permute-done.7.hi_ref
  95.0 0.0 collective-permute-done.3.lo_ref
  95.0 11.0 %grad.1 = (bf16[4,8,64,256]{3,2,1,0:T(8,128)(2,1)}, bf16[4,8,64,256]{3,2,1,0:T(8,128)(2,1)}, bf16[4,8,72,384]{3,2,1,0:T(8,128)(2,1)}) custom-call(f32[8,1,256]{2,1,0:T(1,128)} %fusion.3.gain_ref, bf16[128,1152]{1,0:T(8,128)(2,1)S(1)} %collective-permute-done.3.lo_ref, bf16[128,1152]{1,0:T(8,128)(2,1)S(1)} %collective-permute-done.7.hi_ref, ...), custom_call_target="tpu_custom_call" | custom-call | tf_op jit(solution)/shard_map/grad/pallas_call | solution.py:302
  106.0 3.6 %all-to-all-start.1 = ((bf16[4,8,72,384]{3,2,1,0:T(8,128)(2,1)}), bf16[4,8,72,384]{3,2,1,0:T(8,128)(2,1)S(1)}, u32[]{:S(2)}, u32[]{:S(2)}) async-start(bf16[4,8,72,384]{3,2,1,0:T(8,128)(2,1)} %get-tuple-element.22), calls=%async_computation.1 | async-start | bytes 3538944 | tf_op jit(solution)/shard_map/all_to_all | solution.py:25
  109.6 6.9 %collective-permute-start.8 = (bf16[4,8,64,256]{3,2,1,0:T(8,128)(2,1)}, bf16[4,8,64,256]{3,2,1,0:T(8,128)(2,1)S(1)}, u32[]{:S(2)}, u32[]{:S(2)}) collective-permute-start(bf16[4,8,64,256]{3,2,1,0:T(8,128)(2,1)} %get-tuple-element.17), channel_id=1, source_target_pairs={{0,1},{1,0},{2,3},{3,2},{4,5},{5,4},{6,7},{7,6},{8,9},{9,8},{10,11... | collective-permute-start | bytes 3145736 | tf_op jit(solution)/shard_map/ppermute | solution.py:21
  116.5 10.8 %all-to-all-done.1.got_ref = bf16[4,8,72,384]{3,2,1,0:T(8,128)(2,1)S(1)} async-done(((bf16[4,8,72,384]{3,2,1,0:T(8,128)(2,1)}), bf16[4,8,72,384]{3,2,1,0:T(8,128)(2,1)S(1)}, u32[]{:S(2)}, u32[]{:S(2)}) %all-to-all-start.1) | async-done | bytes 1769504 | tf_op jit(solution)/shard_map/all_to_all | solution.py:25
  127.3 1.7 ysum.1
  129.0 6.8 %all-to-all-start.2 = ((bf16[16,40,384]{2,1,0:T(8,128)(2,1)}), bf16[16,40,384]{2,1,0:T(8,128)(2,1)S(1)}, u32[]{:S(2)}, u32[]{:S(2)}) async-start(bf16[16,40,384]{2,1,0:T(8,128)(2,1)} %ysum.1), calls=%async_computation.2 | async-start | bytes 983040 | tf_op jit(solution)/shard_map/all_to_all | solution.py:25
  135.7 0.0 collective-permute-done.8.theirs_ref
  135.7 2.3 %chip.1 = (bf16[8,64,256]{2,1,0:T(8,128)(2,1)}, bf16[8,64,256]{2,1,0:T(8,128)(2,1)}, bf16[8,64,256]{2,1,0:T(8,128)(2,1)}, bf16[8,64,256]{2,1,0:T(8,128)(2,1)}) custom-call(bf16[4,8,64,256]{3,2,1,0:T(8,128)(2,1)} %get-tuple-element.16.mine_ref, bf16[4,8,64,256]{3,2,1,0:T(8,128)(2,1)S(1)} %collective-permute-done.8.theirs_ref), custom_call_target="tpu_custom_call" | custom-call | tf_op jit(solution)/shard_map/chip/pallas_call | solution.py:327
  138.0 3.1 %collective-permute-start.9 = (bf16[8,64,256]{2,1,0:T(8,128)(2,1)}, bf16[8,64,256]{2,1,0:T(8,128)(2,1)S(1)}, u32[]{:S(2)}, u32[]{:S(2)}) collective-permute-start(bf16[8,64,256]{2,1,0:T(8,128)(2,1)} %get-tuple-element.19), channel_id=1, source_target_pairs={{0,2},{2,4},{4,6},{6,0},{1,3},{3,5},{5,7},{7,1},{8,10},{10,12},{12... | collective-permute-start | bytes 786440 | tf_op jit(solution)/shard_map/ppermute | solution.py:21
  141.1 4.4 %collective-permute-start.10 = (bf16[8,64,256]{2,1,0:T(8,128)(2,1)}, bf16[8,64,256]{2,1,0:T(8,128)(2,1)S(1)}, u32[]{:S(2)}, u32[]{:S(2)}) collective-permute-start(bf16[8,64,256]{2,1,0:T(8,128)(2,1)} %get-tuple-element.20), channel_id=1, source_target_pairs={{0,4},{2,6},{4,0},{6,2},{1,5},{3,7},{5,1},{7,3},{8,12},{10,14},{12... | collective-permute-start | bytes 786440 | tf_op jit(solution)/shard_map/ppermute | solution.py:21
  145.5 3.0 %collective-permute-start.11 = (bf16[8,64,256]{2,1,0:T(8,128)(2,1)}, bf16[8,64,256]{2,1,0:T(8,128)(2,1)S(1)}, u32[]{:S(2)}, u32[]{:S(2)}) collective-permute-start(bf16[8,64,256]{2,1,0:T(8,128)(2,1)} %get-tuple-element.21), channel_id=1, source_target_pairs={{0,6},{2,0},{4,2},{6,4},{1,7},{3,1},{5,3},{7,5},{8,14},{10,8},{12,... | collective-permute-start | bytes 786440 | tf_op jit(solution)/shard_map/ppermute | solution.py:21
  148.5 0.0 collective-permute-done.9.got1
  148.6 2.1 collective-permute-done.10.got2
  150.6 2.5 %collective-permute-done.11.got3 = bf16[8,64,256]{2,1,0:T(8,128)(2,1)S(1)} collective-permute-done((bf16[8,64,256]{2,1,0:T(8,128)(2,1)}, bf16[8,64,256]{2,1,0:T(8,128)(2,1)S(1)}, u32[]{:S(2)}, u32[]{:S(2)}) %collective-permute-start.11) | collective-permute-done | bytes 262176 | tf_op jit(solution)/shard_map/ppermute | solution.py:21
  153.1 2.9 %finish.1.p0 = bf16[64,2048]{1,0:T(8,128)(2,1)} custom-call(s32[3]{0:T(128)} %pad_add_fusion.at_ref, bf16[8,64,256]{2,1,0:T(8,128)(2,1)} %get-tuple-element.18.got0, bf16[8,64,256]{2,1,0:T(8,128)(2,1)S(1)} %collective-permute-done.9.got1, bf16[8,64,256]{2,1,0:T(8,128)(2,1)S(1)} %collective-permute-done.10.got2, ...), custom_call_target="tpu_custom_call" | custom-call | tf_op jit(solution)/shard_map/finish/pallas_call | solution.py:338
  156.0 3.0 %collective-permute-start.14 = (bf16[64,2048]{1,0:T(8,128)(2,1)}, bf16[64,2048]{1,0:T(8,128)(2,1)S(1)}, u32[]{:S(2)}, u32[]{:S(2)}) collective-permute-start(bf16[64,2048]{1,0:T(8,128)(2,1)} %finish.1.p0), channel_id=1, source_target_pairs={{0,2},{2,4},{4,6},{6,0},{1,3},{3,5},{5,7},{7,1},{8,10},{10,12},{12... | collective-permute-start | bytes 786440 | tf_op jit(solution)/shard_map/ppermute | solution.py:21
  159.1 4.3 %collective-permute-start.13 = (bf16[64,2048]{1,0:T(8,128)(2,1)}, bf16[64,2048]{1,0:T(8,128)(2,1)S(1)}, u32[]{:S(2)}, u32[]{:S(2)}) collective-permute-start(bf16[64,2048]{1,0:T(8,128)(2,1)} %finish.1.p0), channel_id=1, source_target_pairs={{0,4},{2,6},{4,0},{6,2},{1,5},{3,7},{5,1},{7,3},{8,12},{10,14},{12... | collective-permute-start | bytes 786440 | tf_op jit(solution)/shard_map/ppermute | solution.py:21
  163.4 2.2 %collective-permute-start.12 = (bf16[64,2048]{1,0:T(8,128)(2,1)}, bf16[64,2048]{1,0:T(8,128)(2,1)S(1)}, u32[]{:S(2)}, u32[]{:S(2)}) collective-permute-start(bf16[64,2048]{1,0:T(8,128)(2,1)} %finish.1.p0), channel_id=1, source_target_pairs={{0,6},{2,0},{4,2},{6,4},{1,7},{3,1},{5,3},{7,5},{8,14},{10,8},{12,... | collective-permute-start | bytes 786440 | tf_op jit(solution)/shard_map/ppermute | solution.py:21
  165.6 0.0 collective-permute-done.14.p3
  165.6 2.6 %collective-permute-done.13.p2 = bf16[64,2048]{1,0:T(8,128)(2,1)S(1)} collective-permute-done((bf16[64,2048]{1,0:T(8,128)(2,1)}, bf16[64,2048]{1,0:T(8,128)(2,1)S(1)}, u32[]{:S(2)}, u32[]{:S(2)}) %collective-permute-start.13) | collective-permute-done | bytes 262176 | tf_op jit(solution)/shard_map/ppermute | solution.py:21
  168.2 2.8 %collective-permute-done.12.p1 = bf16[64,2048]{1,0:T(8,128)(2,1)S(1)} collective-permute-done((bf16[64,2048]{1,0:T(8,128)(2,1)}, bf16[64,2048]{1,0:T(8,128)(2,1)S(1)}, u32[]{:S(2)}, u32[]{:S(2)}) %collective-permute-start.12) | collective-permute-done | bytes 262176 | tf_op jit(solution)/shard_map/ppermute | solution.py:21
  171.0 1.1 pad_maximum_fusion
  172.1 11.4 %collective-permute-start.15 = (bf16[4,64,2048]{2,1,0:T(8,128)(2,1)S(1)}, bf16[4,64,2048]{2,1,0:T(8,128)(2,1)S(1)}, u32[]{:S(2)}, u32[]{:S(2)}) collective-permute-start(bf16[4,64,2048]{2,1,0:T(8,128)(2,1)S(1)} %pad_maximum_fusion), channel_id=1, source_target_pairs={{0,1},{1,0},{2,3},{3,2},{4,5},{5,4},{6,7},{7,6},{8,9},{9,8},{10,11... | collective-permute-start | bytes 3145736 | tf_op jit(solution)/shard_map/ppermute | solution.py:21
  183.5 0.0 all-to-all-done.2.got_ref
  183.5 0.7 zsum.1
  184.2 12.3 %collective-permute-start.16 = (f32[32,384]{1,0:T(8,128)}, f32[32,384]{1,0:T(8,128)S(1)}, u32[]{:S(2)}, u32[]{:S(2)}) collective-permute-start(f32[32,384]{1,0:T(8,128)} %get-tuple-element.24), channel_id=1, source_target_pairs={{0,256},{256,0},{1,257},{257,1},{2,258},{258,2},{3,259},{259,3},{4... | collective-permute-start | bytes 147464 | tf_op jit(solution)/shard_map/ppermute | solution.py:21
  196.5 0.0 copy-start.8
  196.5 0.0 collective-permute-done.15.other_ref
  196.5 2.4 %place.1 = bf16[512,2048]{1,0:T(8,128)(2,1)} custom-call(s32[3]{0:T(128)} %pad_add_fusion.at_ref, bf16[64,2048]{1,0:T(8,128)(2,1)} %finish.1.p0, bf16[64,2048]{1,0:T(8,128)(2,1)S(1)} %collective-permute-done.12.p1, bf16[64,2048]{1,0:T(8,128)(2,1)S(1)} %collective-permute-done.13.p2, bf16[64,2048]{1,0:T(8,128)(2,1)S(1)} %collective-permute-done.14.p3, ...), custom_call_target="tpu_custom_call" | custom-call | tf_op jit(solution)/shard_map/place/pallas_call | solution.py:354
  198.9 3.5 %all-to-all-start.3 = ((f32[8,8,256]{2,1,0:T(8,128)}), f32[8,8,256]{2,1,0:T(8,128)S(1)}, u32[]{:S(2)}, u32[]{:S(2)}) async-start(f32[8,8,256]{2,1,0:T(8,128)} %get-tuple-element.23), calls=%async_computation.3 | async-start | bytes 131072 | tf_op jit(solution)/shard_map/all_to_all | solution.py:25
  202.4 0.0 collective-permute-done.16
  202.4 0.0 copy-done.8
  202.5 0.7 fusion.2
  203.1 4.2 %all-to-all-done.3 = f32[8,8,256]{2,1,0:T(8,128)S(1)} async-done(((f32[8,8,256]{2,1,0:T(8,128)}), f32[8,8,256]{2,1,0:T(8,128)S(1)}, u32[]{:S(2)}, u32[]{:S(2)}) %all-to-all-start.3) | async-done | bytes 65568 | tf_op jit(solution)/shard_map/all_to_all | solution.py:25
  207.3 0.6 copy.9
  (14 shorter events, 0.1 us)
Async XLA Ops:
  13.6 67.5 %copy-start = (bf16[4,64,1152]{2,1,0:T(8,128)(2,1)}, bf16[4,64,1152]{2,1,0:T(8,128)(2,1)S(1)}, u32[]{:S(2)}) copy-start(bf16[4,64,1152]{2,1,0:T(8,128)(2,1)S(1)} %all_to_all.20) | copy-start | bytes 1769476
  13.6 23.4 %collective-permute-start.4 = (bf16[256,1152]{1,0:T(8,128)(2,1)S(1)}, bf16[256,1152]{1,0:T(8,128)(2,1)S(1)}, u32[]{:S(2)}, u32[]{:S(2)}) collective-permute-start(bf16[256,1152]{1,0:T(8,128)(2,1)S(1)} %bitcast.18), channel_id=1, source_target_pairs={{0,480},{32,0},{64,32},{96,64},{128,96},{160,128},{192,160},{224,1... | collective-permute-start | bytes 1769480 | tf_op jit(solution)/shard_map/ppermute | solution.py:21
  26.5 15.9 %collective-permute-start = (bf16[256,1152]{1,0:T(8,128)(2,1)S(1)}, bf16[256,1152]{1,0:T(8,128)(2,1)S(1)}, u32[]{:S(2)}, u32[]{:S(2)}) collective-permute-start(bf16[256,1152]{1,0:T(8,128)(2,1)S(1)} %bitcast.19), channel_id=1, source_target_pairs={{0,32},{32,64},{64,96},{96,128},{128,160},{160,192},{192,224},{224... | collective-permute-start | bytes 1769480 | tf_op jit(solution)/shard_map/ppermute | solution.py:21
  37.1 44.0 %copy-start.1 = (bf16[256,1152]{1,0:T(8,128)(2,1)}, bf16[256,1152]{1,0:T(8,128)(2,1)S(1)}, u32[]{:S(2)}) copy-start(bf16[256,1152]{1,0:T(8,128)(2,1)S(1)} %collective-permute-done.4.refs_1_) | copy-start | bytes 1769476
  37.1 15.0 %collective-permute-start.5 = (bf16[256,1152]{1,0:T(8,128)(2,1)S(1)}, bf16[256,1152]{1,0:T(8,128)(2,1)S(1)}, u32[]{:S(2)}, u32[]{:S(2)}) collective-permute-start(bf16[256,1152]{1,0:T(8,128)(2,1)S(1)} %collective-permute-done.4.refs_1_), channel_id=1, source_target_pairs={{0,480},{32,0},{64,32},{96,64},{128,96},{160,128},{192,160},{224,1... | collective-permute-start | bytes 1769480 | tf_op jit(solution)/shard_map/ppermute | solution.py:21
  42.4 38.7 %copy-start.2 = (bf16[256,1152]{1,0:T(8,128)(2,1)}, bf16[256,1152]{1,0:T(8,128)(2,1)S(1)}, u32[]{:S(2)}) copy-start(bf16[256,1152]{1,0:T(8,128)(2,1)S(1)} %collective-permute-done.refs_2_.refs_6_) | copy-start | bytes 1769476
  42.4 15.0 %collective-permute-start.1 = (bf16[256,1152]{1,0:T(8,128)(2,1)S(1)}, bf16[256,1152]{1,0:T(8,128)(2,1)S(1)}, u32[]{:S(2)}, u32[]{:S(2)}) collective-permute-start(bf16[256,1152]{1,0:T(8,128)(2,1)S(1)} %collective-permute-done.refs_2_.refs_6_), channel_id=1, source_target_pairs={{0,32},{32,64},{64,96},{96,128},{128,160},{160,192},{192,224},{224... | collective-permute-start | bytes 1769480 | tf_op jit(solution)/shard_map/ppermute | solution.py:21
  52.1 29.0 %copy-start.3 = (bf16[256,1152]{1,0:T(8,128)(2,1)}, bf16[256,1152]{1,0:T(8,128)(2,1)S(1)}, u32[]{:S(2)}) copy-start(bf16[256,1152]{1,0:T(8,128)(2,1)S(1)} %collective-permute-done.5.refs_3_.refs_2_) | copy-start | bytes 1769476
  52.1 14.2 %collective-permute-start.6 = (bf16[256,1152]{1,0:T(8,128)(2,1)S(1)}, bf16[256,1152]{1,0:T(8,128)(2,1)S(1)}, u32[]{:S(2)}, u32[]{:S(2)}) collective-permute-start(bf16[256,1152]{1,0:T(8,128)(2,1)S(1)} %collective-permute-done.5.refs_3_.refs_2_), channel_id=1, source_target_pairs={{0,480},{32,0},{64,32},{96,64},{128,96},{160,128},{192,160},{224,1... | collective-permute-start | bytes 1769480 | tf_op jit(solution)/shard_map/ppermute | solution.py:21
  57.4 15.0 %copy-start.4 = (bf16[256,1152]{1,0:T(8,128)(2,1)}, bf16[256,1152]{1,0:T(8,128)(2,1)S(1)}, u32[]{:S(2)}) copy-start(bf16[256,1152]{1,0:T(8,128)(2,1)S(1)} %collective-permute-done.1.refs_4_.refs_5_) | copy-start | bytes 1769476
  57.4 15.0 %collective-permute-start.2 = (bf16[256,1152]{1,0:T(8,128)(2,1)S(1)}, bf16[256,1152]{1,0:T(8,128)(2,1)S(1)}, u32[]{:S(2)}, u32[]{:S(2)}) collective-permute-start(bf16[256,1152]{1,0:T(8,128)(2,1)S(1)} %collective-permute-done.1.refs_4_.refs_5_), channel_id=1, source_target_pairs={{0,32},{32,64},{64,96},{96,128},{128,160},{160,192},{192,224},{224... | collective-permute-start | bytes 1769480 | tf_op jit(solution)/shard_map/ppermute | solution.py:21
  66.3 14.9 %copy-start.5 = (bf16[256,1152]{1,0:T(8,128)(2,1)}, bf16[256,1152]{1,0:T(8,128)(2,1)S(1)}, u32[]{:S(2)}) copy-start(bf16[256,1152]{1,0:T(8,128)(2,1)S(1)} %collective-permute-done.6.refs_3_) | copy-start | bytes 1769476
  67.1 28.0 %collective-permute-start.7 = (bf16[128,1152]{1,0:T(8,128)(2,1)}, bf16[128,1152]{1,0:T(8,128)(2,1)S(1)}, u32[]{:S(2)}, u32[]{:S(2)}) collective-permute-start(bf16[128,1152]{1,0:T(8,128)(2,1)} %slice.9), channel_id=1, source_target_pairs={{0,480},{32,0},{64,32},{96,64},{128,96},{160,128},{192,160},{224,1... | collective-permute-start | bytes 884744 | tf_op jit(solution)/shard_map/ppermute | solution.py:21
  72.4 0.9 copy-start.6
  73.3 21.7 %collective-permute-start.3 = (bf16[128,1152]{1,0:T(8,128)(2,1)}, bf16[128,1152]{1,0:T(8,128)(2,1)S(1)}, u32[]{:S(2)}, u32[]{:S(2)}) collective-permute-start(bf16[128,1152]{1,0:T(8,128)(2,1)} %slice.8), channel_id=1, source_target_pairs={{0,32},{32,64},{64,96},{96,128},{128,160},{160,192},{192,224},{224... | collective-permute-start | bytes 884744 | tf_op jit(solution)/shard_map/ppermute | solution.py:21
  81.1 7.0 %copy-start.7 = (f32[2048]{0:T(1024)S(1)}, f32[2048]{0:T(1024)}, u32[]{:S(2)}) copy-start(f32[2048]{0:T(1024)} %param.7) | copy-start | bytes 24580
  106.0 21.2 %all-to-all-start.1 = ((bf16[4,8,72,384]{3,2,1,0:T(8,128)(2,1)}), bf16[4,8,72,384]{3,2,1,0:T(8,128)(2,1)S(1)}, u32[]{:S(2)}, u32[]{:S(2)}) async-start(bf16[4,8,72,384]{3,2,1,0:T(8,128)(2,1)} %get-tuple-element.22), calls=%async_computation.1 | async-start | bytes 3538944 | tf_op jit(solution)/shard_map/all_to_all | solution.py:25
  109.6 26.1 %collective-permute-start.8 = (bf16[4,8,64,256]{3,2,1,0:T(8,128)(2,1)}, bf16[4,8,64,256]{3,2,1,0:T(8,128)(2,1)S(1)}, u32[]{:S(2)}, u32[]{:S(2)}) collective-permute-start(bf16[4,8,64,256]{3,2,1,0:T(8,128)(2,1)} %get-tuple-element.17), channel_id=1, source_target_pairs={{0,1},{1,0},{2,3},{3,2},{4,5},{5,4},{6,7},{7,6},{8,9},{9,8},{10,11... | collective-permute-start | bytes 3145736 | tf_op jit(solution)/shard_map/ppermute | solution.py:21
  129.0 54.5 %all-to-all-start.2 = ((bf16[16,40,384]{2,1,0:T(8,128)(2,1)}), bf16[16,40,384]{2,1,0:T(8,128)(2,1)S(1)}, u32[]{:S(2)}, u32[]{:S(2)}) async-start(bf16[16,40,384]{2,1,0:T(8,128)(2,1)} %ysum.1), calls=%async_computation.2 | async-start | bytes 983040 | tf_op jit(solution)/shard_map/all_to_all | solution.py:25
  138.0 10.5 %collective-permute-start.9 = (bf16[8,64,256]{2,1,0:T(8,128)(2,1)}, bf16[8,64,256]{2,1,0:T(8,128)(2,1)S(1)}, u32[]{:S(2)}, u32[]{:S(2)}) collective-permute-start(bf16[8,64,256]{2,1,0:T(8,128)(2,1)} %get-tuple-element.19), channel_id=1, source_target_pairs={{0,2},{2,4},{4,6},{6,0},{1,3},{3,5},{5,7},{7,1},{8,10},{10,12},{12... | collective-permute-start | bytes 786440 | tf_op jit(solution)/shard_map/ppermute | solution.py:21
  141.1 9.5 %collective-permute-start.10 = (bf16[8,64,256]{2,1,0:T(8,128)(2,1)}, bf16[8,64,256]{2,1,0:T(8,128)(2,1)S(1)}, u32[]{:S(2)}, u32[]{:S(2)}) collective-permute-start(bf16[8,64,256]{2,1,0:T(8,128)(2,1)} %get-tuple-element.20), channel_id=1, source_target_pairs={{0,4},{2,6},{4,0},{6,2},{1,5},{3,7},{5,1},{7,3},{8,12},{10,14},{12... | collective-permute-start | bytes 786440 | tf_op jit(solution)/shard_map/ppermute | solution.py:21
  145.5 7.6 %collective-permute-start.11 = (bf16[8,64,256]{2,1,0:T(8,128)(2,1)}, bf16[8,64,256]{2,1,0:T(8,128)(2,1)S(1)}, u32[]{:S(2)}, u32[]{:S(2)}) collective-permute-start(bf16[8,64,256]{2,1,0:T(8,128)(2,1)} %get-tuple-element.21), channel_id=1, source_target_pairs={{0,6},{2,0},{4,2},{6,4},{1,7},{3,1},{5,3},{7,5},{8,14},{10,8},{12,... | collective-permute-start | bytes 786440 | tf_op jit(solution)/shard_map/ppermute | solution.py:21
  156.0 9.6 %collective-permute-start.14 = (bf16[64,2048]{1,0:T(8,128)(2,1)}, bf16[64,2048]{1,0:T(8,128)(2,1)S(1)}, u32[]{:S(2)}, u32[]{:S(2)}) collective-permute-start(bf16[64,2048]{1,0:T(8,128)(2,1)} %finish.1.p0), channel_id=1, source_target_pairs={{0,2},{2,4},{4,6},{6,0},{1,3},{3,5},{5,7},{7,1},{8,10},{10,12},{12... | collective-permute-start | bytes 786440 | tf_op jit(solution)/shard_map/ppermute | solution.py:21
  159.1 9.1 %collective-permute-start.13 = (bf16[64,2048]{1,0:T(8,128)(2,1)}, bf16[64,2048]{1,0:T(8,128)(2,1)S(1)}, u32[]{:S(2)}, u32[]{:S(2)}) collective-permute-start(bf16[64,2048]{1,0:T(8,128)(2,1)} %finish.1.p0), channel_id=1, source_target_pairs={{0,4},{2,6},{4,0},{6,2},{1,5},{3,7},{5,1},{7,3},{8,12},{10,14},{12... | collective-permute-start | bytes 786440 | tf_op jit(solution)/shard_map/ppermute | solution.py:21
  163.4 7.6 %collective-permute-start.12 = (bf16[64,2048]{1,0:T(8,128)(2,1)}, bf16[64,2048]{1,0:T(8,128)(2,1)S(1)}, u32[]{:S(2)}, u32[]{:S(2)}) collective-permute-start(bf16[64,2048]{1,0:T(8,128)(2,1)} %finish.1.p0), channel_id=1, source_target_pairs={{0,6},{2,0},{4,2},{6,4},{1,7},{3,1},{5,3},{7,5},{8,14},{10,8},{12,... | collective-permute-start | bytes 786440 | tf_op jit(solution)/shard_map/ppermute | solution.py:21
  172.1 24.4 %collective-permute-start.15 = (bf16[4,64,2048]{2,1,0:T(8,128)(2,1)S(1)}, bf16[4,64,2048]{2,1,0:T(8,128)(2,1)S(1)}, u32[]{:S(2)}, u32[]{:S(2)}) collective-permute-start(bf16[4,64,2048]{2,1,0:T(8,128)(2,1)S(1)} %pad_maximum_fusion), channel_id=1, source_target_pairs={{0,1},{1,0},{2,3},{3,2},{4,5},{5,4},{6,7},{7,6},{8,9},{9,8},{10,11... | collective-permute-start | bytes 3145736 | tf_op jit(solution)/shard_map/ppermute | solution.py:21
  184.2 18.3 %collective-permute-start.16 = (f32[32,384]{1,0:T(8,128)}, f32[32,384]{1,0:T(8,128)S(1)}, u32[]{:S(2)}, u32[]{:S(2)}) collective-permute-start(f32[32,384]{1,0:T(8,128)} %get-tuple-element.24), channel_id=1, source_target_pairs={{0,256},{256,0},{1,257},{257,1},{2,258},{258,2},{3,259},{259,3},{4... | collective-permute-start | bytes 147464 | tf_op jit(solution)/shard_map/ppermute | solution.py:21
  196.5 6.0 %copy-start.8 = (f32[32,384]{1,0:T(8,128)S(1)}, f32[32,384]{1,0:T(8,128)}, u32[]{:S(2)}) copy-start(f32[32,384]{1,0:T(8,128)} %get-tuple-element.24) | copy-start | bytes 147460
  198.9 8.4 %all-to-all-start.3 = ((f32[8,8,256]{2,1,0:T(8,128)}), f32[8,8,256]{2,1,0:T(8,128)S(1)}, u32[]{:S(2)}, u32[]{:S(2)}) async-start(f32[8,8,256]{2,1,0:T(8,128)} %get-tuple-element.23), calls=%async_computation.3 | async-start | bytes 131072 | tf_op jit(solution)/shard_map/all_to_all | solution.py:25

commit v5 on v4

--- a/solution.py
+++ b/solution.py
@@ -54,21 +54,21 @@
 
 
 def forward_kernel(x_ref, c_ref, *refs):
-    w_refs, acc_ref = refs[:-1], refs[-1]
+    acc_ref = refs[-1]
     units = acc_ref.shape[1] // 3
     gu = dh = None
-    for d, w in zip(EARLY, w_refs):
-        a = jnp.dot(x_ref[d], w[:, : 2 * units], preferred_element_type=F32)
-        b = jnp.dot(c_ref[d], w[:, 2 * units :], preferred_element_type=F32)
+    for i, d in enumerate(EARLY):
+        a = jnp.dot(x_ref[d], refs[i][...], preferred_element_type=F32)
+        b = jnp.dot(c_ref[d], refs[len(EARLY) + i][...], preferred_element_type=F32)
         gu = a if gu is None else gu + a
         dh = b if dh is None else dh + b
     acc_ref[:, : 2 * units] = gu
     acc_ref[:, 2 * units :] = dh
 
 
-def grad_kernel(gain_ref, lo_ref, hi_ref, acc_hbm, x_hbm, c_hbm, ct_hbm, *refs):
-    w_hbm, (mine_hbm, other_hbm, dd_hbm) = refs[:7], refs[7:10]
-    acc, xv, cv, ctv, wv, ov, dv, sems = refs[10:]
+def grad_kernel(gain_ref, gu4_ref, down4_ref, acc_hbm, x_hbm, c_hbm, ct_hbm, *refs):
+    w_hbm, down_hbm, (mine_hbm, other_hbm, dd_hbm) = refs[:7], refs[7:9], refs[9:12]
+    acc, xv, cv, ctv, wv, dwv, ov, dv, sems = refs[12:]
     units = acc.shape[1] // 3
     nz, _, cols = xv.shape
     ny, _, longer, _ = dv.shape
@@ -84,11 +84,12 @@
 
     slot = {0: 0, 1: 1, 2: 2, 3: 3, 5: 4, 6: 5, 7: 6}
     acc_in = begin(acc_hbm, acc)
-    x_in, c_in, w_in = {}, {}, {}
+    x_in, c_in, w_in, down_in = {}, {}, {}, {}
     for d in (3, 5):
         w_in[d] = begin(w_hbm[slot[d]], wv.at[slot[d]])
         x_in[d] = begin(x_hbm.at[d], xv.at[d])
         c_in[d] = begin(c_hbm.at[d], cv.at[d - 3])
+        down_in[d] = begin(down_hbm[(d - 3) // 2], dwv.at[(d - 3) // 2])
     x_in[4] = begin(x_hbm.at[4], xv.at[4])
     c_in[4] = begin(c_hbm.at[4], cv.at[1])
     for d in EARLY:
@@ -96,22 +97,19 @@
         x_in[d] = begin(x_hbm.at[d], xv.at[d])
     ct_in = begin(ct_hbm, ctv)
 
-    half = cols // 2
-    halves = ((lo_ref, slice(0, half)), (hi_ref, slice(half, cols)))
     acc_in.wait()
     gu, dh = acc[:, : 2 * units], acc[:, 2 * units :]
     for d in (3, 5):
         w_in[d].wait()
         x_in[d].wait()
         c_in[d].wait()
-        w = wv.at[slot[d]]
-        gu = gu + jnp.dot(xv[d], w[:, : 2 * units], preferred_element_type=F32)
-        dh = dh + jnp.dot(cv[d - 3], w[:, 2 * units :], preferred_element_type=F32)
+        down_in[d].wait()
+        gu = gu + jnp.dot(xv[d], wv[slot[d]], preferred_element_type=F32)
+        dh = dh + jnp.dot(cv[d - 3], dwv[(d - 3) // 2], preferred_element_type=F32)
     x_in[4].wait()
     c_in[4].wait()
-    for w, at in halves:
-        gu = gu + jnp.dot(xv[4, :, at], w[:, : 2 * units], preferred_element_type=F32)
-        dh = dh + jnp.dot(cv[1, :, at], w[:, 2 * units :], preferred_element_type=F32)
+    gu = gu + jnp.dot(xv[4], gu4_ref[...], preferred_element_type=F32)
+    dh = dh + jnp.dot(cv[1], down4_ref[...], preferred_element_type=F32)
     gate, up = gu[:, :units], gu[:, units:]
     dh = 0.5 * dh
     sig = jax.nn.sigmoid(gate)
@@ -126,18 +124,13 @@
         if d in EARLY:
             w_in[d].wait()
             x_in[d].wait()
-        pieces = halves if d == 4 else ((wv.at[slot[d]], slice(0, cols)),)
-        got = []
-        for w, at in pieces:
-            out = lax.dot_general(
-                both, w[:, : 2 * units], (((1,), (1,)), ((), ())), preferred_element_type=F32
-            )
-            terms = jnp.sum(xv[d, :, at].astype(F32) * out, axis=0, keepdims=True)
-            got.append(terms / gain_ref[d, :, at])
-            out = out.astype(BF16)
-            for k in range(2 * nx):
-                ov[k, d, :, at] = out[k * part : (k + 1) * part]
-        sums[d] = got[0] if len(got) == 1 else jnp.concatenate(got, axis=1)
+        w = gu4_ref[...] if d == 4 else wv[slot[d]]
+        out = lax.dot_general(both, w, (((1,), (1,)), ((), ())), preferred_element_type=F32)
+        terms = jnp.sum(xv[d].astype(F32) * out, axis=0, keepdims=True)
+        sums[d] = terms / gain_ref[d]
+        out = out.astype(BF16)
+        for k in range(2 * nx):
+            ov[k, d] = out[k * part : (k + 1) * part]
         out_copies.append(begin(ov.at[pl.ds(nx, nx), d], other_hbm.at[:, d]))
         out_copies.append(begin(ov.at[pl.ds(0, nx), d], mine_hbm.at[:, d]))
     ct_in.wait()
@@ -241,16 +234,19 @@
     gain2 = gain[None]
     at = jnp.stack([zl, c, x]).astype(jnp.int32)
 
-    w = jnp.concatenate([gate_weight, up_weight, down_weight], axis=1)
-    w0 = from_all(w, "fs_1").reshape(ny * rows, 3 * units)
-    fwd, bwd = [w0], [w0]
-    for _ in range(3):
-        fwd.append(shifted(fwd[-1], RING, 1))
-        bwd.append(shifted(bwd[-1], RING, -1))
-    mid = cols // 2
-    last_f = shifted(fwd[-1][:mid], RING, 1)
-    last_b = shifted(bwd[-1][mid:], RING, -1)
-    weights = [w0, bwd[1], bwd[2], bwd[3], fwd[3], fwd[2], fwd[1]]
+    def relay(own):
+        fwd, bwd = [own], [own]
+        for _ in range(3):
+            fwd.append(shifted(fwd[-1], RING, 1))
+            bwd.append(shifted(bwd[-1], RING, -1))
+        return fwd, bwd
+
+    gu0 = from_all(jnp.concatenate([gate_weight, up_weight], axis=1), "fs_1")
+    down0 = from_all(down_weight, "fs_1")
+    gu_f, gu_b = relay(gu0.reshape(ny * rows, 2 * units))
+    down_f, down_b = relay(down0.reshape(ny * rows, units))
+    gu4 = shifted(gu_f[3], RING, 1)
+    down4 = shifted(down_b[3], RING, -1)
 
     def spot(i, at):
         return ((i // nx + at[1]) % 2) * nx + (i + at[2]) % nx
@@ -294,10 +290,13 @@
     acc = pl.pallas_call(
         forward_kernel,
         out_shape=jax.ShapeDtypeStruct((tokens, 3 * units), F32),
-        in_specs=vmem(7),
+        in_specs=vmem(12),
         out_specs=pl.BlockSpec(memory_space=pltpu.VMEM),
         name="forward",
-    )(xr, cr, w0, bwd[1], fwd[1], bwd[2], fwd[2])
+    )(
+        *(xr, cr, gu_f[0], gu_b[1], gu_f[1], gu_b[2], gu_f[2]),
+        *(down_f[0], down_b[1], down_f[1], down_b[2], down_f[2]),
+    )
     anywhere = pl.BlockSpec(memory_space=pl.ANY)
     mine, other, dd = pl.pallas_call(
         grad_kernel,
@@ -306,20 +305,24 @@
             jax.ShapeDtypeStruct((nx, nz, part, cols), BF16),
             jax.ShapeDtypeStruct((ny, nz, rows + 8, units), BF16),
         ),
-        in_specs=vmem(3) + [anywhere] * 11,
+        in_specs=vmem(3) + [anywhere] * 13,
         out_specs=(anywhere,) * 3,
         scratch_shapes=[
             pltpu.VMEM((tokens, 3 * units), F32),
             pltpu.VMEM((nz, tokens, cols), BF16),
             pltpu.VMEM((3, tokens, cols), BF16),
             pltpu.VMEM((nz, cols, tokens), BF16),
-            pltpu.VMEM((7, cols, 3 * units), BF16),
+            pltpu.VMEM((7, cols, 2 * units), BF16),
+            pltpu.VMEM((2, cols, units), BF16),
             pltpu.VMEM((2 * nx, nz, part, cols), BF16),
             pltpu.VMEM((ny, nz, rows + 8, units), BF16),
             pltpu.SemaphoreType.DMA((48,)),
         ],
         name="grad",
-    )(gain_ring, *near(last_f, last_b), acc, xr, cr, ct, *weights)
+    )(
+        *(gain_ring, *near(gu4, down4), acc, xr, cr, ct),
+        *(gu_f[0], gu_b[1], gu_b[2], gu_b[3], gu_f[3], gu_f[2], gu_f[1], down_b[3], down_f[3]),
+    )
     theirs = shifted(other, "c", 1)
     dy = exchanged(dd, "fs_1")
 

time: 209 us -> 217 us (1.038)
  starting transfers between devices: 101 us -> 121 us
  waiting for transfers between devices: 48.2 us -> 29.5 us
  blocking collectives: 12.1 us -> 18.6 us
    ppermute x17 -> x23, starting transfers between devices: 87 us -> 105 us  [shifted(): return lax.ppermute(v, axis, [(i, (i + by) % n) for i in range(n)])]
    ppermute x17 -> x23, waiting for transfers between devices: 33.3 us -> 18.9 us  [shifted(): return lax.ppermute(v, axis, [(i, (i + by) % n) for i in range(n)])]
    all_to_all x1 -> x2, blocking collectives: 12.1 us -> 18.6 us  [exchanged(): return lax.all_to_all(v, axis, 0, 0, tiled=True)]
    all_to_all x3, waiting for transfers between devices: 15 us -> 10.6 us  [exchanged(): return lax.all_to_all(v, axis, 0, 0, tiled=True)]
  transfers between devices with their start and end apart: 20 -> 26, of which waited for: 9 -> 8; matrix products, arithmetic and copies ran while one was open for 2% -> 2% of each run, Pallas kernels for 14% -> 13%
where the time goes in v5:
time: 217 us; the launch traced here: 215 us
  starting transfers between devices  121 us (56%)
  Pallas kernels  39.1 us (18%)
  waiting for transfers between devices  29.5 us (14%)
  blocking collectives  18.6 us (9%)
  other arithmetic  3.88 us (2%)
  local copies, waits for them, and re-layouts  2.25 us (1%)
    ppermute x23, starting transfers between devices, shifted(): return lax.ppermute(v, axis, [(i, (i + by) % n) for i in range(n)])  105 us
    ppermute x23, waiting for transfers between devices, shifted(): return lax.ppermute(v, axis, [(i, (i + by) % n) for i in range(n)])  18.9 us
    all_to_all x2, blocking collectives, exchanged(): return lax.all_to_all(v, axis, 0, 0, tiled=True)  18.6 us
    all_to_all x3, starting transfers between devices, exchanged(): return lax.all_to_all(v, axis, 0, 0, tiled=True)  15.7 us
    pallas_call x1, Pallas kernels, work(): pl.pallas_call(grad_kernel, out_shape=(jax.ShapeDtypeStruct((nx, nz, part...  10.6 us
    all_to_all x3, waiting for transfers between devices, exchanged(): return lax.all_to_all(v, axis, 0, 0, tiled=True)  10.6 us
    pallas_call x1, Pallas kernels, work(): pl.pallas_call(prepare_tokens, out_shape=jax.ShapeDtypeStruct((nz, tokens...  6.97 us
    pallas_call x1, Pallas kernels, work(): pl.pallas_call(forward_kernel, out_shape=jax.ShapeDtypeStruct((tokens, 3...  6.28 us
  transfers between devices with their start and end apart: 26, of which 8 were waited for; matrix products, arithmetic and copies ran while one was open for 2% of the time, Pallas kernels for 13%

profile of v5, /device:TPU:1, one launch (start us, length us, event | category | flops | bytes accessed | tf_op | source)
XLA Modules:
  0.0 215.4 jit_solution(7840901567485054432)
XLA Ops:
  0.6 0.8 pad_maximum_fusion.1
  1.5 11.0 %all_to_all.25 = bf16[4,64,768]{2,1,0:T(8,128)(2,1)S(1)} all-to-all(bf16[4,64,768]{2,1,0:T(8,128)(2,1)S(1)} %broadcast_in_dim.6), channel_id=1, replica_groups=mesh['rep'=2,'fs_0'=8,'fs_1'=4,'x'=4,'c'=2] {'fs_1'}, dimensions={0} | all-to-all | bytes 786432 | tf_op jit(solution)/shard_map/all_to_all | solution.py:25
  12.5 4.5 %collective-permute-start = (bf16[256,768]{1,0:T(8,128)(2,1)S(1)}, bf16[256,768]{1,0:T(8,128)(2,1)S(1)}, u32[]{:S(2)}, u32[]{:S(2)}) collective-permute-start(bf16[256,768]{1,0:T(8,128)(2,1)S(1)} %bitcast.19), channel_id=1, source_target_pairs={{0,32},{32,64},{64,96},{96,128},{128,160},{160,192},{192,224},{224... | collective-permute-start | bytes 1179656 | tf_op jit(solution)/shard_map/ppermute | solution.py:21
  17.1 9.5 %collective-permute-start.8 = (bf16[256,768]{1,0:T(8,128)(2,1)S(1)}, bf16[256,768]{1,0:T(8,128)(2,1)S(1)}, u32[]{:S(2)}, u32[]{:S(2)}) collective-permute-start(bf16[256,768]{1,0:T(8,128)(2,1)S(1)} %bitcast.20), channel_id=1, source_target_pairs={{0,480},{32,0},{64,32},{96,64},{128,96},{160,128},{192,160},{224,1... | collective-permute-start | bytes 1179656 | tf_op jit(solution)/shard_map/ppermute | solution.py:21
  26.6 5.7 %collective-permute-done.refs_2_.refs_6_ = bf16[256,768]{1,0:T(8,128)(2,1)S(1)} collective-permute-done((bf16[256,768]{1,0:T(8,128)(2,1)S(1)}, bf16[256,768]{1,0:T(8,128)(2,1)S(1)}, u32[]{:S(2)}, u32[]{:S(2)}) %collective-permute-start) | collective-permute-done | bytes 393248 | tf_op jit(solution)/shard_map/ppermute | solution.py:21
  32.3 1.9 collective-permute-start.1
  34.2 0.8 broadcast_in_dim.7
  35.1 7.5 %all_to_all.26 = bf16[4,64,384]{2,1,0:T(8,128)(2,1)S(1)} all-to-all(bf16[4,64,384]{2,1,0:T(8,128)(2,1)S(1)} %broadcast_in_dim.7), channel_id=1, replica_groups=mesh['rep'=2,'fs_0'=8,'fs_1'=4,'x'=4,'c'=2] {'fs_1'}, dimensions={0} | all-to-all | bytes 393216 | tf_op jit(solution)/shard_map/all_to_all | solution.py:25
  42.6 4.6 %collective-permute-start.4 = (bf16[256,384]{1,0:T(8,128)(2,1)S(1)}, bf16[256,384]{1,0:T(8,128)(2,1)S(1)}, u32[]{:S(2)}, u32[]{:S(2)}) collective-permute-start(bf16[256,384]{1,0:T(8,128)(2,1)S(1)} %bitcast.24), channel_id=1, source_target_pairs={{0,480},{32,0},{64,32},{96,64},{128,96},{160,128},{192,160},{224,1... | collective-permute-start | bytes 589832 | tf_op jit(solution)/shard_map/ppermute | solution.py:21
  47.2 0.0 collective-permute-done.8.refs_1_
  47.2 1.9 collective-permute-start.9
  49.1 3.4 %collective-permute-start.2 = (bf16[256,768]{1,0:T(8,128)(2,1)S(1)}, bf16[256,768]{1,0:T(8,128)(2,1)S(1)}, u32[]{:S(2)}, u32[]{:S(2)}) collective-permute-start(bf16[256,768]{1,0:T(8,128)(2,1)S(1)} %collective-permute-done.1.refs_4_.refs_5_), channel_id=1, source_target_pairs={{0,32},{32,64},{64,96},{96,128},{128,160},{160,192},{192,224},{224... | collective-permute-start | bytes 1179656 | tf_op jit(solution)/shard_map/ppermute | solution.py:21
  52.5 1.9 collective-permute-start.10
  54.4 0.0 collective-permute-done.4.refs_6_
  54.5 4.6 %collective-permute-start.5 = (bf16[256,384]{1,0:T(8,128)(2,1)S(1)}, bf16[256,384]{1,0:T(8,128)(2,1)}, u32[]{:S(2)}, u32[]{:S(2)}) collective-permute-start(bf16[256,384]{1,0:T(8,128)(2,1)S(1)} %collective-permute-done.4.refs_6_), channel_id=1, source_target_pairs={{0,480},{32,0},{64,32},{96,64},{128,96},{160,128},{192,160},{224,1... | collective-permute-start | bytes 589832 | tf_op jit(solution)/shard_map/ppermute | solution.py:21
  59.0 3.5 %collective-permute-done.10.refs_7_ = bf16[256,384]{1,0:T(8,128)(2,1)S(1)} collective-permute-done((bf16[256,384]{1,0:T(8,128)(2,1)S(1)}, bf16[256,384]{1,0:T(8,128)(2,1)S(1)}, u32[]{:S(2)}, u32[]{:S(2)}) %collective-permute-start.10) | collective-permute-done | bytes 196640 | tf_op jit(solution)/shard_map/ppermute | solution.py:21
  62.5 2.4 %collective-permute-start.11 = (bf16[256,384]{1,0:T(8,128)(2,1)S(1)}, bf16[256,384]{1,0:T(8,128)(2,1)}, u32[]{:S(2)}, u32[]{:S(2)}) collective-permute-start(bf16[256,384]{1,0:T(8,128)(2,1)S(1)} %collective-permute-done.10.refs_7_), channel_id=1, source_target_pairs={{0,32},{32,64},{64,96},{96,128},{128,160},{160,192},{192,224},{224... | collective-permute-start | bytes 589832 | tf_op jit(solution)/shard_map/ppermute | solution.py:21
  64.9 4.1 %collective-permute-start.6 = (bf16[256,384]{1,0:T(8,128)(2,1)}, bf16[256,384]{1,0:T(8,128)(2,1)}, u32[]{:S(2)}, u32[]{:S(2)}) collective-permute-start(bf16[256,384]{1,0:T(8,128)(2,1)} %collective-permute-done.5.refs_8_), channel_id=1, source_target_pairs={{0,480},{32,0},{64,32},{96,64},{128,96},{160,128},{192,160},{224,1... | collective-permute-start | bytes 589832 | tf_op jit(solution)/shard_map/ppermute | solution.py:21
  69.0 0.0 collective-permute-done.9.refs_3_.refs_2_
  69.1 1.9 collective-permute-start.12
  71.0 0.0 collective-permute-done.2.refs_4_
  71.0 3.4 %collective-permute-start.3 = (bf16[256,768]{1,0:T(8,128)(2,1)S(1)}, bf16[256,768]{1,0:T(8,128)(2,1)S(1)}, u32[]{:S(2)}, u32[]{:S(2)}) collective-permute-start(bf16[256,768]{1,0:T(8,128)(2,1)S(1)} %collective-permute-done.2.refs_4_), channel_id=1, source_target_pairs={{0,32},{32,64},{64,96},{96,128},{128,160},{160,192},{192,224},{224... | collective-permute-start | bytes 1179656 | tf_op jit(solution)/shard_map/ppermute | solution.py:21
  74.4 0.0 collective-permute-done.11.refs_9_
  74.4 1.9 collective-permute-start.13
  76.3 0.0 collective-permute-done.6.refs_7_
  76.4 4.6 %collective-permute-start.7 = (bf16[256,384]{1,0:T(8,128)(2,1)}, bf16[256,384]{1,0:T(8,128)(2,1)S(1)}, u32[]{:S(2)}, u32[]{:S(2)}) collective-permute-start(bf16[256,384]{1,0:T(8,128)(2,1)} %collective-permute-done.6.refs_7_), channel_id=1, source_target_pairs={{0,480},{32,0},{64,32},{96,64},{128,96},{160,128},{192,160},{224,1... | collective-permute-start | bytes 589832 | tf_op jit(solution)/shard_map/ppermute | solution.py:21
  80.9 0.7 pad_add_fusion.at_ref
  81.6 5.3 %prepare_c.1 = (bf16[8,512,256]{2,1,0:T(8,128)(2,1)}, bf16[8,256,512]{2,1,0:T(8,128)(2,1)}) custom-call(s32[3]{0:T(128)} %pad_add_fusion.at_ref, bf16[512,2048]{1,0:T(8,128)(2,1)} %c_ref.1, bf16[512,2048]{1,0:T(8,128)(2,1)} %c_ref.1), custom_call_target="tpu_custom_call" | custom-call | tf_op jit(solution)/shard_map/prepare_c/pallas_call | solution.py:268
  86.9 0.0 copy-start.10
  86.9 7.0 %prepare_x.1.x_ref.x_hbm = bf16[8,512,256]{2,1,0:T(8,128)(2,1)} custom-call(s32[3]{0:T(128)} %pad_add_fusion.at_ref, bf16[512,2048]{1,0:T(8,128)(2,1)} %x_ref.3, f32[1,2048]{1,0:T(1,128)} %bitcast.28), custom_call_target="tpu_custom_call" | custom-call | tf_op jit(solution)/shard_map/prepare_x/pallas_call | solution.py:254
  93.9 0.6 fusion.3.gain_ref
  94.5 6.3 %forward.1.acc_hbm = f32[512,1152]{1,0:T(8,128)} custom-call(bf16[8,512,256]{2,1,0:T(8,128)(2,1)} %prepare_x.1.x_ref.x_hbm, bf16[8,512,256]{2,1,0:T(8,128)(2,1)} %get-tuple-element.14.c_ref.c_hbm, bf16[256,768]{1,0:T(8,128)(2,1)} %bitcast.21, bf16[256,768]{1,0:T(8,128)(2,1)} %copy-done.2, bf16[256,768]{1,0:T(8,128)(2,1)} %copy-done.1, ...), custom_call_target="tpu_custom_call" | custom-call | tf_op jit(solution)/shard_map/forward/pallas_call | solution.py:290
  100.8 0.0 collective-permute-done.13.refs_8_
  100.8 0.0 collective-permute-done.7.down4_ref
  100.8 0.7 copy-done.7
  101.6 10.6 %grad.1 = (bf16[4,8,64,256]{3,2,1,0:T(8,128)(2,1)}, bf16[4,8,64,256]{3,2,1,0:T(8,128)(2,1)}, bf16[4,8,72,384]{3,2,1,0:T(8,128)(2,1)}) custom-call(f32[8,1,256]{2,1,0:T(1,128)} %fusion.3.gain_ref, bf16[256,768]{1,0:T(8,128)(2,1)S(1)} %collective-permute-done.3.gu4_ref, bf16[256,384]{1,0:T(8,128)(2,1)S(1)} %collective-permute-done.7.down4_ref, ...), custom_call_target="tpu_custom_call" | custom-call | tf_op jit(solution)/shard_map/grad/pallas_call | solution.py:301
  112.2 3.6 %all-to-all-start.2 = ((bf16[4,8,72,384]{3,2,1,0:T(8,128)(2,1)}), bf16[4,8,72,384]{3,2,1,0:T(8,128)(2,1)S(1)}, u32[]{:S(2)}, u32[]{:S(2)}) async-start(bf16[4,8,72,384]{3,2,1,0:T(8,128)(2,1)} %get-tuple-element.22), calls=%async_computation.2 | async-start | bytes 3538944 | tf_op jit(solution)/shard_map/all_to_all | solution.py:25
  115.8 9.0 %collective-permute-start.14 = (bf16[4,8,64,256]{3,2,1,0:T(8,128)(2,1)}, bf16[4,8,64,256]{3,2,1,0:T(8,128)(2,1)S(1)}, u32[]{:S(2)}, u32[]{:S(2)}) collective-permute-start(bf16[4,8,64,256]{3,2,1,0:T(8,128)(2,1)} %get-tuple-element.17), channel_id=1, source_target_pairs={{0,1},{1,0},{2,3},{3,2},{4,5},{5,4},{6,7},{7,6},{8,9},{9,8},{10,11... | collective-permute-start | bytes 3145736 | tf_op jit(solution)/shard_map/ppermute | solution.py:21
  124.8 6.4 %all-to-all-done.2.got_ref = bf16[4,8,72,384]{3,2,1,0:T(8,128)(2,1)S(1)} async-done(((bf16[4,8,72,384]{3,2,1,0:T(8,128)(2,1)}), bf16[4,8,72,384]{3,2,1,0:T(8,128)(2,1)S(1)}, u32[]{:S(2)}, u32[]{:S(2)}) %all-to-all-start.2) | async-done | bytes 1769504 | tf_op jit(solution)/shard_map/all_to_all | solution.py:25
  131.2 1.7 ysum.1
  132.9 8.5 %all-to-all-start.3 = ((bf16[16,40,384]{2,1,0:T(8,128)(2,1)}), bf16[16,40,384]{2,1,0:T(8,128)(2,1)S(1)}, u32[]{:S(2)}, u32[]{:S(2)}) async-start(bf16[16,40,384]{2,1,0:T(8,128)(2,1)} %ysum.1), calls=%async_computation.3 | async-start | bytes 983040 | tf_op jit(solution)/shard_map/all_to_all | solution.py:25
  141.5 2.3 %chip.1 = (bf16[8,64,256]{2,1,0:T(8,128)(2,1)}, bf16[8,64,256]{2,1,0:T(8,128)(2,1)}, bf16[8,64,256]{2,1,0:T(8,128)(2,1)}, bf16[8,64,256]{2,1,0:T(8,128)(2,1)}) custom-call(bf16[4,8,64,256]{3,2,1,0:T(8,128)(2,1)} %get-tuple-element.16.mine_ref, bf16[4,8,64,256]{3,2,1,0:T(8,128)(2,1)S(1)} %collective-permute-done.14.theirs_ref), custom_call_target="tpu_custom_call" | custom-call | tf_op jit(solution)/shard_map/chip/pallas_call | solution.py:330
  143.7 3.1 %collective-permute-start.15 = (bf16[8,64,256]{2,1,0:T(8,128)(2,1)}, bf16[8,64,256]{2,1,0:T(8,128)(2,1)S(1)}, u32[]{:S(2)}, u32[]{:S(2)}) collective-permute-start(bf16[8,64,256]{2,1,0:T(8,128)(2,1)} %get-tuple-element.19), channel_id=1, source_target_pairs={{0,2},{2,4},{4,6},{6,0},{1,3},{3,5},{5,7},{7,1},{8,10},{10,12},{12... | collective-permute-start | bytes 786440 | tf_op jit(solution)/shard_map/ppermute | solution.py:21
  146.9 4.3 %collective-permute-start.16 = (bf16[8,64,256]{2,1,0:T(8,128)(2,1)}, bf16[8,64,256]{2,1,0:T(8,128)(2,1)S(1)}, u32[]{:S(2)}, u32[]{:S(2)}) collective-permute-start(bf16[8,64,256]{2,1,0:T(8,128)(2,1)} %get-tuple-element.20), channel_id=1, source_target_pairs={{0,4},{2,6},{4,0},{6,2},{1,5},{3,7},{5,1},{7,3},{8,12},{10,14},{12... | collective-permute-start | bytes 786440 | tf_op jit(solution)/shard_map/ppermute | solution.py:21
  151.2 3.1 %collective-permute-start.17 = (bf16[8,64,256]{2,1,0:T(8,128)(2,1)}, bf16[8,64,256]{2,1,0:T(8,128)(2,1)S(1)}, u32[]{:S(2)}, u32[]{:S(2)}) collective-permute-start(bf16[8,64,256]{2,1,0:T(8,128)(2,1)} %get-tuple-element.21), channel_id=1, source_target_pairs={{0,6},{2,0},{4,2},{6,4},{1,7},{3,1},{5,3},{7,5},{8,14},{10,8},{12,... | collective-permute-start | bytes 786440 | tf_op jit(solution)/shard_map/ppermute | solution.py:21
  154.3 0.0 collective-permute-done.15.got1
  154.3 1.8 collective-permute-done.16.got2
  156.1 2.8 %collective-permute-done.17.got3 = bf16[8,64,256]{2,1,0:T(8,128)(2,1)S(1)} collective-permute-done((bf16[8,64,256]{2,1,0:T(8,128)(2,1)}, bf16[8,64,256]{2,1,0:T(8,128)(2,1)S(1)}, u32[]{:S(2)}, u32[]{:S(2)}) %collective-permute-start.17) | collective-permute-done | bytes 262176 | tf_op jit(solution)/shard_map/ppermute | solution.py:21
  158.8 2.9 %finish.1.p0 = bf16[64,2048]{1,0:T(8,128)(2,1)} custom-call(s32[3]{0:T(128)} %pad_add_fusion.at_ref, bf16[8,64,256]{2,1,0:T(8,128)(2,1)} %get-tuple-element.18.got0, bf16[8,64,256]{2,1,0:T(8,128)(2,1)S(1)} %collective-permute-done.15.got1, bf16[8,64,256]{2,1,0:T(8,128)(2,1)S(1)} %collective-permute-done.16.got2, ...), custom_call_target="tpu_custom_call" | custom-call | tf_op jit(solution)/shard_map/finish/pallas_call | solution.py:341
  161.7 3.1 %collective-permute-start.20 = (bf16[64,2048]{1,0:T(8,128)(2,1)}, bf16[64,2048]{1,0:T(8,128)(2,1)S(1)}, u32[]{:S(2)}, u32[]{:S(2)}) collective-permute-start(bf16[64,2048]{1,0:T(8,128)(2,1)} %finish.1.p0), channel_id=1, source_target_pairs={{0,2},{2,4},{4,6},{6,0},{1,3},{3,5},{5,7},{7,1},{8,10},{10,12},{12... | collective-permute-start | bytes 786440 | tf_op jit(solution)/shard_map/ppermute | solution.py:21
  164.8 4.3 %collective-permute-start.19 = (bf16[64,2048]{1,0:T(8,128)(2,1)}, bf16[64,2048]{1,0:T(8,128)(2,1)S(1)}, u32[]{:S(2)}, u32[]{:S(2)}) collective-permute-start(bf16[64,2048]{1,0:T(8,128)(2,1)} %finish.1.p0), channel_id=1, source_target_pairs={{0,4},{2,6},{4,0},{6,2},{1,5},{3,7},{5,1},{7,3},{8,12},{10,14},{12... | collective-permute-start | bytes 786440 | tf_op jit(solution)/shard_map/ppermute | solution.py:21
  169.1 2.2 %collective-permute-start.18 = (bf16[64,2048]{1,0:T(8,128)(2,1)}, bf16[64,2048]{1,0:T(8,128)(2,1)S(1)}, u32[]{:S(2)}, u32[]{:S(2)}) collective-permute-start(bf16[64,2048]{1,0:T(8,128)(2,1)} %finish.1.p0), channel_id=1, source_target_pairs={{0,6},{2,0},{4,2},{6,4},{1,7},{3,1},{5,3},{7,5},{8,14},{10,8},{12,... | collective-permute-start | bytes 786440 | tf_op jit(solution)/shard_map/ppermute | solution.py:21
  171.3 2.6 %collective-permute-done.19.p2 = bf16[64,2048]{1,0:T(8,128)(2,1)S(1)} collective-permute-done((bf16[64,2048]{1,0:T(8,128)(2,1)}, bf16[64,2048]{1,0:T(8,128)(2,1)S(1)}, u32[]{:S(2)}, u32[]{:S(2)}) %collective-permute-start.19) | collective-permute-done | bytes 262176 | tf_op jit(solution)/shard_map/ppermute | solution.py:21
  174.0 2.5 %collective-permute-done.18.p1 = bf16[64,2048]{1,0:T(8,128)(2,1)S(1)} collective-permute-done((bf16[64,2048]{1,0:T(8,128)(2,1)}, bf16[64,2048]{1,0:T(8,128)(2,1)S(1)}, u32[]{:S(2)}, u32[]{:S(2)}) %collective-permute-start.18) | collective-permute-done | bytes 262176 | tf_op jit(solution)/shard_map/ppermute | solution.py:21
  176.4 1.1 pad_maximum_fusion
  177.5 13.4 %collective-permute-start.21 = (bf16[4,64,2048]{2,1,0:T(8,128)(2,1)S(1)}, bf16[4,64,2048]{2,1,0:T(8,128)(2,1)S(1)}, u32[]{:S(2)}, u32[]{:S(2)}) collective-permute-start(bf16[4,64,2048]{2,1,0:T(8,128)(2,1)S(1)} %pad_maximum_fusion), channel_id=1, source_target_pairs={{0,1},{1,0},{2,3},{3,2},{4,5},{5,4},{6,7},{7,6},{8,9},{9,8},{10,11... | collective-permute-start | bytes 3145736 | tf_op jit(solution)/shard_map/ppermute | solution.py:21
  190.9 0.7 zsum.1
  191.6 12.3 %collective-permute-start.22 = (f32[32,384]{1,0:T(8,128)}, f32[32,384]{1,0:T(8,128)S(1)}, u32[]{:S(2)}, u32[]{:S(2)}) collective-permute-start(f32[32,384]{1,0:T(8,128)} %get-tuple-element.24), channel_id=1, source_target_pairs={{0,256},{256,0},{1,257},{257,1},{2,258},{258,2},{3,259},{259,3},{4... | collective-permute-start | bytes 147464 | tf_op jit(solution)/shard_map/ppermute | solution.py:21
  203.9 0.0 copy-start.11
  203.9 2.4 %place.1 = bf16[512,2048]{1,0:T(8,128)(2,1)} custom-call(s32[3]{0:T(128)} %pad_add_fusion.at_ref, bf16[64,2048]{1,0:T(8,128)(2,1)} %finish.1.p0, bf16[64,2048]{1,0:T(8,128)(2,1)S(1)} %collective-permute-done.18.p1, bf16[64,2048]{1,0:T(8,128)(2,1)S(1)} %collective-permute-done.19.p2, bf16[64,2048]{1,0:T(8,128)(2,1)S(1)} %collective-permute-done.20.p3, ...), custom_call_target="tpu_custom_call" | custom-call | tf_op jit(solution)/shard_map/place/pallas_call | solution.py:357
  206.3 3.5 %all-to-all-start.4 = ((f32[8,8,256]{2,1,0:T(8,128)}), f32[8,8,256]{2,1,0:T(8,128)S(1)}, u32[]{:S(2)}, u32[]{:S(2)}) async-start(f32[8,8,256]{2,1,0:T(8,128)} %get-tuple-element.23), calls=%async_computation.4 | async-start | bytes 131072 | tf_op jit(solution)/shard_map/all_to_all | solution.py:25
  209.9 0.7 fusion.2
  210.6 4.2 %all-to-all-done.4 = f32[8,8,256]{2,1,0:T(8,128)S(1)} async-done(((f32[8,8,256]{2,1,0:T(8,128)}), f32[8,8,256]{2,1,0:T(8,128)S(1)}, u32[]{:S(2)}, u32[]{:S(2)}) %all-to-all-start.4) | async-done | bytes 65568 | tf_op jit(solution)/shard_map/all_to_all | solution.py:25
  214.8 0.6 copy.9
  (32 shorter events, 0.1 us)
Async XLA Ops:
  12.5 74.3 %copy-start = (bf16[4,64,768]{2,1,0:T(8,128)(2,1)}, bf16[4,64,768]{2,1,0:T(8,128)(2,1)S(1)}, u32[]{:S(2)}) copy-start(bf16[4,64,768]{2,1,0:T(8,128)(2,1)S(1)} %all_to_all.25) | copy-start | bytes 1179652
  12.5 19.8 %collective-permute-start = (bf16[256,768]{1,0:T(8,128)(2,1)S(1)}, bf16[256,768]{1,0:T(8,128)(2,1)S(1)}, u32[]{:S(2)}, u32[]{:S(2)}) collective-permute-start(bf16[256,768]{1,0:T(8,128)(2,1)S(1)} %bitcast.19), channel_id=1, source_target_pairs={{0,32},{32,64},{64,96},{96,128},{128,160},{160,192},{192,224},{224... | collective-permute-start | bytes 1179656 | tf_op jit(solution)/shard_map/ppermute | solution.py:21
  17.1 30.1 %collective-permute-start.8 = (bf16[256,768]{1,0:T(8,128)(2,1)S(1)}, bf16[256,768]{1,0:T(8,128)(2,1)S(1)}, u32[]{:S(2)}, u32[]{:S(2)}) collective-permute-start(bf16[256,768]{1,0:T(8,128)(2,1)S(1)} %bitcast.20), channel_id=1, source_target_pairs={{0,480},{32,0},{64,32},{96,64},{128,96},{160,128},{192,160},{224,1... | collective-permute-start | bytes 1179656 | tf_op jit(solution)/shard_map/ppermute | solution.py:21
  32.3 54.5 %copy-start.1 = (bf16[256,768]{1,0:T(8,128)(2,1)}, bf16[256,768]{1,0:T(8,128)(2,1)S(1)}, u32[]{:S(2)}) copy-start(bf16[256,768]{1,0:T(8,128)(2,1)S(1)} %collective-permute-done.refs_2_.refs_6_) | copy-start | bytes 1179652
  32.3 16.8 %collective-permute-start.1 = (bf16[256,768]{1,0:T(8,128)(2,1)S(1)}, bf16[256,768]{1,0:T(8,128)(2,1)S(1)}, u32[]{:S(2)}, u32[]{:S(2)}) collective-permute-start(bf16[256,768]{1,0:T(8,128)(2,1)S(1)} %collective-permute-done.refs_2_.refs_6_), channel_id=1, source_target_pairs={{0,32},{32,64},{64,96},{96,128},{128,160},{160,192},{192,224},{224... | collective-permute-start | bytes 1179656 | tf_op jit(solution)/shard_map/ppermute | solution.py:21
  42.6 44.3 %copy-start.5 = (bf16[4,64,384]{2,1,0:T(8,128)(2,1)}, bf16[4,64,384]{2,1,0:T(8,128)(2,1)S(1)}, u32[]{:S(2)}) copy-start(bf16[4,64,384]{2,1,0:T(8,128)(2,1)S(1)} %all_to_all.26) | copy-start | bytes 589828
  42.6 11.8 %collective-permute-start.4 = (bf16[256,384]{1,0:T(8,128)(2,1)S(1)}, bf16[256,384]{1,0:T(8,128)(2,1)S(1)}, u32[]{:S(2)}, u32[]{:S(2)}) collective-permute-start(bf16[256,384]{1,0:T(8,128)(2,1)S(1)} %bitcast.24), channel_id=1, source_target_pairs={{0,480},{32,0},{64,32},{96,64},{128,96},{160,128},{192,160},{224,1... | collective-permute-start | bytes 589832 | tf_op jit(solution)/shard_map/ppermute | solution.py:21
  47.2 39.7 %copy-start.2 = (bf16[256,768]{1,0:T(8,128)(2,1)}, bf16[256,768]{1,0:T(8,128)(2,1)S(1)}, u32[]{:S(2)}) copy-start(bf16[256,768]{1,0:T(8,128)(2,1)S(1)} %collective-permute-done.8.refs_1_) | copy-start | bytes 1179652
  47.2 21.8 %collective-permute-start.9 = (bf16[256,768]{1,0:T(8,128)(2,1)S(1)}, bf16[256,768]{1,0:T(8,128)(2,1)S(1)}, u32[]{:S(2)}, u32[]{:S(2)}) collective-permute-start(bf16[256,768]{1,0:T(8,128)(2,1)S(1)} %collective-permute-done.8.refs_1_), channel_id=1, source_target_pairs={{0,480},{32,0},{64,32},{96,64},{128,96},{160,128},{192,160},{224,1... | collective-permute-start | bytes 1179656 | tf_op jit(solution)/shard_map/ppermute | solution.py:21
  49.1 37.7 %copy-start.3 = (bf16[256,768]{1,0:T(8,128)(2,1)}, bf16[256,768]{1,0:T(8,128)(2,1)S(1)}, u32[]{:S(2)}) copy-start(bf16[256,768]{1,0:T(8,128)(2,1)S(1)} %collective-permute-done.1.refs_4_.refs_5_) | copy-start | bytes 1179652
  49.1 21.9 %collective-permute-start.2 = (bf16[256,768]{1,0:T(8,128)(2,1)S(1)}, bf16[256,768]{1,0:T(8,128)(2,1)S(1)}, u32[]{:S(2)}, u32[]{:S(2)}) collective-permute-start(bf16[256,768]{1,0:T(8,128)(2,1)S(1)} %collective-permute-done.1.refs_4_.refs_5_), channel_id=1, source_target_pairs={{0,32},{32,64},{64,96},{96,128},{128,160},{160,192},{192,224},{224... | collective-permute-start | bytes 1179656 | tf_op jit(solution)/shard_map/ppermute | solution.py:21
  52.5 10.0 %collective-permute-start.10 = (bf16[256,384]{1,0:T(8,128)(2,1)S(1)}, bf16[256,384]{1,0:T(8,128)(2,1)S(1)}, u32[]{:S(2)}, u32[]{:S(2)}) collective-permute-start(bf16[256,384]{1,0:T(8,128)(2,1)S(1)} %bitcast.25), channel_id=1, source_target_pairs={{0,32},{32,64},{64,96},{96,128},{128,160},{160,192},{192,224},{224... | collective-permute-start | bytes 589832 | tf_op jit(solution)/shard_map/ppermute | solution.py:21
  54.4 16.5 %copy-start.8 = (bf16[256,384]{1,0:T(8,128)(2,1)}, bf16[256,384]{1,0:T(8,128)(2,1)S(1)}, u32[]{:S(2)}) copy-start(bf16[256,384]{1,0:T(8,128)(2,1)S(1)} %collective-permute-done.4.refs_6_) | copy-start | bytes 589828
  54.5 10.4 %collective-permute-start.5 = (bf16[256,384]{1,0:T(8,128)(2,1)S(1)}, bf16[256,384]{1,0:T(8,128)(2,1)}, u32[]{:S(2)}, u32[]{:S(2)}) collective-permute-start(bf16[256,384]{1,0:T(8,128)(2,1)S(1)} %collective-permute-done.4.refs_6_), channel_id=1, source_target_pairs={{0,480},{32,0},{64,32},{96,64},{128,96},{160,128},{192,160},{224,1... | collective-permute-start | bytes 589832 | tf_op jit(solution)/shard_map/ppermute | solution.py:21
  62.5 13.8 %copy-start.9 = (bf16[256,384]{1,0:T(8,128)(2,1)}, bf16[256,384]{1,0:T(8,128)(2,1)S(1)}, u32[]{:S(2)}) copy-start(bf16[256,384]{1,0:T(8,128)(2,1)S(1)} %collective-permute-done.10.refs_7_) | copy-start | bytes 589828
  62.5 11.9 %collective-permute-start.11 = (bf16[256,384]{1,0:T(8,128)(2,1)S(1)}, bf16[256,384]{1,0:T(8,128)(2,1)}, u32[]{:S(2)}, u32[]{:S(2)}) collective-permute-start(bf16[256,384]{1,0:T(8,128)(2,1)S(1)} %collective-permute-done.10.refs_7_), channel_id=1, source_target_pairs={{0,32},{32,64},{64,96},{96,128},{128,160},{160,192},{192,224},{224... | collective-permute-start | bytes 589832 | tf_op jit(solution)/shard_map/ppermute | solution.py:21
  64.9 11.4 %collective-permute-start.6 = (bf16[256,384]{1,0:T(8,128)(2,1)}, bf16[256,384]{1,0:T(8,128)(2,1)}, u32[]{:S(2)}, u32[]{:S(2)}) collective-permute-start(bf16[256,384]{1,0:T(8,128)(2,1)} %collective-permute-done.5.refs_8_), channel_id=1, source_target_pairs={{0,480},{32,0},{64,32},{96,64},{128,96},{160,128},{192,160},{224,1... | collective-permute-start | bytes 589832 | tf_op jit(solution)/shard_map/ppermute | solution.py:21
  69.0 17.8 %copy-start.4 = (bf16[256,768]{1,0:T(8,128)(2,1)}, bf16[256,768]{1,0:T(8,128)(2,1)S(1)}, u32[]{:S(2)}) copy-start(bf16[256,768]{1,0:T(8,128)(2,1)S(1)} %collective-permute-done.9.refs_3_.refs_2_) | copy-start | bytes 1179652
  69.1 31.7 %collective-permute-start.12 = (bf16[256,768]{1,0:T(8,128)(2,1)S(1)}, bf16[256,768]{1,0:T(8,128)(2,1)S(1)}, u32[]{:S(2)}, u32[]{:S(2)}) collective-permute-start(bf16[256,768]{1,0:T(8,128)(2,1)S(1)} %collective-permute-done.9.refs_3_.refs_2_), channel_id=1, source_target_pairs={{0,480},{32,0},{64,32},{96,64},{128,96},{160,128},{192,160},{224,1... | collective-permute-start | bytes 1179656 | tf_op jit(solution)/shard_map/ppermute | solution.py:21
  71.0 15.9 %copy-start.6 = (bf16[256,768]{1,0:T(8,128)(2,1)}, bf16[256,768]{1,0:T(8,128)(2,1)S(1)}, u32[]{:S(2)}) copy-start(bf16[256,768]{1,0:T(8,128)(2,1)S(1)} %collective-permute-done.2.refs_4_) | copy-start | bytes 1179652
  71.0 29.8 %collective-permute-start.3 = (bf16[256,768]{1,0:T(8,128)(2,1)S(1)}, bf16[256,768]{1,0:T(8,128)(2,1)S(1)}, u32[]{:S(2)}, u32[]{:S(2)}) collective-permute-start(bf16[256,768]{1,0:T(8,128)(2,1)S(1)} %collective-permute-done.2.refs_4_), channel_id=1, source_target_pairs={{0,32},{32,64},{64,96},{96,128},{128,160},{160,192},{192,224},{224... | collective-permute-start | bytes 1179656 | tf_op jit(solution)/shard_map/ppermute | solution.py:21
  74.4 26.4 %collective-permute-start.13 = (bf16[256,384]{1,0:T(8,128)(2,1)}, bf16[256,384]{1,0:T(8,128)(2,1)}, u32[]{:S(2)}, u32[]{:S(2)}) collective-permute-start(bf16[256,384]{1,0:T(8,128)(2,1)} %collective-permute-done.11.refs_9_), channel_id=1, source_target_pairs={{0,32},{32,64},{64,96},{96,128},{128,160},{160,192},{192,224},{224... | collective-permute-start | bytes 589832 | tf_op jit(solution)/shard_map/ppermute | solution.py:21
  76.4 24.4 %collective-permute-start.7 = (bf16[256,384]{1,0:T(8,128)(2,1)}, bf16[256,384]{1,0:T(8,128)(2,1)S(1)}, u32[]{:S(2)}, u32[]{:S(2)}) collective-permute-start(bf16[256,384]{1,0:T(8,128)(2,1)} %collective-permute-done.6.refs_7_), channel_id=1, source_target_pairs={{0,480},{32,0},{64,32},{96,64},{128,96},{160,128},{192,160},{224,1... | collective-permute-start | bytes 589832 | tf_op jit(solution)/shard_map/ppermute | solution.py:21
  86.9 7.0 %copy-start.10 = (f32[2048]{0:T(1024)S(1)}, f32[2048]{0:T(1024)}, u32[]{:S(2)}) copy-start(f32[2048]{0:T(1024)} %param.7) | copy-start | bytes 24580
  100.8 0.8 copy-start.7
  112.2 19.0 %all-to-all-start.2 = ((bf16[4,8,72,384]{3,2,1,0:T(8,128)(2,1)}), bf16[4,8,72,384]{3,2,1,0:T(8,128)(2,1)S(1)}, u32[]{:S(2)}, u32[]{:S(2)}) async-start(bf16[4,8,72,384]{3,2,1,0:T(8,128)(2,1)} %get-tuple-element.22), calls=%async_computation.2 | async-start | bytes 3538944 | tf_op jit(solution)/shard_map/all_to_all | solution.py:25
  115.8 25.7 %collective-permute-start.14 = (bf16[4,8,64,256]{3,2,1,0:T(8,128)(2,1)}, bf16[4,8,64,256]{3,2,1,0:T(8,128)(2,1)S(1)}, u32[]{:S(2)}, u32[]{:S(2)}) collective-permute-start(bf16[4,8,64,256]{3,2,1,0:T(8,128)(2,1)} %get-tuple-element.17), channel_id=1, source_target_pairs={{0,1},{1,0},{2,3},{3,2},{4,5},{5,4},{6,7},{7,6},{8,9},{9,8},{10,11... | collective-permute-start | bytes 3145736 | tf_op jit(solution)/shard_map/ppermute | solution.py:21
  132.9 58.0 %all-to-all-start.3 = ((bf16[16,40,384]{2,1,0:T(8,128)(2,1)}), bf16[16,40,384]{2,1,0:T(8,128)(2,1)S(1)}, u32[]{:S(2)}, u32[]{:S(2)}) async-start(bf16[16,40,384]{2,1,0:T(8,128)(2,1)} %ysum.1), calls=%async_computation.3 | async-start | bytes 983040 | tf_op jit(solution)/shard_map/all_to_all | solution.py:25
  143.7 10.6 %collective-permute-start.15 = (bf16[8,64,256]{2,1,0:T(8,128)(2,1)}, bf16[8,64,256]{2,1,0:T(8,128)(2,1)S(1)}, u32[]{:S(2)}, u32[]{:S(2)}) collective-permute-start(bf16[8,64,256]{2,1,0:T(8,128)(2,1)} %get-tuple-element.19), channel_id=1, source_target_pairs={{0,2},{2,4},{4,6},{6,0},{1,3},{3,5},{5,7},{7,1},{8,10},{10,12},{12... | collective-permute-start | bytes 786440 | tf_op jit(solution)/shard_map/ppermute | solution.py:21
  146.9 9.2 %collective-permute-start.16 = (bf16[8,64,256]{2,1,0:T(8,128)(2,1)}, bf16[8,64,256]{2,1,0:T(8,128)(2,1)S(1)}, u32[]{:S(2)}, u32[]{:S(2)}) collective-permute-start(bf16[8,64,256]{2,1,0:T(8,128)(2,1)} %get-tuple-element.20), channel_id=1, source_target_pairs={{0,4},{2,6},{4,0},{6,2},{1,5},{3,7},{5,1},{7,3},{8,12},{10,14},{12... | collective-permute-start | bytes 786440 | tf_op jit(solution)/shard_map/ppermute | solution.py:21
  151.2 7.6 %collective-permute-start.17 = (bf16[8,64,256]{2,1,0:T(8,128)(2,1)}, bf16[8,64,256]{2,1,0:T(8,128)(2,1)S(1)}, u32[]{:S(2)}, u32[]{:S(2)}) collective-permute-start(bf16[8,64,256]{2,1,0:T(8,128)(2,1)} %get-tuple-element.21), channel_id=1, source_target_pairs={{0,6},{2,0},{4,2},{6,4},{1,7},{3,1},{5,3},{7,5},{8,14},{10,8},{12,... | collective-permute-start | bytes 786440 | tf_op jit(solution)/shard_map/ppermute | solution.py:21
  161.7 9.6 %collective-permute-start.20 = (bf16[64,2048]{1,0:T(8,128)(2,1)}, bf16[64,2048]{1,0:T(8,128)(2,1)S(1)}, u32[]{:S(2)}, u32[]{:S(2)}) collective-permute-start(bf16[64,2048]{1,0:T(8,128)(2,1)} %finish.1.p0), channel_id=1, source_target_pairs={{0,2},{2,4},{4,6},{6,0},{1,3},{3,5},{5,7},{7,1},{8,10},{10,12},{12... | collective-permute-start | bytes 786440 | tf_op jit(solution)/shard_map/ppermute | solution.py:21
  164.8 9.1 %collective-permute-start.19 = (bf16[64,2048]{1,0:T(8,128)(2,1)}, bf16[64,2048]{1,0:T(8,128)(2,1)S(1)}, u32[]{:S(2)}, u32[]{:S(2)}) collective-permute-start(bf16[64,2048]{1,0:T(8,128)(2,1)} %finish.1.p0), channel_id=1, source_target_pairs={{0,4},{2,6},{4,0},{6,2},{1,5},{3,7},{5,1},{7,3},{8,12},{10,14},{12... | collective-permute-start | bytes 786440 | tf_op jit(solution)/shard_map/ppermute | solution.py:21
  169.1 7.3 %collective-permute-start.18 = (bf16[64,2048]{1,0:T(8,128)(2,1)}, bf16[64,2048]{1,0:T(8,128)(2,1)S(1)}, u32[]{:S(2)}, u32[]{:S(2)}) collective-permute-start(bf16[64,2048]{1,0:T(8,128)(2,1)} %finish.1.p0), channel_id=1, source_target_pairs={{0,6},{2,0},{4,2},{6,4},{1,7},{3,1},{5,3},{7,5},{8,14},{10,8},{12,... | collective-permute-start | bytes 786440 | tf_op jit(solution)/shard_map/ppermute | solution.py:21
  177.5 26.4 %collective-permute-start.21 = (bf16[4,64,2048]{2,1,0:T(8,128)(2,1)S(1)}, bf16[4,64,2048]{2,1,0:T(8,128)(2,1)S(1)}, u32[]{:S(2)}, u32[]{:S(2)}) collective-permute-start(bf16[4,64,2048]{2,1,0:T(8,128)(2,1)S(1)} %pad_maximum_fusion), channel_id=1, source_target_pairs={{0,1},{1,0},{2,3},{3,2},{4,5},{5,4},{6,7},{7,6},{8,9},{9,8},{10,11... | collective-permute-start | bytes 3145736 | tf_op jit(solution)/shard_map/ppermute | solution.py:21
  191.6 18.3 %collective-permute-start.22 = (f32[32,384]{1,0:T(8,128)}, f32[32,384]{1,0:T(8,128)S(1)}, u32[]{:S(2)}, u32[]{:S(2)}) collective-permute-start(f32[32,384]{1,0:T(8,128)} %get-tuple-element.24), channel_id=1, source_target_pairs={{0,256},{256,0},{1,257},{257,1},{2,258},{258,2},{3,259},{259,3},{4... | collective-permute-start | bytes 147464 | tf_op jit(solution)/shard_map/ppermute | solution.py:21
  203.9 6.0 %copy-start.11 = (f32[32,384]{1,0:T(8,128)S(1)}, f32[32,384]{1,0:T(8,128)}, u32[]{:S(2)}) copy-start(f32[32,384]{1,0:T(8,128)} %get-tuple-element.24) | copy-start | bytes 147460
  206.3 8.4 %all-to-all-start.4 = ((f32[8,8,256]{2,1,0:T(8,128)}), f32[8,8,256]{2,1,0:T(8,128)S(1)}, u32[]{:S(2)}, u32[]{:S(2)}) async-start(f32[8,8,256]{2,1,0:T(8,128)} %get-tuple-element.23), calls=%async_computation.4 | async-start | bytes 131072 | tf_op jit(solution)/shard_map/all_to_all | solution.py:25

commit v6 on v4

--- a/solution.py
+++ b/solution.py
@@ -10,6 +10,7 @@
 REP_FS = ("rep", "fs_0", "fs_1")
 TP = ("x", "c")
 RING = ("rep", "fs_0")
+PLANE = ("fs_1", "x", "c")
 EPS = 1e-06
 EARLY = (0, 1, 7, 2, 6)
 F32 = jnp.float32
@@ -66,14 +67,7 @@
     acc_ref[:, 2 * units :] = dh
 
 
-def grad_kernel(gain_ref, lo_ref, hi_ref, acc_hbm, x_hbm, c_hbm, ct_hbm, *refs):
-    w_hbm, (mine_hbm, other_hbm, dd_hbm) = refs[:7], refs[7:10]
-    acc, xv, cv, ctv, wv, ov, dv, sems = refs[10:]
-    units = acc.shape[1] // 3
-    nz, _, cols = xv.shape
-    ny, _, longer, _ = dv.shape
-    nx, part = mine_hbm.shape[0], mine_hbm.shape[2]
-    rows = longer - 8
+def starter(sems):
     used = [0]
 
     def begin(src, dst):
@@ -82,98 +76,112 @@
         copy.start()
         return copy
 
-    slot = {0: 0, 1: 1, 2: 2, 3: 3, 5: 4, 6: 5, 7: 6}
+    return begin
+
+
+def down_kernel(lo_ref, hi_ref, acc_hbm, x_hbm, c_hbm, ct_hbm, w3_hbm, w5_hbm, *refs):
+    dd_hbm, both_ref, acc, xv, cv, ctv, wv, dv, sems = refs
+    units = acc.shape[1] // 3
+    ny, nz, rows, _ = dv.shape
+    cols = xv.shape[2]
+    begin = starter(sems)
     acc_in = begin(acc_hbm, acc)
-    x_in, c_in, w_in = {}, {}, {}
-    for d in (3, 5):
-        w_in[d] = begin(w_hbm[slot[d]], wv.at[slot[d]])
-        x_in[d] = begin(x_hbm.at[d], xv.at[d])
-        c_in[d] = begin(c_hbm.at[d], cv.at[d - 3])
-    x_in[4] = begin(x_hbm.at[4], xv.at[4])
-    c_in[4] = begin(c_hbm.at[4], cv.at[1])
-    for d in EARLY:
-        w_in[d] = begin(w_hbm[slot[d]], wv.at[slot[d]])
-        x_in[d] = begin(x_hbm.at[d], xv.at[d])
+    loads = []
+    for i, w_hbm in enumerate((w3_hbm, w5_hbm)):
+        d = 3 + 2 * i
+        loads.append(
+            (
+                begin(w_hbm, wv.at[i]),
+                begin(x_hbm.at[d], xv.at[2 * i]),
+                begin(c_hbm.at[d], cv.at[2 * i]),
+            )
+        )
+    mid_in = (begin(x_hbm.at[4], xv.at[1]), begin(c_hbm.at[4], cv.at[1]))
     ct_in = begin(ct_hbm, ctv)
-
-    half = cols // 2
-    halves = ((lo_ref, slice(0, half)), (hi_ref, slice(half, cols)))
     acc_in.wait()
     gu, dh = acc[:, : 2 * units], acc[:, 2 * units :]
-    for d in (3, 5):
-        w_in[d].wait()
-        x_in[d].wait()
-        c_in[d].wait()
-        w = wv.at[slot[d]]
-        gu = gu + jnp.dot(xv[d], w[:, : 2 * units], preferred_element_type=F32)
-        dh = dh + jnp.dot(cv[d - 3], w[:, 2 * units :], preferred_element_type=F32)
-    x_in[4].wait()
-    c_in[4].wait()
-    for w, at in halves:
-        gu = gu + jnp.dot(xv[4, :, at], w[:, : 2 * units], preferred_element_type=F32)
+    for i in range(2):
+        for copy in loads[i]:
+            copy.wait()
+        gu = gu + jnp.dot(xv[2 * i], wv[i, :, : 2 * units], preferred_element_type=F32)
+        dh = dh + jnp.dot(cv[2 * i], wv[i, :, 2 * units :], preferred_element_type=F32)
+    for copy in mid_in:
+        copy.wait()
+    half = cols // 2
+    for w, at in ((lo_ref, slice(0, half)), (hi_ref, slice(half, cols))):
+        gu = gu + jnp.dot(xv[1, :, at], w[:, : 2 * units], preferred_element_type=F32)
         dh = dh + jnp.dot(cv[1, :, at], w[:, 2 * units :], preferred_element_type=F32)
     gate, up = gu[:, :units], gu[:, units:]
     dh = 0.5 * dh
     sig = jax.nn.sigmoid(gate)
     act = gate * sig
     hidden = (act * up).astype(BF16)
-    d_gate = (dh * up * sig * (1.0 + gate * (1.0 - sig))).astype(BF16)
-    d_up = (dh * act).astype(BF16)
-    both = jnp.concatenate([d_gate, d_up], axis=1)
+    both_ref[:, :units] = (dh * up * sig * (1.0 + gate * (1.0 - sig))).astype(BF16)
+    both_ref[:, units:] = (dh * act).astype(BF16)
+    ct_in.wait()
     out_copies = []
-    sums = {}
+    for d in range(nz):
+        res = jnp.dot(ctv[d], hidden, preferred_element_type=F32)
+        res = (0.5 * res).astype(BF16)
+        for y in range(ny):
+            dv[y, d] = res[y * rows : (y + 1) * rows]
+        out_copies.append(begin(dv.at[:, d], dd_hbm.at[:, d]))
+    for copy in out_copies:
+        copy.wait()
+
+
+def grad_kernel(gain_ref, lo_ref, hi_ref, both_ref, x_hbm, *refs):
+    w_hbm, (mine_hbm, other_hbm, sum_ref) = refs[:7], refs[7:10]
+    xv, wv, ov, sems = refs[10:]
+    _, _, cols = xv.shape
+    nx, part = mine_hbm.shape[0], mine_hbm.shape[2]
+    units = both_ref.shape[1] // 2
+    begin = starter(sems)
+    slot = {0: 0, 1: 1, 2: 2, 3: 3, 5: 4, 6: 5, 7: 6}
+    x_in, w_in = {}, {}
     for d in (4, 3, 5) + EARLY:
-        if d in EARLY:
+        x_in[d] = begin(x_hbm.at[d], xv.at[d])
+        if d != 4:
+            w_in[d] = begin(w_hbm[slot[d]], wv.at[slot[d]])
+    half = cols // 2
+    halves = ((lo_ref, slice(0, half)), (hi_ref, slice(half, cols)))
+    both = both_ref[...]
+    out_copies = []
+    for d in (4, 3, 5) + EARLY:
+        if d != 4:
             w_in[d].wait()
-            x_in[d].wait()
+        x_in[d].wait()
         pieces = halves if d == 4 else ((wv.at[slot[d]], slice(0, cols)),)
-        got = []
         for w, at in pieces:
             out = lax.dot_general(
                 both, w[:, : 2 * units], (((1,), (1,)), ((), ())), preferred_element_type=F32
             )
             terms = jnp.sum(xv[d, :, at].astype(F32) * out, axis=0, keepdims=True)
-            got.append(terms / gain_ref[d, :, at])
+            sum_ref[d, :, at] = terms / gain_ref[d, :, at]
             out = out.astype(BF16)
             for k in range(2 * nx):
                 ov[k, d, :, at] = out[k * part : (k + 1) * part]
-        sums[d] = got[0] if len(got) == 1 else jnp.concatenate(got, axis=1)
         out_copies.append(begin(ov.at[pl.ds(nx, nx), d], other_hbm.at[:, d]))
         out_copies.append(begin(ov.at[pl.ds(0, nx), d], mine_hbm.at[:, d]))
-    ct_in.wait()
-    for d in range(nz):
-        res = jnp.dot(ctv[d], hidden, preferred_element_type=F32)
-        res = (0.5 * res).astype(BF16)
-        high = sums[d].astype(BF16)
-        left = sums[d] - high.astype(F32)
-        mid = left.astype(BF16)
-        low = (left - mid.astype(F32)).astype(BF16)
-        extra = jnp.concatenate([high, mid, low, jnp.zeros((5, cols), BF16)], axis=0)
-        extra = jnp.concatenate([extra, jnp.zeros((8, units - cols), BF16)], axis=1)
-        for y in range(ny):
-            dv[y, d, :rows] = res[y * rows : (y + 1) * rows]
-            dv[y, d, rows:] = extra
-        out_copies.append(begin(dv.at[:, d], dd_hbm.at[:, d]))
     for copy in out_copies:
         copy.wait()
 
 
-def rows_kernel(at_ref, got_ref, out_ref):
-    ny, nz, longer, _ = got_ref.shape
-    rows = longer - 8
+def rows_kernel(at_ref, own_ref, got_ref, out_ref):
+    ny, nz, rows, units = got_ref.shape
     half = rows // 2
-    sums = []
+    cols = own_ref.shape[2]
     for d in range(nz):
         total = got_ref[0, d].astype(F32)
         for k in range(1, ny):
             total = total + got_ref[k, d].astype(F32)
-        part = total[:rows].astype(BF16)
+        part = total.astype(BF16)
         to = (at_ref[0] + d) % nz
         out_ref[to, :half] = part[:half]
         out_ref[nz + to, :half] = part[half:]
-        sums.append(jnp.sum(total[rows:], axis=0, keepdims=True))
-    extra = jnp.concatenate(sums, axis=0)
+    extra = jnp.concatenate([own_ref[d] for d in range(nz)], axis=0)
     extra = pltpu.roll(extra, at_ref[0], 0).astype(BF16)
+    extra = jnp.concatenate([extra, jnp.zeros((nz, units - cols), BF16)], axis=1)
     for k in range(2 * nz):
         out_ref[k, half:] = extra
 
@@ -299,36 +307,51 @@
         name="forward",
     )(xr, cr, w0, bwd[1], fwd[1], bwd[2], fwd[2])
     anywhere = pl.BlockSpec(memory_space=pl.ANY)
-    mine, other, dd = pl.pallas_call(
+    dd, both = pl.pallas_call(
+        down_kernel,
+        out_shape=(
+            jax.ShapeDtypeStruct((ny, nz, rows, units), BF16),
+            jax.ShapeDtypeStruct((tokens, 2 * units), BF16),
+        ),
+        in_specs=vmem(2) + [anywhere] * 6,
+        out_specs=(anywhere, pl.BlockSpec(memory_space=pltpu.VMEM)),
+        scratch_shapes=[
+            pltpu.VMEM((tokens, 3 * units), F32),
+            pltpu.VMEM((3, tokens, cols), BF16),
+            pltpu.VMEM((3, tokens, cols), BF16),
+            pltpu.VMEM((nz, cols, tokens), BF16),
+            pltpu.VMEM((2, cols, 3 * units), BF16),
+            pltpu.VMEM((ny, nz, rows, units), BF16),
+            pltpu.SemaphoreType.DMA((24,)),
+        ],
+        name="down",
+    )(*near(last_f, last_b), acc, xr, cr, ct, bwd[3], fwd[3])
+    dy = exchanged(dd, "fs_1")
+    mine, other, sums = pl.pallas_call(
         grad_kernel,
         out_shape=(
             jax.ShapeDtypeStruct((nx, nz, part, cols), BF16),
             jax.ShapeDtypeStruct((nx, nz, part, cols), BF16),
-            jax.ShapeDtypeStruct((ny, nz, rows + 8, units), BF16),
-        ),
-        in_specs=vmem(3) + [anywhere] * 11,
-        out_specs=(anywhere,) * 3,
+            jax.ShapeDtypeStruct((nz, 1, cols), F32),
+        ),
+        in_specs=vmem(4) + [anywhere] * 8,
+        out_specs=(anywhere, anywhere, pl.BlockSpec(memory_space=pltpu.VMEM)),
         scratch_shapes=[
-            pltpu.VMEM((tokens, 3 * units), F32),
             pltpu.VMEM((nz, tokens, cols), BF16),
-            pltpu.VMEM((3, tokens, cols), BF16),
-            pltpu.VMEM((nz, cols, tokens), BF16),
             pltpu.VMEM((7, cols, 3 * units), BF16),
             pltpu.VMEM((2 * nx, nz, part, cols), BF16),
-            pltpu.VMEM((ny, nz, rows + 8, units), BF16),
-            pltpu.SemaphoreType.DMA((48,)),
+            pltpu.SemaphoreType.DMA((32,)),
         ],
         name="grad",
-    )(gain_ring, *near(last_f, last_b), acc, xr, cr, ct, *weights)
+    )(gain_ring, *near(last_f, last_b), both, xr, *weights)
     theirs = shifted(other, "c", 1)
-    dy = exchanged(dd, "fs_1")
-
     chunk = jax.ShapeDtypeStruct((nz, part, cols), BF16)
     chip = pl.pallas_call(
         chip_kernel,
         out_shape=(chunk,) * 4,
         in_specs=vmem(2),
         out_specs=tuple(vmem(4)),
+        compiler_params=pltpu.CompilerParams(vmem_limit_bytes=32 << 20),
         name="chip",
     )(mine, *near(theirs))
     got = [chip[0]]
@@ -362,22 +385,22 @@
     dz = pl.pallas_call(
         rows_kernel,
         out_shape=jax.ShapeDtypeStruct((2 * nz, rows // 2 + 8, units), BF16),
-        in_specs=[pl.BlockSpec(memory_space=pltpu.SMEM)] + vmem(1),
+        in_specs=[pl.BlockSpec(memory_space=pltpu.SMEM)] + vmem(2),
         out_specs=pl.BlockSpec(memory_space=pltpu.VMEM),
         name="ysum",
-    )(at, *near(dy))
+    )(at, sums, *near(dy))
     dz = exchanged(dz, RING)
     own, gain_own = pl.pallas_call(
         ring_kernel,
         out_shape=(
             jax.ShapeDtypeStruct((rows // 2, units), F32),
-            jax.ShapeDtypeStruct((lax.axis_size(TP), nz, cols), F32),
+            jax.ShapeDtypeStruct((lax.axis_size(PLANE), nz, cols), F32),
         ),
         in_specs=vmem(1),
         out_specs=tuple(vmem(2)),
         name="zsum",
     )(*near(dz))
-    gain_all = exchanged(gain_own, TP)
+    gain_all = exchanged(gain_own, PLANE)
     gain_gradient = jnp.sum(gain_all, axis=0).reshape(width)
     far = shifted(own, "rep", 1)
     pair = rolled(jnp.stack([own, far]), rep)

time: 209 us -> 202 us (0.967)
  the two profiles are of different devices: /device:TPU:1 before, /device:TPU:2 now
where the time goes in v6:
time: 202 us; the launch traced here: 201 us
  starting transfers between devices  88.8 us (44%)
  waiting for transfers between devices  46.7 us (23%)
  Pallas kernels  43.5 us (22%)
  blocking collectives  14.4 us (7%)
  other arithmetic  3.84 us (2%)
  local copies, waits for them, and re-layouts  2.65 us (1%)
    ppermute x17, starting transfers between devices, shifted(): return lax.ppermute(v, axis, [(i, (i + by) % n) for i in range(n)])  70 us
    ppermute x17, waiting for transfers between devices, shifted(): return lax.ppermute(v, axis, [(i, (i + by) % n) for i in range(n)])  41.3 us
    all_to_all x3, starting transfers between devices, exchanged(): return lax.all_to_all(v, axis, 0, 0, tiled=True)  18.8 us
    all_to_all x1, blocking collectives, exchanged(): return lax.all_to_all(v, axis, 0, 0, tiled=True)  14.4 us
    pallas_call x1, Pallas kernels, work(): pl.pallas_call(grad_kernel, out_shape=(jax.ShapeDtypeStruct((nx, nz, part...  8.68 us
    pallas_call x1, Pallas kernels, work(): pl.pallas_call(down_kernel, out_shape=(jax.ShapeDtypeStruct((ny, nz, rows...  7.13 us
    pallas_call x1, Pallas kernels, work(): pl.pallas_call(prepare_tokens, out_shape=jax.ShapeDtypeStruct((nz, tokens...  6.83 us
    pallas_call x1, Pallas kernels, work(): pl.pallas_call(forward_kernel, out_shape=jax.ShapeDtypeStruct((tokens, 3...  6.3 us
  transfers between devices with their start and end apart: 20, of which 10 were waited for; matrix products, arithmetic and copies ran while one was open for 1% of the time, Pallas kernels for 18%

profile of v6, /device:TPU:2, one launch (start us, length us, event | category | flops | bytes accessed | tf_op | source)
XLA Modules:
  0.0 201.0 jit_solution(15392160691810182929)
XLA Ops:
  0.6 0.9 pad_maximum_fusion.1
  1.5 14.4 %all_to_all.20 = bf16[4,64,1152]{2,1,0:T(8,128)(2,1)S(1)} all-to-all(bf16[4,64,1152]{2,1,0:T(8,128)(2,1)S(1)} %broadcast_in_dim.4), channel_id=1, replica_groups=mesh['rep'=2,'fs_0'=8,'fs_1'=4,'x'=4,'c'=2] {'fs_1'}, dimensions={0} | all-to-all | bytes 1179648 | tf_op jit(solution)/shard_map/all_to_all | solution.py:26
  16.0 3.8 %collective-permute-start = (bf16[256,1152]{1,0:T(8,128)(2,1)S(1)}, bf16[256,1152]{1,0:T(8,128)(2,1)S(1)}, u32[]{:S(2)}, u32[]{:S(2)}) collective-permute-start(bf16[256,1152]{1,0:T(8,128)(2,1)S(1)} %bitcast.18), channel_id=1, source_target_pairs={{0,32},{32,64},{64,96},{96,128},{128,160},{160,192},{192,224},{224... | collective-permute-start | bytes 1769480 | tf_op jit(solution)/shard_map/ppermute | solution.py:22
  19.8 9.5 %collective-permute-start.4 = (bf16[256,1152]{1,0:T(8,128)(2,1)S(1)}, bf16[256,1152]{1,0:T(8,128)(2,1)S(1)}, u32[]{:S(2)}, u32[]{:S(2)}) collective-permute-start(bf16[256,1152]{1,0:T(8,128)(2,1)S(1)} %bitcast.19), channel_id=1, source_target_pairs={{0,480},{32,0},{64,32},{96,64},{128,96},{160,128},{192,160},{224,1... | collective-permute-start | bytes 1769480 | tf_op jit(solution)/shard_map/ppermute | solution.py:22
  29.3 10.0 %collective-permute-done.refs_2_.refs_6_ = bf16[256,1152]{1,0:T(8,128)(2,1)S(1)} collective-permute-done((bf16[256,1152]{1,0:T(8,128)(2,1)S(1)}, bf16[256,1152]{1,0:T(8,128)(2,1)S(1)}, u32[]{:S(2)}, u32[]{:S(2)}) %collective-permute-start) | collective-permute-done | bytes 589856 | tf_op jit(solution)/shard_map/ppermute | solution.py:22
  39.3 1.9 collective-permute-start.1
  41.2 0.0 collective-permute-done.4.refs_1_
  41.2 0.0 copy-start.6
  41.2 5.1 %collective-permute-start.5 = (bf16[256,1152]{1,0:T(8,128)(2,1)S(1)}, bf16[256,1152]{1,0:T(8,128)(2,1)S(1)}, u32[]{:S(2)}, u32[]{:S(2)}) collective-permute-start(bf16[256,1152]{1,0:T(8,128)(2,1)S(1)} %collective-permute-done.4.refs_1_), channel_id=1, source_target_pairs={{0,480},{32,0},{64,32},{96,64},{128,96},{160,128},{192,160},{224,1... | collective-permute-start | bytes 1769480 | tf_op jit(solution)/shard_map/ppermute | solution.py:22
  46.4 9.1 %collective-permute-done.1.refs_4_.refs_5_ = bf16[256,1152]{1,0:T(8,128)(2,1)S(1)} collective-permute-done((bf16[256,1152]{1,0:T(8,128)(2,1)S(1)}, bf16[256,1152]{1,0:T(8,128)(2,1)S(1)}, u32[]{:S(2)}, u32[]{:S(2)}) %collective-permute-start.1) | collective-permute-done | bytes 589856 | tf_op jit(solution)/shard_map/ppermute | solution.py:22
  55.4 1.9 collective-permute-start.2
  57.4 0.0 collective-permute-done.5.refs_3_.refs_2_
  57.4 5.1 %collective-permute-start.6 = (bf16[256,1152]{1,0:T(8,128)(2,1)S(1)}, bf16[256,1152]{1,0:T(8,128)(2,1)S(1)}, u32[]{:S(2)}, u32[]{:S(2)}) collective-permute-start(bf16[256,1152]{1,0:T(8,128)(2,1)S(1)} %collective-permute-done.5.refs_3_.refs_2_), channel_id=1, source_target_pairs={{0,480},{32,0},{64,32},{96,64},{128,96},{160,128},{192,160},{224,1... | collective-permute-start | bytes 1769480 | tf_op jit(solution)/shard_map/ppermute | solution.py:22
  62.5 8.2 %collective-permute-done.2.w5_hbm.refs_4_ = bf16[256,1152]{1,0:T(8,128)(2,1)S(1)} collective-permute-done((bf16[256,1152]{1,0:T(8,128)(2,1)S(1)}, bf16[256,1152]{1,0:T(8,128)(2,1)S(1)}, u32[]{:S(2)}, u32[]{:S(2)}) %collective-permute-start.2) | collective-permute-done | bytes 589856 | tf_op jit(solution)/shard_map/ppermute | solution.py:22
  70.8 1.9 collective-permute-start.3
  72.7 0.0 collective-permute-done.6.w3_hbm.refs_3_
  72.8 5.1 %collective-permute-start.7 = (bf16[128,1152]{1,0:T(8,128)(2,1)S(1)}, bf16[128,1152]{1,0:T(8,128)(2,1)S(1)}, u32[]{:S(2)}, u32[]{:S(2)}) collective-permute-start(bf16[128,1152]{1,0:T(8,128)(2,1)S(1)} %slice.9), channel_id=1, source_target_pairs={{0,480},{32,0},{64,32},{96,64},{128,96},{160,128},{192,160},{224,1... | collective-permute-start | bytes 884744 | tf_op jit(solution)/shard_map/ppermute | solution.py:22
  77.9 0.6 pad_add_fusion.at_ref
  78.5 5.3 %prepare_c.1 = (bf16[8,512,256]{2,1,0:T(8,128)(2,1)}, bf16[8,256,512]{2,1,0:T(8,128)(2,1)}) custom-call(s32[3]{0:T(128)} %pad_add_fusion.at_ref, bf16[512,2048]{1,0:T(8,128)(2,1)} %c_ref.1, bf16[512,2048]{1,0:T(8,128)(2,1)} %c_ref.1), custom_call_target="tpu_custom_call" | custom-call | tf_op jit(solution)/shard_map/prepare_c/pallas_call | solution.py:280
  83.8 0.0 copy-done.3
  83.8 0.0 copy-done.4
  83.8 6.8 %prepare_x.1.x_ref.x_hbm = bf16[8,512,256]{2,1,0:T(8,128)(2,1)} custom-call(s32[3]{0:T(128)} %pad_add_fusion.at_ref, bf16[512,2048]{1,0:T(8,128)(2,1)} %x_ref.3, f32[1,2048]{1,0:T(1,128)} %bitcast.24), custom_call_target="tpu_custom_call" | custom-call | tf_op jit(solution)/shard_map/prepare_x/pallas_call | solution.py:266
  90.7 6.3 %forward.1.acc_hbm = f32[512,1152]{1,0:T(8,128)} custom-call(bf16[8,512,256]{2,1,0:T(8,128)(2,1)} %prepare_x.1.x_ref.x_hbm, bf16[8,512,256]{2,1,0:T(8,128)(2,1)} %get-tuple-element.16.c_ref.c_hbm, bf16[256,1152]{1,0:T(8,128)(2,1)} %bitcast.20, bf16[256,1152]{1,0:T(8,128)(2,1)} %copy-done.6, bf16[256,1152]{1,0:T(8,128)(2,1)} %copy-done.5, ...), custom_call_target="tpu_custom_call" | custom-call | tf_op jit(solution)/shard_map/forward/pallas_call | solution.py:302
  97.0 0.0 collective-permute-done.3.lo_ref
  97.0 0.0 collective-permute-done.7.hi_ref
  97.0 7.1 %down.1 = (bf16[4,8,64,384]{3,2,1,0:T(8,128)(2,1)}, bf16[512,768]{1,0:T(8,128)(2,1)}) custom-call(bf16[128,1152]{1,0:T(8,128)(2,1)S(1)} %collective-permute-done.3.lo_ref, bf16[128,1152]{1,0:T(8,128)(2,1)S(1)} %collective-permute-done.7.hi_ref, f32[512,1152]{1,0:T(8,128)} %forward.1.acc_hbm, bf16[8,512,256]{2,1,0:T(8,128)(2,1)} %prepare_x.1.x_ref.x_hbm, ...), custom_call_target="tpu_custom_call" | custom-call | tf_op jit(solution)/shard_map/down/pallas_call | solution.py:310
  104.1 0.0 copy-start.9
  104.1 3.6 %all-to-all-start.1 = ((bf16[4,8,64,384]{3,2,1,0:T(8,128)(2,1)}), bf16[4,8,64,384]{3,2,1,0:T(8,128)(2,1)S(1)}, u32[]{:S(2)}, u32[]{:S(2)}) async-start(bf16[4,8,64,384]{3,2,1,0:T(8,128)(2,1)} %get-tuple-element.26), calls=%async_computation.1 | async-start | bytes 3145728 | tf_op jit(solution)/shard_map/all_to_all | solution.py:26
  107.7 0.6 fusion.3.gain_ref
  108.4 8.7 %grad.1 = (bf16[4,8,64,256]{3,2,1,0:T(8,128)(2,1)}, bf16[4,8,64,256]{3,2,1,0:T(8,128)(2,1)}, f32[8,1,256]{2,1,0:T(1,128)}) custom-call(f32[8,1,256]{2,1,0:T(1,128)} %fusion.3.gain_ref, bf16[128,1152]{1,0:T(8,128)(2,1)S(1)} %collective-permute-done.3.lo_ref, bf16[128,1152]{1,0:T(8,128)(2,1)S(1)} %collective-permute-done.7.hi_ref, ...), custom_call_target="tpu_custom_call" | custom-call | tf_op jit(solution)/shard_map/grad/pallas_call | solution.py:330
  117.1 1.9 collective-permute-start.8
  119.0 5.4 %all-to-all-done.1.got_ref = bf16[4,8,64,384]{3,2,1,0:T(8,128)(2,1)S(1)} async-done(((bf16[4,8,64,384]{3,2,1,0:T(8,128)(2,1)}), bf16[4,8,64,384]{3,2,1,0:T(8,128)(2,1)S(1)}, u32[]{:S(2)}, u32[]{:S(2)}) %all-to-all-start.1) | async-done | bytes 1572896 | tf_op jit(solution)/shard_map/all_to_all | solution.py:26
  124.4 1.7 ysum.1
  126.1 7.8 %all-to-all-start.2 = ((bf16[16,40,384]{2,1,0:T(8,128)(2,1)}), bf16[16,40,384]{2,1,0:T(8,128)(2,1)S(1)}, u32[]{:S(2)}, u32[]{:S(2)}) async-start(bf16[16,40,384]{2,1,0:T(8,128)(2,1)} %ysum.1), calls=%async_computation.2 | async-start | bytes 983040 | tf_op jit(solution)/shard_map/all_to_all | solution.py:26
  133.9 0.0 collective-permute-done.8.theirs_ref
  133.9 1.2 copy-done
  135.1 1.5 chip.1
  136.6 0.7 copy-done.1
  137.3 4.0 %collective-permute-start.10 = (bf16[8,64,256]{2,1,0:T(8,128)(2,1)S(1)}, bf16[8,64,256]{2,1,0:T(8,128)(2,1)S(1)}, u32[]{:S(2)}, u32[]{:S(2)}) collective-permute-start(bf16[8,64,256]{2,1,0:T(8,128)(2,1)S(1)} %get-tuple-element.23), channel_id=1, source_target_pairs={{0,4},{2,6},{4,0},{6,2},{1,5},{3,7},{5,1},{7,3},{8,12},{10,14},{12... | collective-permute-start | bytes 786440 | tf_op jit(solution)/shard_map/ppermute | solution.py:22
  141.3 3.3 %collective-permute-start.11 = (bf16[8,64,256]{2,1,0:T(8,128)(2,1)S(1)}, bf16[8,64,256]{2,1,0:T(8,128)(2,1)S(1)}, u32[]{:S(2)}, u32[]{:S(2)}) collective-permute-start(bf16[8,64,256]{2,1,0:T(8,128)(2,1)S(1)} %get-tuple-element.24), channel_id=1, source_target_pairs={{0,6},{2,0},{4,2},{6,4},{1,7},{3,1},{5,3},{7,5},{8,14},{10,8},{12,... | collective-permute-start | bytes 786440 | tf_op jit(solution)/shard_map/ppermute | solution.py:22
  144.7 2.5 %collective-permute-start.9 = (bf16[8,64,256]{2,1,0:T(8,128)(2,1)S(1)}, bf16[8,64,256]{2,1,0:T(8,128)(2,1)S(1)}, u32[]{:S(2)}, u32[]{:S(2)}) collective-permute-start(bf16[8,64,256]{2,1,0:T(8,128)(2,1)S(1)} %get-tuple-element.22), channel_id=1, source_target_pairs={{0,2},{2,4},{4,6},{6,0},{1,3},{3,5},{5,7},{7,1},{8,10},{10,12},{12... | collective-permute-start | bytes 786440 | tf_op jit(solution)/shard_map/ppermute | solution.py:22
  147.2 0.0 collective-permute-done.10.got2
  147.2 2.7 %collective-permute-done.11.got3 = bf16[8,64,256]{2,1,0:T(8,128)(2,1)S(1)} collective-permute-done((bf16[8,64,256]{2,1,0:T(8,128)(2,1)S(1)}, bf16[8,64,256]{2,1,0:T(8,128)(2,1)S(1)}, u32[]{:S(2)}, u32[]{:S(2)}) %collective-permute-start.11) | collective-permute-done | bytes 262176 | tf_op jit(solution)/shard_map/ppermute | solution.py:22
  149.9 3.1 %collective-permute-done.9.got1 = bf16[8,64,256]{2,1,0:T(8,128)(2,1)S(1)} collective-permute-done((bf16[8,64,256]{2,1,0:T(8,128)(2,1)S(1)}, bf16[8,64,256]{2,1,0:T(8,128)(2,1)S(1)}, u32[]{:S(2)}, u32[]{:S(2)}) %collective-permute-start.9) | collective-permute-done | bytes 262176 | tf_op jit(solution)/shard_map/ppermute | solution.py:22
  152.9 2.9 %finish.1.p0 = bf16[64,2048]{1,0:T(8,128)(2,1)} custom-call(s32[3]{0:T(128)} %pad_add_fusion.at_ref, bf16[8,64,256]{2,1,0:T(8,128)(2,1)} %copy-done.1, bf16[8,64,256]{2,1,0:T(8,128)(2,1)S(1)} %collective-permute-done.9.got1, bf16[8,64,256]{2,1,0:T(8,128)(2,1)S(1)} %collective-permute-done.10.got2, bf16[8,64,256]{2,1,0:T(8,128)(2,1)S(1)} %collective-permute-done.11.got3, ...), custom_call_target="tpu_custom_call" | custom-call | tf_op jit(solution)/shard_map/finish/pallas_call | solution.py:361
  155.8 4.2 %collective-permute-start.12 = (bf16[64,2048]{1,0:T(8,128)(2,1)}, bf16[64,2048]{1,0:T(8,128)(2,1)S(1)}, u32[]{:S(2)}, u32[]{:S(2)}) collective-permute-start(bf16[64,2048]{1,0:T(8,128)(2,1)} %finish.1.p0), channel_id=1, source_target_pairs={{0,6},{2,0},{4,2},{6,4},{1,7},{3,1},{5,3},{7,5},{8,14},{10,8},{12,... | collective-permute-start | bytes 786440 | tf_op jit(solution)/shard_map/ppermute | solution.py:22
  160.1 1.9 collective-permute-start.13
  162.0 3.4 %collective-permute-start.14 = (bf16[64,2048]{1,0:T(8,128)(2,1)}, bf16[64,2048]{1,0:T(8,128)(2,1)S(1)}, u32[]{:S(2)}, u32[]{:S(2)}) collective-permute-start(bf16[64,2048]{1,0:T(8,128)(2,1)} %finish.1.p0), channel_id=1, source_target_pairs={{0,2},{2,4},{4,6},{6,0},{1,3},{3,5},{5,7},{7,1},{8,10},{10,12},{12... | collective-permute-start | bytes 786440 | tf_op jit(solution)/shard_map/ppermute | solution.py:22
  165.4 1.6 collective-permute-done.12.p1
  167.0 3.1 %collective-permute-done.13.p2 = bf16[64,2048]{1,0:T(8,128)(2,1)S(1)} collective-permute-done((bf16[64,2048]{1,0:T(8,128)(2,1)}, bf16[64,2048]{1,0:T(8,128)(2,1)S(1)}, u32[]{:S(2)}, u32[]{:S(2)}) %collective-permute-start.13) | collective-permute-done | bytes 262176 | tf_op jit(solution)/shard_map/ppermute | solution.py:22
  170.1 1.3 collective-permute-done.14.p3
  171.4 1.1 pad_maximum_fusion
  172.5 1.9 collective-permute-start.15
  174.4 0.0 all-to-all-done.2.got_ref
  174.4 0.8 zsum.1
  175.2 7.4 %all-to-all-start.3 = ((f32[32,8,256]{2,1,0:T(8,128)}), f32[32,8,256]{2,1,0:T(8,128)S(1)}, u32[]{:S(2)}, u32[]{:S(2)}) async-start(f32[32,8,256]{2,1,0:T(8,128)} %get-tuple-element.27), calls=%async_computation.3 | async-start | bytes 524288 | tf_op jit(solution)/shard_map/all_to_all | solution.py:26
  182.6 12.3 %collective-permute-start.16 = (f32[32,384]{1,0:T(8,128)}, f32[32,384]{1,0:T(8,128)S(1)}, u32[]{:S(2)}, u32[]{:S(2)}) collective-permute-start(f32[32,384]{1,0:T(8,128)} %get-tuple-element.28), channel_id=1, source_target_pairs={{0,256},{256,0},{1,257},{257,1},{2,258},{258,2},{3,259},{259,3},{4... | collective-permute-start | bytes 147464 | tf_op jit(solution)/shard_map/ppermute | solution.py:22
  194.9 0.0 copy-start.10
  194.9 0.0 collective-permute-done.15.other_ref
  194.9 2.4 %place.1 = bf16[512,2048]{1,0:T(8,128)(2,1)} custom-call(s32[3]{0:T(128)} %pad_add_fusion.at_ref, bf16[64,2048]{1,0:T(8,128)(2,1)} %finish.1.p0, bf16[64,2048]{1,0:T(8,128)(2,1)S(1)} %collective-permute-done.12.p1, bf16[64,2048]{1,0:T(8,128)(2,1)S(1)} %collective-permute-done.13.p2, bf16[64,2048]{1,0:T(8,128)(2,1)S(1)} %collective-permute-done.14.p3, ...), custom_call_target="tpu_custom_call" | custom-call | tf_op jit(solution)/shard_map/place/pallas_call | solution.py:377
  197.4 2.3 %collective-permute-done.16 = f32[32,384]{1,0:T(8,128)S(1)} collective-permute-done((f32[32,384]{1,0:T(8,128)}, f32[32,384]{1,0:T(8,128)S(1)}, u32[]{:S(2)}, u32[]{:S(2)}) %collective-permute-start.16) | collective-permute-done | bytes 49184 | tf_op jit(solution)/shard_map/ppermute | solution.py:22
  199.7 0.7 fusion.2
  200.4 0.0 all-to-all-done.3
  200.4 0.6 copy.9
  (19 shorter events, 0.2 us)
Async XLA Ops:
  16.0 67.8 %copy-start.2 = (bf16[4,64,1152]{2,1,0:T(8,128)(2,1)}, bf16[4,64,1152]{2,1,0:T(8,128)(2,1)S(1)}, u32[]{:S(2)}) copy-start(bf16[4,64,1152]{2,1,0:T(8,128)(2,1)S(1)} %all_to_all.20) | copy-start | bytes 1769476
  16.0 23.3 %collective-permute-start = (bf16[256,1152]{1,0:T(8,128)(2,1)S(1)}, bf16[256,1152]{1,0:T(8,128)(2,1)S(1)}, u32[]{:S(2)}, u32[]{:S(2)}) collective-permute-start(bf16[256,1152]{1,0:T(8,128)(2,1)S(1)} %bitcast.18), channel_id=1, source_target_pairs={{0,32},{32,64},{64,96},{96,128},{128,160},{160,192},{192,224},{224... | collective-permute-start | bytes 1769480 | tf_op jit(solution)/shard_map/ppermute | solution.py:22
  19.8 21.4 %collective-permute-start.4 = (bf16[256,1152]{1,0:T(8,128)(2,1)S(1)}, bf16[256,1152]{1,0:T(8,128)(2,1)S(1)}, u32[]{:S(2)}, u32[]{:S(2)}) collective-permute-start(bf16[256,1152]{1,0:T(8,128)(2,1)S(1)} %bitcast.19), channel_id=1, source_target_pairs={{0,480},{32,0},{64,32},{96,64},{128,96},{160,128},{192,160},{224,1... | collective-permute-start | bytes 1769480 | tf_op jit(solution)/shard_map/ppermute | solution.py:22
  39.3 44.5 %copy-start.5 = (bf16[256,1152]{1,0:T(8,128)(2,1)}, bf16[256,1152]{1,0:T(8,128)(2,1)S(1)}, u32[]{:S(2)}) copy-start(bf16[256,1152]{1,0:T(8,128)(2,1)S(1)} %collective-permute-done.refs_2_.refs_6_) | copy-start | bytes 1769476
  39.3 16.2 %collective-permute-start.1 = (bf16[256,1152]{1,0:T(8,128)(2,1)S(1)}, bf16[256,1152]{1,0:T(8,128)(2,1)S(1)}, u32[]{:S(2)}, u32[]{:S(2)}) collective-permute-start(bf16[256,1152]{1,0:T(8,128)(2,1)S(1)} %collective-permute-done.refs_2_.refs_6_), channel_id=1, source_target_pairs={{0,32},{32,64},{64,96},{96,128},{128,160},{160,192},{192,224},{224... | collective-permute-start | bytes 1769480 | tf_op jit(solution)/shard_map/ppermute | solution.py:22
  41.2 16.2 %copy-start.6 = (bf16[256,1152]{1,0:T(8,128)(2,1)}, bf16[256,1152]{1,0:T(8,128)(2,1)S(1)}, u32[]{:S(2)}) copy-start(bf16[256,1152]{1,0:T(8,128)(2,1)S(1)} %collective-permute-done.4.refs_1_) | copy-start | bytes 1769476
  41.2 16.2 %collective-permute-start.5 = (bf16[256,1152]{1,0:T(8,128)(2,1)S(1)}, bf16[256,1152]{1,0:T(8,128)(2,1)S(1)}, u32[]{:S(2)}, u32[]{:S(2)}) collective-permute-start(bf16[256,1152]{1,0:T(8,128)(2,1)S(1)} %collective-permute-done.4.refs_1_), channel_id=1, source_target_pairs={{0,480},{32,0},{64,32},{96,64},{128,96},{160,128},{192,160},{224,1... | collective-permute-start | bytes 1769480 | tf_op jit(solution)/shard_map/ppermute | solution.py:22
  55.4 1.9 copy-start.7
  55.4 15.3 %collective-permute-start.2 = (bf16[256,1152]{1,0:T(8,128)(2,1)S(1)}, bf16[256,1152]{1,0:T(8,128)(2,1)S(1)}, u32[]{:S(2)}, u32[]{:S(2)}) collective-permute-start(bf16[256,1152]{1,0:T(8,128)(2,1)S(1)} %collective-permute-done.1.refs_4_.refs_5_), channel_id=1, source_target_pairs={{0,32},{32,64},{64,96},{96,128},{128,160},{160,192},{192,224},{224... | collective-permute-start | bytes 1769480 | tf_op jit(solution)/shard_map/ppermute | solution.py:22
  57.4 15.3 %copy-start.8 = (bf16[256,1152]{1,0:T(8,128)(2,1)}, bf16[256,1152]{1,0:T(8,128)(2,1)S(1)}, u32[]{:S(2)}) copy-start(bf16[256,1152]{1,0:T(8,128)(2,1)S(1)} %collective-permute-done.5.refs_3_.refs_2_) | copy-start | bytes 1769476
  57.4 15.3 %collective-permute-start.6 = (bf16[256,1152]{1,0:T(8,128)(2,1)S(1)}, bf16[256,1152]{1,0:T(8,128)(2,1)S(1)}, u32[]{:S(2)}, u32[]{:S(2)}) collective-permute-start(bf16[256,1152]{1,0:T(8,128)(2,1)S(1)} %collective-permute-done.5.refs_3_.refs_2_), channel_id=1, source_target_pairs={{0,480},{32,0},{64,32},{96,64},{128,96},{160,128},{192,160},{224,1... | collective-permute-start | bytes 1769480 | tf_op jit(solution)/shard_map/ppermute | solution.py:22
  70.7 13.1 %copy-start.3 = (bf16[256,1152]{1,0:T(8,128)(2,1)}, bf16[256,1152]{1,0:T(8,128)(2,1)S(1)}, u32[]{:S(2)}) copy-start(bf16[256,1152]{1,0:T(8,128)(2,1)S(1)} %collective-permute-done.2.w5_hbm.refs_4_) | copy-start | bytes 1769476
  70.8 26.2 %collective-permute-start.3 = (bf16[128,1152]{1,0:T(8,128)(2,1)S(1)}, bf16[128,1152]{1,0:T(8,128)(2,1)S(1)}, u32[]{:S(2)}, u32[]{:S(2)}) collective-permute-start(bf16[128,1152]{1,0:T(8,128)(2,1)S(1)} %slice.8), channel_id=1, source_target_pairs={{0,32},{32,64},{64,96},{96,128},{128,160},{160,192},{192,224},{224... | collective-permute-start | bytes 884744 | tf_op jit(solution)/shard_map/ppermute | solution.py:22
  72.7 11.1 %copy-start.4 = (bf16[256,1152]{1,0:T(8,128)(2,1)}, bf16[256,1152]{1,0:T(8,128)(2,1)S(1)}, u32[]{:S(2)}) copy-start(bf16[256,1152]{1,0:T(8,128)(2,1)S(1)} %collective-permute-done.6.w3_hbm.refs_3_) | copy-start | bytes 1769476
  72.8 24.2 %collective-permute-start.7 = (bf16[128,1152]{1,0:T(8,128)(2,1)S(1)}, bf16[128,1152]{1,0:T(8,128)(2,1)S(1)}, u32[]{:S(2)}, u32[]{:S(2)}) collective-permute-start(bf16[128,1152]{1,0:T(8,128)(2,1)S(1)} %slice.9), channel_id=1, source_target_pairs={{0,480},{32,0},{64,32},{96,64},{128,96},{160,128},{192,160},{224,1... | collective-permute-start | bytes 884744 | tf_op jit(solution)/shard_map/ppermute | solution.py:22
  104.1 3.6 %copy-start.9 = (f32[2048]{0:T(1024)S(1)}, f32[2048]{0:T(1024)}, u32[]{:S(2)}) copy-start(f32[2048]{0:T(1024)} %param.7) | copy-start | bytes 24580
  104.1 20.3 %all-to-all-start.1 = ((bf16[4,8,64,384]{3,2,1,0:T(8,128)(2,1)}), bf16[4,8,64,384]{3,2,1,0:T(8,128)(2,1)S(1)}, u32[]{:S(2)}, u32[]{:S(2)}) async-start(bf16[4,8,64,384]{3,2,1,0:T(8,128)(2,1)} %get-tuple-element.26), calls=%async_computation.1 | async-start | bytes 3145728 | tf_op jit(solution)/shard_map/all_to_all | solution.py:26
  117.1 16.8 %collective-permute-start.8 = (bf16[4,8,64,256]{3,2,1,0:T(8,128)(2,1)}, bf16[4,8,64,256]{3,2,1,0:T(8,128)(2,1)}, u32[]{:S(2)}, u32[]{:S(2)}) collective-permute-start(bf16[4,8,64,256]{3,2,1,0:T(8,128)(2,1)} %get-tuple-element.20), channel_id=1, source_target_pairs={{0,1},{1,0},{2,3},{3,2},{4,5},{5,4},{6,7},{7,6},{8,9},{9,8},{10,11... | collective-permute-start | bytes 3145736 | tf_op jit(solution)/shard_map/ppermute | solution.py:22
  126.1 48.3 %all-to-all-start.2 = ((bf16[16,40,384]{2,1,0:T(8,128)(2,1)}), bf16[16,40,384]{2,1,0:T(8,128)(2,1)S(1)}, u32[]{:S(2)}, u32[]{:S(2)}) async-start(bf16[16,40,384]{2,1,0:T(8,128)(2,1)} %ysum.1), calls=%async_computation.2 | async-start | bytes 983040 | tf_op jit(solution)/shard_map/all_to_all | solution.py:26
  133.9 1.2 copy-start
  136.6 0.7 copy-start.1
  137.3 9.9 %collective-permute-start.10 = (bf16[8,64,256]{2,1,0:T(8,128)(2,1)S(1)}, bf16[8,64,256]{2,1,0:T(8,128)(2,1)S(1)}, u32[]{:S(2)}, u32[]{:S(2)}) collective-permute-start(bf16[8,64,256]{2,1,0:T(8,128)(2,1)S(1)} %get-tuple-element.23), channel_id=1, source_target_pairs={{0,4},{2,6},{4,0},{6,2},{1,5},{3,7},{5,1},{7,3},{8,12},{10,14},{12... | collective-permute-start | bytes 786440 | tf_op jit(solution)/shard_map/ppermute | solution.py:22
  141.3 8.5 %collective-permute-start.11 = (bf16[8,64,256]{2,1,0:T(8,128)(2,1)S(1)}, bf16[8,64,256]{2,1,0:T(8,128)(2,1)S(1)}, u32[]{:S(2)}, u32[]{:S(2)}) collective-permute-start(bf16[8,64,256]{2,1,0:T(8,128)(2,1)S(1)} %get-tuple-element.24), channel_id=1, source_target_pairs={{0,6},{2,0},{4,2},{6,4},{1,7},{3,1},{5,3},{7,5},{8,14},{10,8},{12,... | collective-permute-start | bytes 786440 | tf_op jit(solution)/shard_map/ppermute | solution.py:22
  144.7 8.3 %collective-permute-start.9 = (bf16[8,64,256]{2,1,0:T(8,128)(2,1)S(1)}, bf16[8,64,256]{2,1,0:T(8,128)(2,1)S(1)}, u32[]{:S(2)}, u32[]{:S(2)}) collective-permute-start(bf16[8,64,256]{2,1,0:T(8,128)(2,1)S(1)} %get-tuple-element.22), channel_id=1, source_target_pairs={{0,2},{2,4},{4,6},{6,0},{1,3},{3,5},{5,7},{7,1},{8,10},{10,12},{12... | collective-permute-start | bytes 786440 | tf_op jit(solution)/shard_map/ppermute | solution.py:22
  155.8 11.2 %collective-permute-start.12 = (bf16[64,2048]{1,0:T(8,128)(2,1)}, bf16[64,2048]{1,0:T(8,128)(2,1)S(1)}, u32[]{:S(2)}, u32[]{:S(2)}) collective-permute-start(bf16[64,2048]{1,0:T(8,128)(2,1)} %finish.1.p0), channel_id=1, source_target_pairs={{0,6},{2,0},{4,2},{6,4},{1,7},{3,1},{5,3},{7,5},{8,14},{10,8},{12,... | collective-permute-start | bytes 786440 | tf_op jit(solution)/shard_map/ppermute | solution.py:22
  160.1 10.0 %collective-permute-start.13 = (bf16[64,2048]{1,0:T(8,128)(2,1)}, bf16[64,2048]{1,0:T(8,128)(2,1)S(1)}, u32[]{:S(2)}, u32[]{:S(2)}) collective-permute-start(bf16[64,2048]{1,0:T(8,128)(2,1)} %finish.1.p0), channel_id=1, source_target_pairs={{0,4},{2,6},{4,0},{6,2},{1,5},{3,7},{5,1},{7,3},{8,12},{10,14},{12... | collective-permute-start | bytes 786440 | tf_op jit(solution)/shard_map/ppermute | solution.py:22
  162.0 9.3 %collective-permute-start.14 = (bf16[64,2048]{1,0:T(8,128)(2,1)}, bf16[64,2048]{1,0:T(8,128)(2,1)S(1)}, u32[]{:S(2)}, u32[]{:S(2)}) collective-permute-start(bf16[64,2048]{1,0:T(8,128)(2,1)} %finish.1.p0), channel_id=1, source_target_pairs={{0,2},{2,4},{4,6},{6,0},{1,3},{3,5},{5,7},{7,1},{8,10},{10,12},{12... | collective-permute-start | bytes 786440 | tf_op jit(solution)/shard_map/ppermute | solution.py:22
  172.5 22.5 %collective-permute-start.15 = (bf16[4,64,2048]{2,1,0:T(8,128)(2,1)S(1)}, bf16[4,64,2048]{2,1,0:T(8,128)(2,1)S(1)}, u32[]{:S(2)}, u32[]{:S(2)}) collective-permute-start(bf16[4,64,2048]{2,1,0:T(8,128)(2,1)S(1)} %pad_maximum_fusion), channel_id=1, source_target_pairs={{0,1},{1,0},{2,3},{3,2},{4,5},{5,4},{6,7},{7,6},{8,9},{9,8},{10,11... | collective-permute-start | bytes 3145736 | tf_op jit(solution)/shard_map/ppermute | solution.py:22
  175.2 25.2 %all-to-all-start.3 = ((f32[32,8,256]{2,1,0:T(8,128)}), f32[32,8,256]{2,1,0:T(8,128)S(1)}, u32[]{:S(2)}, u32[]{:S(2)}) async-start(f32[32,8,256]{2,1,0:T(8,128)} %get-tuple-element.27), calls=%async_computation.3 | async-start | bytes 524288 | tf_op jit(solution)/shard_map/all_to_all | solution.py:26
  182.6 17.1 %collective-permute-start.16 = (f32[32,384]{1,0:T(8,128)}, f32[32,384]{1,0:T(8,128)S(1)}, u32[]{:S(2)}, u32[]{:S(2)}) collective-permute-start(f32[32,384]{1,0:T(8,128)} %get-tuple-element.28), channel_id=1, source_target_pairs={{0,256},{256,0},{1,257},{257,1},{2,258},{258,2},{3,259},{259,3},{4... | collective-permute-start | bytes 147464 | tf_op jit(solution)/shard_map/ppermute | solution.py:22
  194.9 4.8 %copy-start.10 = (f32[32,384]{1,0:T(8,128)S(1)}, f32[32,384]{1,0:T(8,128)}, u32[]{:S(2)}) copy-start(f32[32,384]{1,0:T(8,128)} %get-tuple-element.28) | copy-start | bytes 147460

commit v7 on v4

--- a/solution.py
+++ b/solution.py
@@ -91,10 +91,6 @@
         c_in[d] = begin(c_hbm.at[d], cv.at[d - 3])
     x_in[4] = begin(x_hbm.at[4], xv.at[4])
     c_in[4] = begin(c_hbm.at[4], cv.at[1])
-    for d in EARLY:
-        w_in[d] = begin(w_hbm[slot[d]], wv.at[slot[d]])
-        x_in[d] = begin(x_hbm.at[d], xv.at[d])
-    ct_in = begin(ct_hbm, ctv)
 
     half = cols // 2
     halves = ((lo_ref, slice(0, half)), (hi_ref, slice(half, cols)))
@@ -104,6 +100,9 @@
         w_in[d].wait()
         x_in[d].wait()
         c_in[d].wait()
+        for e in EARLY if d == 3 else ():
+            w_in[e] = begin(w_hbm[slot[e]], wv.at[slot[e]])
+            x_in[e] = begin(x_hbm.at[e], xv.at[e])
         w = wv.at[slot[d]]
         gu = gu + jnp.dot(xv[d], w[:, : 2 * units], preferred_element_type=F32)
         dh = dh + jnp.dot(cv[d - 3], w[:, 2 * units :], preferred_element_type=F32)
@@ -120,6 +119,7 @@
     d_gate = (dh * up * sig * (1.0 + gate * (1.0 - sig))).astype(BF16)
     d_up = (dh * act).astype(BF16)
     both = jnp.concatenate([d_gate, d_up], axis=1)
+    ct_in = begin(ct_hbm, ctv)
     out_copies = []
     sums = {}
     for d in (4, 3, 5) + EARLY:

time: 209 us -> 209 us (level)
  no operation moved by 1% of the time
where the time goes in v7:
time: 209 us; the launch traced here: 208 us
  starting transfers between devices  101 us (48%)
  waiting for transfers between devices  48.2 us (23%)
  Pallas kernels  39.5 us (19%)
  blocking collectives  12.1 us (6%)
  other arithmetic  3.85 us (2%)
  local copies, waits for them, and re-layouts  2.41 us (1%)
    ppermute x17, starting transfers between devices, shifted(): return lax.ppermute(v, axis, [(i, (i + by) % n) for i in range(n)])  87 us
    ppermute x17, waiting for transfers between devices, shifted(): return lax.ppermute(v, axis, [(i, (i + by) % n) for i in range(n)])  33.3 us
    all_to_all x3, waiting for transfers between devices, exchanged(): return lax.all_to_all(v, axis, 0, 0, tiled=True)  15 us
    all_to_all x3, starting transfers between devices, exchanged(): return lax.all_to_all(v, axis, 0, 0, tiled=True)  13.9 us
    all_to_all x1, blocking collectives, exchanged(): return lax.all_to_all(v, axis, 0, 0, tiled=True)  12.1 us
    pallas_call x1, Pallas kernels, work(): pl.pallas_call(grad_kernel, out_shape=(jax.ShapeDtypeStruct((nx, nz, part...  11 us
    pallas_call x1, Pallas kernels, work(): pl.pallas_call(prepare_tokens, out_shape=jax.ShapeDtypeStruct((nz, tokens...  6.97 us
    pallas_call x1, Pallas kernels, work(): pl.pallas_call(forward_kernel, out_shape=jax.ShapeDtypeStruct((tokens, 3...  6.29 us
  transfers between devices with their start and end apart: 20, of which 9 were waited for; matrix products, arithmetic and copies ran while one was open for 2% of the time, Pallas kernels for 14%

profile of v7, /device:TPU:1, one launch (start us, length us, event | category | flops | bytes accessed | tf_op | source)
XLA Modules:
  0.0 207.9 jit_solution(3000043101005842293)
XLA Ops:
  0.6 0.9 pad_maximum_fusion.1
  1.5 12.1 %all_to_all.20 = bf16[4,64,1152]{2,1,0:T(8,128)(2,1)S(1)} all-to-all(bf16[4,64,1152]{2,1,0:T(8,128)(2,1)S(1)} %broadcast_in_dim.4), channel_id=1, replica_groups=mesh['rep'=2,'fs_0'=8,'fs_1'=4,'x'=4,'c'=2] {'fs_1'}, dimensions={0} | all-to-all | bytes 1179648 | tf_op jit(solution)/shard_map/all_to_all | solution.py:25
  13.6 12.9 %collective-permute-start.4 = (bf16[256,1152]{1,0:T(8,128)(2,1)S(1)}, bf16[256,1152]{1,0:T(8,128)(2,1)S(1)}, u32[]{:S(2)}, u32[]{:S(2)}) collective-permute-start(bf16[256,1152]{1,0:T(8,128)(2,1)S(1)} %bitcast.18), channel_id=1, source_target_pairs={{0,480},{32,0},{64,32},{96,64},{128,96},{160,128},{192,160},{224,1... | collective-permute-start | bytes 1769480 | tf_op jit(solution)/shard_map/ppermute | solution.py:21
  26.5 1.9 collective-permute-start
  28.4 8.6 %collective-permute-done.4.refs_1_ = bf16[256,1152]{1,0:T(8,128)(2,1)S(1)} collective-permute-done((bf16[256,1152]{1,0:T(8,128)(2,1)S(1)}, bf16[256,1152]{1,0:T(8,128)(2,1)S(1)}, u32[]{:S(2)}, u32[]{:S(2)}) %collective-permute-start.4) | collective-permute-done | bytes 589856 | tf_op jit(solution)/shard_map/ppermute | solution.py:21
  37.1 5.3 %collective-permute-start.5 = (bf16[256,1152]{1,0:T(8,128)(2,1)S(1)}, bf16[256,1152]{1,0:T(8,128)(2,1)S(1)}, u32[]{:S(2)}, u32[]{:S(2)}) collective-permute-start(bf16[256,1152]{1,0:T(8,128)(2,1)S(1)} %collective-permute-done.4.refs_1_), channel_id=1, source_target_pairs={{0,480},{32,0},{64,32},{96,64},{128,96},{160,128},{192,160},{224,1... | collective-permute-start | bytes 1769480 | tf_op jit(solution)/shard_map/ppermute | solution.py:21
  42.4 0.0 collective-permute-done.refs_2_.refs_6_
  42.4 0.0 copy-start.2
  42.4 1.9 collective-permute-start.1
  44.3 7.8 %collective-permute-done.5.refs_3_.refs_2_ = bf16[256,1152]{1,0:T(8,128)(2,1)S(1)} collective-permute-done((bf16[256,1152]{1,0:T(8,128)(2,1)S(1)}, bf16[256,1152]{1,0:T(8,128)(2,1)S(1)}, u32[]{:S(2)}, u32[]{:S(2)}) %collective-permute-start.5) | collective-permute-done | bytes 589856 | tf_op jit(solution)/shard_map/ppermute | solution.py:21
  52.1 5.3 %collective-permute-start.6 = (bf16[256,1152]{1,0:T(8,128)(2,1)S(1)}, bf16[256,1152]{1,0:T(8,128)(2,1)S(1)}, u32[]{:S(2)}, u32[]{:S(2)}) collective-permute-start(bf16[256,1152]{1,0:T(8,128)(2,1)S(1)} %collective-permute-done.5.refs_3_.refs_2_), channel_id=1, source_target_pairs={{0,480},{32,0},{64,32},{96,64},{128,96},{160,128},{192,160},{224,1... | collective-permute-start | bytes 1769480 | tf_op jit(solution)/shard_map/ppermute | solution.py:21
  57.4 0.0 collective-permute-done.1.refs_4_.refs_5_
  57.4 0.0 copy-start.4
  57.4 1.9 collective-permute-start.2
  59.4 6.9 %collective-permute-done.6.refs_3_ = bf16[256,1152]{1,0:T(8,128)(2,1)S(1)} collective-permute-done((bf16[256,1152]{1,0:T(8,128)(2,1)S(1)}, bf16[256,1152]{1,0:T(8,128)(2,1)S(1)}, u32[]{:S(2)}, u32[]{:S(2)}) %collective-permute-start.6) | collective-permute-done | bytes 589856 | tf_op jit(solution)/shard_map/ppermute | solution.py:21
  66.3 0.8 slice.9
  67.1 5.3 %collective-permute-start.7 = (bf16[128,1152]{1,0:T(8,128)(2,1)}, bf16[128,1152]{1,0:T(8,128)(2,1)S(1)}, u32[]{:S(2)}, u32[]{:S(2)}) collective-permute-start(bf16[128,1152]{1,0:T(8,128)(2,1)} %slice.9), channel_id=1, source_target_pairs={{0,480},{32,0},{64,32},{96,64},{128,96},{160,128},{192,160},{224,1... | collective-permute-start | bytes 884744 | tf_op jit(solution)/shard_map/ppermute | solution.py:21
  72.4 0.0 collective-permute-done.2.refs_4_
  72.4 0.8 slice.8
  73.2 0.1 copy-done.6
  73.3 1.9 collective-permute-start.3
  75.3 0.6 pad_add_fusion.at_ref
  75.8 5.2 %prepare_c.1 = (bf16[8,512,256]{2,1,0:T(8,128)(2,1)}, bf16[8,256,512]{2,1,0:T(8,128)(2,1)}) custom-call(s32[3]{0:T(128)} %pad_add_fusion.at_ref, bf16[512,2048]{1,0:T(8,128)(2,1)} %c_ref.1, bf16[512,2048]{1,0:T(8,128)(2,1)} %c_ref.1), custom_call_target="tpu_custom_call" | custom-call | tf_op jit(solution)/shard_map/prepare_c/pallas_call | solution.py:272
  81.1 0.0 copy-done
  81.1 0.0 copy-start.7
  81.1 7.0 %prepare_x.1.x_ref.x_hbm = bf16[8,512,256]{2,1,0:T(8,128)(2,1)} custom-call(s32[3]{0:T(128)} %pad_add_fusion.at_ref, bf16[512,2048]{1,0:T(8,128)(2,1)} %x_ref.3, f32[1,2048]{1,0:T(1,128)} %bitcast.24), custom_call_target="tpu_custom_call" | custom-call | tf_op jit(solution)/shard_map/prepare_x/pallas_call | solution.py:258
  88.1 0.6 fusion.3.gain_ref
  88.7 6.3 %forward.1.acc_hbm = f32[512,1152]{1,0:T(8,128)} custom-call(bf16[8,512,256]{2,1,0:T(8,128)(2,1)} %prepare_x.1.x_ref.x_hbm, bf16[8,512,256]{2,1,0:T(8,128)(2,1)} %get-tuple-element.14.c_ref.c_hbm, bf16[256,1152]{1,0:T(8,128)(2,1)} %bitcast.20, bf16[256,1152]{1,0:T(8,128)(2,1)} %copy-done.1, bf16[256,1152]{1,0:T(8,128)(2,1)} %copy-done.2, ...), custom_call_target="tpu_custom_call" | custom-call | tf_op jit(solution)/shard_map/forward/pallas_call | solution.py:294
  95.0 0.0 collective-permute-done.7.hi_ref
  95.0 0.0 collective-permute-done.3.lo_ref
  95.0 11.0 %grad.1 = (bf16[4,8,64,256]{3,2,1,0:T(8,128)(2,1)}, bf16[4,8,64,256]{3,2,1,0:T(8,128)(2,1)}, bf16[4,8,72,384]{3,2,1,0:T(8,128)(2,1)}) custom-call(f32[8,1,256]{2,1,0:T(1,128)} %fusion.3.gain_ref, bf16[128,1152]{1,0:T(8,128)(2,1)S(1)} %collective-permute-done.3.lo_ref, bf16[128,1152]{1,0:T(8,128)(2,1)S(1)} %collective-permute-done.7.hi_ref, ...), custom_call_target="tpu_custom_call" | custom-call | tf_op jit(solution)/shard_map/grad/pallas_call | solution.py:302
  106.0 3.6 %all-to-all-start.1 = ((bf16[4,8,72,384]{3,2,1,0:T(8,128)(2,1)}), bf16[4,8,72,384]{3,2,1,0:T(8,128)(2,1)S(1)}, u32[]{:S(2)}, u32[]{:S(2)}) async-start(bf16[4,8,72,384]{3,2,1,0:T(8,128)(2,1)} %get-tuple-element.22), calls=%async_computation.1 | async-start | bytes 3538944 | tf_op jit(solution)/shard_map/all_to_all | solution.py:25
  109.6 6.9 %collective-permute-start.8 = (bf16[4,8,64,256]{3,2,1,0:T(8,128)(2,1)}, bf16[4,8,64,256]{3,2,1,0:T(8,128)(2,1)S(1)}, u32[]{:S(2)}, u32[]{:S(2)}) collective-permute-start(bf16[4,8,64,256]{3,2,1,0:T(8,128)(2,1)} %get-tuple-element.17), channel_id=1, source_target_pairs={{0,1},{1,0},{2,3},{3,2},{4,5},{5,4},{6,7},{7,6},{8,9},{9,8},{10,11... | collective-permute-start | bytes 3145736 | tf_op jit(solution)/shard_map/ppermute | solution.py:21
  116.5 10.8 %all-to-all-done.1.got_ref = bf16[4,8,72,384]{3,2,1,0:T(8,128)(2,1)S(1)} async-done(((bf16[4,8,72,384]{3,2,1,0:T(8,128)(2,1)}), bf16[4,8,72,384]{3,2,1,0:T(8,128)(2,1)S(1)}, u32[]{:S(2)}, u32[]{:S(2)}) %all-to-all-start.1) | async-done | bytes 1769504 | tf_op jit(solution)/shard_map/all_to_all | solution.py:25
  127.3 1.7 ysum.1
  129.0 6.8 %all-to-all-start.2 = ((bf16[16,40,384]{2,1,0:T(8,128)(2,1)}), bf16[16,40,384]{2,1,0:T(8,128)(2,1)S(1)}, u32[]{:S(2)}, u32[]{:S(2)}) async-start(bf16[16,40,384]{2,1,0:T(8,128)(2,1)} %ysum.1), calls=%async_computation.2 | async-start | bytes 983040 | tf_op jit(solution)/shard_map/all_to_all | solution.py:25
  135.7 0.0 collective-permute-done.8.theirs_ref
  135.7 2.3 %chip.1 = (bf16[8,64,256]{2,1,0:T(8,128)(2,1)}, bf16[8,64,256]{2,1,0:T(8,128)(2,1)}, bf16[8,64,256]{2,1,0:T(8,128)(2,1)}, bf16[8,64,256]{2,1,0:T(8,128)(2,1)}) custom-call(bf16[4,8,64,256]{3,2,1,0:T(8,128)(2,1)} %get-tuple-element.16.mine_ref, bf16[4,8,64,256]{3,2,1,0:T(8,128)(2,1)S(1)} %collective-permute-done.8.theirs_ref), custom_call_target="tpu_custom_call" | custom-call | tf_op jit(solution)/shard_map/chip/pallas_call | solution.py:327
  138.0 3.1 %collective-permute-start.9 = (bf16[8,64,256]{2,1,0:T(8,128)(2,1)}, bf16[8,64,256]{2,1,0:T(8,128)(2,1)S(1)}, u32[]{:S(2)}, u32[]{:S(2)}) collective-permute-start(bf16[8,64,256]{2,1,0:T(8,128)(2,1)} %get-tuple-element.19), channel_id=1, source_target_pairs={{0,2},{2,4},{4,6},{6,0},{1,3},{3,5},{5,7},{7,1},{8,10},{10,12},{12... | collective-permute-start | bytes 786440 | tf_op jit(solution)/shard_map/ppermute | solution.py:21
  141.1 4.4 %collective-permute-start.10 = (bf16[8,64,256]{2,1,0:T(8,128)(2,1)}, bf16[8,64,256]{2,1,0:T(8,128)(2,1)S(1)}, u32[]{:S(2)}, u32[]{:S(2)}) collective-permute-start(bf16[8,64,256]{2,1,0:T(8,128)(2,1)} %get-tuple-element.20), channel_id=1, source_target_pairs={{0,4},{2,6},{4,0},{6,2},{1,5},{3,7},{5,1},{7,3},{8,12},{10,14},{12... | collective-permute-start | bytes 786440 | tf_op jit(solution)/shard_map/ppermute | solution.py:21
  145.5 3.1 %collective-permute-start.11 = (bf16[8,64,256]{2,1,0:T(8,128)(2,1)}, bf16[8,64,256]{2,1,0:T(8,128)(2,1)S(1)}, u32[]{:S(2)}, u32[]{:S(2)}) collective-permute-start(bf16[8,64,256]{2,1,0:T(8,128)(2,1)} %get-tuple-element.21), channel_id=1, source_target_pairs={{0,6},{2,0},{4,2},{6,4},{1,7},{3,1},{5,3},{7,5},{8,14},{10,8},{12,... | collective-permute-start | bytes 786440 | tf_op jit(solution)/shard_map/ppermute | solution.py:21
  148.6 0.0 collective-permute-done.9.got1
  148.6 2.0 collective-permute-done.10.got2
  150.6 2.5 %collective-permute-done.11.got3 = bf16[8,64,256]{2,1,0:T(8,128)(2,1)S(1)} collective-permute-done((bf16[8,64,256]{2,1,0:T(8,128)(2,1)}, bf16[8,64,256]{2,1,0:T(8,128)(2,1)S(1)}, u32[]{:S(2)}, u32[]{:S(2)}) %collective-permute-start.11) | collective-permute-done | bytes 262176 | tf_op jit(solution)/shard_map/ppermute | solution.py:21
  153.1 2.9 %finish.1.p0 = bf16[64,2048]{1,0:T(8,128)(2,1)} custom-call(s32[3]{0:T(128)} %pad_add_fusion.at_ref, bf16[8,64,256]{2,1,0:T(8,128)(2,1)} %get-tuple-element.18.got0, bf16[8,64,256]{2,1,0:T(8,128)(2,1)S(1)} %collective-permute-done.9.got1, bf16[8,64,256]{2,1,0:T(8,128)(2,1)S(1)} %collective-permute-done.10.got2, ...), custom_call_target="tpu_custom_call" | custom-call | tf_op jit(solution)/shard_map/finish/pallas_call | solution.py:338
  156.0 3.1 %collective-permute-start.14 = (bf16[64,2048]{1,0:T(8,128)(2,1)}, bf16[64,2048]{1,0:T(8,128)(2,1)S(1)}, u32[]{:S(2)}, u32[]{:S(2)}) collective-permute-start(bf16[64,2048]{1,0:T(8,128)(2,1)} %finish.1.p0), channel_id=1, source_target_pairs={{0,2},{2,4},{4,6},{6,0},{1,3},{3,5},{5,7},{7,1},{8,10},{10,12},{12... | collective-permute-start | bytes 786440 | tf_op jit(solution)/shard_map/ppermute | solution.py:21
  159.1 4.3 %collective-permute-start.13 = (bf16[64,2048]{1,0:T(8,128)(2,1)}, bf16[64,2048]{1,0:T(8,128)(2,1)S(1)}, u32[]{:S(2)}, u32[]{:S(2)}) collective-permute-start(bf16[64,2048]{1,0:T(8,128)(2,1)} %finish.1.p0), channel_id=1, source_target_pairs={{0,4},{2,6},{4,0},{6,2},{1,5},{3,7},{5,1},{7,3},{8,12},{10,14},{12... | collective-permute-start | bytes 786440 | tf_op jit(solution)/shard_map/ppermute | solution.py:21
  163.4 2.2 %collective-permute-start.12 = (bf16[64,2048]{1,0:T(8,128)(2,1)}, bf16[64,2048]{1,0:T(8,128)(2,1)S(1)}, u32[]{:S(2)}, u32[]{:S(2)}) collective-permute-start(bf16[64,2048]{1,0:T(8,128)(2,1)} %finish.1.p0), channel_id=1, source_target_pairs={{0,6},{2,0},{4,2},{6,4},{1,7},{3,1},{5,3},{7,5},{8,14},{10,8},{12,... | collective-permute-start | bytes 786440 | tf_op jit(solution)/shard_map/ppermute | solution.py:21
  165.6 0.0 collective-permute-done.14.p3
  165.6 2.6 %collective-permute-done.13.p2 = bf16[64,2048]{1,0:T(8,128)(2,1)S(1)} collective-permute-done((bf16[64,2048]{1,0:T(8,128)(2,1)}, bf16[64,2048]{1,0:T(8,128)(2,1)S(1)}, u32[]{:S(2)}, u32[]{:S(2)}) %collective-permute-start.13) | collective-permute-done | bytes 262176 | tf_op jit(solution)/shard_map/ppermute | solution.py:21
  168.2 2.8 %collective-permute-done.12.p1 = bf16[64,2048]{1,0:T(8,128)(2,1)S(1)} collective-permute-done((bf16[64,2048]{1,0:T(8,128)(2,1)}, bf16[64,2048]{1,0:T(8,128)(2,1)S(1)}, u32[]{:S(2)}, u32[]{:S(2)}) %collective-permute-start.12) | collective-permute-done | bytes 262176 | tf_op jit(solution)/shard_map/ppermute | solution.py:21
  171.0 1.1 pad_maximum_fusion
  172.1 11.4 %collective-permute-start.15 = (bf16[4,64,2048]{2,1,0:T(8,128)(2,1)S(1)}, bf16[4,64,2048]{2,1,0:T(8,128)(2,1)S(1)}, u32[]{:S(2)}, u32[]{:S(2)}) collective-permute-start(bf16[4,64,2048]{2,1,0:T(8,128)(2,1)S(1)} %pad_maximum_fusion), channel_id=1, source_target_pairs={{0,1},{1,0},{2,3},{3,2},{4,5},{5,4},{6,7},{7,6},{8,9},{9,8},{10,11... | collective-permute-start | bytes 3145736 | tf_op jit(solution)/shard_map/ppermute | solution.py:21
  183.5 0.0 all-to-all-done.2.got_ref
  183.5 0.7 zsum.1
  184.2 12.3 %collective-permute-start.16 = (f32[32,384]{1,0:T(8,128)}, f32[32,384]{1,0:T(8,128)S(1)}, u32[]{:S(2)}, u32[]{:S(2)}) collective-permute-start(f32[32,384]{1,0:T(8,128)} %get-tuple-element.24), channel_id=1, source_target_pairs={{0,256},{256,0},{1,257},{257,1},{2,258},{258,2},{3,259},{259,3},{4... | collective-permute-start | bytes 147464 | tf_op jit(solution)/shard_map/ppermute | solution.py:21
  196.5 0.0 copy-start.8
  196.5 0.0 collective-permute-done.15.other_ref
  196.5 2.4 %place.1 = bf16[512,2048]{1,0:T(8,128)(2,1)} custom-call(s32[3]{0:T(128)} %pad_add_fusion.at_ref, bf16[64,2048]{1,0:T(8,128)(2,1)} %finish.1.p0, bf16[64,2048]{1,0:T(8,128)(2,1)S(1)} %collective-permute-done.12.p1, bf16[64,2048]{1,0:T(8,128)(2,1)S(1)} %collective-permute-done.13.p2, bf16[64,2048]{1,0:T(8,128)(2,1)S(1)} %collective-permute-done.14.p3, ...), custom_call_target="tpu_custom_call" | custom-call | tf_op jit(solution)/shard_map/place/pallas_call | solution.py:354
  198.9 3.5 %all-to-all-start.3 = ((f32[8,8,256]{2,1,0:T(8,128)}), f32[8,8,256]{2,1,0:T(8,128)S(1)}, u32[]{:S(2)}, u32[]{:S(2)}) async-start(f32[8,8,256]{2,1,0:T(8,128)} %get-tuple-element.23), calls=%async_computation.3 | async-start | bytes 131072 | tf_op jit(solution)/shard_map/all_to_all | solution.py:25
  202.5 0.0 collective-permute-done.16
  202.5 0.7 fusion.2
  203.1 4.2 %all-to-all-done.3 = f32[8,8,256]{2,1,0:T(8,128)S(1)} async-done(((f32[8,8,256]{2,1,0:T(8,128)}), f32[8,8,256]{2,1,0:T(8,128)S(1)}, u32[]{:S(2)}, u32[]{:S(2)}) %all-to-all-start.3) | async-done | bytes 65568 | tf_op jit(solution)/shard_map/all_to_all | solution.py:25
  207.3 0.6 copy.9
  (14 shorter events, 0.1 us)
Async XLA Ops:
  13.6 67.5 %copy-start = (bf16[4,64,1152]{2,1,0:T(8,128)(2,1)}, bf16[4,64,1152]{2,1,0:T(8,128)(2,1)S(1)}, u32[]{:S(2)}) copy-start(bf16[4,64,1152]{2,1,0:T(8,128)(2,1)S(1)} %all_to_all.20) | copy-start | bytes 1769476
  13.6 23.4 %collective-permute-start.4 = (bf16[256,1152]{1,0:T(8,128)(2,1)S(1)}, bf16[256,1152]{1,0:T(8,128)(2,1)S(1)}, u32[]{:S(2)}, u32[]{:S(2)}) collective-permute-start(bf16[256,1152]{1,0:T(8,128)(2,1)S(1)} %bitcast.18), channel_id=1, source_target_pairs={{0,480},{32,0},{64,32},{96,64},{128,96},{160,128},{192,160},{224,1... | collective-permute-start | bytes 1769480 | tf_op jit(solution)/shard_map/ppermute | solution.py:21
  26.5 15.9 %collective-permute-start = (bf16[256,1152]{1,0:T(8,128)(2,1)S(1)}, bf16[256,1152]{1,0:T(8,128)(2,1)S(1)}, u32[]{:S(2)}, u32[]{:S(2)}) collective-permute-start(bf16[256,1152]{1,0:T(8,128)(2,1)S(1)} %bitcast.19), channel_id=1, source_target_pairs={{0,32},{32,64},{64,96},{96,128},{128,160},{160,192},{192,224},{224... | collective-permute-start | bytes 1769480 | tf_op jit(solution)/shard_map/ppermute | solution.py:21
  37.1 44.0 %copy-start.1 = (bf16[256,1152]{1,0:T(8,128)(2,1)}, bf16[256,1152]{1,0:T(8,128)(2,1)S(1)}, u32[]{:S(2)}) copy-start(bf16[256,1152]{1,0:T(8,128)(2,1)S(1)} %collective-permute-done.4.refs_1_) | copy-start | bytes 1769476
  37.1 15.0 %collective-permute-start.5 = (bf16[256,1152]{1,0:T(8,128)(2,1)S(1)}, bf16[256,1152]{1,0:T(8,128)(2,1)S(1)}, u32[]{:S(2)}, u32[]{:S(2)}) collective-permute-start(bf16[256,1152]{1,0:T(8,128)(2,1)S(1)} %collective-permute-done.4.refs_1_), channel_id=1, source_target_pairs={{0,480},{32,0},{64,32},{96,64},{128,96},{160,128},{192,160},{224,1... | collective-permute-start | bytes 1769480 | tf_op jit(solution)/shard_map/ppermute | solution.py:21
  42.4 38.7 %copy-start.2 = (bf16[256,1152]{1,0:T(8,128)(2,1)}, bf16[256,1152]{1,0:T(8,128)(2,1)S(1)}, u32[]{:S(2)}) copy-start(bf16[256,1152]{1,0:T(8,128)(2,1)S(1)} %collective-permute-done.refs_2_.refs_6_) | copy-start | bytes 1769476
  42.4 15.0 %collective-permute-start.1 = (bf16[256,1152]{1,0:T(8,128)(2,1)S(1)}, bf16[256,1152]{1,0:T(8,128)(2,1)S(1)}, u32[]{:S(2)}, u32[]{:S(2)}) collective-permute-start(bf16[256,1152]{1,0:T(8,128)(2,1)S(1)} %collective-permute-done.refs_2_.refs_6_), channel_id=1, source_target_pairs={{0,32},{32,64},{64,96},{96,128},{128,160},{160,192},{192,224},{224... | collective-permute-start | bytes 1769480 | tf_op jit(solution)/shard_map/ppermute | solution.py:21
  52.1 29.0 %copy-start.3 = (bf16[256,1152]{1,0:T(8,128)(2,1)}, bf16[256,1152]{1,0:T(8,128)(2,1)S(1)}, u32[]{:S(2)}) copy-start(bf16[256,1152]{1,0:T(8,128)(2,1)S(1)} %collective-permute-done.5.refs_3_.refs_2_) | copy-start | bytes 1769476
  52.1 14.2 %collective-permute-start.6 = (bf16[256,1152]{1,0:T(8,128)(2,1)S(1)}, bf16[256,1152]{1,0:T(8,128)(2,1)S(1)}, u32[]{:S(2)}, u32[]{:S(2)}) collective-permute-start(bf16[256,1152]{1,0:T(8,128)(2,1)S(1)} %collective-permute-done.5.refs_3_.refs_2_), channel_id=1, source_target_pairs={{0,480},{32,0},{64,32},{96,64},{128,96},{160,128},{192,160},{224,1... | collective-permute-start | bytes 1769480 | tf_op jit(solution)/shard_map/ppermute | solution.py:21
  57.4 15.0 %copy-start.4 = (bf16[256,1152]{1,0:T(8,128)(2,1)}, bf16[256,1152]{1,0:T(8,128)(2,1)S(1)}, u32[]{:S(2)}) copy-start(bf16[256,1152]{1,0:T(8,128)(2,1)S(1)} %collective-permute-done.1.refs_4_.refs_5_) | copy-start | bytes 1769476
  57.4 15.0 %collective-permute-start.2 = (bf16[256,1152]{1,0:T(8,128)(2,1)S(1)}, bf16[256,1152]{1,0:T(8,128)(2,1)S(1)}, u32[]{:S(2)}, u32[]{:S(2)}) collective-permute-start(bf16[256,1152]{1,0:T(8,128)(2,1)S(1)} %collective-permute-done.1.refs_4_.refs_5_), channel_id=1, source_target_pairs={{0,32},{32,64},{64,96},{96,128},{128,160},{160,192},{192,224},{224... | collective-permute-start | bytes 1769480 | tf_op jit(solution)/shard_map/ppermute | solution.py:21
  66.3 14.9 %copy-start.5 = (bf16[256,1152]{1,0:T(8,128)(2,1)}, bf16[256,1152]{1,0:T(8,128)(2,1)S(1)}, u32[]{:S(2)}) copy-start(bf16[256,1152]{1,0:T(8,128)(2,1)S(1)} %collective-permute-done.6.refs_3_) | copy-start | bytes 1769476
  67.1 28.0 %collective-permute-start.7 = (bf16[128,1152]{1,0:T(8,128)(2,1)}, bf16[128,1152]{1,0:T(8,128)(2,1)S(1)}, u32[]{:S(2)}, u32[]{:S(2)}) collective-permute-start(bf16[128,1152]{1,0:T(8,128)(2,1)} %slice.9), channel_id=1, source_target_pairs={{0,480},{32,0},{64,32},{96,64},{128,96},{160,128},{192,160},{224,1... | collective-permute-start | bytes 884744 | tf_op jit(solution)/shard_map/ppermute | solution.py:21
  72.4 0.9 copy-start.6
  73.3 21.7 %collective-permute-start.3 = (bf16[128,1152]{1,0:T(8,128)(2,1)}, bf16[128,1152]{1,0:T(8,128)(2,1)S(1)}, u32[]{:S(2)}, u32[]{:S(2)}) collective-permute-start(bf16[128,1152]{1,0:T(8,128)(2,1)} %slice.8), channel_id=1, source_target_pairs={{0,32},{32,64},{64,96},{96,128},{128,160},{160,192},{192,224},{224... | collective-permute-start | bytes 884744 | tf_op jit(solution)/shard_map/ppermute | solution.py:21
  81.1 7.0 %copy-start.7 = (f32[2048]{0:T(1024)S(1)}, f32[2048]{0:T(1024)}, u32[]{:S(2)}) copy-start(f32[2048]{0:T(1024)} %param.7) | copy-start | bytes 24580
  106.0 21.2 %all-to-all-start.1 = ((bf16[4,8,72,384]{3,2,1,0:T(8,128)(2,1)}), bf16[4,8,72,384]{3,2,1,0:T(8,128)(2,1)S(1)}, u32[]{:S(2)}, u32[]{:S(2)}) async-start(bf16[4,8,72,384]{3,2,1,0:T(8,128)(2,1)} %get-tuple-element.22), calls=%async_computation.1 | async-start | bytes 3538944 | tf_op jit(solution)/shard_map/all_to_all | solution.py:25
  109.6 26.1 %collective-permute-start.8 = (bf16[4,8,64,256]{3,2,1,0:T(8,128)(2,1)}, bf16[4,8,64,256]{3,2,1,0:T(8,128)(2,1)S(1)}, u32[]{:S(2)}, u32[]{:S(2)}) collective-permute-start(bf16[4,8,64,256]{3,2,1,0:T(8,128)(2,1)} %get-tuple-element.17), channel_id=1, source_target_pairs={{0,1},{1,0},{2,3},{3,2},{4,5},{5,4},{6,7},{7,6},{8,9},{9,8},{10,11... | collective-permute-start | bytes 3145736 | tf_op jit(solution)/shard_map/ppermute | solution.py:21
  129.0 54.5 %all-to-all-start.2 = ((bf16[16,40,384]{2,1,0:T(8,128)(2,1)}), bf16[16,40,384]{2,1,0:T(8,128)(2,1)S(1)}, u32[]{:S(2)}, u32[]{:S(2)}) async-start(bf16[16,40,384]{2,1,0:T(8,128)(2,1)} %ysum.1), calls=%async_computation.2 | async-start | bytes 983040 | tf_op jit(solution)/shard_map/all_to_all | solution.py:25
  138.0 10.5 %collective-permute-start.9 = (bf16[8,64,256]{2,1,0:T(8,128)(2,1)}, bf16[8,64,256]{2,1,0:T(8,128)(2,1)S(1)}, u32[]{:S(2)}, u32[]{:S(2)}) collective-permute-start(bf16[8,64,256]{2,1,0:T(8,128)(2,1)} %get-tuple-element.19), channel_id=1, source_target_pairs={{0,2},{2,4},{4,6},{6,0},{1,3},{3,5},{5,7},{7,1},{8,10},{10,12},{12... | collective-permute-start | bytes 786440 | tf_op jit(solution)/shard_map/ppermute | solution.py:21
  141.1 9.5 %collective-permute-start.10 = (bf16[8,64,256]{2,1,0:T(8,128)(2,1)}, bf16[8,64,256]{2,1,0:T(8,128)(2,1)S(1)}, u32[]{:S(2)}, u32[]{:S(2)}) collective-permute-start(bf16[8,64,256]{2,1,0:T(8,128)(2,1)} %get-tuple-element.20), channel_id=1, source_target_pairs={{0,4},{2,6},{4,0},{6,2},{1,5},{3,7},{5,1},{7,3},{8,12},{10,14},{12... | collective-permute-start | bytes 786440 | tf_op jit(solution)/shard_map/ppermute | solution.py:21
  145.5 7.6 %collective-permute-start.11 = (bf16[8,64,256]{2,1,0:T(8,128)(2,1)}, bf16[8,64,256]{2,1,0:T(8,128)(2,1)S(1)}, u32[]{:S(2)}, u32[]{:S(2)}) collective-permute-start(bf16[8,64,256]{2,1,0:T(8,128)(2,1)} %get-tuple-element.21), channel_id=1, source_target_pairs={{0,6},{2,0},{4,2},{6,4},{1,7},{3,1},{5,3},{7,5},{8,14},{10,8},{12,... | collective-permute-start | bytes 786440 | tf_op jit(solution)/shard_map/ppermute | solution.py:21
  156.0 9.6 %collective-permute-start.14 = (bf16[64,2048]{1,0:T(8,128)(2,1)}, bf16[64,2048]{1,0:T(8,128)(2,1)S(1)}, u32[]{:S(2)}, u32[]{:S(2)}) collective-permute-start(bf16[64,2048]{1,0:T(8,128)(2,1)} %finish.1.p0), channel_id=1, source_target_pairs={{0,2},{2,4},{4,6},{6,0},{1,3},{3,5},{5,7},{7,1},{8,10},{10,12},{12... | collective-permute-start | bytes 786440 | tf_op jit(solution)/shard_map/ppermute | solution.py:21
  159.1 9.1 %collective-permute-start.13 = (bf16[64,2048]{1,0:T(8,128)(2,1)}, bf16[64,2048]{1,0:T(8,128)(2,1)S(1)}, u32[]{:S(2)}, u32[]{:S(2)}) collective-permute-start(bf16[64,2048]{1,0:T(8,128)(2,1)} %finish.1.p0), channel_id=1, source_target_pairs={{0,4},{2,6},{4,0},{6,2},{1,5},{3,7},{5,1},{7,3},{8,12},{10,14},{12... | collective-permute-start | bytes 786440 | tf_op jit(solution)/shard_map/ppermute | solution.py:21
  163.4 7.6 %collective-permute-start.12 = (bf16[64,2048]{1,0:T(8,128)(2,1)}, bf16[64,2048]{1,0:T(8,128)(2,1)S(1)}, u32[]{:S(2)}, u32[]{:S(2)}) collective-permute-start(bf16[64,2048]{1,0:T(8,128)(2,1)} %finish.1.p0), channel_id=1, source_target_pairs={{0,6},{2,0},{4,2},{6,4},{1,7},{3,1},{5,3},{7,5},{8,14},{10,8},{12,... | collective-permute-start | bytes 786440 | tf_op jit(solution)/shard_map/ppermute | solution.py:21
  172.1 24.4 %collective-permute-start.15 = (bf16[4,64,2048]{2,1,0:T(8,128)(2,1)S(1)}, bf16[4,64,2048]{2,1,0:T(8,128)(2,1)S(1)}, u32[]{:S(2)}, u32[]{:S(2)}) collective-permute-start(bf16[4,64,2048]{2,1,0:T(8,128)(2,1)S(1)} %pad_maximum_fusion), channel_id=1, source_target_pairs={{0,1},{1,0},{2,3},{3,2},{4,5},{5,4},{6,7},{7,6},{8,9},{9,8},{10,11... | collective-permute-start | bytes 3145736 | tf_op jit(solution)/shard_map/ppermute | solution.py:21
  184.2 18.3 %collective-permute-start.16 = (f32[32,384]{1,0:T(8,128)}, f32[32,384]{1,0:T(8,128)S(1)}, u32[]{:S(2)}, u32[]{:S(2)}) collective-permute-start(f32[32,384]{1,0:T(8,128)} %get-tuple-element.24), channel_id=1, source_target_pairs={{0,256},{256,0},{1,257},{257,1},{2,258},{258,2},{3,259},{259,3},{4... | collective-permute-start | bytes 147464 | tf_op jit(solution)/shard_map/ppermute | solution.py:21
  196.5 6.0 %copy-start.8 = (f32[32,384]{1,0:T(8,128)S(1)}, f32[32,384]{1,0:T(8,128)}, u32[]{:S(2)}) copy-start(f32[32,384]{1,0:T(8,128)} %get-tuple-element.24) | copy-start | bytes 147460
  198.9 8.4 %all-to-all-start.3 = ((f32[8,8,256]{2,1,0:T(8,128)}), f32[8,8,256]{2,1,0:T(8,128)S(1)}, u32[]{:S(2)}, u32[]{:S(2)}) async-start(f32[8,8,256]{2,1,0:T(8,128)} %get-tuple-element.23), calls=%async_computation.3 | async-start | bytes 131072 | tf_op jit(solution)/shard_map/all_to_all | solution.py:25

commit v8 on v7

--- a/solution.py
+++ b/solution.py
@@ -11,6 +11,8 @@
 TP = ("x", "c")
 RING = ("rep", "fs_0")
 EPS = 1e-06
+LANES = 128
+TILES = 3
 EARLY = (0, 1, 7, 2, 6)
 F32 = jnp.float32
 BF16 = jnp.bfloat16
@@ -73,7 +75,8 @@
     nz, _, cols = xv.shape
     ny, _, longer, _ = dv.shape
     nx, part = mine_hbm.shape[0], mine_hbm.shape[2]
-    rows = longer - 8
+    tiles = units // LANES
+    rows = (longer - 8) // tiles
     used = [0]
 
     def begin(src, dst):
@@ -148,11 +151,14 @@
         left = sums[d] - high.astype(F32)
         mid = left.astype(BF16)
         low = (left - mid.astype(F32)).astype(BF16)
-        extra = jnp.concatenate([high, mid, low, jnp.zeros((5, cols), BF16)], axis=0)
-        extra = jnp.concatenate([extra, jnp.zeros((8, units - cols), BF16)], axis=1)
+        ends = [v[:, at : at + LANES] for at in (0, LANES) for v in (high, mid, low)]
+        extra = jnp.concatenate(ends + [jnp.zeros((2, LANES), BF16)], axis=0)
         for y in range(ny):
-            dv[y, d, :rows] = res[y * rows : (y + 1) * rows]
-            dv[y, d, rows:] = extra
+            for j in range(tiles):
+                dv[y, d, j * rows : (j + 1) * rows] = res[
+                    y * rows : (y + 1) * rows, j * LANES : (j + 1) * LANES
+                ]
+            dv[y, d, tiles * rows :] = extra
         out_copies.append(begin(dv.at[:, d], dd_hbm.at[:, d]))
     for copy in out_copies:
         copy.wait()
@@ -160,33 +166,45 @@
 
 def rows_kernel(at_ref, got_ref, out_ref):
     ny, nz, longer, _ = got_ref.shape
-    rows = longer - 8
+    ends = out_ref.shape[1] - 16
+    rows = (longer - 8) // TILES
+    tiles = TILES
     half = rows // 2
     sums = []
     for d in range(nz):
         total = got_ref[0, d].astype(F32)
         for k in range(1, ny):
             total = total + got_ref[k, d].astype(F32)
-        part = total[:rows].astype(BF16)
         to = (at_ref[0] + d) % nz
-        out_ref[to, :half] = part[:half]
-        out_ref[nz + to, :half] = part[half:]
-        sums.append(jnp.sum(total[rows:], axis=0, keepdims=True))
+        for j in range(tiles):
+            part = total[j * rows : (j + 1) * rows].astype(BF16)
+            out_ref[to, j * half : (j + 1) * half] = part[:half]
+            out_ref[nz + to, j * half : (j + 1) * half] = part[half:]
+        base = tiles * rows
+        one = jnp.sum(total[base : base + 3], axis=0, keepdims=True)
+        two = jnp.sum(total[base + 3 : base + 6], axis=0, keepdims=True)
+        sums.append(jnp.concatenate([one, two], axis=1))
     extra = jnp.concatenate(sums, axis=0)
     extra = pltpu.roll(extra, at_ref[0], 0).astype(BF16)
     for k in range(2 * nz):
-        out_ref[k, half:] = extra
-
-
-def ring_kernel(got_ref, out_ref, sum_ref):
-    half = out_ref.shape[0]
-    cols = sum_ref.shape[2]
+        out_ref[k, ends : ends + 8] = extra[:, :LANES]
+        out_ref[k, ends + 8 :] = extra[:, LANES:]
+
+
+def ring_kernel(got_ref, out_ref, short_ref, sum_ref):
+    half, units = out_ref.shape
+    tiles = units // LANES
     total = got_ref[0].astype(F32)
     for k in range(1, got_ref.shape[0]):
         total = total + got_ref[k].astype(F32)
-    out_ref[...] = total[:half]
+    for j in range(tiles):
+        part = total[j * half : (j + 1) * half]
+        out_ref[:, j * LANES : (j + 1) * LANES] = part
+        short_ref[:, j * LANES : (j + 1) * LANES] = part.astype(BF16)
+    ends = tiles * half
     for k in range(sum_ref.shape[0]):
-        sum_ref[k] = total[half:, :cols]
+        sum_ref[k, :, :LANES] = total[ends : ends + 8]
+        sum_ref[k, :, LANES:] = total[ends + 8 :]
 
 
 def chip_kernel(mine_ref, theirs_ref, *out_refs):
@@ -304,7 +322,7 @@
         out_shape=(
             jax.ShapeDtypeStruct((nx, nz, part, cols), BF16),
             jax.ShapeDtypeStruct((nx, nz, part, cols), BF16),
-            jax.ShapeDtypeStruct((ny, nz, rows + 8, units), BF16),
+            jax.ShapeDtypeStruct((ny, nz, TILES * rows + 8, LANES), BF16),
         ),
         in_specs=vmem(3) + [anywhere] * 11,
         out_specs=(anywhere,) * 3,
@@ -315,7 +333,7 @@
             pltpu.VMEM((nz, cols, tokens), BF16),
             pltpu.VMEM((7, cols, 3 * units), BF16),
             pltpu.VMEM((2 * nx, nz, part, cols), BF16),
-            pltpu.VMEM((ny, nz, rows + 8, units), BF16),
+            pltpu.VMEM((ny, nz, TILES * rows + 8, LANES), BF16),
             pltpu.SemaphoreType.DMA((48,)),
         ],
         name="grad",
@@ -361,25 +379,26 @@
 
     dz = pl.pallas_call(
         rows_kernel,
-        out_shape=jax.ShapeDtypeStruct((2 * nz, rows // 2 + 8, units), BF16),
+        out_shape=jax.ShapeDtypeStruct((2 * nz, TILES * rows // 2 + 16, LANES), BF16),
         in_specs=[pl.BlockSpec(memory_space=pltpu.SMEM)] + vmem(1),
         out_specs=pl.BlockSpec(memory_space=pltpu.VMEM),
         name="ysum",
     )(at, *near(dy))
     dz = exchanged(dz, RING)
-    own, gain_own = pl.pallas_call(
+    own, short, gain_own = pl.pallas_call(
         ring_kernel,
         out_shape=(
             jax.ShapeDtypeStruct((rows // 2, units), F32),
+            jax.ShapeDtypeStruct((rows // 2, units), BF16),
             jax.ShapeDtypeStruct((lax.axis_size(TP), nz, cols), F32),
         ),
         in_specs=vmem(1),
-        out_specs=tuple(vmem(2)),
+        out_specs=tuple(vmem(3)),
         name="zsum",
     )(*near(dz))
     gain_all = exchanged(gain_own, TP)
     gain_gradient = jnp.sum(gain_all, axis=0).reshape(width)
-    far = shifted(own, "rep", 1)
+    far = shifted(short, "rep", 1).astype(F32)
     pair = rolled(jnp.stack([own, far]), rep)
     d_down = pair.reshape(rows, units)
     return (out, gain_gradient, d_down)

time: 209 us -> 195 us (0.933)
  waiting for transfers between devices: 48.2 us -> 37.3 us
  starting transfers between devices: 101 us -> 95.5 us
  local copies, waits for them, and re-layouts: 2.41 us -> 4.61 us
    all_to_all x3, waiting for transfers between devices: 15 us -> 4.16 us  [exchanged(): return lax.all_to_all(v, axis, 0, 0, tiled=True)]
    ppermute x17, starting transfers between devices: 87 us -> 80.3 us  [shifted(): return lax.ppermute(v, axis, [(i, (i + by) % n) for i in range(n)])]
    unnamed x19 -> x25, local copies, waits for them, and re-layouts: 0.77 us -> 2.98 us
  transfers between devices with their start and end apart: 20 -> 20, of which waited for: 9 -> 7; matrix products, arithmetic and copies ran while one was open for 2% -> 2% of each run, Pallas kernels for 14% -> 15%
where the time goes in v8:
time: 195 us; the launch traced here: 194 us
  starting transfers between devices  95.5 us (49%)
  Pallas kernels  39.6 us (20%)
  waiting for transfers between devices  37.3 us (19%)
  blocking collectives  12.1 us (6%)
  local copies, waits for them, and re-layouts  4.61 us (2%)
  other arithmetic  3.93 us (2%)
    ppermute x17, starting transfers between devices, shifted(): return lax.ppermute(v, axis, [(i, (i + by) % n) for i in range(n)])  80.3 us
    ppermute x17, waiting for transfers between devices, shifted(): return lax.ppermute(v, axis, [(i, (i + by) % n) for i in range(n)])  33.2 us
    all_to_all x3, starting transfers between devices, exchanged(): return lax.all_to_all(v, axis, 0, 0, tiled=True)  15.3 us
    all_to_all x1, blocking collectives, exchanged(): return lax.all_to_all(v, axis, 0, 0, tiled=True)  12.1 us
    pallas_call x1, Pallas kernels, work(): pl.pallas_call(grad_kernel, out_shape=(jax.ShapeDtypeStruct((nx, nz, part...  11 us
    pallas_call x1, Pallas kernels, work(): pl.pallas_call(prepare_tokens, out_shape=jax.ShapeDtypeStruct((nz, tokens...  6.97 us
    pallas_call x1, Pallas kernels, work(): pl.pallas_call(forward_kernel, out_shape=jax.ShapeDtypeStruct((tokens, 3...  6.3 us
    pallas_call x1, Pallas kernels, work(): pl.pallas_call(prepare_cotangent, out_shape=(jax.ShapeDtypeStruct((nz, to...  5.34 us
  transfers between devices with their start and end apart: 20, of which 7 were waited for; matrix products, arithmetic and copies ran while one was open for 2% of the time, Pallas kernels for 15%

profile of v8, /device:TPU:1, one launch (start us, length us, event | category | flops | bytes accessed | tf_op | source)
XLA Modules:
  0.0 194.0 jit_solution(14058360231651252387)
XLA Ops:
  0.6 0.9 pad_maximum_fusion.1
  1.5 12.1 %all_to_all.20 = bf16[4,64,1152]{2,1,0:T(8,128)(2,1)S(1)} all-to-all(bf16[4,64,1152]{2,1,0:T(8,128)(2,1)S(1)} %broadcast_in_dim.4), channel_id=1, replica_groups=mesh['rep'=2,'fs_0'=8,'fs_1'=4,'x'=4,'c'=2] {'fs_1'}, dimensions={0} | all-to-all | bytes 1179648 | tf_op jit(solution)/shard_map/all_to_all | solution.py:27
  13.6 12.9 %collective-permute-start.4 = (bf16[256,1152]{1,0:T(8,128)(2,1)S(1)}, bf16[256,1152]{1,0:T(8,128)(2,1)S(1)}, u32[]{:S(2)}, u32[]{:S(2)}) collective-permute-start(bf16[256,1152]{1,0:T(8,128)(2,1)S(1)} %bitcast.20), channel_id=1, source_target_pairs={{0,480},{32,0},{64,32},{96,64},{128,96},{160,128},{192,160},{224,1... | collective-permute-start | bytes 1769480 | tf_op jit(solution)/shard_map/ppermute | solution.py:23
  26.5 1.9 collective-permute-start
  28.4 8.6 %collective-permute-done.4.refs_1_ = bf16[256,1152]{1,0:T(8,128)(2,1)S(1)} collective-permute-done((bf16[256,1152]{1,0:T(8,128)(2,1)S(1)}, bf16[256,1152]{1,0:T(8,128)(2,1)S(1)}, u32[]{:S(2)}, u32[]{:S(2)}) %collective-permute-start.4) | collective-permute-done | bytes 589856 | tf_op jit(solution)/shard_map/ppermute | solution.py:23
  37.1 5.3 %collective-permute-start.5 = (bf16[256,1152]{1,0:T(8,128)(2,1)S(1)}, bf16[256,1152]{1,0:T(8,128)(2,1)S(1)}, u32[]{:S(2)}, u32[]{:S(2)}) collective-permute-start(bf16[256,1152]{1,0:T(8,128)(2,1)S(1)} %collective-permute-done.4.refs_1_), channel_id=1, source_target_pairs={{0,480},{32,0},{64,32},{96,64},{128,96},{160,128},{192,160},{224,1... | collective-permute-start | bytes 1769480 | tf_op jit(solution)/shard_map/ppermute | solution.py:23
  42.4 0.0 collective-permute-done.refs_2_.refs_6_
  42.4 1.9 collective-permute-start.1
  44.3 7.8 %collective-permute-done.5.refs_3_.refs_2_ = bf16[256,1152]{1,0:T(8,128)(2,1)S(1)} collective-permute-done((bf16[256,1152]{1,0:T(8,128)(2,1)S(1)}, bf16[256,1152]{1,0:T(8,128)(2,1)S(1)}, u32[]{:S(2)}, u32[]{:S(2)}) %collective-permute-start.5) | collective-permute-done | bytes 589856 | tf_op jit(solution)/shard_map/ppermute | solution.py:23
  52.1 5.3 %collective-permute-start.6 = (bf16[256,1152]{1,0:T(8,128)(2,1)S(1)}, bf16[256,1152]{1,0:T(8,128)(2,1)S(1)}, u32[]{:S(2)}, u32[]{:S(2)}) collective-permute-start(bf16[256,1152]{1,0:T(8,128)(2,1)S(1)} %collective-permute-done.5.refs_3_.refs_2_), channel_id=1, source_target_pairs={{0,480},{32,0},{64,32},{96,64},{128,96},{160,128},{192,160},{224,1... | collective-permute-start | bytes 1769480 | tf_op jit(solution)/shard_map/ppermute | solution.py:23
  57.4 0.0 collective-permute-done.1.refs_4_.refs_5_
  57.4 1.9 collective-permute-start.2
  59.4 6.9 %collective-permute-done.6.refs_3_ = bf16[256,1152]{1,0:T(8,128)(2,1)S(1)} collective-permute-done((bf16[256,1152]{1,0:T(8,128)(2,1)S(1)}, bf16[256,1152]{1,0:T(8,128)(2,1)S(1)}, u32[]{:S(2)}, u32[]{:S(2)}) %collective-permute-start.6) | collective-permute-done | bytes 589856 | tf_op jit(solution)/shard_map/ppermute | solution.py:23
  66.3 0.8 slice.9
  67.1 5.3 %collective-permute-start.7 = (bf16[128,1152]{1,0:T(8,128)(2,1)}, bf16[128,1152]{1,0:T(8,128)(2,1)S(1)}, u32[]{:S(2)}, u32[]{:S(2)}) collective-permute-start(bf16[128,1152]{1,0:T(8,128)(2,1)} %slice.9), channel_id=1, source_target_pairs={{0,480},{32,0},{64,32},{96,64},{128,96},{160,128},{192,160},{224,1... | collective-permute-start | bytes 884744 | tf_op jit(solution)/shard_map/ppermute | solution.py:23
  72.4 0.0 collective-permute-done.2.refs_4_
  72.4 0.8 slice.8
  73.2 0.1 copy-done.8
  73.3 1.9 collective-permute-start.3
  75.3 0.7 pad_add_fusion.at_ref
  75.9 5.3 %prepare_c.1 = (bf16[8,512,256]{2,1,0:T(8,128)(2,1)}, bf16[8,256,512]{2,1,0:T(8,128)(2,1)}) custom-call(s32[3]{0:T(128)} %pad_add_fusion.at_ref, bf16[512,2048]{1,0:T(8,128)(2,1)} %c_ref.1, bf16[512,2048]{1,0:T(8,128)(2,1)} %c_ref.1), custom_call_target="tpu_custom_call" | custom-call | tf_op jit(solution)/shard_map/prepare_c/pallas_call | solution.py:290
  81.3 0.0 copy-done.3
  81.3 0.0 copy-start.9
  81.3 7.0 %prepare_x.1.x_ref.x_hbm = bf16[8,512,256]{2,1,0:T(8,128)(2,1)} custom-call(s32[3]{0:T(128)} %pad_add_fusion.at_ref, bf16[512,2048]{1,0:T(8,128)(2,1)} %x_ref.3, f32[1,2048]{1,0:T(1,128)} %bitcast.26), custom_call_target="tpu_custom_call" | custom-call | tf_op jit(solution)/shard_map/prepare_x/pallas_call | solution.py:276
  88.3 0.6 fusion.3.gain_ref
  88.9 6.3 %forward.1.acc_hbm = f32[512,1152]{1,0:T(8,128)} custom-call(bf16[8,512,256]{2,1,0:T(8,128)(2,1)} %prepare_x.1.x_ref.x_hbm, bf16[8,512,256]{2,1,0:T(8,128)(2,1)} %get-tuple-element.15.c_ref.c_hbm, bf16[256,1152]{1,0:T(8,128)(2,1)} %bitcast.22, bf16[256,1152]{1,0:T(8,128)(2,1)} %copy-done.3, bf16[256,1152]{1,0:T(8,128)(2,1)} %copy-done.4, ...), custom_call_target="tpu_custom_call" | custom-call | tf_op jit(solution)/shard_map/forward/pallas_call | solution.py:312
  95.2 0.0 collective-permute-done.7.hi_ref
  95.2 0.0 collective-permute-done.3.lo_ref
  95.2 11.0 %grad.1 = (bf16[4,8,64,256]{3,2,1,0:T(8,128)(2,1)}, bf16[4,8,64,256]{3,2,1,0:T(8,128)(2,1)}, bf16[4,8,200,128]{3,2,1,0:T(8,128)(2,1)}) custom-call(f32[8,1,256]{2,1,0:T(1,128)} %fusion.3.gain_ref, bf16[128,1152]{1,0:T(8,128)(2,1)S(1)} %collective-permute-done.3.lo_ref, bf16[128,1152]{1,0:T(8,128)(2,1)S(1)} %collective-permute-done.7.hi_ref, ...), custom_call_target="tpu_custom_call" | custom-call | tf_op jit(solution)/shard_map/grad/pallas_call | solution.py:320
  106.2 3.7 %all-to-all-start.1 = ((bf16[4,8,200,128]{3,2,1,0:T(8,128)(2,1)}), bf16[4,8,200,128]{3,2,1,0:T(8,128)(2,1)S(1)}, u32[]{:S(2)}, u32[]{:S(2)}) async-start(bf16[4,8,200,128]{3,2,1,0:T(8,128)(2,1)} %get-tuple-element.23), calls=%async_computation.1 | async-start | bytes 3276800 | tf_op jit(solution)/shard_map/all_to_all | solution.py:27
  109.9 6.9 %collective-permute-start.8 = (bf16[4,8,64,256]{3,2,1,0:T(8,128)(2,1)S(1)}, bf16[4,8,64,256]{3,2,1,0:T(8,128)(2,1)S(1)}, u32[]{:S(2)}, u32[]{:S(2)}) collective-permute-start(bf16[4,8,64,256]{3,2,1,0:T(8,128)(2,1)S(1)} %copy-done.11), channel_id=1, source_target_pairs={{0,1},{1,0},{2,3},{3,2},{4,5},{5,4},{6,7},{7,6},{8,9},{9,8},{10,11... | collective-permute-start | bytes 3145736 | tf_op jit(solution)/shard_map/ppermute | solution.py:23
  116.8 2.3 %collective-permute-done.8.theirs_ref = bf16[4,8,64,256]{3,2,1,0:T(8,128)(2,1)S(1)} collective-permute-done((bf16[4,8,64,256]{3,2,1,0:T(8,128)(2,1)S(1)}, bf16[4,8,64,256]{3,2,1,0:T(8,128)(2,1)S(1)}, u32[]{:S(2)}, u32[]{:S(2)}) %collective-permute-start.8) | collective-permute-done | bytes 1048608 | tf_op jit(solution)/shard_map/ppermute | solution.py:23
  119.1 1.0 copy-done
  120.1 1.2 copy-done.1
  121.3 2.3 %chip.1 = (bf16[8,64,256]{2,1,0:T(8,128)(2,1)}, bf16[8,64,256]{2,1,0:T(8,128)(2,1)}, bf16[8,64,256]{2,1,0:T(8,128)(2,1)}, bf16[8,64,256]{2,1,0:T(8,128)(2,1)}) custom-call(bf16[4,8,64,256]{3,2,1,0:T(8,128)(2,1)} %get-tuple-element.17.mine_ref, bf16[4,8,64,256]{3,2,1,0:T(8,128)(2,1)S(1)} %copy-done.1), custom_call_target="tpu_custom_call" | custom-call | tf_op jit(solution)/shard_map/chip/pallas_call | solution.py:345
  123.5 3.1 %collective-permute-start.9 = (bf16[8,64,256]{2,1,0:T(8,128)(2,1)}, bf16[8,64,256]{2,1,0:T(8,128)(2,1)S(1)}, u32[]{:S(2)}, u32[]{:S(2)}) collective-permute-start(bf16[8,64,256]{2,1,0:T(8,128)(2,1)} %get-tuple-element.20), channel_id=1, source_target_pairs={{0,2},{2,4},{4,6},{6,0},{1,3},{3,5},{5,7},{7,1},{8,10},{10,12},{12... | collective-permute-start | bytes 786440 | tf_op jit(solution)/shard_map/ppermute | solution.py:23
  126.7 4.4 %collective-permute-start.10 = (bf16[8,64,256]{2,1,0:T(8,128)(2,1)}, bf16[8,64,256]{2,1,0:T(8,128)(2,1)S(1)}, u32[]{:S(2)}, u32[]{:S(2)}) collective-permute-start(bf16[8,64,256]{2,1,0:T(8,128)(2,1)} %get-tuple-element.21), channel_id=1, source_target_pairs={{0,4},{2,6},{4,0},{6,2},{1,5},{3,7},{5,1},{7,3},{8,12},{10,14},{12... | collective-permute-start | bytes 786440 | tf_op jit(solution)/shard_map/ppermute | solution.py:23
  131.0 3.1 %collective-permute-start.11 = (bf16[8,64,256]{2,1,0:T(8,128)(2,1)}, bf16[8,64,256]{2,1,0:T(8,128)(2,1)S(1)}, u32[]{:S(2)}, u32[]{:S(2)}) collective-permute-start(bf16[8,64,256]{2,1,0:T(8,128)(2,1)} %get-tuple-element.22), channel_id=1, source_target_pairs={{0,6},{2,0},{4,2},{6,4},{1,7},{3,1},{5,3},{7,5},{8,14},{10,8},{12,... | collective-permute-start | bytes 786440 | tf_op jit(solution)/shard_map/ppermute | solution.py:23
  134.1 0.0 all-to-all-done.1.got_ref
  134.1 1.7 ysum.1
  135.8 7.3 %all-to-all-start.2 = ((bf16[16,112,128]{2,1,0:T(8,128)(2,1)}), bf16[16,112,128]{2,1,0:T(8,128)(2,1)S(1)}, u32[]{:S(2)}, u32[]{:S(2)}) async-start(bf16[16,112,128]{2,1,0:T(8,128)(2,1)} %ysum.1), calls=%async_computation.2 | async-start | bytes 917504 | tf_op jit(solution)/shard_map/all_to_all | solution.py:27
  143.1 0.0 collective-permute-done.9.got1
  143.1 0.0 collective-permute-done.10.got2
  143.1 0.0 collective-permute-done.11.got3
  143.1 2.9 %finish.1.p0 = bf16[64,2048]{1,0:T(8,128)(2,1)} custom-call(s32[3]{0:T(128)} %pad_add_fusion.at_ref, bf16[8,64,256]{2,1,0:T(8,128)(2,1)} %get-tuple-element.19.got0, bf16[8,64,256]{2,1,0:T(8,128)(2,1)S(1)} %collective-permute-done.9.got1, bf16[8,64,256]{2,1,0:T(8,128)(2,1)S(1)} %collective-permute-done.10.got2, ...), custom_call_target="tpu_custom_call" | custom-call | tf_op jit(solution)/shard_map/finish/pallas_call | solution.py:356
  146.0 4.1 %collective-permute-start.14 = (bf16[64,2048]{1,0:T(8,128)(2,1)}, bf16[64,2048]{1,0:T(8,128)(2,1)S(1)}, u32[]{:S(2)}, u32[]{:S(2)}) collective-permute-start(bf16[64,2048]{1,0:T(8,128)(2,1)} %finish.1.p0), channel_id=1, source_target_pairs={{0,2},{2,4},{4,6},{6,0},{1,3},{3,5},{5,7},{7,1},{8,10},{10,12},{12... | collective-permute-start | bytes 786440 | tf_op jit(solution)/shard_map/ppermute | solution.py:23
  150.1 3.1 %collective-permute-start.13 = (bf16[64,2048]{1,0:T(8,128)(2,1)}, bf16[64,2048]{1,0:T(8,128)(2,1)S(1)}, u32[]{:S(2)}, u32[]{:S(2)}) collective-permute-start(bf16[64,2048]{1,0:T(8,128)(2,1)} %finish.1.p0), channel_id=1, source_target_pairs={{0,4},{2,6},{4,0},{6,2},{1,5},{3,7},{5,1},{7,3},{8,12},{10,14},{12... | collective-permute-start | bytes 786440 | tf_op jit(solution)/shard_map/ppermute | solution.py:23
  153.3 3.1 %collective-permute-start.12 = (bf16[64,2048]{1,0:T(8,128)(2,1)}, bf16[64,2048]{1,0:T(8,128)(2,1)S(1)}, u32[]{:S(2)}, u32[]{:S(2)}) collective-permute-start(bf16[64,2048]{1,0:T(8,128)(2,1)} %finish.1.p0), channel_id=1, source_target_pairs={{0,6},{2,0},{4,2},{6,4},{1,7},{3,1},{5,3},{7,5},{8,14},{10,8},{12,... | collective-permute-start | bytes 786440 | tf_op jit(solution)/shard_map/ppermute | solution.py:23
  156.4 0.0 collective-permute-done.14.p3
  156.4 6.4 %collective-permute-done.13.p2 = bf16[64,2048]{1,0:T(8,128)(2,1)S(1)} collective-permute-done((bf16[64,2048]{1,0:T(8,128)(2,1)}, bf16[64,2048]{1,0:T(8,128)(2,1)S(1)}, u32[]{:S(2)}, u32[]{:S(2)}) %collective-permute-start.13) | collective-permute-done | bytes 262176 | tf_op jit(solution)/shard_map/ppermute | solution.py:23
  162.8 1.1 collective-permute-done.12.p1
  163.9 1.1 pad_maximum_fusion
  165.0 4.1 %collective-permute-start.15 = (bf16[4,64,2048]{2,1,0:T(8,128)(2,1)S(1)}, bf16[4,64,2048]{2,1,0:T(8,128)(2,1)S(1)}, u32[]{:S(2)}, u32[]{:S(2)}) collective-permute-start(bf16[4,64,2048]{2,1,0:T(8,128)(2,1)S(1)} %pad_maximum_fusion), channel_id=1, source_target_pairs={{0,1},{1,0},{2,3},{3,2},{4,5},{5,4},{6,7},{7,6},{8,9},{9,8},{10,11... | collective-permute-start | bytes 3145736 | tf_op jit(solution)/shard_map/ppermute | solution.py:23
  169.2 0.0 all-to-all-done.2.got_ref
  169.2 0.7 zsum.1
  169.9 12.0 %collective-permute-start.16 = (bf16[32,384]{1,0:T(8,128)(2,1)}, bf16[32,384]{1,0:T(8,128)(2,1)S(1)}, u32[]{:S(2)}, u32[]{:S(2)}) collective-permute-start(bf16[32,384]{1,0:T(8,128)(2,1)} %get-tuple-element.26), channel_id=1, source_target_pairs={{0,256},{256,0},{1,257},{257,1},{2,258},{258,2},{3,259},{259,3},{4... | collective-permute-start | bytes 73736 | tf_op jit(solution)/shard_map/ppermute | solution.py:23
  181.9 0.0 copy-start.10
  181.9 0.0 collective-permute-done.15.other_ref
  181.9 2.4 %place.1 = bf16[512,2048]{1,0:T(8,128)(2,1)} custom-call(s32[3]{0:T(128)} %pad_add_fusion.at_ref, bf16[64,2048]{1,0:T(8,128)(2,1)} %finish.1.p0, bf16[64,2048]{1,0:T(8,128)(2,1)S(1)} %collective-permute-done.12.p1, bf16[64,2048]{1,0:T(8,128)(2,1)S(1)} %collective-permute-done.13.p2, bf16[64,2048]{1,0:T(8,128)(2,1)S(1)} %collective-permute-done.14.p3, ...), custom_call_target="tpu_custom_call" | custom-call | tf_op jit(solution)/shard_map/place/pallas_call | solution.py:372
  184.3 4.2 %all-to-all-start.3 = ((f32[8,8,256]{2,1,0:T(8,128)}), f32[8,8,256]{2,1,0:T(8,128)S(1)}, u32[]{:S(2)}, u32[]{:S(2)}) async-start(f32[8,8,256]{2,1,0:T(8,128)} %get-tuple-element.24), calls=%async_computation.3 | async-start | bytes 131072 | tf_op jit(solution)/shard_map/all_to_all | solution.py:27
  188.6 0.0 collective-permute-done.16
  188.6 0.7 fusion.2
  189.3 4.2 %all-to-all-done.3 = f32[8,8,256]{2,1,0:T(8,128)S(1)} async-done(((f32[8,8,256]{2,1,0:T(8,128)}), f32[8,8,256]{2,1,0:T(8,128)S(1)}, u32[]{:S(2)}, u32[]{:S(2)}) %all-to-all-start.3) | async-done | bytes 65568 | tf_op jit(solution)/shard_map/all_to_all | solution.py:27
  193.4 0.6 copy.9
  (21 shorter events, 0.1 us)
Async XLA Ops:
  13.6 67.6 %copy-start.2 = (bf16[4,64,1152]{2,1,0:T(8,128)(2,1)}, bf16[4,64,1152]{2,1,0:T(8,128)(2,1)S(1)}, u32[]{:S(2)}) copy-start(bf16[4,64,1152]{2,1,0:T(8,128)(2,1)S(1)} %all_to_all.20) | copy-start | bytes 1769476
  13.6 23.4 %collective-permute-start.4 = (bf16[256,1152]{1,0:T(8,128)(2,1)S(1)}, bf16[256,1152]{1,0:T(8,128)(2,1)S(1)}, u32[]{:S(2)}, u32[]{:S(2)}) collective-permute-start(bf16[256,1152]{1,0:T(8,128)(2,1)S(1)} %bitcast.20), channel_id=1, source_target_pairs={{0,480},{32,0},{64,32},{96,64},{128,96},{160,128},{192,160},{224,1... | collective-permute-start | bytes 1769480 | tf_op jit(solution)/shard_map/ppermute | solution.py:23
  26.5 15.9 %collective-permute-start = (bf16[256,1152]{1,0:T(8,128)(2,1)S(1)}, bf16[256,1152]{1,0:T(8,128)(2,1)S(1)}, u32[]{:S(2)}, u32[]{:S(2)}) collective-permute-start(bf16[256,1152]{1,0:T(8,128)(2,1)S(1)} %bitcast.21), channel_id=1, source_target_pairs={{0,32},{32,64},{64,96},{96,128},{128,160},{160,192},{192,224},{224... | collective-permute-start | bytes 1769480 | tf_op jit(solution)/shard_map/ppermute | solution.py:23
  37.1 44.2 %copy-start.3 = (bf16[256,1152]{1,0:T(8,128)(2,1)}, bf16[256,1152]{1,0:T(8,128)(2,1)S(1)}, u32[]{:S(2)}) copy-start(bf16[256,1152]{1,0:T(8,128)(2,1)S(1)} %collective-permute-done.4.refs_1_) | copy-start | bytes 1769476
  37.1 15.0 %collective-permute-start.5 = (bf16[256,1152]{1,0:T(8,128)(2,1)S(1)}, bf16[256,1152]{1,0:T(8,128)(2,1)S(1)}, u32[]{:S(2)}, u32[]{:S(2)}) collective-permute-start(bf16[256,1152]{1,0:T(8,128)(2,1)S(1)} %collective-permute-done.4.refs_1_), channel_id=1, source_target_pairs={{0,480},{32,0},{64,32},{96,64},{128,96},{160,128},{192,160},{224,1... | collective-permute-start | bytes 1769480 | tf_op jit(solution)/shard_map/ppermute | solution.py:23
  42.4 38.9 %copy-start.4 = (bf16[256,1152]{1,0:T(8,128)(2,1)}, bf16[256,1152]{1,0:T(8,128)(2,1)S(1)}, u32[]{:S(2)}) copy-start(bf16[256,1152]{1,0:T(8,128)(2,1)S(1)} %collective-permute-done.refs_2_.refs_6_) | copy-start | bytes 1769476
  42.4 15.0 %collective-permute-start.1 = (bf16[256,1152]{1,0:T(8,128)(2,1)S(1)}, bf16[256,1152]{1,0:T(8,128)(2,1)S(1)}, u32[]{:S(2)}, u32[]{:S(2)}) collective-permute-start(bf16[256,1152]{1,0:T(8,128)(2,1)S(1)} %collective-permute-done.refs_2_.refs_6_), channel_id=1, source_target_pairs={{0,32},{32,64},{64,96},{96,128},{128,160},{160,192},{192,224},{224... | collective-permute-start | bytes 1769480 | tf_op jit(solution)/shard_map/ppermute | solution.py:23
  52.1 29.2 %copy-start.5 = (bf16[256,1152]{1,0:T(8,128)(2,1)}, bf16[256,1152]{1,0:T(8,128)(2,1)S(1)}, u32[]{:S(2)}) copy-start(bf16[256,1152]{1,0:T(8,128)(2,1)S(1)} %collective-permute-done.5.refs_3_.refs_2_) | copy-start | bytes 1769476
  52.1 14.2 %collective-permute-start.6 = (bf16[256,1152]{1,0:T(8,128)(2,1)S(1)}, bf16[256,1152]{1,0:T(8,128)(2,1)S(1)}, u32[]{:S(2)}, u32[]{:S(2)}) collective-permute-start(bf16[256,1152]{1,0:T(8,128)(2,1)S(1)} %collective-permute-done.5.refs_3_.refs_2_), channel_id=1, source_target_pairs={{0,480},{32,0},{64,32},{96,64},{128,96},{160,128},{192,160},{224,1... | collective-permute-start | bytes 1769480 | tf_op jit(solution)/shard_map/ppermute | solution.py:23
  57.4 15.0 %copy-start.6 = (bf16[256,1152]{1,0:T(8,128)(2,1)}, bf16[256,1152]{1,0:T(8,128)(2,1)S(1)}, u32[]{:S(2)}) copy-start(bf16[256,1152]{1,0:T(8,128)(2,1)S(1)} %collective-permute-done.1.refs_4_.refs_5_) | copy-start | bytes 1769476
  57.4 14.9 %collective-permute-start.2 = (bf16[256,1152]{1,0:T(8,128)(2,1)S(1)}, bf16[256,1152]{1,0:T(8,128)(2,1)S(1)}, u32[]{:S(2)}, u32[]{:S(2)}) collective-permute-start(bf16[256,1152]{1,0:T(8,128)(2,1)S(1)} %collective-permute-done.1.refs_4_.refs_5_), channel_id=1, source_target_pairs={{0,32},{32,64},{64,96},{96,128},{128,160},{160,192},{192,224},{224... | collective-permute-start | bytes 1769480 | tf_op jit(solution)/shard_map/ppermute | solution.py:23
  66.3 15.0 %copy-start.7 = (bf16[256,1152]{1,0:T(8,128)(2,1)}, bf16[256,1152]{1,0:T(8,128)(2,1)S(1)}, u32[]{:S(2)}) copy-start(bf16[256,1152]{1,0:T(8,128)(2,1)S(1)} %collective-permute-done.6.refs_3_) | copy-start | bytes 1769476
  67.1 28.2 %collective-permute-start.7 = (bf16[128,1152]{1,0:T(8,128)(2,1)}, bf16[128,1152]{1,0:T(8,128)(2,1)S(1)}, u32[]{:S(2)}, u32[]{:S(2)}) collective-permute-start(bf16[128,1152]{1,0:T(8,128)(2,1)} %slice.9), channel_id=1, source_target_pairs={{0,480},{32,0},{64,32},{96,64},{128,96},{160,128},{192,160},{224,1... | collective-permute-start | bytes 884744 | tf_op jit(solution)/shard_map/ppermute | solution.py:23
  72.4 0.9 copy-start.8
  73.3 21.9 %collective-permute-start.3 = (bf16[128,1152]{1,0:T(8,128)(2,1)}, bf16[128,1152]{1,0:T(8,128)(2,1)S(1)}, u32[]{:S(2)}, u32[]{:S(2)}) collective-permute-start(bf16[128,1152]{1,0:T(8,128)(2,1)} %slice.8), channel_id=1, source_target_pairs={{0,32},{32,64},{64,96},{96,128},{128,160},{160,192},{192,224},{224... | collective-permute-start | bytes 884744 | tf_op jit(solution)/shard_map/ppermute | solution.py:23
  81.3 7.0 %copy-start.9 = (f32[2048]{0:T(1024)S(1)}, f32[2048]{0:T(1024)}, u32[]{:S(2)}) copy-start(f32[2048]{0:T(1024)} %param.7) | copy-start | bytes 24580
  106.2 3.7 %copy-start.11 = (bf16[4,8,64,256]{3,2,1,0:T(8,128)(2,1)S(1)}, bf16[4,8,64,256]{3,2,1,0:T(8,128)(2,1)}, u32[]{:S(2)}) copy-start(bf16[4,8,64,256]{3,2,1,0:T(8,128)(2,1)} %get-tuple-element.18) | copy-start | bytes 3145732
  106.2 27.9 %all-to-all-start.1 = ((bf16[4,8,200,128]{3,2,1,0:T(8,128)(2,1)}), bf16[4,8,200,128]{3,2,1,0:T(8,128)(2,1)S(1)}, u32[]{:S(2)}, u32[]{:S(2)}) async-start(bf16[4,8,200,128]{3,2,1,0:T(8,128)(2,1)} %get-tuple-element.23), calls=%async_computation.1 | async-start | bytes 3276800 | tf_op jit(solution)/shard_map/all_to_all | solution.py:27
  109.9 9.1 %collective-permute-start.8 = (bf16[4,8,64,256]{3,2,1,0:T(8,128)(2,1)S(1)}, bf16[4,8,64,256]{3,2,1,0:T(8,128)(2,1)S(1)}, u32[]{:S(2)}, u32[]{:S(2)}) collective-permute-start(bf16[4,8,64,256]{3,2,1,0:T(8,128)(2,1)S(1)} %copy-done.11), channel_id=1, source_target_pairs={{0,1},{1,0},{2,3},{3,2},{4,5},{5,4},{6,7},{7,6},{8,9},{9,8},{10,11... | collective-permute-start | bytes 3145736 | tf_op jit(solution)/shard_map/ppermute | solution.py:23
  119.1 1.0 copy-start
  120.0 1.2 copy-start.1
  123.5 19.5 %collective-permute-start.9 = (bf16[8,64,256]{2,1,0:T(8,128)(2,1)}, bf16[8,64,256]{2,1,0:T(8,128)(2,1)S(1)}, u32[]{:S(2)}, u32[]{:S(2)}) collective-permute-start(bf16[8,64,256]{2,1,0:T(8,128)(2,1)} %get-tuple-element.20), channel_id=1, source_target_pairs={{0,2},{2,4},{4,6},{6,0},{1,3},{3,5},{5,7},{7,1},{8,10},{10,12},{12... | collective-permute-start | bytes 786440 | tf_op jit(solution)/shard_map/ppermute | solution.py:23
  126.7 16.4 %collective-permute-start.10 = (bf16[8,64,256]{2,1,0:T(8,128)(2,1)}, bf16[8,64,256]{2,1,0:T(8,128)(2,1)S(1)}, u32[]{:S(2)}, u32[]{:S(2)}) collective-permute-start(bf16[8,64,256]{2,1,0:T(8,128)(2,1)} %get-tuple-element.21), channel_id=1, source_target_pairs={{0,4},{2,6},{4,0},{6,2},{1,5},{3,7},{5,1},{7,3},{8,12},{10,14},{12... | collective-permute-start | bytes 786440 | tf_op jit(solution)/shard_map/ppermute | solution.py:23
  131.0 12.1 %collective-permute-start.11 = (bf16[8,64,256]{2,1,0:T(8,128)(2,1)}, bf16[8,64,256]{2,1,0:T(8,128)(2,1)S(1)}, u32[]{:S(2)}, u32[]{:S(2)}) collective-permute-start(bf16[8,64,256]{2,1,0:T(8,128)(2,1)} %get-tuple-element.22), channel_id=1, source_target_pairs={{0,6},{2,0},{4,2},{6,4},{1,7},{3,1},{5,3},{7,5},{8,14},{10,8},{12,... | collective-permute-start | bytes 786440 | tf_op jit(solution)/shard_map/ppermute | solution.py:23
  135.8 33.4 %all-to-all-start.2 = ((bf16[16,112,128]{2,1,0:T(8,128)(2,1)}), bf16[16,112,128]{2,1,0:T(8,128)(2,1)S(1)}, u32[]{:S(2)}, u32[]{:S(2)}) async-start(bf16[16,112,128]{2,1,0:T(8,128)(2,1)} %ysum.1), calls=%async_computation.2 | async-start | bytes 917504 | tf_op jit(solution)/shard_map/all_to_all | solution.py:27
  146.0 10.3 %collective-permute-start.14 = (bf16[64,2048]{1,0:T(8,128)(2,1)}, bf16[64,2048]{1,0:T(8,128)(2,1)S(1)}, u32[]{:S(2)}, u32[]{:S(2)}) collective-permute-start(bf16[64,2048]{1,0:T(8,128)(2,1)} %finish.1.p0), channel_id=1, source_target_pairs={{0,2},{2,4},{4,6},{6,0},{1,3},{3,5},{5,7},{7,1},{8,10},{10,12},{12... | collective-permute-start | bytes 786440 | tf_op jit(solution)/shard_map/ppermute | solution.py:23
  150.1 12.7 %collective-permute-start.13 = (bf16[64,2048]{1,0:T(8,128)(2,1)}, bf16[64,2048]{1,0:T(8,128)(2,1)S(1)}, u32[]{:S(2)}, u32[]{:S(2)}) collective-permute-start(bf16[64,2048]{1,0:T(8,128)(2,1)} %finish.1.p0), channel_id=1, source_target_pairs={{0,4},{2,6},{4,0},{6,2},{1,5},{3,7},{5,1},{7,3},{8,12},{10,14},{12... | collective-permute-start | bytes 786440 | tf_op jit(solution)/shard_map/ppermute | solution.py:23
  153.3 10.7 %collective-permute-start.12 = (bf16[64,2048]{1,0:T(8,128)(2,1)}, bf16[64,2048]{1,0:T(8,128)(2,1)S(1)}, u32[]{:S(2)}, u32[]{:S(2)}) collective-permute-start(bf16[64,2048]{1,0:T(8,128)(2,1)} %finish.1.p0), channel_id=1, source_target_pairs={{0,6},{2,0},{4,2},{6,4},{1,7},{3,1},{5,3},{7,5},{8,14},{10,8},{12,... | collective-permute-start | bytes 786440 | tf_op jit(solution)/shard_map/ppermute | solution.py:23
  165.0 16.9 %collective-permute-start.15 = (bf16[4,64,2048]{2,1,0:T(8,128)(2,1)S(1)}, bf16[4,64,2048]{2,1,0:T(8,128)(2,1)S(1)}, u32[]{:S(2)}, u32[]{:S(2)}) collective-permute-start(bf16[4,64,2048]{2,1,0:T(8,128)(2,1)S(1)} %pad_maximum_fusion), channel_id=1, source_target_pairs={{0,1},{1,0},{2,3},{3,2},{4,5},{5,4},{6,7},{7,6},{8,9},{9,8},{10,11... | collective-permute-start | bytes 3145736 | tf_op jit(solution)/shard_map/ppermute | solution.py:23
  169.9 18.7 %collective-permute-start.16 = (bf16[32,384]{1,0:T(8,128)(2,1)}, bf16[32,384]{1,0:T(8,128)(2,1)S(1)}, u32[]{:S(2)}, u32[]{:S(2)}) collective-permute-start(bf16[32,384]{1,0:T(8,128)(2,1)} %get-tuple-element.26), channel_id=1, source_target_pairs={{0,256},{256,0},{1,257},{257,1},{2,258},{258,2},{3,259},{259,3},{4... | collective-permute-start | bytes 73736 | tf_op jit(solution)/shard_map/ppermute | solution.py:23
  181.9 6.7 %copy-start.10 = (f32[32,384]{1,0:T(8,128)S(1)}, f32[32,384]{1,0:T(8,128)}, u32[]{:S(2)}) copy-start(f32[32,384]{1,0:T(8,128)} %get-tuple-element.25) | copy-start | bytes 147460
  184.3 9.1 %all-to-all-start.3 = ((f32[8,8,256]{2,1,0:T(8,128)}), f32[8,8,256]{2,1,0:T(8,128)S(1)}, u32[]{:S(2)}, u32[]{:S(2)}) async-start(f32[8,8,256]{2,1,0:T(8,128)} %get-tuple-element.24), calls=%async_computation.3 | async-start | bytes 131072 | tf_op jit(solution)/shard_map/all_to_all | solution.py:27

commit v9 on v8

--- a/solution.py
+++ b/solution.py
@@ -36,7 +36,11 @@
     return lax.dynamic_slice_in_dim(jnp.concatenate([v, v], axis=0), start, v.shape[0], axis=0)
 
 
-def prepare_tokens(at_ref, x_ref, gain_ref, out_ref):
+def prepare_tokens(at_ref, x_ref, gain_ref, out_ref, own_ref):
+    @pl.when(pl.program_id(0) == 0)
+    def _():
+        own_ref[...] = x_ref[...]
+
     nz, _, cols = out_ref.shape
     v = x_ref[...].astype(F32)
     inv = lax.rsqrt(jnp.mean(v * v, axis=-1, keepdims=True) + EPS)
@@ -46,7 +50,11 @@
         out_ref[d] = (part * inv * gain_ref[:, own]).astype(BF16)
 
 
-def prepare_cotangent(at_ref, lo_ref, hi_ref, out_ref, turned_ref):
+def prepare_cotangent(at_ref, lo_ref, hi_ref, out_ref, turned_ref, own_ref):
+    @pl.when(pl.program_id(0) == 0)
+    def _():
+        own_ref[...] = lo_ref[...]
+
     nz, _, cols = out_ref.shape
     for d in range(nz):
         own = pl.ds(pl.multiple_of(((at_ref[0] + d) % nz) * cols, cols), cols)
@@ -70,7 +78,7 @@
 
 def grad_kernel(gain_ref, lo_ref, hi_ref, acc_hbm, x_hbm, c_hbm, ct_hbm, *refs):
     w_hbm, (mine_hbm, other_hbm, dd_hbm) = refs[:7], refs[7:10]
-    acc, xv, cv, ctv, wv, ov, dv, sems = refs[10:]
+    acc, xv, cv, ctv, wv, ev, ov, dv, sems = refs[10:]
     units = acc.shape[1] // 3
     nz, _, cols = xv.shape
     ny, _, longer, _ = dv.shape
@@ -89,7 +97,7 @@
     acc_in = begin(acc_hbm, acc)
     x_in, c_in, w_in = {}, {}, {}
     for d in (3, 5):
-        w_in[d] = begin(w_hbm[slot[d]], wv.at[slot[d]])
+        w_in[d] = begin(w_hbm[slot[d]], wv.at[(d - 3) // 2])
         x_in[d] = begin(x_hbm.at[d], xv.at[d])
         c_in[d] = begin(c_hbm.at[d], cv.at[d - 3])
     x_in[4] = begin(x_hbm.at[4], xv.at[4])
@@ -103,10 +111,10 @@
         w_in[d].wait()
         x_in[d].wait()
         c_in[d].wait()
-        for e in EARLY if d == 3 else ():
-            w_in[e] = begin(w_hbm[slot[e]], wv.at[slot[e]])
+        for i, e in enumerate(EARLY) if d == 3 else ():
+            w_in[e] = begin(w_hbm[slot[e]].at[:, pl.ds(0, 2 * units)], ev.at[i])
             x_in[e] = begin(x_hbm.at[e], xv.at[e])
-        w = wv.at[slot[d]]
+        w = wv.at[(d - 3) // 2]
         gu = gu + jnp.dot(xv[d], w[:, : 2 * units], preferred_element_type=F32)
         dh = dh + jnp.dot(cv[d - 3], w[:, 2 * units :], preferred_element_type=F32)
     x_in[4].wait()
@@ -129,7 +137,11 @@
         if d in EARLY:
             w_in[d].wait()
             x_in[d].wait()
-        pieces = halves if d == 4 else ((wv.at[slot[d]], slice(0, cols)),)
+        if d == 4:
+            pieces = halves
+        else:
+            block = ev.at[EARLY.index(d)] if d in EARLY else wv.at[(d - 3) // 2]
+            pieces = ((block, slice(0, cols)),)
         got = []
         for w, at in pieces:
             out = lax.dot_general(
@@ -273,9 +285,12 @@
     def spot(i, at):
         return ((i // nx + at[1]) % 2) * nx + (i + at[2]) % nx
 
-    xr = pl.pallas_call(
+    xr, own_x = pl.pallas_call(
         prepare_tokens,
-        out_shape=jax.ShapeDtypeStruct((nz, tokens, cols), BF16),
+        out_shape=(
+            jax.ShapeDtypeStruct((nz, tokens, cols), BF16),
+            jax.ShapeDtypeStruct((part, width), BF16),
+        ),
         grid_spec=pltpu.PrefetchScalarGridSpec(
             num_scalar_prefetch=1,
             grid=(2 * nx,),
@@ -283,15 +298,19 @@
                 pl.BlockSpec((part, width), lambda i, at: (spot(i, at), 0)),
                 pl.BlockSpec((1, width), lambda i, at: (0, 0)),
             ],
-            out_specs=pl.BlockSpec((nz, part, cols), lambda i, at: (0, i, 0)),
+            out_specs=(
+                pl.BlockSpec((nz, part, cols), lambda i, at: (0, i, 0)),
+                pl.BlockSpec((part, width), lambda i, at: (0, 0)),
+            ),
         ),
         name="prepare_x",
     )(at, inputs, gain2)
-    cr, ct = pl.pallas_call(
+    cr, ct, own_c = pl.pallas_call(
         prepare_cotangent,
         out_shape=(
             jax.ShapeDtypeStruct((nz, tokens, cols), BF16),
             jax.ShapeDtypeStruct((nz, cols, tokens), BF16),
+            jax.ShapeDtypeStruct((part, width), BF16),
         ),
         grid_spec=pltpu.PrefetchScalarGridSpec(
             num_scalar_prefetch=1,
@@ -303,6 +322,7 @@
             out_specs=(
                 pl.BlockSpec((nz, 2 * part, cols), lambda i, at: (0, i, 0)),
                 pl.BlockSpec((nz, cols, 2 * part), lambda i, at: (0, 0, i)),
+                pl.BlockSpec((part, width), lambda i, at: (0, 0)),
             ),
         ),
         name="prepare_c",
@@ -331,7 +351,8 @@
             pltpu.VMEM((nz, tokens, cols), BF16),
             pltpu.VMEM((3, tokens, cols), BF16),
             pltpu.VMEM((nz, cols, tokens), BF16),
-            pltpu.VMEM((7, cols, 3 * units), BF16),
+            pltpu.VMEM((2, cols, 3 * units), BF16),
+            pltpu.VMEM((5, cols, 2 * units), BF16),
             pltpu.VMEM((2 * nx, nz, part, cols), BF16),
             pltpu.VMEM((ny, nz, TILES * rows + 8, LANES), BF16),
             pltpu.SemaphoreType.DMA((48,)),
@@ -347,24 +368,24 @@
         out_shape=(chunk,) * 4,
         in_specs=vmem(2),
         out_specs=tuple(vmem(4)),
+        compiler_params=pltpu.CompilerParams(vmem_limit_bytes=48 << 20),
         name="chip",
     )(mine, *near(theirs))
     got = [chip[0]]
     for k in (1, 2, 3):
         got.append(shifted(chip[k], "x", k))
-    own = pl.BlockSpec((part, width), lambda i, at: (at[1] * nx + at[2], 0))
     ig = pl.pallas_call(
         finish_kernel,
         out_shape=jax.ShapeDtypeStruct((part, width), BF16),
         grid_spec=pltpu.PrefetchScalarGridSpec(
             num_scalar_prefetch=1,
             grid=(1,),
-            in_specs=vmem(4) + [own, own, pl.BlockSpec((1, width), lambda i, at: (0, 0))],
+            in_specs=vmem(7),
             out_specs=pl.BlockSpec((part, width), lambda i, at: (0, 0)),
             scratch_shapes=[pltpu.VMEM((part, width), BF16)],
         ),
         name="finish",
-    )(at, got[0], *near(*got[1:]), inputs, cotangent, gain2)
+    )(at, got[0], *near(*got[1:]), own_x, own_c, gain2)
     pieces = [ig]
     for k in (1, 2, 3):
         pieces.append(shifted(ig, "x", -k))

time: 195 us -> 192 us (0.985)
  local copies, waits for them, and re-layouts: 4.61 us -> 0.74 us
    unnamed x25 -> x23, local copies, waits for them, and re-layouts: 2.98 us -> 0.65 us
  transfers between devices with their start and end apart: 20 -> 20, of which waited for: 7 -> 7; matrix products, arithmetic and copies ran while one was open for 2% -> 2% of each run, Pallas kernels for 15% -> 14%
where the time goes in v9:
time: 192 us; the launch traced here: 190 us
  starting transfers between devices  95.7 us (50%)
  Pallas kernels  38.5 us (20%)
  waiting for transfers between devices  37.4 us (19%)
  blocking collectives  12.1 us (6%)
  other arithmetic  4.84 us (3%)
    ppermute x17, starting transfers between devices, shifted(): return lax.ppermute(v, axis, [(i, (i + by) % n) for i in range(n)])  80.4 us
    ppermute x17, waiting for transfers between devices, shifted(): return lax.ppermute(v, axis, [(i, (i + by) % n) for i in range(n)])  33.2 us
    all_to_all x3, starting transfers between devices, exchanged(): return lax.all_to_all(v, axis, 0, 0, tiled=True)  15.3 us
    all_to_all x1, blocking collectives, exchanged(): return lax.all_to_all(v, axis, 0, 0, tiled=True)  12.1 us
    pallas_call x1, Pallas kernels, work(): pl.pallas_call(grad_kernel, out_shape=(jax.ShapeDtypeStruct((nx, nz, part...  11 us
    pallas_call x1, Pallas kernels, work(): pl.pallas_call(prepare_tokens, out_shape=(jax.ShapeDtypeStruct((nz, token...  7.08 us
    pallas_call x1, Pallas kernels, work(): pl.pallas_call(forward_kernel, out_shape=jax.ShapeDtypeStruct((tokens, 3...  6.3 us
    pallas_call x1, Pallas kernels, work(): pl.pallas_call(prepare_cotangent, out_shape=(jax.ShapeDtypeStruct((nz, to...  5.48 us
  transfers between devices with their start and end apart: 20, of which 7 were waited for; matrix products, arithmetic and copies ran while one was open for 2% of the time, Pallas kernels for 14%

profile of v9, /device:TPU:1, one launch (start us, length us, event | category | flops | bytes accessed | tf_op | source)
XLA Modules:
  0.0 190.3 jit_solution(15870884599179689512)
XLA Ops:
  0.6 0.9 pad_maximum_fusion.1
  1.5 12.1 %all_to_all.20 = bf16[4,64,1152]{2,1,0:T(8,128)(2,1)S(1)} all-to-all(bf16[4,64,1152]{2,1,0:T(8,128)(2,1)S(1)} %broadcast_in_dim.4), channel_id=1, replica_groups=mesh['rep'=2,'fs_0'=8,'fs_1'=4,'x'=4,'c'=2] {'fs_1'}, dimensions={0} | all-to-all | bytes 1179648 | tf_op jit(solution)/shard_map/all_to_all | solution.py:27
  13.6 12.9 %collective-permute-start.4 = (bf16[256,1152]{1,0:T(8,128)(2,1)S(1)}, bf16[256,1152]{1,0:T(8,128)(2,1)S(1)}, u32[]{:S(2)}, u32[]{:S(2)}) collective-permute-start(bf16[256,1152]{1,0:T(8,128)(2,1)S(1)} %bitcast.20), channel_id=1, source_target_pairs={{0,480},{32,0},{64,32},{96,64},{128,96},{160,128},{192,160},{224,1... | collective-permute-start | bytes 1769480 | tf_op jit(solution)/shard_map/ppermute | solution.py:23
  26.5 1.9 %collective-permute-start = (bf16[256,1152]{1,0:T(8,128)(2,1)S(1)}, bf16[256,1152]{1,0:T(8,128)(2,1)S(1)}, u32[]{:S(2)}, u32[]{:S(2)}) collective-permute-start(bf16[256,1152]{1,0:T(8,128)(2,1)S(1)} %bitcast.21), channel_id=1, source_target_pairs={{0,32},{32,64},{64,96},{96,128},{128,160},{160,192},{192,224},{224... | collective-permute-start | bytes 1769480 | tf_op jit(solution)/shard_map/ppermute | solution.py:23
  28.4 8.6 %collective-permute-done.4.refs_1_ = bf16[256,1152]{1,0:T(8,128)(2,1)S(1)} collective-permute-done((bf16[256,1152]{1,0:T(8,128)(2,1)S(1)}, bf16[256,1152]{1,0:T(8,128)(2,1)S(1)}, u32[]{:S(2)}, u32[]{:S(2)}) %collective-permute-start.4) | collective-permute-done | bytes 589856 | tf_op jit(solution)/shard_map/ppermute | solution.py:23
  37.1 5.3 %collective-permute-start.5 = (bf16[256,1152]{1,0:T(8,128)(2,1)S(1)}, bf16[256,1152]{1,0:T(8,128)(2,1)S(1)}, u32[]{:S(2)}, u32[]{:S(2)}) collective-permute-start(bf16[256,1152]{1,0:T(8,128)(2,1)S(1)} %collective-permute-done.4.refs_1_), channel_id=1, source_target_pairs={{0,480},{32,0},{64,32},{96,64},{128,96},{160,128},{192,160},{224,1... | collective-permute-start | bytes 1769480 | tf_op jit(solution)/shard_map/ppermute | solution.py:23
  42.4 0.0 collective-permute-done.refs_2_.refs_6_
  42.4 0.0 copy-start.4
  42.4 1.9 %collective-permute-start.1 = (bf16[256,1152]{1,0:T(8,128)(2,1)S(1)}, bf16[256,1152]{1,0:T(8,128)(2,1)S(1)}, u32[]{:S(2)}, u32[]{:S(2)}) collective-permute-start(bf16[256,1152]{1,0:T(8,128)(2,1)S(1)} %collective-permute-done.refs_2_.refs_6_), channel_id=1, source_target_pairs={{0,32},{32,64},{64,96},{96,128},{128,160},{160,192},{192,224},{224... | collective-permute-start | bytes 1769480 | tf_op jit(solution)/shard_map/ppermute | solution.py:23
  44.3 7.8 %collective-permute-done.5.refs_3_.refs_2_ = bf16[256,1152]{1,0:T(8,128)(2,1)S(1)} collective-permute-done((bf16[256,1152]{1,0:T(8,128)(2,1)S(1)}, bf16[256,1152]{1,0:T(8,128)(2,1)S(1)}, u32[]{:S(2)}, u32[]{:S(2)}) %collective-permute-start.5) | collective-permute-done | bytes 589856 | tf_op jit(solution)/shard_map/ppermute | solution.py:23
  52.1 5.3 %collective-permute-start.6 = (bf16[256,1152]{1,0:T(8,128)(2,1)S(1)}, bf16[256,1152]{1,0:T(8,128)(2,1)S(1)}, u32[]{:S(2)}, u32[]{:S(2)}) collective-permute-start(bf16[256,1152]{1,0:T(8,128)(2,1)S(1)} %collective-permute-done.5.refs_3_.refs_2_), channel_id=1, source_target_pairs={{0,480},{32,0},{64,32},{96,64},{128,96},{160,128},{192,160},{224,1... | collective-permute-start | bytes 1769480 | tf_op jit(solution)/shard_map/ppermute | solution.py:23
  57.4 0.0 collective-permute-done.1.refs_4_.refs_5_
  57.4 0.0 copy-start.6
  57.4 1.9 %collective-permute-start.2 = (bf16[256,1152]{1,0:T(8,128)(2,1)S(1)}, bf16[256,1152]{1,0:T(8,128)(2,1)S(1)}, u32[]{:S(2)}, u32[]{:S(2)}) collective-permute-start(bf16[256,1152]{1,0:T(8,128)(2,1)S(1)} %collective-permute-done.1.refs_4_.refs_5_), channel_id=1, source_target_pairs={{0,32},{32,64},{64,96},{96,128},{128,160},{160,192},{192,224},{224... | collective-permute-start | bytes 1769480 | tf_op jit(solution)/shard_map/ppermute | solution.py:23
  59.4 6.9 %collective-permute-done.6.refs_3_ = bf16[256,1152]{1,0:T(8,128)(2,1)S(1)} collective-permute-done((bf16[256,1152]{1,0:T(8,128)(2,1)S(1)}, bf16[256,1152]{1,0:T(8,128)(2,1)S(1)}, u32[]{:S(2)}, u32[]{:S(2)}) %collective-permute-start.6) | collective-permute-done | bytes 589856 | tf_op jit(solution)/shard_map/ppermute | solution.py:23
  66.3 5.3 %collective-permute-start.7 = (bf16[128,1152]{1,0:T(8,128)(2,1)S(1)}, bf16[128,1152]{1,0:T(8,128)(2,1)S(1)}, u32[]{:S(2)}, u32[]{:S(2)}) collective-permute-start(bf16[128,1152]{1,0:T(8,128)(2,1)S(1)} %slice.9), channel_id=1, source_target_pairs={{0,480},{32,0},{64,32},{96,64},{128,96},{160,128},{192,160},{224,1... | collective-permute-start | bytes 884744 | tf_op jit(solution)/shard_map/ppermute | solution.py:23
  71.6 0.0 collective-permute-done.2.refs_4_
  71.6 0.0 copy-done.6
  71.6 0.0 copy-start.8
  71.7 0.0 copy-done.7
  71.7 1.9 %collective-permute-start.3 = (bf16[128,1152]{1,0:T(8,128)(2,1)S(1)}, bf16[128,1152]{1,0:T(8,128)(2,1)S(1)}, u32[]{:S(2)}, u32[]{:S(2)}) collective-permute-start(bf16[128,1152]{1,0:T(8,128)(2,1)S(1)} %slice.8), channel_id=1, source_target_pairs={{0,32},{32,64},{64,96},{96,128},{128,160},{160,192},{192,224},{224... | collective-permute-start | bytes 884744 | tf_op jit(solution)/shard_map/ppermute | solution.py:23
  73.6 0.0 copy-done.8
  73.6 0.6 pad_add_fusion.at_ref
  74.2 5.5 %prepare_c.1 = (bf16[8,512,256]{2,1,0:T(8,128)(2,1)}, bf16[8,256,512]{2,1,0:T(8,128)(2,1)}, bf16[64,2048]{1,0:T(8,128)(2,1)}) custom-call(s32[3]{0:T(128)} %pad_add_fusion.at_ref, bf16[512,2048]{1,0:T(8,128)(2,1)} %hi_ref.1, bf16[512,2048]{1,0:T(8,128)(2,1)} %hi_ref.1), custom_call_target="tpu_custom_call" | custom-call | tf_op jit(solution)/shard_map/prepare_c/pallas_call | solution.py:308
  79.8 0.0 copy-start.9
  79.8 7.1 %prepare_x.1 = (bf16[8,512,256]{2,1,0:T(8,128)(2,1)}, bf16[64,2048]{1,0:T(8,128)(2,1)}) custom-call(s32[3]{0:T(128)} %pad_add_fusion.at_ref, bf16[512,2048]{1,0:T(8,128)(2,1)} %x_ref.1, f32[1,2048]{1,0:T(1,128)} %bitcast.26), custom_call_target="tpu_custom_call" | custom-call | tf_op jit(solution)/shard_map/prepare_x/pallas_call | solution.py:288
  86.9 0.6 fusion.3.gain_ref
  87.5 6.3 %forward.1.acc_hbm = f32[512,1152]{1,0:T(8,128)} custom-call(bf16[8,512,256]{2,1,0:T(8,128)(2,1)} %get-tuple-element.18.x_ref.x_hbm, bf16[8,512,256]{2,1,0:T(8,128)(2,1)} %get-tuple-element.19.c_ref.c_hbm, bf16[256,1152]{1,0:T(8,128)(2,1)} %bitcast.22, bf16[256,1152]{1,0:T(8,128)(2,1)} %copy-done.3, bf16[256,1152]{1,0:T(8,128)(2,1)} %copy-done.4, ...), custom_call_target="tpu_custom_call" | custom-call | tf_op jit(solution)/shard_map/forward/pallas_call | solution.py:332
  93.8 0.0 collective-permute-done.7.hi_ref
  93.8 0.0 collective-permute-done.3.lo_ref
  93.8 11.0 %grad.1 = (bf16[4,8,64,256]{3,2,1,0:T(8,128)(2,1)}, bf16[4,8,64,256]{3,2,1,0:T(8,128)(2,1)}, bf16[4,8,200,128]{3,2,1,0:T(8,128)(2,1)}) custom-call(f32[8,1,256]{2,1,0:T(1,128)} %fusion.3.gain_ref, bf16[128,1152]{1,0:T(8,128)(2,1)S(1)} %collective-permute-done.3.lo_ref, bf16[128,1152]{1,0:T(8,128)(2,1)S(1)} %collective-permute-done.7.hi_ref, ...), custom_call_target="tpu_custom_call" | custom-call | tf_op jit(solution)/shard_map/grad/pallas_call | solution.py:340
  104.8 3.7 %all-to-all-start.1 = ((bf16[4,8,200,128]{3,2,1,0:T(8,128)(2,1)}), bf16[4,8,200,128]{3,2,1,0:T(8,128)(2,1)S(1)}, u32[]{:S(2)}, u32[]{:S(2)}) async-start(bf16[4,8,200,128]{3,2,1,0:T(8,128)(2,1)} %get-tuple-element.29), calls=%async_computation.1 | async-start | bytes 3276800 | tf_op jit(solution)/shard_map/all_to_all | solution.py:27
  108.5 6.9 %collective-permute-start.8 = (bf16[4,8,64,256]{3,2,1,0:T(8,128)(2,1)}, bf16[4,8,64,256]{3,2,1,0:T(8,128)(2,1)S(1)}, u32[]{:S(2)}, u32[]{:S(2)}) collective-permute-start(bf16[4,8,64,256]{3,2,1,0:T(8,128)(2,1)} %get-tuple-element.22), channel_id=1, source_target_pairs={{0,1},{1,0},{2,3},{3,2},{4,5},{5,4},{6,7},{7,6},{8,9},{9,8},{10,11... | collective-permute-start | bytes 3145736 | tf_op jit(solution)/shard_map/ppermute | solution.py:23
  115.4 2.5 %collective-permute-done.8.theirs_ref = bf16[4,8,64,256]{3,2,1,0:T(8,128)(2,1)S(1)} collective-permute-done((bf16[4,8,64,256]{3,2,1,0:T(8,128)(2,1)}, bf16[4,8,64,256]{3,2,1,0:T(8,128)(2,1)S(1)}, u32[]{:S(2)}, u32[]{:S(2)}) %collective-permute-start.8) | collective-permute-done | bytes 1048608 | tf_op jit(solution)/shard_map/ppermute | solution.py:23
  117.8 1.0 chip.1
  118.8 3.1 %collective-permute-start.9 = (bf16[8,64,256]{2,1,0:T(8,128)(2,1)}, bf16[8,64,256]{2,1,0:T(8,128)(2,1)S(1)}, u32[]{:S(2)}, u32[]{:S(2)}) collective-permute-start(bf16[8,64,256]{2,1,0:T(8,128)(2,1)} %get-tuple-element.24), channel_id=1, source_target_pairs={{0,2},{2,4},{4,6},{6,0},{1,3},{3,5},{5,7},{7,1},{8,10},{10,12},{12... | collective-permute-start | bytes 786440 | tf_op jit(solution)/shard_map/ppermute | solution.py:23
  121.9 4.4 %collective-permute-start.10 = (bf16[8,64,256]{2,1,0:T(8,128)(2,1)}, bf16[8,64,256]{2,1,0:T(8,128)(2,1)S(1)}, u32[]{:S(2)}, u32[]{:S(2)}) collective-permute-start(bf16[8,64,256]{2,1,0:T(8,128)(2,1)} %get-tuple-element.25), channel_id=1, source_target_pairs={{0,4},{2,6},{4,0},{6,2},{1,5},{3,7},{5,1},{7,3},{8,12},{10,14},{12... | collective-permute-start | bytes 786440 | tf_op jit(solution)/shard_map/ppermute | solution.py:23
  126.3 3.1 %collective-permute-start.11 = (bf16[8,64,256]{2,1,0:T(8,128)(2,1)S(1)}, bf16[8,64,256]{2,1,0:T(8,128)(2,1)S(1)}, u32[]{:S(2)}, u32[]{:S(2)}) collective-permute-start(bf16[8,64,256]{2,1,0:T(8,128)(2,1)S(1)} %get-tuple-element.26), channel_id=1, source_target_pairs={{0,6},{2,0},{4,2},{6,4},{1,7},{3,1},{5,3},{7,5},{8,14},{10,8},{12,... | collective-permute-start | bytes 786440 | tf_op jit(solution)/shard_map/ppermute | solution.py:23
  129.4 0.0 all-to-all-done.1.got_ref
  129.4 1.7 ysum.1
  131.0 7.3 %all-to-all-start.2 = ((bf16[16,112,128]{2,1,0:T(8,128)(2,1)}), bf16[16,112,128]{2,1,0:T(8,128)(2,1)S(1)}, u32[]{:S(2)}, u32[]{:S(2)}) async-start(bf16[16,112,128]{2,1,0:T(8,128)(2,1)} %ysum.1), calls=%async_computation.2 | async-start | bytes 917504 | tf_op jit(solution)/shard_map/all_to_all | solution.py:27
  138.4 0.0 collective-permute-done.9.got1
  138.4 0.0 collective-permute-done.10.got2
  138.4 0.0 collective-permute-done.11.got3
  138.4 2.9 %finish.1.p0 = bf16[64,2048]{1,0:T(8,128)(2,1)} custom-call(s32[3]{0:T(128)} %pad_add_fusion.at_ref, bf16[8,64,256]{2,1,0:T(8,128)(2,1)} %copy-done.1, bf16[8,64,256]{2,1,0:T(8,128)(2,1)S(1)} %collective-permute-done.9.got1, bf16[8,64,256]{2,1,0:T(8,128)(2,1)S(1)} %collective-permute-done.10.got2, bf16[8,64,256]{2,1,0:T(8,128)(2,1)S(1)} %collective-permute-done.11.got3, ...), custom_call_target="tpu_custom_call" | custom-call | tf_op jit(solution)/shard_map/finish/pallas_call | solution.py:377
  141.3 4.1 %collective-permute-start.14 = (bf16[64,2048]{1,0:T(8,128)(2,1)}, bf16[64,2048]{1,0:T(8,128)(2,1)S(1)}, u32[]{:S(2)}, u32[]{:S(2)}) collective-permute-start(bf16[64,2048]{1,0:T(8,128)(2,1)} %finish.1.p0), channel_id=1, source_target_pairs={{0,2},{2,4},{4,6},{6,0},{1,3},{3,5},{5,7},{7,1},{8,10},{10,12},{12... | collective-permute-start | bytes 786440 | tf_op jit(solution)/shard_map/ppermute | solution.py:23
  145.4 3.2 %collective-permute-start.13 = (bf16[64,2048]{1,0:T(8,128)(2,1)}, bf16[64,2048]{1,0:T(8,128)(2,1)S(1)}, u32[]{:S(2)}, u32[]{:S(2)}) collective-permute-start(bf16[64,2048]{1,0:T(8,128)(2,1)} %finish.1.p0), channel_id=1, source_target_pairs={{0,4},{2,6},{4,0},{6,2},{1,5},{3,7},{5,1},{7,3},{8,12},{10,14},{12... | collective-permute-start | bytes 786440 | tf_op jit(solution)/shard_map/ppermute | solution.py:23
  148.6 3.0 %collective-permute-start.12 = (bf16[64,2048]{1,0:T(8,128)(2,1)}, bf16[64,2048]{1,0:T(8,128)(2,1)S(1)}, u32[]{:S(2)}, u32[]{:S(2)}) collective-permute-start(bf16[64,2048]{1,0:T(8,128)(2,1)} %finish.1.p0), channel_id=1, source_target_pairs={{0,6},{2,0},{4,2},{6,4},{1,7},{3,1},{5,3},{7,5},{8,14},{10,8},{12,... | collective-permute-start | bytes 786440 | tf_op jit(solution)/shard_map/ppermute | solution.py:23
  151.6 0.0 collective-permute-done.14.p3
  151.6 5.7 %collective-permute-done.13.p2 = bf16[64,2048]{1,0:T(8,128)(2,1)S(1)} collective-permute-done((bf16[64,2048]{1,0:T(8,128)(2,1)}, bf16[64,2048]{1,0:T(8,128)(2,1)S(1)}, u32[]{:S(2)}, u32[]{:S(2)}) %collective-permute-start.13) | collective-permute-done | bytes 262176 | tf_op jit(solution)/shard_map/ppermute | solution.py:23
  157.3 1.7 collective-permute-done.12.p1
  159.0 2.1 %pad_maximum_fusion = bf16[4,64,2048]{2,1,0:T(8,128)(2,1)} fusion(bf16[1,64,2048]{2,1,0:T(8,128)(2,1)S(1)} %bitcast.17, bf16[1,64,2048]{2,1,0:T(8,128)(2,1)S(1)} %bitcast.18, bf16[1,64,2048]{2,1,0:T(8,128)(2,1)S(1)} %bitcast.19, bf16[1,64,2048]{2,1,0:T(8,128)(2,1)} %bitcast.24), kind=kLoop, calls=%fused_computation | loop fusion | flops 1572864 | bytes 2097152 | tf_op jit(solution)/shard_map/stack | solution.py:392
  161.1 4.3 %collective-permute-start.15 = (bf16[4,64,2048]{2,1,0:T(8,128)(2,1)}, bf16[4,64,2048]{2,1,0:T(8,128)(2,1)S(1)}, u32[]{:S(2)}, u32[]{:S(2)}) collective-permute-start(bf16[4,64,2048]{2,1,0:T(8,128)(2,1)} %pad_maximum_fusion), channel_id=1, source_target_pairs={{0,1},{1,0},{2,3},{3,2},{4,5},{5,4},{6,7},{7,6},{8,9},{9,8},{10,11... | collective-permute-start | bytes 3145736 | tf_op jit(solution)/shard_map/ppermute | solution.py:23
  165.4 0.0 all-to-all-done.2.got_ref
  165.4 0.7 zsum.1
  166.1 12.0 %collective-permute-start.16 = (bf16[32,384]{1,0:T(8,128)(2,1)}, bf16[32,384]{1,0:T(8,128)(2,1)S(1)}, u32[]{:S(2)}, u32[]{:S(2)}) collective-permute-start(bf16[32,384]{1,0:T(8,128)(2,1)} %get-tuple-element.32), channel_id=1, source_target_pairs={{0,256},{256,0},{1,257},{257,1},{2,258},{258,2},{3,259},{259,3},{4... | collective-permute-start | bytes 73736 | tf_op jit(solution)/shard_map/ppermute | solution.py:23
  178.1 0.0 copy-start.10
  178.1 0.0 collective-permute-done.15.other_ref
  178.1 2.4 %place.1 = bf16[512,2048]{1,0:T(8,128)(2,1)} custom-call(s32[3]{0:T(128)} %pad_add_fusion.at_ref, bf16[64,2048]{1,0:T(8,128)(2,1)} %finish.1.p0, bf16[64,2048]{1,0:T(8,128)(2,1)S(1)} %collective-permute-done.12.p1, bf16[64,2048]{1,0:T(8,128)(2,1)S(1)} %collective-permute-done.13.p2, bf16[64,2048]{1,0:T(8,128)(2,1)S(1)} %collective-permute-done.14.p3, ...), custom_call_target="tpu_custom_call" | custom-call | tf_op jit(solution)/shard_map/place/pallas_call | solution.py:393
  180.5 4.2 %all-to-all-start.3 = ((f32[8,8,256]{2,1,0:T(8,128)}), f32[8,8,256]{2,1,0:T(8,128)S(1)}, u32[]{:S(2)}, u32[]{:S(2)}) async-start(f32[8,8,256]{2,1,0:T(8,128)} %get-tuple-element.30), calls=%async_computation.3 | async-start | bytes 131072 | tf_op jit(solution)/shard_map/all_to_all | solution.py:27
  184.8 0.0 collective-permute-done.16
  184.8 0.7 fusion.2
  185.5 4.2 %all-to-all-done.3 = f32[8,8,256]{2,1,0:T(8,128)S(1)} async-done(((f32[8,8,256]{2,1,0:T(8,128)}), f32[8,8,256]{2,1,0:T(8,128)S(1)}, u32[]{:S(2)}, u32[]{:S(2)}) %all-to-all-start.3) | async-done | bytes 65568 | tf_op jit(solution)/shard_map/all_to_all | solution.py:27
  189.6 0.6 copy.9
  (19 shorter events, 0.1 us)
Async XLA Ops:
  13.6 66.1 %copy-start.2 = (bf16[4,64,1152]{2,1,0:T(8,128)(2,1)}, bf16[4,64,1152]{2,1,0:T(8,128)(2,1)S(1)}, u32[]{:S(2)}) copy-start(bf16[4,64,1152]{2,1,0:T(8,128)(2,1)S(1)} %all_to_all.20) | copy-start | bytes 1769476
  13.6 23.4 %collective-permute-start.4 = (bf16[256,1152]{1,0:T(8,128)(2,1)S(1)}, bf16[256,1152]{1,0:T(8,128)(2,1)S(1)}, u32[]{:S(2)}, u32[]{:S(2)}) collective-permute-start(bf16[256,1152]{1,0:T(8,128)(2,1)S(1)} %bitcast.20), channel_id=1, source_target_pairs={{0,480},{32,0},{64,32},{96,64},{128,96},{160,128},{192,160},{224,1... | collective-permute-start | bytes 1769480 | tf_op jit(solution)/shard_map/ppermute | solution.py:23
  26.5 15.9 %collective-permute-start = (bf16[256,1152]{1,0:T(8,128)(2,1)S(1)}, bf16[256,1152]{1,0:T(8,128)(2,1)S(1)}, u32[]{:S(2)}, u32[]{:S(2)}) collective-permute-start(bf16[256,1152]{1,0:T(8,128)(2,1)S(1)} %bitcast.21), channel_id=1, source_target_pairs={{0,32},{32,64},{64,96},{96,128},{128,160},{160,192},{192,224},{224... | collective-permute-start | bytes 1769480 | tf_op jit(solution)/shard_map/ppermute | solution.py:23
  37.1 42.7 %copy-start.3 = (bf16[256,1152]{1,0:T(8,128)(2,1)}, bf16[256,1152]{1,0:T(8,128)(2,1)S(1)}, u32[]{:S(2)}) copy-start(bf16[256,1152]{1,0:T(8,128)(2,1)S(1)} %collective-permute-done.4.refs_1_) | copy-start | bytes 1769476
  37.1 15.0 %collective-permute-start.5 = (bf16[256,1152]{1,0:T(8,128)(2,1)S(1)}, bf16[256,1152]{1,0:T(8,128)(2,1)S(1)}, u32[]{:S(2)}, u32[]{:S(2)}) collective-permute-start(bf16[256,1152]{1,0:T(8,128)(2,1)S(1)} %collective-permute-done.4.refs_1_), channel_id=1, source_target_pairs={{0,480},{32,0},{64,32},{96,64},{128,96},{160,128},{192,160},{224,1... | collective-permute-start | bytes 1769480 | tf_op jit(solution)/shard_map/ppermute | solution.py:23
  42.4 37.4 %copy-start.4 = (bf16[256,1152]{1,0:T(8,128)(2,1)}, bf16[256,1152]{1,0:T(8,128)(2,1)S(1)}, u32[]{:S(2)}) copy-start(bf16[256,1152]{1,0:T(8,128)(2,1)S(1)} %collective-permute-done.refs_2_.refs_6_) | copy-start | bytes 1769476
  42.4 15.0 %collective-permute-start.1 = (bf16[256,1152]{1,0:T(8,128)(2,1)S(1)}, bf16[256,1152]{1,0:T(8,128)(2,1)S(1)}, u32[]{:S(2)}, u32[]{:S(2)}) collective-permute-start(bf16[256,1152]{1,0:T(8,128)(2,1)S(1)} %collective-permute-done.refs_2_.refs_6_), channel_id=1, source_target_pairs={{0,32},{32,64},{64,96},{96,128},{128,160},{160,192},{192,224},{224... | collective-permute-start | bytes 1769480 | tf_op jit(solution)/shard_map/ppermute | solution.py:23
  52.1 27.7 %copy-start.5 = (bf16[256,1152]{1,0:T(8,128)(2,1)}, bf16[256,1152]{1,0:T(8,128)(2,1)S(1)}, u32[]{:S(2)}) copy-start(bf16[256,1152]{1,0:T(8,128)(2,1)S(1)} %collective-permute-done.5.refs_3_.refs_2_) | copy-start | bytes 1769476
  52.1 14.2 %collective-permute-start.6 = (bf16[256,1152]{1,0:T(8,128)(2,1)S(1)}, bf16[256,1152]{1,0:T(8,128)(2,1)S(1)}, u32[]{:S(2)}, u32[]{:S(2)}) collective-permute-start(bf16[256,1152]{1,0:T(8,128)(2,1)S(1)} %collective-permute-done.5.refs_3_.refs_2_), channel_id=1, source_target_pairs={{0,480},{32,0},{64,32},{96,64},{128,96},{160,128},{192,160},{224,1... | collective-permute-start | bytes 1769480 | tf_op jit(solution)/shard_map/ppermute | solution.py:23
  57.4 14.2 %copy-start.6 = (bf16[256,1152]{1,0:T(8,128)(2,1)}, bf16[256,1152]{1,0:T(8,128)(2,1)S(1)}, u32[]{:S(2)}) copy-start(bf16[256,1152]{1,0:T(8,128)(2,1)S(1)} %collective-permute-done.1.refs_4_.refs_5_) | copy-start | bytes 1769476
  57.4 14.2 %collective-permute-start.2 = (bf16[256,1152]{1,0:T(8,128)(2,1)S(1)}, bf16[256,1152]{1,0:T(8,128)(2,1)S(1)}, u32[]{:S(2)}, u32[]{:S(2)}) collective-permute-start(bf16[256,1152]{1,0:T(8,128)(2,1)S(1)} %collective-permute-done.1.refs_4_.refs_5_), channel_id=1, source_target_pairs={{0,32},{32,64},{64,96},{96,128},{128,160},{160,192},{192,224},{224... | collective-permute-start | bytes 1769480 | tf_op jit(solution)/shard_map/ppermute | solution.py:23
  66.3 5.4 %copy-start.7 = (bf16[256,1152]{1,0:T(8,128)(2,1)}, bf16[256,1152]{1,0:T(8,128)(2,1)S(1)}, u32[]{:S(2)}) copy-start(bf16[256,1152]{1,0:T(8,128)(2,1)S(1)} %collective-permute-done.6.refs_3_) | copy-start | bytes 1769476
  66.3 27.5 %collective-permute-start.7 = (bf16[128,1152]{1,0:T(8,128)(2,1)S(1)}, bf16[128,1152]{1,0:T(8,128)(2,1)S(1)}, u32[]{:S(2)}, u32[]{:S(2)}) collective-permute-start(bf16[128,1152]{1,0:T(8,128)(2,1)S(1)} %slice.9), channel_id=1, source_target_pairs={{0,480},{32,0},{64,32},{96,64},{128,96},{160,128},{192,160},{224,1... | collective-permute-start | bytes 884744 | tf_op jit(solution)/shard_map/ppermute | solution.py:23
  71.6 2.0 %copy-start.8 = (bf16[256,1152]{1,0:T(8,128)(2,1)}, bf16[256,1152]{1,0:T(8,128)(2,1)S(1)}, u32[]{:S(2)}) copy-start(bf16[256,1152]{1,0:T(8,128)(2,1)S(1)} %collective-permute-done.2.refs_4_) | copy-start | bytes 1769476
  71.7 22.1 %collective-permute-start.3 = (bf16[128,1152]{1,0:T(8,128)(2,1)S(1)}, bf16[128,1152]{1,0:T(8,128)(2,1)S(1)}, u32[]{:S(2)}, u32[]{:S(2)}) collective-permute-start(bf16[128,1152]{1,0:T(8,128)(2,1)S(1)} %slice.8), channel_id=1, source_target_pairs={{0,32},{32,64},{64,96},{96,128},{128,160},{160,192},{192,224},{224... | collective-permute-start | bytes 884744 | tf_op jit(solution)/shard_map/ppermute | solution.py:23
  79.8 7.1 %copy-start.9 = (f32[2048]{0:T(1024)S(1)}, f32[2048]{0:T(1024)}, u32[]{:S(2)}) copy-start(f32[2048]{0:T(1024)} %param.7) | copy-start | bytes 24580
  104.8 13.1 %copy-start = (bf16[4,8,64,256]{3,2,1,0:T(8,128)(2,1)S(1)}, bf16[4,8,64,256]{3,2,1,0:T(8,128)(2,1)}, u32[]{:S(2)}) copy-start(bf16[4,8,64,256]{3,2,1,0:T(8,128)(2,1)} %get-tuple-element.21.mine_ref) | copy-start | bytes 3145732
  104.8 24.6 %all-to-all-start.1 = ((bf16[4,8,200,128]{3,2,1,0:T(8,128)(2,1)}), bf16[4,8,200,128]{3,2,1,0:T(8,128)(2,1)S(1)}, u32[]{:S(2)}, u32[]{:S(2)}) async-start(bf16[4,8,200,128]{3,2,1,0:T(8,128)(2,1)} %get-tuple-element.29), calls=%async_computation.1 | async-start | bytes 3276800 | tf_op jit(solution)/shard_map/all_to_all | solution.py:27
  108.5 9.3 %collective-permute-start.8 = (bf16[4,8,64,256]{3,2,1,0:T(8,128)(2,1)}, bf16[4,8,64,256]{3,2,1,0:T(8,128)(2,1)S(1)}, u32[]{:S(2)}, u32[]{:S(2)}) collective-permute-start(bf16[4,8,64,256]{3,2,1,0:T(8,128)(2,1)} %get-tuple-element.22), channel_id=1, source_target_pairs={{0,1},{1,0},{2,3},{3,2},{4,5},{5,4},{6,7},{7,6},{8,9},{9,8},{10,11... | collective-permute-start | bytes 3145736 | tf_op jit(solution)/shard_map/ppermute | solution.py:23
  118.8 12.2 %copy-start.1 = (bf16[8,64,256]{2,1,0:T(8,128)(2,1)}, bf16[8,64,256]{2,1,0:T(8,128)(2,1)S(1)}, u32[]{:S(2)}) copy-start(bf16[8,64,256]{2,1,0:T(8,128)(2,1)S(1)} %get-tuple-element.23.got0) | copy-start | bytes 786436
  118.8 19.6 %collective-permute-start.9 = (bf16[8,64,256]{2,1,0:T(8,128)(2,1)}, bf16[8,64,256]{2,1,0:T(8,128)(2,1)S(1)}, u32[]{:S(2)}, u32[]{:S(2)}) collective-permute-start(bf16[8,64,256]{2,1,0:T(8,128)(2,1)} %get-tuple-element.24), channel_id=1, source_target_pairs={{0,2},{2,4},{4,6},{6,0},{1,3},{3,5},{5,7},{7,1},{8,10},{10,12},{12... | collective-permute-start | bytes 786440 | tf_op jit(solution)/shard_map/ppermute | solution.py:23
  121.9 16.5 %collective-permute-start.10 = (bf16[8,64,256]{2,1,0:T(8,128)(2,1)}, bf16[8,64,256]{2,1,0:T(8,128)(2,1)S(1)}, u32[]{:S(2)}, u32[]{:S(2)}) collective-permute-start(bf16[8,64,256]{2,1,0:T(8,128)(2,1)} %get-tuple-element.25), channel_id=1, source_target_pairs={{0,4},{2,6},{4,0},{6,2},{1,5},{3,7},{5,1},{7,3},{8,12},{10,14},{12... | collective-permute-start | bytes 786440 | tf_op jit(solution)/shard_map/ppermute | solution.py:23
  126.3 12.1 %collective-permute-start.11 = (bf16[8,64,256]{2,1,0:T(8,128)(2,1)S(1)}, bf16[8,64,256]{2,1,0:T(8,128)(2,1)S(1)}, u32[]{:S(2)}, u32[]{:S(2)}) collective-permute-start(bf16[8,64,256]{2,1,0:T(8,128)(2,1)S(1)} %get-tuple-element.26), channel_id=1, source_target_pairs={{0,6},{2,0},{4,2},{6,4},{1,7},{3,1},{5,3},{7,5},{8,14},{10,8},{12,... | collective-permute-start | bytes 786440 | tf_op jit(solution)/shard_map/ppermute | solution.py:23
  131.0 34.4 %all-to-all-start.2 = ((bf16[16,112,128]{2,1,0:T(8,128)(2,1)}), bf16[16,112,128]{2,1,0:T(8,128)(2,1)S(1)}, u32[]{:S(2)}, u32[]{:S(2)}) async-start(bf16[16,112,128]{2,1,0:T(8,128)(2,1)} %ysum.1), calls=%async_computation.2 | async-start | bytes 917504 | tf_op jit(solution)/shard_map/all_to_all | solution.py:27
  141.3 10.3 %collective-permute-start.14 = (bf16[64,2048]{1,0:T(8,128)(2,1)}, bf16[64,2048]{1,0:T(8,128)(2,1)S(1)}, u32[]{:S(2)}, u32[]{:S(2)}) collective-permute-start(bf16[64,2048]{1,0:T(8,128)(2,1)} %finish.1.p0), channel_id=1, source_target_pairs={{0,2},{2,4},{4,6},{6,0},{1,3},{3,5},{5,7},{7,1},{8,10},{10,12},{12... | collective-permute-start | bytes 786440 | tf_op jit(solution)/shard_map/ppermute | solution.py:23
  145.4 11.9 %collective-permute-start.13 = (bf16[64,2048]{1,0:T(8,128)(2,1)}, bf16[64,2048]{1,0:T(8,128)(2,1)S(1)}, u32[]{:S(2)}, u32[]{:S(2)}) collective-permute-start(bf16[64,2048]{1,0:T(8,128)(2,1)} %finish.1.p0), channel_id=1, source_target_pairs={{0,4},{2,6},{4,0},{6,2},{1,5},{3,7},{5,1},{7,3},{8,12},{10,14},{12... | collective-permute-start | bytes 786440 | tf_op jit(solution)/shard_map/ppermute | solution.py:23
  148.6 10.4 %collective-permute-start.12 = (bf16[64,2048]{1,0:T(8,128)(2,1)}, bf16[64,2048]{1,0:T(8,128)(2,1)S(1)}, u32[]{:S(2)}, u32[]{:S(2)}) collective-permute-start(bf16[64,2048]{1,0:T(8,128)(2,1)} %finish.1.p0), channel_id=1, source_target_pairs={{0,6},{2,0},{4,2},{6,4},{1,7},{3,1},{5,3},{7,5},{8,14},{10,8},{12,... | collective-permute-start | bytes 786440 | tf_op jit(solution)/shard_map/ppermute | solution.py:23
  161.1 17.0 %collective-permute-start.15 = (bf16[4,64,2048]{2,1,0:T(8,128)(2,1)}, bf16[4,64,2048]{2,1,0:T(8,128)(2,1)S(1)}, u32[]{:S(2)}, u32[]{:S(2)}) collective-permute-start(bf16[4,64,2048]{2,1,0:T(8,128)(2,1)} %pad_maximum_fusion), channel_id=1, source_target_pairs={{0,1},{1,0},{2,3},{3,2},{4,5},{5,4},{6,7},{7,6},{8,9},{9,8},{10,11... | collective-permute-start | bytes 3145736 | tf_op jit(solution)/shard_map/ppermute | solution.py:23
  166.1 18.7 %collective-permute-start.16 = (bf16[32,384]{1,0:T(8,128)(2,1)}, bf16[32,384]{1,0:T(8,128)(2,1)S(1)}, u32[]{:S(2)}, u32[]{:S(2)}) collective-permute-start(bf16[32,384]{1,0:T(8,128)(2,1)} %get-tuple-element.32), channel_id=1, source_target_pairs={{0,256},{256,0},{1,257},{257,1},{2,258},{258,2},{3,259},{259,3},{4... | collective-permute-start | bytes 73736 | tf_op jit(solution)/shard_map/ppermute | solution.py:23
  178.1 6.7 %copy-start.10 = (f32[32,384]{1,0:T(8,128)S(1)}, f32[32,384]{1,0:T(8,128)}, u32[]{:S(2)}) copy-start(f32[32,384]{1,0:T(8,128)} %get-tuple-element.31) | copy-start | bytes 147460
  180.5 9.1 %all-to-all-start.3 = ((f32[8,8,256]{2,1,0:T(8,128)}), f32[8,8,256]{2,1,0:T(8,128)S(1)}, u32[]{:S(2)}, u32[]{:S(2)}) async-start(f32[8,8,256]{2,1,0:T(8,128)} %get-tuple-element.30), calls=%async_computation.3 | async-start | bytes 131072 | tf_op jit(solution)/shard_map/all_to_all | solution.py:27
